TPU v7x, 512 devices: a whole 4x4x16 slice. The times are simulated.
512 devices in a mesh: rep: 2 (over z_hi), fs: 32 (over z_lo, y), tp: 8 (over x, core).
Axes of the slice: x: 4, y: 4, z: 16 (z_hi: 2, z_lo: 8; z = z_hi * 8 + z_lo), core: 2. Of those that a mesh axis runs over, the one named last changes fastest.
Arguments:
- x_next: bfloat16 [24576, 2048], P(('rep', 'fs')), may hold values from -6 to 6
- value_next: bfloat16 [24576, 3072], P(('rep', 'fs'), 'tp'), may hold values from -6 to 6
- x_prev: bfloat16 [24576, 2048], P(('rep', 'fs')), may hold values from -16 to 16
- value_prev: bfloat16 [24576, 3072], P(('rep', 'fs'), 'tp'), may hold values from -6 to 6
- cotangent: bfloat16 [24576, 3072], P(('rep', 'fs'), 'tp'), may hold values from -16 to 16
- w_gate: bfloat16 [2048, 3072], P('fs', 'tp'), may hold values from -0.125 to 0.125
- conv_taps: float32 [3, 3072], P(None, 'tp'), may hold values from -3.5 to 3.5
- conv_bias: float32 [3072], P('tp'), may hold values from -3 to 3
- sum_w: float32 [2048, 3072], P('fs', 'tp'), may hold values from -6 to 6
- sum_taps: float32 [3, 3072], P(None, 'tp'), may hold values from -6 to 6
- sum_bias: float32 [3072], P('tp'), may hold values from -6 to 6
Outputs:
- hidden_next: bfloat16 [24576, 3072], P(('rep', 'fs'), 'tp')
- grad_input: bfloat16 [24576, 2048], P(('rep', 'fs'))
- grad_value: bfloat16 [24576, 3072], P(('rep', 'fs'), 'tp')
- new_sum_w: float32 [2048, 3072], P('fs', 'tp')
- new_sum_taps: float32 [3, 3072], P(None, 'tp')
- new_sum_bias: float32 [3072], P('tp')
All inputs are finite; a program needn't handle non-finite values.
Results may differ from a plain program's by a relative error of at most 0.015.
Values may be sent and summed in bfloat16 or wider, within the bound.
No kernel may reach another device: no remote copies, remote signals or barrier semaphores. Data moves between devices by JAX's collectives and lax.ppermute only.
A program may use at most 64 MiB of HBM per device.

v0:
```python
import jax
import jax.numpy as jnp
from jax import lax
from jax.sharding import PartitionSpec as P

SEQ_LEN = 128


def joined_along(parts, dim):
    shape = list(parts.shape[1:])
    shape[dim] *= parts.shape[0]
    return jnp.moveaxis(parts, 0, dim).reshape(shape)


def copy_for_each(shard, axis):
    copies = jnp.broadcast_to(shard, (lax.axis_size(axis), *shard.shape))
    return lax.all_to_all(copies, axis, split_axis=0, concat_axis=0, tiled=True)


def gathered_copies(shard, axis, dim):
    return joined_along(copy_for_each(shard, axis), dim)


def split_up(shard, dim, length):
    shape = shard.shape
    parts = shard.reshape(*shape[:dim], length, shape[dim] // length, *shape[dim + 1 :])
    return jnp.moveaxis(parts, dim, 0)


def summed_on_arrival(shard, axis, dim):
    length = lax.axis_size(axis)
    parts = lax.all_to_all(split_up(shard, dim, length), axis, 0, 0, tiled=True)
    return jnp.sum(parts.astype(jnp.float32), axis=0)


def of_everyone(shard, axis):
    return copy_for_each(shard, axis).sum(axis=0)


def packed_total(arrays, axis):
    vector, at, finished = (jnp.concatenate([a.reshape(-1) for a in arrays]), 0, [])
    subtotal = of_everyone(vector, axis)
    for a in arrays:
        finished.append(subtotal[at : at + a.size].reshape(a.shape))
        at += a.size
    return tuple(finished)


def lagged(values, offset, position):
    count_rows = values.shape[0]
    shifted_rows = jnp.concatenate(
        (jnp.zeros((offset, values.shape[1]), values.dtype), values[: count_rows - offset]), axis=0
    )
    return jnp.where((position >= offset)[:, None], shifted_rows, jnp.zeros_like(shifted_rows))


def leading(values, offset, position):
    shifted_rows = jnp.concatenate(
        (values[offset:], jnp.zeros((offset, values.shape[1]), values.dtype)), axis=0
    )
    return jnp.where(
        (position < SEQ_LEN - offset)[:, None], shifted_rows, jnp.zeros_like(shifted_rows)
    )


def convolve(up_rows, conv_taps, conv_bias, position):
    values = up_rows.astype(jnp.float32)
    tap_count = conv_taps.shape[0]
    result = jnp.zeros(values.shape, jnp.float32) + conv_bias[None, :]
    for tap_index in range(tap_count):
        result = result + conv_taps[tap_index][None, :] * lagged(
            values, tap_count - 1 - tap_index, position
        )
    return result


def per_device(
    x_next,
    value_next,
    x_prev,
    value_prev,
    cotangent,
    w_gate,
    conv_taps,
    conv_bias,
    sum_w,
    sum_taps,
    sum_bias,
):
    row_count = x_next.shape[0]
    tap_count = conv_taps.shape[0]
    position = jnp.arange(row_count) % SEQ_LEN
    gathered = gathered_copies(w_gate, "fs", 0)
    up_next = jnp.dot(x_next, gathered, preferred_element_type=jnp.float32)
    up_prev = jnp.dot(x_prev, gathered, preferred_element_type=jnp.float32)
    up_next = up_next.astype(jnp.bfloat16)
    up_prev = up_prev.astype(jnp.bfloat16)
    gate_next = convolve(up_next, conv_taps, conv_bias, position)
    hidden_next = (gate_next * jax.nn.sigmoid(gate_next) * value_next.astype(jnp.float32)).astype(
        jnp.bfloat16
    )
    gate_prev = convolve(up_prev, conv_taps, conv_bias, position)
    sigmoid_gate = jax.nn.sigmoid(gate_prev)
    cot_values = cotangent.astype(jnp.float32)
    grad_value = (cot_values * gate_prev * sigmoid_gate).astype(jnp.bfloat16)
    grad_gate = (
        cot_values
        * value_prev.astype(jnp.float32)
        * sigmoid_gate
        * (1.0 + gate_prev * (1.0 - sigmoid_gate))
    )
    grad_up = jnp.zeros(grad_gate.shape, jnp.float32)
    for tap_index in range(tap_count):
        grad_up = grad_up + conv_taps[tap_index][None, :] * leading(
            grad_gate, tap_count - 1 - tap_index, position
        )
    grad_up = grad_up.astype(jnp.bfloat16)
    contract_units = (((1,), (1,)), ((), ()))
    partial_input = lax.dot_general(
        grad_up, gathered, contract_units, preferred_element_type=jnp.float32
    )
    grad_input = lax.psum(partial_input.astype(jnp.bfloat16), "tp")
    rep_count = lax.axis_size("rep")
    fs_count = lax.axis_size("fs")
    grad_scale = float(row_count * rep_count * fs_count) ** (-0.5)
    up_values = up_prev.astype(jnp.float32)
    tap_terms = (
        jnp.stack(
            [
                jnp.sum(grad_gate * lagged(up_values, tap_count - 1 - tap_index, position), axis=0)
                for tap_index in range(tap_count)
            ],
            axis=0,
        )
        * grad_scale
    )
    bias_terms = jnp.sum(grad_gate, axis=0) * grad_scale
    grad_rows = summed_on_arrival(
        (
            lax.dot_general(
                x_prev, grad_up, (((0,), (0,)), ((), ())), preferred_element_type=jnp.float32
            )
            * grad_scale
        ).astype(jnp.bfloat16),
        "fs",
        0,
    )
    tap_terms, bias_terms = packed_total((tap_terms, bias_terms), "fs")
    grad_rows, tap_terms, bias_terms = packed_total((grad_rows, tap_terms, bias_terms), "rep")
    return (
        hidden_next,
        grad_input,
        grad_value,
        sum_w + grad_rows,
        sum_taps + tap_terms,
        sum_bias + bias_terms,
    )


def solution(mesh):
    in_specs = (
        P(("rep", "fs"), None),
        P(("rep", "fs"), "tp"),
        P(("rep", "fs"), None),
        P(("rep", "fs"), "tp"),
        P(("rep", "fs"), "tp"),
        P("fs", "tp"),
        P(None, "tp"),
        P("tp"),
        P("fs", "tp"),
        P(None, "tp"),
        P("tp"),
    )
    out_specs = (
        P(("rep", "fs"), "tp"),
        P(("rep", "fs"), None),
        P(("rep", "fs"), "tp"),
        P("fs", "tp"),
        P(None, "tp"),
        P("tp"),
    )
    return jax.shard_map(
        per_device, mesh=mesh, in_specs=in_specs, out_specs=out_specs, check_vma=False
    )
```

profile of v0, /device:TPU:1, one launch (start us, length us, event | category | flops | bytes accessed | tf_op | source)
XLA Modules:
  0.0 239.3 jit_solution(13440346699739339541)
XLA Ops:
  7.2 0.0 copy-start
  7.2 2.3 broadcast_in_dim.81
  9.5 0.0 copy-start.8
  9.5 16.2 %all-to-all-start = ((bf16[32,64,384]{2,1,0:T(8,128)(2,1)}), bf16[32,64,384]{2,1,0:T(8,128)(2,1)S(1)}, u32[]{:S(2)}, u32[]{:S(2)}) async-start(bf16[32,64,384]{2,1,0:T(8,128)(2,1)} %broadcast_in_dim.81), calls=%async_computation | async-start | bytes 3145728 | tf_op jit(solution)/shard_map/all_to_all | solution.py:17
  25.7 0.0 copy-done.8
  25.8 72.1 %all-to-all-done = bf16[32,64,384]{2,1,0:T(8,128)(2,1)S(1)} async-done(((bf16[32,64,384]{2,1,0:T(8,128)(2,1)}), bf16[32,64,384]{2,1,0:T(8,128)(2,1)S(1)}, u32[]{:S(2)}, u32[]{:S(2)}) %all-to-all-start) | async-done | bytes 1572896 | tf_op jit(solution)/shard_map/all_to_all | solution.py:17
  97.9 0.0 copy-start.1
  97.9 0.0 copy-done
  97.9 0.0 copy-start.11
  97.9 1.0 fusion.1
  98.9 0.2 copy-done.1
  99.0 0.8 copy-done.11
  99.9 0.0 copy-start.2
  99.9 0.0 copy-start.4
  99.9 0.0 copy-start.5
  99.9 0.0 copy-start.9
  99.9 1.0 fusion.2
  100.9 0.0 copy-done.2
  100.9 0.1 copy-done.4
  100.9 0.1 copy-done.5
  101.0 0.0 copy-done.9
  101.0 2.2 multiply_reduce_fusion.2
  103.3 0.8 broadcast_in_dim.87
  104.0 8.1 %all-to-all-start.2 = ((f32[32,1,1536]{2,1,0:T(1,128)}), f32[32,1,1536]{2,1,0:T(1,128)}, u32[]{:S(2)}, u32[]{:S(2)}) async-start(f32[32,1,1536]{2,1,0:T(1,128)} %broadcast_in_dim.87), calls=%async_computation.2 | async-start | bytes 393216 | tf_op jit(solution)/shard_map/all_to_all | solution.py:17
  112.3 0.3 add_convert_fusion
  112.6 0.0 copy-start.3
  112.6 0.7 copy-done.3
  113.3 1.0 fusion
  114.3 1.6 copy.19
  115.9 10.0 %all-to-all-done.2 = f32[32,1,1536]{2,1,0:T(1,128)} async-done(((f32[32,1,1536]{2,1,0:T(1,128)}), f32[32,1,1536]{2,1,0:T(1,128)}, u32[]{:S(2)}, u32[]{:S(2)}) %all-to-all-start.2) | async-done | bytes 196640 | tf_op jit(solution)/shard_map/all_to_all | solution.py:17
  125.8 7.9 %all-to-all-start.1 = ((bf16[32,64,384]{2,1,0:T(8,128)(2,1)}), bf16[32,64,384]{2,1,0:T(8,128)(2,1)S(1)}, u32[]{:S(2)}, u32[]{:S(2)}) async-start(bf16[32,64,384]{2,1,0:T(8,128)(2,1)} %bitcast.2), calls=%async_computation.1 | async-start | bytes 3145728 | tf_op jit(solution)/shard_map/all_to_all | solution.py:32
  133.8 0.0 all-reduce.8.cloned.1.call-start
  133.8 3.7 %convolution_convert_fusion = bf16[384,2048]{1,0:T(8,128)(2,1)} fusion(bf16[384,384]{1,0:T(8,128)(2,1)} %copy-done.3, bf16[2048,384]{1,0:T(8,128)(2,1)} %bitcast.18), kind=kOutput, calls=%fused_computation.2 | convolution fusion | flops 604766208 | bytes 3440640 | tf_op jit(solution)/shard_map/dot_general | solution.py:119
  137.5 0.0 all-reduce.8.cloned.1.call-update
  137.5 1.1 reduce_sum.68
  138.6 67.3 %all-to-all-done.1 = bf16[32,64,384]{2,1,0:T(8,128)(2,1)S(1)} async-done(((bf16[32,64,384]{2,1,0:T(8,128)(2,1)}), bf16[32,64,384]{2,1,0:T(8,128)(2,1)S(1)}, u32[]{:S(2)}, u32[]{:S(2)}) %all-to-all-start.1) | async-done | bytes 1572896 | tf_op jit(solution)/shard_map/all_to_all | solution.py:32
  205.8 0.2 convert_reduce_fusion
  206.0 0.0 copy-start.7
  206.0 0.0 copy-start.6
  206.1 0.0 copy-start.10
  206.1 0.8 broadcast_in_dim.88
  206.9 7.3 %all-to-all-start.3 = ((f32[2,1,26112]{2,1,0:T(1,128)}), f32[2,1,26112]{2,1,0:T(1,128)S(1)}, u32[]{:S(2)}, u32[]{:S(2)}) async-start(f32[2,1,26112]{2,1,0:T(1,128)} %broadcast_in_dim.88), calls=%async_computation.3 | async-start | bytes 417792 | tf_op jit(solution)/shard_map/all_to_all | solution.py:17
  214.2 1.9 fusion.6
  216.1 11.4 %all-to-all-done.3 = f32[2,1,26112]{2,1,0:T(1,128)S(1)} async-done(((f32[2,1,26112]{2,1,0:T(1,128)}), f32[2,1,26112]{2,1,0:T(1,128)S(1)}, u32[]{:S(2)}, u32[]{:S(2)}) %all-to-all-start.3) | async-done | bytes 208928 | tf_op jit(solution)/shard_map/all_to_all | solution.py:17
  227.5 0.3 reduce_sum.69
  227.9 0.0 copy-done.7
  227.9 0.6 add.119
  228.5 0.0 copy-done.6
  228.5 0.7 add.118
  229.2 0.0 copy-done.10
  229.2 0.6 slice_add_fusion
  229.8 0.0 all-reduce.8.cloned.1.call-done
  229.8 2.7 %copy.28 = bf16[384,2048]{1,0:T(8,128)(2,1)} copy(bf16[384,2048]{1,0:T(8,128)(2,1)} %all-reduce.8.cloned.1.call-done) | data formatting | bytes 3145728
  (20 shorter events, 0.2 us)
Async XLA Ops:
  7.2 90.7 %copy-start = (bf16[384,2048]{1,0:T(8,128)(2,1)S(1)}, bf16[384,2048]{1,0:T(8,128)(2,1)}, u32[]{:S(2)}) copy-start(bf16[384,2048]{1,0:T(8,128)(2,1)} %param.13) | copy-start | bytes 4718596
  9.5 16.3 %copy-start.8 = (f32[3,384]{1,0:T(4,128)S(1)}, f32[3,384]{1,0:T(4,128)}, u32[]{:S(2)}) copy-start(f32[3,384]{1,0:T(4,128)} %param.17) | copy-start | bytes 13828
  9.5 88.4 %all-to-all-start = ((bf16[32,64,384]{2,1,0:T(8,128)(2,1)}), bf16[32,64,384]{2,1,0:T(8,128)(2,1)S(1)}, u32[]{:S(2)}, u32[]{:S(2)}) async-start(bf16[32,64,384]{2,1,0:T(8,128)(2,1)} %broadcast_in_dim.81), calls=%async_computation | async-start | bytes 3145728 | tf_op jit(solution)/shard_map/all_to_all | solution.py:17
  97.9 1.1 copy-start.1
  97.9 2.0 copy-start.11
  99.9 1.0 copy-start.2
  99.9 1.0 copy-start.4
  99.9 1.1 copy-start.5
  99.9 1.1 copy-start.9
  104.0 21.8 %all-to-all-start.2 = ((f32[32,1,1536]{2,1,0:T(1,128)}), f32[32,1,1536]{2,1,0:T(1,128)}, u32[]{:S(2)}, u32[]{:S(2)}) async-start(f32[32,1,1536]{2,1,0:T(1,128)} %broadcast_in_dim.87), calls=%async_computation.2 | async-start | bytes 393216 | tf_op jit(solution)/shard_map/all_to_all | solution.py:17
  112.6 0.7 copy-start.3
  125.8 80.0 %all-to-all-start.1 = ((bf16[32,64,384]{2,1,0:T(8,128)(2,1)}), bf16[32,64,384]{2,1,0:T(8,128)(2,1)S(1)}, u32[]{:S(2)}, u32[]{:S(2)}) async-start(bf16[32,64,384]{2,1,0:T(8,128)(2,1)} %bitcast.2), calls=%async_computation.1 | async-start | bytes 3145728 | tf_op jit(solution)/shard_map/all_to_all | solution.py:32
  133.8 96.0 %all-reduce.8.cloned.1.call-start = ((), (), s32[]{:S(2)}) async-start(), calls=%async_computation.4 | async-start | bytes 3145728 | tf_op jit(solution)/shard_map/psum | solution.py:122
  206.0 21.9 %copy-start.7 = (f32[3,384]{1,0:T(4,128)S(1)}, f32[3,384]{1,0:T(4,128)}, u32[]{:S(2)}) copy-start(f32[3,384]{1,0:T(4,128)} %param.20) | copy-start | bytes 13828
  206.0 22.5 %copy-start.6 = (f32[64,384]{1,0:T(8,128)S(1)}, f32[64,384]{1,0:T(8,128)}, u32[]{:S(2)}) copy-start(f32[64,384]{1,0:T(8,128)} %param.19) | copy-start | bytes 294916
  206.1 23.1 %copy-start.10 = (f32[384]{0:T(512)S(1)}, f32[384]{0:T(512)}, u32[]{:S(2)}) copy-start(f32[384]{0:T(512)} %param.21) | copy-start | bytes 4612
  206.9 20.6 %all-to-all-start.3 = ((f32[2,1,26112]{2,1,0:T(1,128)}), f32[2,1,26112]{2,1,0:T(1,128)S(1)}, u32[]{:S(2)}, u32[]{:S(2)}) async-start(f32[2,1,26112]{2,1,0:T(1,128)} %broadcast_in_dim.88), calls=%async_computation.3 | async-start | bytes 417792 | tf_op jit(solution)/shard_map/all_to_all | solution.py:17
Sparse Core Ops, SparseCore 0:
  137.6 78.2 all-reduce.7
where the time goes:
time: 243 us; the launch traced here: 239 us
  waiting for transfers between devices  161 us (66%)
  starting transfers between devices  39.6 us (16%)
  between operations  14.3 us (6%)
  local copies, waits for them, and re-layouts  10.2 us (4%)
  other arithmetic  7.85 us (3%)
  matrix products  6.62 us (3%)
    all_to_all x3, waiting for transfers between devices, copy_for_each(): return lax.all_to_all(copies, axis, split_axis=0, concat_axis=0, tiled=True)  93.5 us
    all_to_all x1, waiting for transfers between devices, summed_on_arrival(): parts = lax.all_to_all(split_up(shard, dim, length), axis, 0, 0, tiled=True)  67.3 us
    all_to_all x3, starting transfers between devices, copy_for_each(): return lax.all_to_all(copies, axis, split_axis=0, concat_axis=0, tiled=True)  31.6 us
    all_to_all x1, starting transfers between devices, summed_on_arrival(): parts = lax.all_to_all(split_up(shard, dim, length), axis, 0, 0, tiled=True)  7.92 us
  transfers between devices with their start and end apart: 5, of which 4 were waited for; matrix products, arithmetic and copies ran while one was open for 5% of the time, Pallas kernels for 0%

commit v1 on v0

v1 whole, which is shorter than its diff:
```python
import jax
import jax.numpy as jnp
from jax import lax
from jax.sharding import Mesh
from jax.sharding import PartitionSpec as P

SEQ_LEN = 128
SMALL_ROWS = 8


def copies_to(block, axis, size):
    copies = jnp.broadcast_to(block, (size, *block.shape))
    return lax.all_to_all(copies, axis, 0, 0, tiled=True)


def exchange(blocks, axis):
    return lax.all_to_all(blocks, axis, 0, 0, tiled=True)


def summed(blocks):
    return jnp.sum(blocks.astype(jnp.float32), axis=0)


def lagged(values, offset, position):
    count_rows = values.shape[0]
    shifted_rows = jnp.concatenate(
        (jnp.zeros((offset, values.shape[1]), values.dtype), values[: count_rows - offset]), axis=0
    )
    return jnp.where((position >= offset)[:, None], shifted_rows, jnp.zeros_like(shifted_rows))


def leading(values, offset, position):
    shifted_rows = jnp.concatenate(
        (values[offset:], jnp.zeros((offset, values.shape[1]), values.dtype)), axis=0
    )
    return jnp.where(
        (position < SEQ_LEN - offset)[:, None], shifted_rows, jnp.zeros_like(shifted_rows)
    )


def convolve(up_rows, conv_taps, conv_bias, position):
    values = up_rows.astype(jnp.float32)
    tap_count = conv_taps.shape[0]
    result = jnp.zeros(values.shape, jnp.float32) + conv_bias[None, :]
    for tap_index in range(tap_count):
        result = result + conv_taps[tap_index][None, :] * lagged(
            values, tap_count - 1 - tap_index, position
        )
    return result


def high_and_low(rows):
    high = rows.astype(jnp.bfloat16)
    low = (rows - high.astype(jnp.float32)).astype(jnp.bfloat16)
    return jnp.concatenate([high, low], axis=0)


def with_small(blocks, small):
    rows = jnp.broadcast_to(high_and_low(small), (blocks.shape[0], SMALL_ROWS, small.shape[1]))
    return jnp.concatenate([blocks, rows], axis=1)


def split_small(total):
    rows = total.shape[0] - SMALL_ROWS
    half = SMALL_ROWS // 2
    return total[:rows], total[rows : rows + half] + total[rows + half :]


def per_device(
    x_next,
    value_next,
    x_prev,
    value_prev,
    cotangent,
    w_gate,
    conv_taps,
    conv_bias,
    sum_w,
    sum_taps,
    sum_bias,
):
    row_count, width = x_next.shape
    shard_rows, units = w_gate.shape
    tap_count = conv_taps.shape[0]
    position = jnp.arange(row_count) % SEQ_LEN
    n_zh, n_zm, n_zq, n_y = (lax.axis_size(a) for a in ("zh", "zm", "zq", "y"))
    n_x, n_c = lax.axis_size("x"), lax.axis_size("c")

    pair = copies_to(w_gate, "zm", n_zm)
    quad = copies_to(pair, "zq", n_zq)
    plane = copies_to(quad, "y", n_y)
    gathered = jnp.transpose(plane, (2, 1, 0, 3, 4)).reshape(width, units)

    up_prev = jnp.dot(x_prev, gathered, preferred_element_type=jnp.float32).astype(jnp.bfloat16)
    gate_prev = convolve(up_prev, conv_taps, conv_bias, position)
    sigmoid_gate = jax.nn.sigmoid(gate_prev)
    cot_values = cotangent.astype(jnp.float32)
    grad_value = (cot_values * gate_prev * sigmoid_gate).astype(jnp.bfloat16)
    grad_gate = (
        cot_values
        * value_prev.astype(jnp.float32)
        * sigmoid_gate
        * (1.0 + gate_prev * (1.0 - sigmoid_gate))
    )
    grad_up = jnp.zeros(grad_gate.shape, jnp.float32)
    for tap_index in range(tap_count):
        grad_up = grad_up + conv_taps[tap_index][None, :] * leading(
            grad_gate, tap_count - 1 - tap_index, position
        )
    grad_up = grad_up.astype(jnp.bfloat16)
    token_count = row_count * n_zh * n_zm * n_zq * n_y
    grad_scale = float(token_count) ** (-0.5)
    up_values = up_prev.astype(jnp.float32)
    small = (
        jnp.stack(
            [
                jnp.sum(grad_gate * lagged(up_values, tap_count - 1 - tap_index, position), axis=0)
                for tap_index in range(tap_count)
            ]
            + [jnp.sum(grad_gate, axis=0)],
            axis=0,
        )
        * grad_scale
    )

    grad_w = (
        lax.dot_general(
            x_prev, grad_up, (((0,), (0,)), ((), ())), preferred_element_type=jnp.float32
        )
        * grad_scale
    ).astype(jnp.bfloat16)
    by_y = jnp.transpose(grad_w.reshape(n_zm, n_zq, n_y, shard_rows, units), (2, 1, 0, 3, 4))
    by_y = with_small(by_y.reshape(n_y, n_zq * n_zm * shard_rows, units), small)
    part, small = split_small(summed(exchange(by_y, "y")))
    by_q = part.astype(jnp.bfloat16).reshape(n_zq, n_zm * shard_rows, units)
    part, small = split_small(summed(exchange(with_small(by_q, small), "zq")))
    by_half = part.astype(jnp.bfloat16).reshape(n_zm, shard_rows, units)
    by_half = with_small(by_half, small)
    by_half = jnp.broadcast_to(by_half, (n_zh, *by_half.shape)).reshape(-1, *by_half.shape[1:])
    grad_rows, small = split_small(summed(exchange(by_half, ("zh", "zm"))))

    partial_input = lax.dot_general(
        grad_up, gathered, (((1,), (1,)), ((), ())), preferred_element_type=jnp.float32
    ).astype(jnp.bfloat16)
    half = summed(exchange(partial_input.reshape(n_c, -1, width), "c")).astype(jnp.bfloat16)
    eighth = summed(exchange(half.reshape(n_x, -1, width), "x")).astype(jnp.bfloat16)
    half = copies_to(eighth, "x", n_x).reshape(-1, width)
    grad_input = copies_to(half, "c", n_c).reshape(-1, width)

    up_next = jnp.dot(x_next, gathered, preferred_element_type=jnp.float32).astype(jnp.bfloat16)
    gate_next = convolve(up_next, conv_taps, conv_bias, position)
    hidden_next = (gate_next * jax.nn.sigmoid(gate_next) * value_next.astype(jnp.float32)).astype(
        jnp.bfloat16
    )
    return (
        hidden_next,
        grad_input,
        grad_value,
        sum_w + grad_rows,
        sum_taps + small[:tap_count],
        sum_bias + small[tap_count],
    )


def solution(mesh):
    n_fs, n_tp = mesh.shape["fs"], mesh.shape["tp"]
    n_y, n_zq, n_c = 4, 4, 2
    fine = Mesh(
        mesh.devices.reshape(
            mesh.shape["rep"], n_fs // (n_y * n_zq), n_zq, n_y, n_tp // n_c, n_c
        ),
        ("zh", "zm", "zq", "y", "x", "c"),
    )
    fs, tp = ("zm", "zq", "y"), ("x", "c")
    tokens = ("zh", *fs)
    in_specs = (
        P(tokens, None),
        P(tokens, tp),
        P(tokens, None),
        P(tokens, tp),
        P(tokens, tp),
        P(fs, tp),
        P(None, tp),
        P(tp),
        P(fs, tp),
        P(None, tp),
        P(tp),
    )
    out_specs = (
        P(tokens, tp),
        P(tokens, None),
        P(tokens, tp),
        P(fs, tp),
        P(None, tp),
        P(tp),
    )
    return jax.shard_map(
        per_device, mesh=fine, in_specs=in_specs, out_specs=out_specs, check_vma=False
    )
```

time: 243 us -> 182 us (0.75)
  waiting for transfers between devices: 161 us -> 63.7 us
  blocking collectives: 0 us -> 51.6 us
  between operations: 14.3 us -> 1 us
  starting transfers between devices: 39.6 us -> 30 us
  other arithmetic: 7.85 us -> 14.9 us
    all_to_all x4 -> x6, waiting for transfers between devices: 161 us -> 63.7 us  [the longest x3 36.5 us: exchange(): return lax.all_to_all(blocks, axis, 0, 0, tiled=True)]
    all_to_all x0 -> x4, blocking collectives: none -> 51.6 us  [the longest x2 30.9 us: copies_to(): return lax.all_to_all(copies, axis, 0, 0, tiled=True)]
    all_to_all x4 -> x6, starting transfers between devices: 39.6 us -> 30 us  [the longest x3 17 us: copies_to(): return lax.all_to_all(copies, axis, 0, 0, tiled=True)]
    broadcast_in_dim x3 -> x9, local copies, waits for them, and re-layouts: 3.86 us -> 8.32 us  [the longest x5 6.71 us: copies_to(): copies = jnp.broadcast_to(block, (size, *block.shape))]
    reduce_sum x3 -> x5, other arithmetic: 1.57 us -> 5.69 us  [summed(): return jnp.sum(blocks.astype(jnp.float32), axis=0)]
    unnamed x25 -> x23, local copies, waits for them, and re-layouts: 4.61 us -> 1.71 us
    dot_general x3, matrix products: 5.61 us -> 2.99 us  [the longest x1 1.01 us: per_device(): lax.dot_general(grad_up, gathered, (((1,), (1,)), ((), ())), preferred_el...]
  transfers between devices with their start and end apart: 5 -> 6, of which waited for: 4 -> 6; matrix products, arithmetic and copies ran while one was open for 5% -> 7% of each run, Pallas kernels for 0% -> 0%
where the time goes in v1:
time: 182 us; the launch traced here: 179 us
  waiting for transfers between devices  63.7 us (35%)
  blocking collectives  51.6 us (28%)
  starting transfers between devices  30 us (16%)
  other arithmetic  14.9 us (8%)
  local copies, waits for them, and re-layouts  12.5 us (7%)
  matrix products  5.14 us (3%)
    all_to_all x3, waiting for transfers between devices, exchange(): return lax.all_to_all(blocks, axis, 0, 0, tiled=True)  36.5 us
    all_to_all x2, blocking collectives, copies_to(): return lax.all_to_all(copies, axis, 0, 0, tiled=True)  30.9 us
    all_to_all x3, waiting for transfers between devices, copies_to(): return lax.all_to_all(copies, axis, 0, 0, tiled=True)  27.2 us
    all_to_all x2, blocking collectives, exchange(): return lax.all_to_all(blocks, axis, 0, 0, tiled=True)  20.7 us
    all_to_all x3, starting transfers between devices, copies_to(): return lax.all_to_all(copies, axis, 0, 0, tiled=True)  17 us
    all_to_all x3, starting transfers between devices, exchange(): return lax.all_to_all(blocks, axis, 0, 0, tiled=True)  13 us
    broadcast_in_dim x5, local copies, waits for them, and re-layouts, copies_to(): copies = jnp.broadcast_to(block, (size, *block.shape))  6.71 us
    reduce_sum x5, other arithmetic, summed(): return jnp.sum(blocks.astype(jnp.float32), axis=0)  5.69 us
  transfers between devices with their start and end apart: 6, of which 6 were waited for; matrix products, arithmetic and copies ran while one was open for 7% of the time, Pallas kernels for 0%

profile of v1, /device:TPU:1, one launch (start us, length us, event | category | flops | bytes accessed | tf_op | source)
XLA Modules:
  0.0 179.0 jit_solution(11645867407816321327)
XLA Ops:
  0.6 0.0 copy-start
  0.6 0.9 broadcast_in_dim.99
  1.6 15.8 %all_to_all.50 = bf16[2,64,384]{2,1,0:T(8,128)(2,1)S(1)} all-to-all(bf16[2,64,384]{2,1,0:T(8,128)(2,1)S(1)} %broadcast_in_dim.99), channel_id=1, replica_groups=mesh['zh'=2,'zm'=2,'zq'=4,'y'=4,'x'=4,'c'=2] {'zm'}, dimensions={0} | all-to-all | bytes 196608 | tf_op jit(solution)/shard_map/all_to_all | solution.py:13
  17.5 15.1 %all_to_all.51 = bf16[4,2,64,384]{3,2,1,0:T(8,128)(2,1)S(1)} all-to-all(bf16[4,2,64,384]{3,2,1,0:T(8,128)(2,1)S(1)} %broadcast_in_dim.100), channel_id=1, replica_groups=mesh['zh'=2,'zm'=2,'zq'=4,'y'=4,'x'=4,'c'=2] {'zq'}, dimensions={0} | all-to-all | bytes 786432 | tf_op jit(solution)/shard_map/all_to_all | solution.py:13
  32.6 1.4 broadcast_in_dim.101
  33.9 0.0 copy-start.7
  34.0 4.3 %all-to-all-start.2 = ((bf16[4,4,2,64,384]{4,3,1,2,0:T(8,128)(2,1)}), bf16[4,4,2,64,384]{4,3,1,2,0:T(8,128)(2,1)S(1)}, u32[]{:S(2)}, u32[]{:S(2)}) async-start(bf16[4,4,2,64,384]{4,3,1,2,0:T(8,128)(2,1)} %broadcast_in_dim.101), calls=%async_computation.2 | async-start | bytes 3145728 | tf_op jit(solution)/shard_map/all_to_all | solution.py:13
  38.3 0.0 copy-done.7
  38.3 17.4 %all-to-all-done.2 = bf16[4,4,2,64,384]{4,3,1,2,0:T(8,128)(2,1)S(1)} async-done(((bf16[4,4,2,64,384]{4,3,1,2,0:T(8,128)(2,1)}), bf16[4,4,2,64,384]{4,3,1,2,0:T(8,128)(2,1)S(1)}, u32[]{:S(2)}, u32[]{:S(2)}) %all-to-all-start.2) | async-done | bytes 1572896 | tf_op jit(solution)/shard_map/all_to_all | solution.py:13
  55.7 0.2 copy.24
  55.9 0.0 copy-done
  55.9 0.0 copy-start.10
  56.0 1.0 fusion.1
  57.0 0.4 copy-done.10
  57.4 0.0 copy-start.1
  57.4 0.0 copy-start.4
  57.4 0.0 copy-start.5
  57.4 0.0 copy-start.8
  57.4 1.0 fusion.2
  58.4 0.0 copy-done.1
  58.4 0.0 copy-done.4
  58.4 0.1 copy-done.5
  58.5 0.0 copy-done.8
  58.5 2.2 %multiply_reduce_fusion.2 = (f32[384]{0:T(512)S(1)}, f32[384]{0:T(512)S(1)}, f32[384]{0:T(512)S(1)}, f32[384]{0:T(512)S(1)}, f32[384,384]{1,0:T(8,128)S(1)}, /*index=5*/f32[384,384]{1,0:T(8,128)}, bf16[384,384]{1,0:T(8,128)(2,1)}) fusion(f32[382,384]{1,0:T(8,128)S(1)} %bitcast.35, pred[384]{0:T(512)(128)(4,1)S(1)} %fusion.14, f32[384,384]{1,0:T(8,128)S(1)} %fusion.1, ...), kind=kLoop, calls=%fused_computation.19 | loop fusion | flops 6339072 | bytes 5902464 | tf_op jit(solution)/shard_map/reduce_sum | solution.py:117
  60.8 0.3 add_convert_fusion
  61.1 0.0 copy-start.2
  61.1 1.0 convolution_convert_fusion
  62.1 0.0 copy-done.2
  62.1 8.8 %all_to_all.52 = bf16[2,192,2048]{2,1,0:T(8,128)(2,1)S(1)} all-to-all(bf16[2,192,2048]{2,1,0:T(8,128)(2,1)S(1)} %bitcast.34), channel_id=1, replica_groups=mesh['zh'=2,'zm'=2,'zq'=4,'y'=4,'x'=4,'c'=2] {'c'}, dimensions={0} | all-to-all | bytes 3145728 | tf_op jit(solution)/shard_map/all_to_all | solution.py:17
  70.9 1.4 reduce_sum.87
  72.4 0.0 copy-start.3
  72.4 4.3 %all-to-all-start.4 = ((bf16[4,48,2048]{2,1,0:T(8,128)(2,1)}), bf16[4,48,2048]{2,1,0:T(8,128)(2,1)}, u32[]{:S(2)}, u32[]{:S(2)}) async-start(bf16[4,48,2048]{2,1,0:T(8,128)(2,1)} %bitcast.39), calls=%async_computation.4 | async-start | bytes 1572864 | tf_op jit(solution)/shard_map/all_to_all | solution.py:17
  76.7 0.0 copy-done.3
  76.7 2.2 %fusion = bf16[2048,384]{0,1:T(8,128)(2,1)} fusion(bf16[384,384]{1,0:T(8,128)(2,1)S(1)} %copy-done.3, bf16[384,2048]{1,0:T(8,128)(2,1)S(1)} %copy-done), kind=kOutput, calls=%fused_computation.3 | convolution fusion | flops 605552640 | bytes 3440640 | tf_op jit(solution)/shard_map/dot_general | solution.py:127
  78.9 1.9 %copy.25 = bf16[2048,384]{1,0:T(8,128)(2,1)S(1)} copy(bf16[2048,384]{0,1:T(8,128)(2,1)} %fusion) | data formatting | bytes 3145728 | tf_op jit(solution)/shard_map/convert_element_type | solution.py:131
  80.7 0.2 copy.26
  81.0 1.3 pad_maximum_fusion
  82.3 6.3 %all-to-all-done.4 = bf16[4,48,2048]{2,1,0:T(8,128)(2,1)} async-done(((bf16[4,48,2048]{2,1,0:T(8,128)(2,1)}), bf16[4,48,2048]{2,1,0:T(8,128)(2,1)}, u32[]{:S(2)}, u32[]{:S(2)}) %all-to-all-start.4) | async-done | bytes 786464 | tf_op jit(solution)/shard_map/all_to_all | solution.py:17
  88.6 3.6 %all-to-all-start.7 = ((bf16[4,520,384]{2,1,0:T(8,128)(2,1)}), bf16[4,520,384]{2,1,0:T(8,128)(2,1)S(1)}, u32[]{:S(2)}, u32[]{:S(2)}) async-start(bf16[4,520,384]{2,1,0:T(8,128)(2,1)} %pad_maximum_fusion), calls=%async_computation.7 | async-start | bytes 3194880 | tf_op jit(solution)/shard_map/all_to_all | solution.py:17
  92.2 2.0 %reduce_sum.88 = bf16[48,2048]{1,0:T(8,128)(2,1)} reduce(bf16[4,48,2048]{2,1,0:T(8,128)(2,1)} %all-to-all-done.4, bf16[]{:T(256)} %constant.36.clone.1), dimensions={0}, to_apply=%region_1.2 | reduce | flops 294912 | bytes 983042 | tf_op jit(solution)/shard_map/reduce_sum | solution.py:21
  94.2 17.7 %all-to-all-done.7 = bf16[4,520,384]{2,1,0:T(8,128)(2,1)S(1)} async-done(((bf16[4,520,384]{2,1,0:T(8,128)(2,1)}), bf16[4,520,384]{2,1,0:T(8,128)(2,1)S(1)}, u32[]{:S(2)}, u32[]{:S(2)}) %all-to-all-start.7) | async-done | bytes 1597472 | tf_op jit(solution)/shard_map/all_to_all | solution.py:17
  111.9 1.9 %broadcast_in_dim.107 = bf16[4,48,2048]{2,1,0:T(8,128)(2,1)} broadcast(bf16[48,2048]{1,0:T(8,128)(2,1)} %reduce_sum.88), dimensions={1,2} | broadcast | bytes 983040 | tf_op jit(solution)/shard_map/broadcast_in_dim | solution.py:12
  113.7 4.2 %all-to-all-start.5 = ((bf16[4,48,2048]{2,1,0:T(8,128)(2,1)}), bf16[4,48,2048]{2,1,0:T(8,128)(2,1)}, u32[]{:S(2)}, u32[]{:S(2)}) async-start(bf16[4,48,2048]{2,1,0:T(8,128)(2,1)} %broadcast_in_dim.107), calls=%async_computation.5 | async-start | bytes 1572864 | tf_op jit(solution)/shard_map/all_to_all | solution.py:13
  117.9 0.2 convert_reduce_fusion
  118.3 9.5 %all-to-all-done.5 = bf16[4,48,2048]{2,1,0:T(8,128)(2,1)} async-done(((bf16[4,48,2048]{2,1,0:T(8,128)(2,1)}), bf16[4,48,2048]{2,1,0:T(8,128)(2,1)}, u32[]{:S(2)}, u32[]{:S(2)}) %all-to-all-start.5) | async-done | bytes 786464 | tf_op jit(solution)/shard_map/all_to_all | solution.py:13
  127.9 11.9 %all_to_all.53 = bf16[4,136,384]{2,1,0:T(8,128)(2,1)} all-to-all(bf16[4,136,384]{2,1,0:T(8,128)(2,1)S(1)} %pad_maximum_fusion.1), channel_id=1, replica_groups=mesh['zh'=2,'zm'=2,'zq'=4,'y'=4,'x'=4,'c'=2] {'zq'}, dimensions={0} | all-to-all | bytes 835584 | tf_op jit(solution)/shard_map/all_to_all | solution.py:17
  139.8 2.5 %broadcast_in_dim.108 = bf16[2,192,2048]{2,1,0:T(8,128)(2,1)} broadcast(bf16[192,2048]{1,0:T(8,128)(2,1)} %bitcast.5), dimensions={1,2} | broadcast | bytes 2359296 | tf_op jit(solution)/shard_map/broadcast_in_dim | solution.py:12
  142.3 8.5 %all-to-all-start.6 = ((bf16[2,192,2048]{2,1,0:T(8,128)(2,1)}), bf16[2,192,2048]{2,1,0:T(8,128)(2,1)S(1)}, u32[]{:S(2)}, u32[]{:S(2)}) async-start(bf16[2,192,2048]{2,1,0:T(8,128)(2,1)} %broadcast_in_dim.108), calls=%async_computation.6 | async-start | bytes 3145728 | tf_op jit(solution)/shard_map/all_to_all | solution.py:13
  150.8 1.1 convert_reduce_fusion.1
  151.9 0.0 copy-start.6
  151.9 0.0 copy-start.9
  152.0 0.7 pad_maximum_fusion.2
  152.6 0.3 all-to-all-done.6
  152.9 1.6 broadcast_in_dim.112
  154.5 5.1 %all-to-all-start.9 = ((bf16[4,72,384]{2,1,0:T(8,128)(2,1)}), bf16[4,72,384]{2,1,0:T(8,128)(2,1)}, u32[]{:S(2)}, u32[]{:S(2)}) async-start(bf16[4,72,384]{2,1,0:T(8,128)(2,1)} %bitcast.41), calls=%async_computation.9 | async-start | bytes 442368 | tf_op jit(solution)/shard_map/all_to_all | solution.py:17
  159.6 1.9 %fusion.6 = bf16[384,384]{1,0:T(8,128)(2,1)} fusion(f32[384,384]{1,0:T(8,128)} %get-tuple-element.18, bf16[384,384]{1,0:T(8,128)(2,1)S(1)} %copy-done.1), kind=kLoop, calls=%fused_computation.16 | loop fusion | flops 1032192 | bytes 1179648 | tf_op jit(solution)/shard_map/convert_element_type | solution.py:98
  161.6 12.5 %all-to-all-done.9 = bf16[4,72,384]{2,1,0:T(8,128)(2,1)} async-done(((bf16[4,72,384]{2,1,0:T(8,128)(2,1)}), bf16[4,72,384]{2,1,0:T(8,128)(2,1)}, u32[]{:S(2)}, u32[]{:S(2)}) %all-to-all-start.9) | async-done | bytes 221216 | tf_op jit(solution)/shard_map/all_to_all | solution.py:17
  174.1 1.0 convert_reduce_fusion.2
  175.1 1.6 slice_add_fusion
  176.7 0.0 copy-done.6
  176.7 0.6 slice_add_fusion.1
  177.3 0.0 copy-done.9
  177.3 0.6 add.130
  177.9 1.1 copy.28
  (27 shorter events, 0.4 us)
Async XLA Ops:
  0.6 55.3 %copy-start = (bf16[384,2048]{1,0:T(8,128)(2,1)S(1)}, bf16[384,2048]{1,0:T(8,128)(2,1)}, u32[]{:S(2)}) copy-start(bf16[384,2048]{1,0:T(8,128)(2,1)} %param.13) | copy-start | bytes 4718596
  33.9 4.4 %copy-start.7 = (f32[3,384]{1,0:T(4,128)S(1)}, f32[3,384]{1,0:T(4,128)}, u32[]{:S(2)}) copy-start(f32[3,384]{1,0:T(4,128)} %param.17) | copy-start | bytes 13828
  34.0 21.8 %all-to-all-start.2 = ((bf16[4,4,2,64,384]{4,3,1,2,0:T(8,128)(2,1)}), bf16[4,4,2,64,384]{4,3,1,2,0:T(8,128)(2,1)S(1)}, u32[]{:S(2)}, u32[]{:S(2)}) async-start(bf16[4,4,2,64,384]{4,3,1,2,0:T(8,128)(2,1)} %broadcast_in_dim.101), calls=%async_computation.2 | async-start | bytes 3145728 | tf_op jit(solution)/shard_map/all_to_all | solution.py:13
  55.9 1.4 copy-start.10
  57.4 1.0 copy-start.1
  57.4 1.0 copy-start.4
  57.4 1.1 copy-start.5
  57.4 1.1 copy-start.8
  61.1 1.0 copy-start.2
  72.4 4.3 %copy-start.3 = (bf16[384,384]{1,0:T(8,128)(2,1)S(1)}, bf16[384,384]{1,0:T(8,128)(2,1)}, u32[]{:S(2)}) copy-start(bf16[384,384]{1,0:T(8,128)(2,1)} %copy-done.2) | copy-start | bytes 884740
  72.4 16.3 %all-to-all-start.4 = ((bf16[4,48,2048]{2,1,0:T(8,128)(2,1)}), bf16[4,48,2048]{2,1,0:T(8,128)(2,1)}, u32[]{:S(2)}, u32[]{:S(2)}) async-start(bf16[4,48,2048]{2,1,0:T(8,128)(2,1)} %bitcast.39), calls=%async_computation.4 | async-start | bytes 1572864 | tf_op jit(solution)/shard_map/all_to_all | solution.py:17
  88.6 23.2 %all-to-all-start.7 = ((bf16[4,520,384]{2,1,0:T(8,128)(2,1)}), bf16[4,520,384]{2,1,0:T(8,128)(2,1)S(1)}, u32[]{:S(2)}, u32[]{:S(2)}) async-start(bf16[4,520,384]{2,1,0:T(8,128)(2,1)} %pad_maximum_fusion), calls=%async_computation.7 | async-start | bytes 3194880 | tf_op jit(solution)/shard_map/all_to_all | solution.py:17
  113.7 14.1 %all-to-all-start.5 = ((bf16[4,48,2048]{2,1,0:T(8,128)(2,1)}), bf16[4,48,2048]{2,1,0:T(8,128)(2,1)}, u32[]{:S(2)}, u32[]{:S(2)}) async-start(bf16[4,48,2048]{2,1,0:T(8,128)(2,1)} %broadcast_in_dim.107), calls=%async_computation.5 | async-start | bytes 1572864 | tf_op jit(solution)/shard_map/all_to_all | solution.py:13
  142.3 10.7 %all-to-all-start.6 = ((bf16[2,192,2048]{2,1,0:T(8,128)(2,1)}), bf16[2,192,2048]{2,1,0:T(8,128)(2,1)S(1)}, u32[]{:S(2)}, u32[]{:S(2)}) async-start(bf16[2,192,2048]{2,1,0:T(8,128)(2,1)} %broadcast_in_dim.108), calls=%async_computation.6 | async-start | bytes 3145728 | tf_op jit(solution)/shard_map/all_to_all | solution.py:13
  151.9 24.8 %copy-start.6 = (f32[3,384]{1,0:T(4,128)S(1)}, f32[3,384]{1,0:T(4,128)}, u32[]{:S(2)}) copy-start(f32[3,384]{1,0:T(4,128)} %param.20) | copy-start | bytes 13828
  151.9 25.4 %copy-start.9 = (f32[384]{0:T(512)S(1)}, f32[384]{0:T(512)}, u32[]{:S(2)}) copy-start(f32[384]{0:T(512)} %param.21) | copy-start | bytes 4612
  154.5 19.6 %all-to-all-start.9 = ((bf16[4,72,384]{2,1,0:T(8,128)(2,1)}), bf16[4,72,384]{2,1,0:T(8,128)(2,1)}, u32[]{:S(2)}, u32[]{:S(2)}) async-start(bf16[4,72,384]{2,1,0:T(8,128)(2,1)} %bitcast.41), calls=%async_computation.9 | async-start | bytes 442368 | tf_op jit(solution)/shard_map/all_to_all | solution.py:17

commit v2 on v1

--- a/solution.py
+++ b/solution.py
@@ -1,6 +1,8 @@
 import jax
 import jax.numpy as jnp
 from jax import lax
+from jax.experimental import pallas as pl
+from jax.experimental.pallas import tpu as pltpu
 from jax.sharding import Mesh
 from jax.sharding import PartitionSpec as P
 
@@ -15,6 +17,44 @@
 
 def exchange(blocks, axis):
     return lax.all_to_all(blocks, axis, 0, 0, tiled=True)
+
+
+def send_on(block, axis, shift):
+    size = lax.axis_size(axis)
+    return lax.ppermute(block, axis, [(i, (i + shift) % size) for i in range(size)])
+
+
+def put_in_order(own, other, n_c):
+    n_x = own.shape[0]
+
+    def body(own_ref, other_ref, out_ref, sems):
+        at_x, at_c = lax.axis_index("x"), lax.axis_index("c")
+        moves = []
+        for k in range(n_x):
+            spot = (at_x + n_x - k) % n_x
+            moves.append(
+                pltpu.make_async_copy(own_ref.at[k], out_ref.at[at_c * n_x + spot], sems.at[k])
+            )
+            moves.append(
+                pltpu.make_async_copy(
+                    other_ref.at[k], out_ref.at[(1 - at_c) * n_x + spot], sems.at[n_x + k]
+                )
+            )
+        for move in moves:
+            move.start()
+        for move in moves:
+            move.wait()
+
+    return pl.pallas_call(
+        body,
+        out_shape=jax.ShapeDtypeStruct((n_c * n_x, *own.shape[1:]), own.dtype),
+        in_specs=[pl.BlockSpec(memory_space=pl.ANY)] * 2,
+        out_specs=pl.BlockSpec(memory_space=pl.ANY),
+        scratch_shapes=[pltpu.SemaphoreType.DMA((2 * n_x,))],
+        cost_estimate=pl.CostEstimate(
+            flops=0, bytes_accessed=4 * own.size * own.dtype.itemsize, transcendentals=0
+        ),
+    )(own, other)
 
 
 def summed(blocks):
@@ -131,21 +171,37 @@
     ).astype(jnp.bfloat16)
     by_y = jnp.transpose(grad_w.reshape(n_zm, n_zq, n_y, shard_rows, units), (2, 1, 0, 3, 4))
     by_y = with_small(by_y.reshape(n_y, n_zq * n_zm * shard_rows, units), small)
-    part, small = split_small(summed(exchange(by_y, "y")))
+    by_y, grad_up, x_next = lax.optimization_barrier((by_y, grad_up, x_next))
+    from_y = exchange(by_y, "y")
+
+    at_x, at_c = lax.axis_index("x"), lax.axis_index("c")
+    block_rows = row_count // (n_x * n_c)
+
+    def partial_half(which):
+        rows = lax.dynamic_slice_in_dim(grad_up, which * n_x * block_rows, n_x * block_rows, 0)
+        turned = lax.dynamic_slice_in_dim(
+            jnp.concatenate([rows, rows], axis=0), at_x * block_rows, n_x * block_rows, 0
+        )
+        return lax.dot_general(
+            turned, gathered, (((1,), (1,)), ((), ())), preferred_element_type=jnp.float32
+        )
+
+    from_core = send_on(partial_half(1 - at_c).astype(jnp.bfloat16), "c", 1)
+    half = (partial_half(at_c) + from_core.astype(jnp.float32)).astype(jnp.bfloat16)
+    half = half.reshape(n_x, block_rows, width)
+    arrived = [half[0]] + [send_on(half[k], "x", k) for k in range(1, n_x)]
+    from_y, *arrived = lax.optimization_barrier((from_y, *arrived))
+    eighth = sum(block.astype(jnp.float32) for block in arrived).astype(jnp.bfloat16)
+    half = jnp.stack([eighth] + [send_on(eighth, "x", k) for k in range(1, n_x)])
+    grad_input = put_in_order(half, send_on(half, "c", 1), n_c).reshape(row_count, width)
+
+    part, small = split_small(summed(from_y))
     by_q = part.astype(jnp.bfloat16).reshape(n_zq, n_zm * shard_rows, units)
     part, small = split_small(summed(exchange(with_small(by_q, small), "zq")))
     by_half = part.astype(jnp.bfloat16).reshape(n_zm, shard_rows, units)
     by_half = with_small(by_half, small)
     by_half = jnp.broadcast_to(by_half, (n_zh, *by_half.shape)).reshape(-1, *by_half.shape[1:])
     grad_rows, small = split_small(summed(exchange(by_half, ("zh", "zm"))))
-
-    partial_input = lax.dot_general(
-        grad_up, gathered, (((1,), (1,)), ((), ())), preferred_element_type=jnp.float32
-    ).astype(jnp.bfloat16)
-    half = summed(exchange(partial_input.reshape(n_c, -1, width), "c")).astype(jnp.bfloat16)
-    eighth = summed(exchange(half.reshape(n_x, -1, width), "x")).astype(jnp.bfloat16)
-    half = copies_to(eighth, "x", n_x).reshape(-1, width)
-    grad_input = copies_to(half, "c", n_c).reshape(-1, width)
 
     up_next = jnp.dot(x_next, gathered, preferred_element_type=jnp.float32).astype(jnp.bfloat16)
     gate_next = convolve(up_next, conv_taps, conv_bias, position)

time: 182 us -> 196 us (1.077)
  Pallas kernels: 0 us -> 48.8 us
  waiting for transfers between devices: 63.7 us -> 35.4 us
  blocking collectives: 51.6 us -> 30.9 us
  starting transfers between devices: 30 us -> 46.4 us
  matrix products: 5.14 us -> 9.16 us
  other arithmetic: 14.9 us -> 12.3 us
    pallas_call x0 -> x1, Pallas kernels: none -> 48.8 us  [put_in_order(): pl.pallas_call(body, out_shape=jax.ShapeDtypeStruct((n_c * n_x, *own.shap...]
    all_to_all x3, waiting for transfers between devices: 36.5 us -> 0.17 us  [exchange(): return lax.all_to_all(blocks, axis, 0, 0, tiled=True)]
    ppermute x0 -> x8, starting transfers between devices: none -> 27.8 us  [send_on(): lax.ppermute(block, axis, [(i, (i + shift) % size) for i in range(size)])]
    all_to_all x2 -> x0, blocking collectives: 20.7 us -> none  [exchange(): return lax.all_to_all(blocks, axis, 0, 0, tiled=True)]
    ppermute x0 -> x8, waiting for transfers between devices: none -> 17.7 us  [send_on(): lax.ppermute(block, axis, [(i, (i + shift) % size) for i in range(size)])]
    all_to_all x3 -> x1, starting transfers between devices: 17 us -> 4.47 us  [copies_to(): return lax.all_to_all(copies, axis, 0, 0, tiled=True)]
    all_to_all x3 -> x1, waiting for transfers between devices: 27.2 us -> 17.5 us  [copies_to(): return lax.all_to_all(copies, axis, 0, 0, tiled=True)]
    broadcast_in_dim x5 -> x3, local copies, waits for them, and re-layouts: 6.71 us -> 2.34 us  [copies_to(): copies = jnp.broadcast_to(block, (size, *block.shape))]
  transfers between devices with their start and end apart: 6 -> 12, of which waited for: 6 -> 7; matrix products, arithmetic and copies ran while one was open for 7% -> 5% of each run, Pallas kernels for 0% -> 25%
where the time goes in v2:
time: 196 us; the launch traced here: 195 us
  Pallas kernels  48.8 us (25%)
  starting transfers between devices  46.4 us (24%)
  waiting for transfers between devices  35.4 us (18%)
  blocking collectives  30.9 us (16%)
  other arithmetic  12.3 us (6%)
  local copies, waits for them, and re-layouts  10.6 us (5%)
  matrix products  9.16 us (5%)
    pallas_call x1, Pallas kernels, put_in_order(): pl.pallas_call(body, out_shape=jax.ShapeDtypeStruct((n_c * n_x, *own.shap...  48.8 us
    all_to_all x2, blocking collectives, copies_to(): return lax.all_to_all(copies, axis, 0, 0, tiled=True)  30.9 us
    ppermute x8, starting transfers between devices, send_on(): lax.ppermute(block, axis, [(i, (i + shift) % size) for i in range(size)])  27.8 us
    ppermute x8, waiting for transfers between devices, send_on(): lax.ppermute(block, axis, [(i, (i + shift) % size) for i in range(size)])  17.7 us
    all_to_all x1, waiting for transfers between devices, copies_to(): return lax.all_to_all(copies, axis, 0, 0, tiled=True)  17.5 us
    all_to_all x3, starting transfers between devices, exchange(): return lax.all_to_all(blocks, axis, 0, 0, tiled=True)  14.1 us
    all_to_all x1, starting transfers between devices, copies_to(): return lax.all_to_all(copies, axis, 0, 0, tiled=True)  4.47 us
  transfers between devices with their start and end apart: 12, of which 7 were waited for; matrix products, arithmetic and copies ran while one was open for 5% of the time, Pallas kernels for 25%

profile of v2, /device:TPU:1, one launch (start us, length us, event | category | flops | bytes accessed | tf_op | source)
XLA Modules:
  0.0 194.8 jit_solution(1673530489764940176)
XLA Ops:
  0.6 0.0 copy-start
  0.6 0.9 broadcast_in_dim.94
  1.6 15.8 %all_to_all.30 = bf16[2,64,384]{2,1,0:T(8,128)(2,1)S(1)} all-to-all(bf16[2,64,384]{2,1,0:T(8,128)(2,1)S(1)} %broadcast_in_dim.94), channel_id=1, replica_groups=mesh['zh'=2,'zm'=2,'zq'=4,'y'=4,'x'=4,'c'=2] {'zm'}, dimensions={0} | all-to-all | bytes 196608 | tf_op jit(solution)/shard_map/all_to_all | solution.py:15
  17.5 15.1 %all_to_all.31 = bf16[4,2,64,384]{3,2,1,0:T(8,128)(2,1)S(1)} all-to-all(bf16[4,2,64,384]{3,2,1,0:T(8,128)(2,1)S(1)} %broadcast_in_dim.95), channel_id=1, replica_groups=mesh['zh'=2,'zm'=2,'zq'=4,'y'=4,'x'=4,'c'=2] {'zq'}, dimensions={0} | all-to-all | bytes 786432 | tf_op jit(solution)/shard_map/all_to_all | solution.py:15
  32.6 1.4 broadcast_in_dim.96
  34.0 4.5 %all-to-all-start.2 = ((bf16[4,4,2,64,384]{4,3,1,2,0:T(8,128)(2,1)}), bf16[4,4,2,64,384]{4,3,1,2,0:T(8,128)(2,1)}, u32[]{:S(2)}, u32[]{:S(2)}) async-start(bf16[4,4,2,64,384]{4,3,1,2,0:T(8,128)(2,1)} %broadcast_in_dim.96), calls=%async_computation.2 | async-start | bytes 3145728 | tf_op jit(solution)/shard_map/all_to_all | solution.py:15
  38.5 0.0 copy-start.9
  38.5 0.0 copy-start.11
  38.5 0.0 copy-start.13
  38.6 17.5 %all-to-all-done.2 = bf16[4,4,2,64,384]{4,3,1,2,0:T(8,128)(2,1)} async-done(((bf16[4,4,2,64,384]{4,3,1,2,0:T(8,128)(2,1)}), bf16[4,4,2,64,384]{4,3,1,2,0:T(8,128)(2,1)}, u32[]{:S(2)}, u32[]{:S(2)}) %all-to-all-start.2) | async-done | bytes 1572896 | tf_op jit(solution)/shard_map/all_to_all | solution.py:15
  56.1 1.6 copy.24
  57.7 0.0 copy-start.1
  57.7 0.0 copy-start.7
  57.7 1.0 fusion.2
  58.7 0.0 copy-start.4
  58.7 1.2 fusion.6
  60.0 0.0 copy-done.11
  60.0 0.6 multiply_reduce_fusion.2
  60.7 0.3 add_convert_fusion.1
  61.0 2.2 %fusion = bf16[2048,384]{0,1:T(8,128)(2,1)} fusion(bf16[384,384]{1,0:T(8,128)(2,1)S(1)} %add_convert_fusion.1, bf16[384,2048]{1,0:T(8,128)(2,1)S(1)} %copy-done), kind=kOutput, calls=%fused_computation.2 | convolution fusion | flops 605552640 | bytes 3440640 | tf_op jit(solution)/shard_map/dot_general | solution.py:167
  63.1 2.6 %copy.25 = bf16[2048,384]{1,0:T(8,128)(2,1)} copy(bf16[2048,384]{0,1:T(8,128)(2,1)} %fusion) | data formatting | bytes 3145728 | tf_op jit(solution)/shard_map/convert_element_type | solution.py:171
  65.7 1.6 copy.26
  67.4 1.3 pad_maximum_fusion
  68.7 0.7 constant_dynamic-slice_fusion.1
  69.4 1.7 convolution_convert_fusion
  71.1 6.1 %collective-permute-start = (bf16[192,2048]{1,0:T(8,128)(2,1)}, bf16[192,2048]{1,0:T(8,128)(2,1)}, u32[]{:S(2)}, u32[]{:S(2)}) collective-permute-start(bf16[192,2048]{1,0:T(8,128)(2,1)} %convolution_convert_fusion), channel_id=1, source_target_pairs={{0,1},{1,0},{2,3},{3,2},{4,5},{5,4},{6,7},{7,6},{8,9},{9,8},{10,11... | collective-permute-start | bytes 2359304 | tf_op jit(solution)/shard_map/ppermute | solution.py:24
  77.2 4.4 %all-to-all-start.3 = ((bf16[4,520,384]{2,1,0:T(8,128)(2,1)}), bf16[4,520,384]{2,1,0:T(8,128)(2,1)}, u32[]{:S(2)}, u32[]{:S(2)}) async-start(bf16[4,520,384]{2,1,0:T(8,128)(2,1)} %pad_maximum_fusion), calls=%async_computation.3 | async-start | bytes 3194880 | tf_op jit(solution)/shard_map/all_to_all | solution.py:19
  81.5 0.0 collective-permute-done
  81.6 1.9 add_convert_fusion
  83.5 0.1 fusion.33
  83.6 4.4 %collective-permute-start.3 = (bf16[48,2048]{1,0:T(8,128)(2,1)S(1)}, bf16[48,2048]{1,0:T(8,128)(2,1)S(1)}, u32[]{:S(2)}, u32[]{:S(2)}) collective-permute-start(bf16[48,2048]{1,0:T(8,128)(2,1)S(1)} %get-tuple-element.36), channel_id=1, source_target_pairs={{0,6},{2,0},{4,2},{6,4},{1,7},{3,1},{5,3},{7,5},{8,14},{10,8},{12,... | collective-permute-start | bytes 589832 | tf_op jit(solution)/shard_map/ppermute | solution.py:24
  88.0 2.5 %collective-permute-start.2 = (bf16[48,2048]{1,0:T(8,128)(2,1)S(1)}, bf16[48,2048]{1,0:T(8,128)(2,1)S(1)}, u32[]{:S(2)}, u32[]{:S(2)}) collective-permute-start(bf16[48,2048]{1,0:T(8,128)(2,1)S(1)} %get-tuple-element.37), channel_id=1, source_target_pairs={{0,4},{2,6},{4,0},{6,2},{1,5},{3,7},{5,1},{7,3},{8,12},{10,14},{12... | collective-permute-start | bytes 589832 | tf_op jit(solution)/shard_map/ppermute | solution.py:24
  90.4 2.5 %collective-permute-start.1 = (bf16[48,2048]{1,0:T(8,128)(2,1)S(1)}, bf16[48,2048]{1,0:T(8,128)(2,1)}, u32[]{:S(2)}, u32[]{:S(2)}) collective-permute-start(bf16[48,2048]{1,0:T(8,128)(2,1)S(1)} %get-tuple-element.38), channel_id=1, source_target_pairs={{0,2},{2,4},{4,6},{6,0},{1,3},{3,5},{5,7},{7,1},{8,10},{10,12},{12... | collective-permute-start | bytes 589832 | tf_op jit(solution)/shard_map/ppermute | solution.py:24
  93.0 3.3 %collective-permute-done.3 = bf16[48,2048]{1,0:T(8,128)(2,1)S(1)} collective-permute-done((bf16[48,2048]{1,0:T(8,128)(2,1)S(1)}, bf16[48,2048]{1,0:T(8,128)(2,1)S(1)}, u32[]{:S(2)}, u32[]{:S(2)}) %collective-permute-start.3) | collective-permute-done | bytes 196640 | tf_op jit(solution)/shard_map/ppermute | solution.py:24
  96.3 1.4 collective-permute-done.2
  97.6 0.7 copy-done.5
  98.3 4.2 %collective-permute-done.1 = bf16[48,2048]{1,0:T(8,128)(2,1)} collective-permute-done((bf16[48,2048]{1,0:T(8,128)(2,1)S(1)}, bf16[48,2048]{1,0:T(8,128)(2,1)}, u32[]{:S(2)}, u32[]{:S(2)}) %collective-permute-start.1) | collective-permute-done | bytes 196640 | tf_op jit(solution)/shard_map/ppermute | solution.py:24
  102.5 0.2 all-to-all-done.3
  102.7 1.8 convert_reduce_fusion
  104.5 0.8 pad_maximum_fusion.2
  105.3 4.1 %all-to-all-start.4 = ((bf16[4,136,384]{2,1,0:T(8,128)(2,1)}), bf16[4,136,384]{2,1,0:T(8,128)(2,1)}, u32[]{:S(2)}, u32[]{:S(2)}) async-start(bf16[4,136,384]{2,1,0:T(8,128)(2,1)} %pad_maximum_fusion.2), calls=%async_computation.4 | async-start | bytes 835584 | tf_op jit(solution)/shard_map/all_to_all | solution.py:19
  109.4 1.1 add_convert_fusion.2
  110.6 4.4 %collective-permute-start.6 = (bf16[48,2048]{1,0:T(8,128)(2,1)S(1)}, bf16[48,2048]{1,0:T(8,128)(2,1)S(1)}, u32[]{:S(2)}, u32[]{:S(2)}) collective-permute-start(bf16[48,2048]{1,0:T(8,128)(2,1)S(1)} %add_convert_fusion.2), channel_id=1, source_target_pairs={{0,6},{2,0},{4,2},{6,4},{1,7},{3,1},{5,3},{7,5},{8,14},{10,8},{12,... | collective-permute-start | bytes 589832 | tf_op jit(solution)/shard_map/ppermute | solution.py:24
  115.0 2.4 %collective-permute-start.5 = (bf16[48,2048]{1,0:T(8,128)(2,1)S(1)}, bf16[48,2048]{1,0:T(8,128)(2,1)S(1)}, u32[]{:S(2)}, u32[]{:S(2)}) collective-permute-start(bf16[48,2048]{1,0:T(8,128)(2,1)S(1)} %add_convert_fusion.2), channel_id=1, source_target_pairs={{0,4},{2,6},{4,0},{6,2},{1,5},{3,7},{5,1},{7,3},{8,12},{10,14},{12... | collective-permute-start | bytes 589832 | tf_op jit(solution)/shard_map/ppermute | solution.py:24
  117.4 2.5 %collective-permute-start.4 = (bf16[48,2048]{1,0:T(8,128)(2,1)S(1)}, bf16[48,2048]{1,0:T(8,128)(2,1)S(1)}, u32[]{:S(2)}, u32[]{:S(2)}) collective-permute-start(bf16[48,2048]{1,0:T(8,128)(2,1)S(1)} %add_convert_fusion.2), channel_id=1, source_target_pairs={{0,2},{2,4},{4,6},{6,0},{1,3},{3,5},{5,7},{7,1},{8,10},{10,12},{12... | collective-permute-start | bytes 589832 | tf_op jit(solution)/shard_map/ppermute | solution.py:24
  119.9 0.0 collective-permute-done.6
  120.0 3.7 %collective-permute-done.5 = bf16[48,2048]{1,0:T(8,128)(2,1)S(1)} collective-permute-done((bf16[48,2048]{1,0:T(8,128)(2,1)S(1)}, bf16[48,2048]{1,0:T(8,128)(2,1)S(1)}, u32[]{:S(2)}, u32[]{:S(2)}) %collective-permute-start.5) | collective-permute-done | bytes 196640 | tf_op jit(solution)/shard_map/ppermute | solution.py:24
  123.7 5.1 %collective-permute-done.4 = bf16[48,2048]{1,0:T(8,128)(2,1)S(1)} collective-permute-done((bf16[48,2048]{1,0:T(8,128)(2,1)S(1)}, bf16[48,2048]{1,0:T(8,128)(2,1)S(1)}, u32[]{:S(2)}, u32[]{:S(2)}) %collective-permute-start.4) | collective-permute-done | bytes 196640 | tf_op jit(solution)/shard_map/ppermute | solution.py:24
  128.8 1.0 pad_maximum_fusion.1.own_ref
  129.8 3.0 %collective-permute-start.7 = (bf16[4,48,2048]{2,1,0:T(8,128)(2,1)}, bf16[4,48,2048]{2,1,0:T(8,128)(2,1)}, u32[]{:S(2)}, u32[]{:S(2)}) collective-permute-start(bf16[4,48,2048]{2,1,0:T(8,128)(2,1)} %pad_maximum_fusion.1.own_ref), channel_id=1, source_target_pairs={{0,1},{1,0},{2,3},{3,2},{4,5},{5,4},{6,7},{7,6},{8,9},{9,8},{10,11... | collective-permute-start | bytes 2359304 | tf_op jit(solution)/shard_map/ppermute | solution.py:24
  132.8 0.0 all-to-all-done.4
  132.8 1.1 convert_reduce_fusion.1
  134.0 0.7 broadcast_in_dim.104
  134.7 5.7 %all-to-all-start.5 = ((bf16[4,72,384]{2,1,0:T(8,128)(2,1)}), bf16[4,72,384]{2,1,0:T(8,128)(2,1)S(1)}, u32[]{:S(2)}, u32[]{:S(2)}) async-start(bf16[4,72,384]{2,1,0:T(8,128)(2,1)} %bitcast.43), calls=%async_computation.5 | async-start | bytes 442368 | tf_op jit(solution)/shard_map/all_to_all | solution.py:19
  140.3 0.0 copy-start.14
  140.3 2.4 %fusion.1 = f32[384,384]{1,0:T(8,128)S(1)} fusion(bf16[384,2048]{1,0:T(8,128)(2,1)} %param.11, bf16[2048,384]{1,0:T(8,128)(2,1)S(1)} %bitcast.36), kind=kOutput, calls=%fused_computation.7 | convolution fusion | flops 604274688 | bytes 3735552 | tf_op jit(solution)/shard_map/dot_general | solution.py:206
  142.8 0.0 copy-done.3
  142.8 1.2 multiply_convert_fusion.1
  144.0 0.0 collective-permute-done.7.other_ref
  144.0 48.8 %shard_map.154 = bf16[8,48,2048]{2,1,0:T(8,128)(2,1)} custom-call(bf16[4,48,2048]{2,1,0:T(8,128)(2,1)} %pad_maximum_fusion.1.own_ref, bf16[4,48,2048]{2,1,0:T(8,128)(2,1)} %collective-permute-done.7.other_ref), custom_call_target="tpu_custom_call" | custom-call | bytes 3145728 | tf_op jit(solution)/shard_map/pallas_call | solution.py:48
  192.9 0.0 all-to-all-done.5
  193.0 0.7 slice_add_fusion
  193.6 0.6 slice_add_fusion.1
  194.2 0.6 add.159
  (50 shorter events, 0.5 us)
Async XLA Ops:
  0.6 57.1 %copy-start = (bf16[384,2048]{1,0:T(8,128)(2,1)S(1)}, bf16[384,2048]{1,0:T(8,128)(2,1)}, u32[]{:S(2)}) copy-start(bf16[384,2048]{1,0:T(8,128)(2,1)} %param.13) | copy-start | bytes 4718596
  33.9 4.6 %copy-start.15 = (f32[3,384]{1,0:T(4,128)S(1)}, f32[3,384]{1,0:T(4,128)}, u32[]{:S(2)}) copy-start(f32[3,384]{1,0:T(4,128)} %param.17) | copy-start | bytes 13828
  34.0 22.1 %all-to-all-start.2 = ((bf16[4,4,2,64,384]{4,3,1,2,0:T(8,128)(2,1)}), bf16[4,4,2,64,384]{4,3,1,2,0:T(8,128)(2,1)}, u32[]{:S(2)}, u32[]{:S(2)}) async-start(bf16[4,4,2,64,384]{4,3,1,2,0:T(8,128)(2,1)} %broadcast_in_dim.96), calls=%async_computation.2 | async-start | bytes 3145728 | tf_op jit(solution)/shard_map/all_to_all | solution.py:15
  38.5 21.5 %copy-start.9 = (pred[384]{0:T(512)(128)(4,1)}, pred[384]{0:T(512)(128)(4,1)S(1)}, u32[]{:S(2)}) copy-start(pred[384]{0:T(512)(128)(4,1)S(1)} %get-tuple-element.49) | copy-start | bytes 1156
  38.5 21.5 %copy-start.11 = (pred[384]{0:T(512)(128)(4,1)}, pred[384]{0:T(512)(128)(4,1)S(1)}, u32[]{:S(2)}) copy-start(pred[384]{0:T(512)(128)(4,1)S(1)} %get-tuple-element.46) | copy-start | bytes 1156
  38.5 21.5 %copy-start.13 = (pred[384]{0:T(512)(128)(4,1)}, pred[384]{0:T(512)(128)(4,1)S(1)}, u32[]{:S(2)}) copy-start(pred[384]{0:T(512)(128)(4,1)S(1)} %get-tuple-element.47) | copy-start | bytes 1156
  57.7 1.0 copy-start.1
  57.7 1.0 copy-start.7
  58.7 1.3 copy-start.4
  71.1 10.5 %copy-start.2 = (bf16[192,384]{1,0:T(8,128)(2,1)S(1)}, bf16[192,384]{1,0:T(8,128)(2,1)}, u32[]{:S(2)}) copy-start(bf16[192,384]{1,0:T(8,128)(2,1)} %get-tuple-element.40) | copy-start | bytes 442372
  71.1 10.5 %collective-permute-start = (bf16[192,2048]{1,0:T(8,128)(2,1)}, bf16[192,2048]{1,0:T(8,128)(2,1)}, u32[]{:S(2)}, u32[]{:S(2)}) collective-permute-start(bf16[192,2048]{1,0:T(8,128)(2,1)} %convolution_convert_fusion), channel_id=1, source_target_pairs={{0,1},{1,0},{2,3},{3,2},{4,5},{5,4},{6,7},{7,6},{8,9},{9,8},{10,11... | collective-permute-start | bytes 2359304 | tf_op jit(solution)/shard_map/ppermute | solution.py:24
  77.2 25.5 %all-to-all-start.3 = ((bf16[4,520,384]{2,1,0:T(8,128)(2,1)}), bf16[4,520,384]{2,1,0:T(8,128)(2,1)}, u32[]{:S(2)}, u32[]{:S(2)}) async-start(bf16[4,520,384]{2,1,0:T(8,128)(2,1)} %pad_maximum_fusion), calls=%async_computation.3 | async-start | bytes 3194880 | tf_op jit(solution)/shard_map/all_to_all | solution.py:19
  83.6 12.7 %collective-permute-start.3 = (bf16[48,2048]{1,0:T(8,128)(2,1)S(1)}, bf16[48,2048]{1,0:T(8,128)(2,1)S(1)}, u32[]{:S(2)}, u32[]{:S(2)}) collective-permute-start(bf16[48,2048]{1,0:T(8,128)(2,1)S(1)} %get-tuple-element.36), channel_id=1, source_target_pairs={{0,6},{2,0},{4,2},{6,4},{1,7},{3,1},{5,3},{7,5},{8,14},{10,8},{12,... | collective-permute-start | bytes 589832 | tf_op jit(solution)/shard_map/ppermute | solution.py:24
  88.0 9.7 %collective-permute-start.2 = (bf16[48,2048]{1,0:T(8,128)(2,1)S(1)}, bf16[48,2048]{1,0:T(8,128)(2,1)S(1)}, u32[]{:S(2)}, u32[]{:S(2)}) collective-permute-start(bf16[48,2048]{1,0:T(8,128)(2,1)S(1)} %get-tuple-element.37), channel_id=1, source_target_pairs={{0,4},{2,6},{4,0},{6,2},{1,5},{3,7},{5,1},{7,3},{8,12},{10,14},{12... | collective-permute-start | bytes 589832 | tf_op jit(solution)/shard_map/ppermute | solution.py:24
  90.4 12.1 %collective-permute-start.1 = (bf16[48,2048]{1,0:T(8,128)(2,1)S(1)}, bf16[48,2048]{1,0:T(8,128)(2,1)}, u32[]{:S(2)}, u32[]{:S(2)}) collective-permute-start(bf16[48,2048]{1,0:T(8,128)(2,1)S(1)} %get-tuple-element.38), channel_id=1, source_target_pairs={{0,2},{2,4},{4,6},{6,0},{1,3},{3,5},{5,7},{7,1},{8,10},{10,12},{12... | collective-permute-start | bytes 589832 | tf_op jit(solution)/shard_map/ppermute | solution.py:24
  97.6 0.7 copy-start.5
  105.3 27.5 %all-to-all-start.4 = ((bf16[4,136,384]{2,1,0:T(8,128)(2,1)}), bf16[4,136,384]{2,1,0:T(8,128)(2,1)}, u32[]{:S(2)}, u32[]{:S(2)}) async-start(bf16[4,136,384]{2,1,0:T(8,128)(2,1)} %pad_maximum_fusion.2), calls=%async_computation.4 | async-start | bytes 835584 | tf_op jit(solution)/shard_map/all_to_all | solution.py:19
  110.6 9.4 %collective-permute-start.6 = (bf16[48,2048]{1,0:T(8,128)(2,1)S(1)}, bf16[48,2048]{1,0:T(8,128)(2,1)S(1)}, u32[]{:S(2)}, u32[]{:S(2)}) collective-permute-start(bf16[48,2048]{1,0:T(8,128)(2,1)S(1)} %add_convert_fusion.2), channel_id=1, source_target_pairs={{0,6},{2,0},{4,2},{6,4},{1,7},{3,1},{5,3},{7,5},{8,14},{10,8},{12,... | collective-permute-start | bytes 589832 | tf_op jit(solution)/shard_map/ppermute | solution.py:24
  115.0 8.7 %collective-permute-start.5 = (bf16[48,2048]{1,0:T(8,128)(2,1)S(1)}, bf16[48,2048]{1,0:T(8,128)(2,1)S(1)}, u32[]{:S(2)}, u32[]{:S(2)}) collective-permute-start(bf16[48,2048]{1,0:T(8,128)(2,1)S(1)} %add_convert_fusion.2), channel_id=1, source_target_pairs={{0,4},{2,6},{4,0},{6,2},{1,5},{3,7},{5,1},{7,3},{8,12},{10,14},{12... | collective-permute-start | bytes 589832 | tf_op jit(solution)/shard_map/ppermute | solution.py:24
  117.4 11.4 %collective-permute-start.4 = (bf16[48,2048]{1,0:T(8,128)(2,1)S(1)}, bf16[48,2048]{1,0:T(8,128)(2,1)S(1)}, u32[]{:S(2)}, u32[]{:S(2)}) collective-permute-start(bf16[48,2048]{1,0:T(8,128)(2,1)S(1)} %add_convert_fusion.2), channel_id=1, source_target_pairs={{0,2},{2,4},{4,6},{6,0},{1,3},{3,5},{5,7},{7,1},{8,10},{10,12},{12... | collective-permute-start | bytes 589832 | tf_op jit(solution)/shard_map/ppermute | solution.py:24
  129.8 14.3 %collective-permute-start.7 = (bf16[4,48,2048]{2,1,0:T(8,128)(2,1)}, bf16[4,48,2048]{2,1,0:T(8,128)(2,1)}, u32[]{:S(2)}, u32[]{:S(2)}) collective-permute-start(bf16[4,48,2048]{2,1,0:T(8,128)(2,1)} %pad_maximum_fusion.1.own_ref), channel_id=1, source_target_pairs={{0,1},{1,0},{2,3},{3,2},{4,5},{5,4},{6,7},{7,6},{8,9},{9,8},{10,11... | collective-permute-start | bytes 2359304 | tf_op jit(solution)/shard_map/ppermute | solution.py:24
  134.7 58.2 %all-to-all-start.5 = ((bf16[4,72,384]{2,1,0:T(8,128)(2,1)}), bf16[4,72,384]{2,1,0:T(8,128)(2,1)S(1)}, u32[]{:S(2)}, u32[]{:S(2)}) async-start(bf16[4,72,384]{2,1,0:T(8,128)(2,1)} %bitcast.43), calls=%async_computation.5 | async-start | bytes 442368 | tf_op jit(solution)/shard_map/all_to_all | solution.py:19
  140.3 2.4 %copy-start.3 = (bf16[384,384]{1,0:T(8,128)(2,1)S(1)}, bf16[384,384]{1,0:T(8,128)(2,1)}, u32[]{:S(2)}) copy-start(bf16[384,384]{1,0:T(8,128)(2,1)} %param.12) | copy-start | bytes 884740
  140.3 2.5 %copy-start.10 = (pred[384]{0:T(512)(128)(4,1)S(1)}, pred[384]{0:T(512)(128)(4,1)}, u32[]{:S(2)}) copy-start(pred[384]{0:T(512)(128)(4,1)} %copy-done.9) | copy-start | bytes 1156
  140.3 2.5 %copy-start.12 = (pred[384]{0:T(512)(128)(4,1)S(1)}, pred[384]{0:T(512)(128)(4,1)}, u32[]{:S(2)}) copy-start(pred[384]{0:T(512)(128)(4,1)} %copy-done.11) | copy-start | bytes 1156
  140.3 2.5 %copy-start.14 = (pred[384]{0:T(512)(128)(4,1)S(1)}, pred[384]{0:T(512)(128)(4,1)}, u32[]{:S(2)}) copy-start(pred[384]{0:T(512)(128)(4,1)} %copy-done.13) | copy-start | bytes 1156
  144.0 48.9 %copy-start.6 = (f32[64,384]{1,0:T(8,128)S(1)}, f32[64,384]{1,0:T(8,128)}, u32[]{:S(2)}) copy-start(f32[64,384]{1,0:T(8,128)} %param.19) | copy-start | bytes 294916
  144.0 49.6 %copy-start.8 = (f32[3,384]{1,0:T(4,128)S(1)}, f32[3,384]{1,0:T(4,128)}, u32[]{:S(2)}) copy-start(f32[3,384]{1,0:T(4,128)} %param.20) | copy-start | bytes 13828
  144.0 50.2 %copy-start.16 = (f32[384]{0:T(512)S(1)}, f32[384]{0:T(512)}, u32[]{:S(2)}) copy-start(f32[384]{0:T(512)} %param.21) | copy-start | bytes 4612

commit v3 on v1

v3 whole, which is shorter than its diff:
```python
import jax
import jax.numpy as jnp
from jax import lax
from jax.experimental import pallas as pl
from jax.experimental.pallas import tpu as pltpu
from jax.sharding import Mesh
from jax.sharding import PartitionSpec as P


SEQ_LEN = 128
SMALL_ROWS = 8


def copies_to(block, axis, size):
    copies = jnp.broadcast_to(block, (size, *block.shape))
    return lax.all_to_all(copies, axis, 0, 0, tiled=True)


def exchange(blocks, axis):
    return lax.all_to_all(blocks, axis, 0, 0, tiled=True)


def send_on(block, axis, shift):
    size = lax.axis_size(axis)
    return lax.ppermute(block, axis, [(i, (i + shift) % size) for i in range(size)])


def whole(shape):
    return pl.BlockSpec(shape, lambda *_: (0,) * len(shape))


def cost(flops, count, exps=0):
    return pl.CostEstimate(flops=flops, bytes_accessed=count, transcendentals=exps)


def put_in_order(own, other, n_c):
    n_x = len(own)
    rows, width = own[0].shape

    def body(*refs):
        out_ref = refs[-1]
        at_x, at_c = lax.axis_index("x"), lax.axis_index("c")
        for k in range(n_x):
            spot = (at_x + n_x - k) % n_x
            out_ref[at_c * n_x + spot] = refs[k][...]
            out_ref[(1 - at_c) * n_x + spot] = refs[n_x + k][...]

    return pl.pallas_call(
        body,
        out_shape=jax.ShapeDtypeStruct((n_c * n_x, rows, width), own[0].dtype),
        cost_estimate=cost(0, 32 * own[0].size),
        name="put_in_order",
    )(*own, *other)


def later(values, offset):
    rows = lax.broadcasted_iota(jnp.int32, values.shape, 0)
    return values if offset == 0 else jnp.where(
        rows >= offset, pltpu.roll(values, offset, 0), 0.0
    )


def earlier(values, offset):
    count = values.shape[0]
    rows = lax.broadcasted_iota(jnp.int32, values.shape, 0)
    return values if offset == 0 else jnp.where(
        rows < count - offset, pltpu.roll(values, count - offset, 0), 0.0
    )


def gated(up, taps_ref, bias_ref):
    tap_count = taps_ref.shape[0]
    total = bias_ref[...]
    for j in range(tap_count):
        total = total + taps_ref[j : j + 1, :] * later(up, tap_count - 1 - j)
    return total


def previous_branch(x_prev, plane, cotangent, value_prev, conv_taps, conv_bias, n_c):
    row_count, width = x_prev.shape
    n_y, n_zq, n_zm, shard_rows, units = plane.shape
    tap_count = conv_taps.shape[0]
    n_x = lax.axis_size("x")
    half_rows = row_count // n_c
    block_rows = half_rows // n_x
    steps = row_count // SEQ_LEN

    def body(
        x_ref,
        w_ref,
        cot_ref,
        value_ref,
        taps_ref,
        bias_ref,
        gv_ref,
        gu_ref,
        small_ref,
        natural_ref,
        turned_ref,
        send_ref,
    ):
        step = pl.program_id(0)

        @pl.when(step == 0)
        def _():
            small_ref[...] = jnp.zeros_like(small_ref)
            for y in range(n_y):
                for q in range(n_zq):
                    for m in range(n_zm):
                        at = ((m * n_zq + q) * n_y + y) * shard_rows
                        natural_ref[at : at + shard_rows] = w_ref[y, q, m]

        up = jnp.dot(x_ref[...], natural_ref[...], preferred_element_type=jnp.float32)
        up = up.astype(jnp.bfloat16).astype(jnp.float32)
        gate = gated(up, taps_ref, bias_ref)
        sig = jax.nn.sigmoid(gate)
        cot = cot_ref[...].astype(jnp.float32)
        gv_ref[...] = (cot * gate * sig).astype(jnp.bfloat16)
        grad_gate = cot * value_ref[...].astype(jnp.float32) * sig * (1.0 + gate * (1.0 - sig))
        grad_up = jnp.zeros_like(grad_gate)
        for j in range(tap_count):
            grad_up = grad_up + taps_ref[j : j + 1, :] * earlier(grad_gate, tap_count - 1 - j)
        start = pl.multiple_of(step * SEQ_LEN, SEQ_LEN)
        gu_ref[pl.ds(start, SEQ_LEN)] = grad_up.astype(jnp.bfloat16)
        for j in range(tap_count):
            small_ref[j : j + 1, :] += jnp.sum(
                grad_gate * later(up, tap_count - 1 - j), axis=0, keepdims=True
            )
        small_ref[tap_count : tap_count + 1, :] += jnp.sum(grad_gate, axis=0, keepdims=True)

        @pl.when(step == steps - 1)
        def _():
            at_x, at_c = lax.axis_index("x"), lax.axis_index("c")
            for i in range(n_c):
                core = (at_c + 1 + i) % n_c
                for k in range(n_x):
                    row = core * half_rows + ((at_x + k) % n_x) * block_rows
                    turned_ref[i, k * block_rows : (k + 1) * block_rows] = gu_ref[
                        pl.ds(pl.multiple_of(row, block_rows), block_rows)
                    ]
            send_ref[...] = lax.dot_general(
                turned_ref[0],
                natural_ref[...],
                (((1,), (1,)), ((), ())),
                preferred_element_type=jnp.float32,
            ).astype(jnp.bfloat16)

    rows = pl.BlockSpec((SEQ_LEN, units), lambda i: (i, 0))
    half = jax.ShapeDtypeStruct((row_count, units), jnp.bfloat16)
    outs = [
        half,
        half,
        jax.ShapeDtypeStruct((SMALL_ROWS, units), jnp.float32),
        jax.ShapeDtypeStruct((width, units), jnp.bfloat16),
        jax.ShapeDtypeStruct((n_c, half_rows, units), jnp.bfloat16),
        jax.ShapeDtypeStruct((half_rows, width), jnp.bfloat16),
    ]
    return pl.pallas_call(
        body,
        grid=(steps,),
        in_specs=[
            pl.BlockSpec((SEQ_LEN, width), lambda i: (i, 0)),
            whole(plane.shape),
            rows,
            rows,
            whole(conv_taps.shape),
            whole((1, units)),
        ],
        out_specs=[rows] + [whole(o.shape) for o in outs[1:]],
        out_shape=outs,
        cost_estimate=cost(3 * row_count * width * units, 8 * width * units, row_count * units),
        name="previous_branch",
    )(x_prev, plane, cotangent, value_prev, conv_taps, conv_bias.reshape(1, units))


def next_branch(x_next, weights, value_next, conv_taps, conv_bias):
    row_count, width = x_next.shape
    units = weights.shape[1]

    def body(x_ref, w_ref, value_ref, taps_ref, bias_ref, out_ref):
        up = jnp.dot(x_ref[...], w_ref[...], preferred_element_type=jnp.float32)
        gate = gated(up.astype(jnp.bfloat16).astype(jnp.float32), taps_ref, bias_ref)
        hidden = gate * jax.nn.sigmoid(gate) * value_ref[...].astype(jnp.float32)
        out_ref[...] = hidden.astype(jnp.bfloat16)

    rows = pl.BlockSpec((SEQ_LEN, units), lambda i: (i, 0))
    return pl.pallas_call(
        body,
        grid=(row_count // SEQ_LEN,),
        in_specs=[
            pl.BlockSpec((SEQ_LEN, width), lambda i: (i, 0)),
            whole(weights.shape),
            rows,
            whole(conv_taps.shape),
            whole((1, units)),
        ],
        out_specs=rows,
        out_shape=jax.ShapeDtypeStruct((row_count, units), jnp.bfloat16),
        cost_estimate=cost(2 * row_count * width * units, 4 * width * units, row_count * units),
        name="next_branch",
    )(x_next, weights, value_next, conv_taps, conv_bias.reshape(1, units))


def high_and_low(rows):
    high = rows.astype(jnp.bfloat16).astype(jnp.float32)
    return jnp.concatenate([high, rows - high], axis=0).astype(jnp.bfloat16)


def turned_columns(x, parts):
    row_count, width = x.shape
    each = width // parts

    def body(x_ref, out_ref):
        out_ref[...] = x_ref[...].T

    return pl.pallas_call(
        body,
        grid=(parts,),
        in_specs=[pl.BlockSpec((row_count, each), lambda i: (0, i))],
        out_specs=pl.BlockSpec((each, row_count), lambda i: (i, 0)),
        out_shape=jax.ShapeDtypeStruct((width, row_count), x.dtype),
        cost_estimate=cost(2 * row_count * row_count * width, 4 * x.size),
        name="turned_columns",
    )(x)


def weight_gradient(x_turned, grad_up, small, grad_scale, n_zm, n_zq, n_y):
    width, row_count = x_turned.shape
    units = grad_up.shape[1]
    each = width // n_y
    shard_rows = each // (n_zm * n_zq)

    def body(x_ref, g_ref, small_ref, out_ref):
        grad = jnp.dot(
            x_ref[...].reshape(each, row_count), g_ref[...], preferred_element_type=jnp.float32
        )
        grad = (grad * grad_scale).astype(jnp.bfloat16)
        for q in range(n_zq):
            for m in range(n_zm):
                to, at = (q * n_zm + m) * shard_rows, (m * n_zq + q) * shard_rows
                out_ref[0, to : to + shard_rows] = grad[at : at + shard_rows]
        out_ref[0, each:] = high_and_low(small_ref[...] * grad_scale)

    return pl.pallas_call(
        body,
        grid=(n_y,),
        in_specs=[
            pl.BlockSpec((n_zm * n_zq, 1, shard_rows, row_count), lambda i: (0, i, 0, 0)),
            whole(grad_up.shape),
            whole(small.shape),
        ],
        out_specs=pl.BlockSpec((1, each + 2 * SMALL_ROWS, units), lambda i: (i, 0, 0)),
        out_shape=jax.ShapeDtypeStruct((n_y, each + 2 * SMALL_ROWS, units), jnp.bfloat16),
        cost_estimate=cost(2 * row_count * width * units, 4 * width * units),
        name="weight_gradient",
    )(x_turned.reshape(n_zm * n_zq, n_y, shard_rows, row_count), grad_up, small)


def summed(block):
    return jnp.sum(block.astype(jnp.float32), axis=0)


def small_total(block):
    total = summed(block)
    return total[:SMALL_ROWS] + total[SMALL_ROWS:]


def sum_and_repack(arrived, parts, repeats):
    count, rows, units = arrived.shape
    extra = 2 * SMALL_ROWS
    each = (rows - extra) // parts

    def body(main_ref, small_ref, out_ref):
        main = summed(main_ref[...]).astype(jnp.bfloat16)
        small = high_and_low(small_total(small_ref[...]))
        for r in range(repeats):
            out_ref[r, 0, :each] = main
            out_ref[r, 0, each:] = small

    out = pl.pallas_call(
        body,
        grid=(parts,),
        in_specs=[
            pl.BlockSpec((count, each, units), lambda i: (0, i, 0)),
            pl.BlockSpec((count, extra, units), lambda i: (0, (rows - extra) // extra, 0)),
        ],
        out_specs=pl.BlockSpec((repeats, 1, each + extra, units), lambda i: (0, i, 0, 0)),
        out_shape=jax.ShapeDtypeStruct((repeats, parts, each + extra, units), jnp.bfloat16),
        cost_estimate=cost(2 * arrived.size, 4 * arrived.size),
        name="sum_and_repack",
    )(arrived, arrived)
    return out.reshape(repeats * parts, each + extra, units)


def last_sum(arrived, sum_w, sum_taps, sum_bias):
    rows, units = sum_w.shape
    tap_count = sum_taps.shape[0]

    def body(in_ref, w_ref, taps_ref, bias_ref, new_w_ref, new_taps_ref, new_bias_ref):
        new_w_ref[...] = w_ref[...] + summed(in_ref[:, :rows])
        small = small_total(in_ref[:, rows:])
        new_taps_ref[...] = taps_ref[...] + small[:tap_count]
        new_bias_ref[...] = bias_ref[...] + small[tap_count : tap_count + 1]

    new_w, new_taps, new_bias = pl.pallas_call(
        body,
        out_shape=[
            jax.ShapeDtypeStruct(sum_w.shape, jnp.float32),
            jax.ShapeDtypeStruct(sum_taps.shape, jnp.float32),
            jax.ShapeDtypeStruct((1, units), jnp.float32),
        ],
        cost_estimate=cost(2 * arrived.size, 4 * arrived.size),
        name="last_sum",
    )(arrived, sum_w, sum_taps, sum_bias.reshape(1, units))
    return new_w, new_taps, new_bias.reshape(units)


def per_device(
    x_next,
    value_next,
    x_prev,
    value_prev,
    cotangent,
    w_gate,
    conv_taps,
    conv_bias,
    sum_w,
    sum_taps,
    sum_bias,
):
    row_count, width = x_next.shape
    n_zh, n_zm, n_zq, n_y = (lax.axis_size(a) for a in ("zh", "zm", "zq", "y"))
    n_x, n_c = lax.axis_size("x"), lax.axis_size("c")

    pair = copies_to(w_gate, "zm", n_zm)
    quad = copies_to(pair, "zq", n_zq)
    x_turned = turned_columns(x_prev, 8)
    quad, x_turned = lax.optimization_barrier((quad, x_turned))
    plane = copies_to(quad, "y", n_y)

    grad_value, grad_up, small, gathered, turned, to_core = previous_branch(
        x_prev, plane, cotangent, value_prev, conv_taps, conv_bias, n_c
    )
    from_core = send_on(to_core, "c", 1)
    grad_scale = float(row_count * n_zh * n_zm * n_zq * n_y) ** (-0.5)
    by_y = weight_gradient(x_turned, grad_up, small, grad_scale, n_zm, n_zq, n_y)
    by_y, turned = lax.optimization_barrier((by_y, turned))
    from_y = exchange(by_y, "y")

    block_rows = row_count // (n_x * n_c)
    kept = lax.dot_general(
        turned[1], gathered, (((1,), (1,)), ((), ())), preferred_element_type=jnp.float32
    )
    half = (kept + from_core.astype(jnp.float32)).astype(jnp.bfloat16)
    half = half.reshape(n_x, block_rows, width)
    arrived = [half[0]] + [send_on(half[k], "x", k) for k in range(1, n_x)]
    from_y, *arrived = lax.optimization_barrier((from_y, *arrived))
    eighth = sum(block.astype(jnp.float32) for block in arrived).astype(jnp.bfloat16)
    spread = [eighth]
    for k in range(1, n_x):
        spread.append(send_on(eighth, "x", k))

    from_q = exchange(sum_and_repack(from_y, n_zq, 1), "zq")
    by_half = sum_and_repack(from_q, n_zm, n_zh)
    by_half, x_next = lax.optimization_barrier((by_half, x_next))
    from_half = exchange(by_half, ("zh", "zm"))
    hidden_next = next_branch(x_next, gathered, value_next, conv_taps, conv_bias)
    hidden_next, *spread = lax.optimization_barrier((hidden_next, *spread))
    other = [send_on(block, "c", 1) for block in spread]
    from_half, *other = lax.optimization_barrier((from_half, *other))
    grad_input = put_in_order(spread, other, n_c).reshape(row_count, width)
    new_w, new_taps, new_bias = last_sum(from_half, sum_w, sum_taps, sum_bias)
    return hidden_next, grad_input, grad_value, new_w, new_taps, new_bias


def solution(mesh):
    n_fs, n_tp = mesh.shape["fs"], mesh.shape["tp"]
    n_y, n_zq, n_c = 4, 4, 2
    fine = Mesh(
        mesh.devices.reshape(
            mesh.shape["rep"], n_fs // (n_y * n_zq), n_zq, n_y, n_tp // n_c, n_c
        ),
        ("zh", "zm", "zq", "y", "x", "c"),
    )
    fs, tp = ("zm", "zq", "y"), ("x", "c")
    tokens = ("zh", *fs)
    in_specs = (
        P(tokens, None),
        P(tokens, tp),
        P(tokens, None),
        P(tokens, tp),
        P(tokens, tp),
        P(fs, tp),
        P(None, tp),
        P(tp),
        P(fs, tp),
        P(None, tp),
        P(tp),
    )
    out_specs = (
        P(tokens, tp),
        P(tokens, None),
        P(tokens, tp),
        P(fs, tp),
        P(None, tp),
        P(tp),
    )
    return jax.shard_map(
        per_device, mesh=fine, in_specs=in_specs, out_specs=out_specs, check_vma=False
    )
```

time: 182 us -> 164 us (0.901)
  waiting for transfers between devices: 63.7 us -> 29.2 us
  Pallas kernels: 0 us -> 30.9 us
  starting transfers between devices: 30 us -> 58.9 us
  blocking collectives: 51.6 us -> 32.2 us
  other arithmetic: 14.9 us -> 1.31 us
  local copies, waits for them, and re-layouts: 12.5 us -> 7.29 us
  matrix products: 5.14 us -> 1.83 us
    ppermute x0 -> x11, starting transfers between devices: none -> 38.7 us  [send_on(): lax.ppermute(block, axis, [(i, (i + shift) % size) for i in range(size)])]
    all_to_all x3 -> x2, waiting for transfers between devices: 36.5 us -> 3.2 us  [exchange(): return lax.all_to_all(blocks, axis, 0, 0, tiled=True)]
    pallas_call x0 -> x8, Pallas kernels: none -> 30.9 us  [the longest x1 6.75 us: previous_branch(): pl.pallas_call(body, grid=(steps,), in_specs=[pl.BlockSpec((SEQ_LEN, widt...]
    all_to_all x2 -> x1, blocking collectives: 30.9 us -> 15.8 us  [copies_to(): return lax.all_to_all(copies, axis, 0, 0, tiled=True)]
    reduce_sum x6 -> x0, other arithmetic: 7.87 us -> none  [the longest x5 5.69 us: summed(): return jnp.sum(blocks.astype(jnp.float32), axis=0)]
    all_to_all x3 -> x2, waiting for transfers between devices: 27.2 us -> 19.6 us  [copies_to(): return lax.all_to_all(copies, axis, 0, 0, tiled=True)]
    all_to_all x3 -> x2, starting transfers between devices: 17 us -> 9.98 us  [copies_to(): return lax.all_to_all(copies, axis, 0, 0, tiled=True)]
    ppermute x0 -> x11, waiting for transfers between devices: none -> 6.43 us  [send_on(): lax.ppermute(block, axis, [(i, (i + shift) % size) for i in range(size)])]
  transfers between devices with their start and end apart: 6 -> 15, of which waited for: 6 -> 6; matrix products, arithmetic and copies ran while one was open for 7% -> 2% of each run, Pallas kernels for 0% -> 9%
where the time goes in v3:
time: 164 us; the launch traced here: 163 us
  starting transfers between devices  58.9 us (36%)
  blocking collectives  32.2 us (20%)
  Pallas kernels  30.9 us (19%)
  waiting for transfers between devices  29.2 us (18%)
  local copies, waits for them, and re-layouts  7.29 us (4%)
  matrix products  1.83 us (1%)
    ppermute x11, starting transfers between devices, send_on(): lax.ppermute(block, axis, [(i, (i + shift) % size) for i in range(size)])  38.7 us
    all_to_all x2, waiting for transfers between devices, copies_to(): return lax.all_to_all(copies, axis, 0, 0, tiled=True)  19.6 us
    all_to_all x1, blocking collectives, exchange(): return lax.all_to_all(blocks, axis, 0, 0, tiled=True)  16.3 us
    all_to_all x1, blocking collectives, copies_to(): return lax.all_to_all(copies, axis, 0, 0, tiled=True)  15.8 us
    all_to_all x2, starting transfers between devices, exchange(): return lax.all_to_all(blocks, axis, 0, 0, tiled=True)  10.2 us
    all_to_all x2, starting transfers between devices, copies_to(): return lax.all_to_all(copies, axis, 0, 0, tiled=True)  9.98 us
    pallas_call x1, Pallas kernels, previous_branch(): pl.pallas_call(body, grid=(steps,), in_specs=[pl.BlockSpec((SEQ_LEN, widt...  6.75 us
    ppermute x11, waiting for transfers between devices, send_on(): lax.ppermute(block, axis, [(i, (i + shift) % size) for i in range(size)])  6.43 us
  transfers between devices with their start and end apart: 15, of which 6 were waited for; matrix products, arithmetic and copies ran while one was open for 2% of the time, Pallas kernels for 9%

profile of v3, /device:TPU:1, one launch (start us, length us, event | category | flops | bytes accessed | tf_op | source)
XLA Modules:
  0.0 162.5 jit_solution(3517891814430822186)
XLA Ops:
  0.6 0.8 broadcast_in_dim.9
  1.4 15.8 %all_to_all.30 = bf16[2,64,384]{2,1,0:T(8,128)(2,1)S(1)} all-to-all(bf16[2,64,384]{2,1,0:T(8,128)(2,1)S(1)} %broadcast_in_dim.9), channel_id=1, replica_groups=mesh['zh'=2,'zm'=2,'zq'=4,'y'=4,'x'=4,'c'=2] {'zm'}, dimensions={0} | all-to-all | bytes 196608 | tf_op jit(solution)/shard_map/all_to_all | solution.py:16
  17.3 0.8 broadcast_in_dim.10
  18.1 5.7 %all-to-all-start.1 = ((bf16[4,2,64,384]{3,2,1,0:T(8,128)(2,1)}), bf16[4,2,64,384]{3,2,1,0:T(8,128)(2,1)S(1)}, u32[]{:S(2)}, u32[]{:S(2)}) async-start(bf16[4,2,64,384]{3,2,1,0:T(8,128)(2,1)} %broadcast_in_dim.10), calls=%async_computation.1 | async-start | bytes 786432 | tf_op jit(solution)/shard_map/all_to_all | solution.py:16
  23.7 5.8 %turned_columns.1 = bf16[2048,384]{1,0:T(8,128)(2,1)} custom-call(bf16[384,2048]{1,0:T(8,128)(2,1)} %x_ref.3), custom_call_target="tpu_custom_call" | custom-call | flops 603979776 | bytes 3145728 | tf_op jit(solution)/shard_map/turned_columns/pallas_call | solution.py:216
  29.5 3.4 %all-to-all-done.1 = bf16[4,2,64,384]{3,2,1,0:T(8,128)(2,1)S(1)} async-done(((bf16[4,2,64,384]{3,2,1,0:T(8,128)(2,1)}), bf16[4,2,64,384]{3,2,1,0:T(8,128)(2,1)S(1)}, u32[]{:S(2)}, u32[]{:S(2)}) %all-to-all-start.1) | async-done | bytes 393248 | tf_op jit(solution)/shard_map/all_to_all | solution.py:16
  32.9 1.4 broadcast_in_dim.11
  34.3 4.3 %all-to-all-start.2 = ((bf16[4,4,2,64,384]{4,3,2,1,0:T(8,128)(2,1)}), bf16[4,4,2,64,384]{4,3,2,1,0:T(8,128)(2,1)S(1)}, u32[]{:S(2)}, u32[]{:S(2)}) async-start(bf16[4,4,2,64,384]{4,3,2,1,0:T(8,128)(2,1)} %broadcast_in_dim.11), calls=%async_computation.2 | async-start | bytes 3145728 | tf_op jit(solution)/shard_map/all_to_all | solution.py:16
  38.6 0.0 copy-done.13
  38.6 0.6 reshape.44.bias_ref
  39.2 16.2 %all-to-all-done.2.w_ref = bf16[4,4,2,64,384]{4,3,2,1,0:T(8,128)(2,1)S(1)} async-done(((bf16[4,4,2,64,384]{4,3,2,1,0:T(8,128)(2,1)}), bf16[4,4,2,64,384]{4,3,2,1,0:T(8,128)(2,1)S(1)}, u32[]{:S(2)}, u32[]{:S(2)}) %all-to-all-start.2) | async-done | bytes 1572896 | tf_op jit(solution)/shard_map/all_to_all | solution.py:16
  55.3 1.1 copy-done.2
  56.5 6.8 %previous_branch.1 = (bf16[384,384]{1,0:T(8,128)(2,1)}, bf16[384,384]{1,0:T(8,128)(2,1)}, f32[8,384]{1,0:T(8,128)}, bf16[2048,384]{1,0:T(8,128)(2,1)}, bf16[2,19...) custom-call(bf16[384,2048]{1,0:T(8,128)(2,1)} %x_ref.3, bf16[4,4,2,64,384]{4,3,2,1,0:T(8,128)(2,1)} %copy-done.2, ...), custom_call_target="tpu_custom_call" | custom-call | flops 905969664 | bytes 6291456 | tf_op jit(solution)/shard_map/previous_branch/pallas_call | solution.py:158
  63.2 6.8 %collective-permute-start = (bf16[192,2048]{1,0:T(8,128)(2,1)}, bf16[192,2048]{1,0:T(8,128)(2,1)}, u32[]{:S(2)}, u32[]{:S(2)}) collective-permute-start(bf16[192,2048]{1,0:T(8,128)(2,1)} %get-tuple-element.44), channel_id=1, source_target_pairs={{0,1},{1,0},{2,3},{3,2},{4,5},{5,4},{6,7},{7,6},{8,9},{9,8},{10,11... | collective-permute-start | bytes 2359304 | tf_op jit(solution)/shard_map/ppermute | solution.py:25
  70.1 4.4 %weight_gradient.1 = bf16[4,528,384]{2,1,0:T(8,128)(2,1)} custom-call(bf16[8,4,64,384]{3,2,1,0:T(8,128)(2,1)} %bitcast.10, bf16[384,384]{1,0:T(8,128)(2,1)} %get-tuple-element.38.g_ref, f32[8,384]{1,0:T(8,128)} %get-tuple-element.39.small_ref), custom_call_target="tpu_custom_call" | custom-call | flops 603979776 | bytes 3145728 | tf_op jit(solution)/shard_map/weight_gradient/pallas_call | solution.py:244
  74.5 3.7 %all-to-all-start.3 = ((bf16[4,528,384]{2,1,0:T(8,128)(2,1)}), bf16[4,528,384]{2,1,0:T(8,128)(2,1)S(1)}, u32[]{:S(2)}, u32[]{:S(2)}) async-start(bf16[4,528,384]{2,1,0:T(8,128)(2,1)} %weight_gradient.1), calls=%async_computation.3 | async-start | bytes 3244032 | tf_op jit(solution)/shard_map/all_to_all | solution.py:20
  78.2 0.0 collective-permute-done
  78.2 0.0 copy-done.1
  78.2 0.0 copy-done.12
  78.2 1.8 %add_convert_fusion = bf16[192,2048]{1,0:T(8,128)(2,1)S(1)} fusion(bf16[192,2048]{1,0:T(8,128)(2,1)} %collective-permute-done, bf16[2048,384]{1,0:T(8,128)(2,1)S(1)} %copy-done.1, bf16[2,192,384]{2,1,0:T(8,128)(2,1)S(1)} %copy-done.12), kind=kOutput, calls=%fused_computation | convolution fusion | flops 303169536 | bytes 3293184 | tf_op jit(solution)/shard_map/dot_general | solution.py:351
  80.1 0.1 fusion.5
  80.1 3.1 %collective-permute-start.1 = (bf16[48,2048]{1,0:T(8,128)(2,1)S(1)}, bf16[48,2048]{1,0:T(8,128)(2,1)S(1)}, u32[]{:S(2)}, u32[]{:S(2)}) collective-permute-start(bf16[48,2048]{1,0:T(8,128)(2,1)S(1)} %get-tuple-element.68), channel_id=1, source_target_pairs={{0,2},{2,4},{4,6},{6,0},{1,3},{3,5},{5,7},{7,1},{8,10},{10,12},{12... | collective-permute-start | bytes 589832 | tf_op jit(solution)/shard_map/ppermute | solution.py:25
  83.3 4.3 %collective-permute-start.2 = (bf16[48,2048]{1,0:T(8,128)(2,1)S(1)}, bf16[48,2048]{1,0:T(8,128)(2,1)S(1)}, u32[]{:S(2)}, u32[]{:S(2)}) collective-permute-start(bf16[48,2048]{1,0:T(8,128)(2,1)S(1)} %get-tuple-element.67), channel_id=1, source_target_pairs={{0,4},{2,6},{4,0},{6,2},{1,5},{3,7},{5,1},{7,3},{8,12},{10,14},{12... | collective-permute-start | bytes 589832 | tf_op jit(solution)/shard_map/ppermute | solution.py:25
  87.6 3.1 %collective-permute-start.3 = (bf16[48,2048]{1,0:T(8,128)(2,1)S(1)}, bf16[48,2048]{1,0:T(8,128)(2,1)S(1)}, u32[]{:S(2)}, u32[]{:S(2)}) collective-permute-start(bf16[48,2048]{1,0:T(8,128)(2,1)S(1)} %get-tuple-element.66), channel_id=1, source_target_pairs={{0,6},{2,0},{4,2},{6,4},{1,7},{3,1},{5,3},{7,5},{8,14},{10,8},{12,... | collective-permute-start | bytes 589832 | tf_op jit(solution)/shard_map/ppermute | solution.py:25
  90.7 0.0 collective-permute-done.1
  90.7 4.2 %collective-permute-done.2 = bf16[48,2048]{1,0:T(8,128)(2,1)S(1)} collective-permute-done((bf16[48,2048]{1,0:T(8,128)(2,1)S(1)}, bf16[48,2048]{1,0:T(8,128)(2,1)S(1)}, u32[]{:S(2)}, u32[]{:S(2)}) %collective-permute-start.2) | collective-permute-done | bytes 196640 | tf_op jit(solution)/shard_map/ppermute | solution.py:25
  94.9 1.4 collective-permute-done.3
  96.3 3.2 %all-to-all-done.3.main_ref.small_ref = bf16[4,528,384]{2,1,0:T(8,128)(2,1)S(1)} async-done(((bf16[4,528,384]{2,1,0:T(8,128)(2,1)}), bf16[4,528,384]{2,1,0:T(8,128)(2,1)S(1)}, u32[]{:S(2)}, u32[]{:S(2)}) %all-to-all-start.3) | async-done | bytes 1622048 | tf_op jit(solution)/shard_map/all_to_all | solution.py:20
  99.5 1.2 copy-done
  100.7 3.4 %sum_and_repack.2 = bf16[1,4,144,384]{3,2,1,0:T(8,128)(2,1)} custom-call(bf16[4,528,384]{2,1,0:T(8,128)(2,1)} %copy-done, bf16[4,528,384]{2,1,0:T(8,128)(2,1)} %copy-done), custom_call_target="tpu_custom_call" | custom-call | flops 1622016 | bytes 3244032 | tf_op jit(solution)/shard_map/sum_and_repack/pallas_call | solution.py:280
  104.1 16.3 %all_to_all.31.main_ref.small_ref = bf16[4,144,384]{2,1,0:T(8,128)(2,1)} all-to-all(bf16[4,144,384]{2,1,0:T(8,128)(2,1)} %bitcast.11), channel_id=1, replica_groups=mesh['zh'=2,'zm'=2,'zq'=4,'y'=4,'x'=4,'c'=2] {'zq'}, dimensions={0} | all-to-all | bytes 884736 | tf_op jit(solution)/shard_map/all_to_all | solution.py:20
  120.5 1.7 %sum_and_repack.3 = bf16[2,2,80,384]{3,2,1,0:T(8,128)(2,1)} custom-call(bf16[4,144,384]{2,1,0:T(8,128)(2,1)} %all_to_all.31.main_ref.small_ref, bf16[4,144,384]{2,1,0:T(8,128)(2,1)} %all_to_all.31.main_ref.small_ref), custom_call_target="tpu_custom_call" | custom-call | flops 442368 | bytes 884736 | tf_op jit(solution)/shard_map/sum_and_repack/pallas_call | solution.py:280
  122.2 6.5 %all-to-all-start.5 = ((bf16[4,80,384]{2,1,0:T(8,128)(2,1)}), bf16[4,80,384]{2,1,0:T(8,128)(2,1)S(1)}, u32[]{:S(2)}, u32[]{:S(2)}) async-start(bf16[4,80,384]{2,1,0:T(8,128)(2,1)} %bitcast.13), calls=%async_computation.5 | async-start | bytes 491520 | tf_op jit(solution)/shard_map/all_to_all | solution.py:20
  128.7 0.1 add_convert_fusion.1.refs_0_
  128.8 0.0 copy-start.4
  128.8 0.0 copy-start.14
  128.8 3.2 %collective-permute-start.4 = (bf16[48,2048]{1,0:T(8,128)(2,1)S(1)}, bf16[48,2048]{1,0:T(8,128)(2,1)S(1)}, u32[]{:S(2)}, u32[]{:S(2)}) collective-permute-start(bf16[48,2048]{1,0:T(8,128)(2,1)S(1)} %add_convert_fusion.1.refs_0_), channel_id=1, source_target_pairs={{0,2},{2,4},{4,6},{6,0},{1,3},{3,5},{5,7},{7,1},{8,10},{10,12},{12... | collective-permute-start | bytes 589832 | tf_op jit(solution)/shard_map/ppermute | solution.py:25
  132.1 4.4 %collective-permute-start.5 = (bf16[48,2048]{1,0:T(8,128)(2,1)S(1)}, bf16[48,2048]{1,0:T(8,128)(2,1)S(1)}, u32[]{:S(2)}, u32[]{:S(2)}) collective-permute-start(bf16[48,2048]{1,0:T(8,128)(2,1)S(1)} %add_convert_fusion.1.refs_0_), channel_id=1, source_target_pairs={{0,4},{2,6},{4,0},{6,2},{1,5},{3,7},{5,1},{7,3},{8,12},{10,14},{12... | collective-permute-start | bytes 589832 | tf_op jit(solution)/shard_map/ppermute | solution.py:25
  136.5 3.1 %collective-permute-start.6 = (bf16[48,2048]{1,0:T(8,128)(2,1)S(1)}, bf16[48,2048]{1,0:T(8,128)(2,1)S(1)}, u32[]{:S(2)}, u32[]{:S(2)}) collective-permute-start(bf16[48,2048]{1,0:T(8,128)(2,1)S(1)} %add_convert_fusion.1.refs_0_), channel_id=1, source_target_pairs={{0,6},{2,0},{4,2},{6,4},{1,7},{3,1},{5,3},{7,5},{8,14},{10,8},{12,... | collective-permute-start | bytes 589832 | tf_op jit(solution)/shard_map/ppermute | solution.py:25
  139.5 4.4 %next_branch.1 = bf16[384,384]{1,0:T(8,128)(2,1)} custom-call(bf16[384,2048]{1,0:T(8,128)(2,1)} %x_ref.4, bf16[2048,384]{1,0:T(8,128)(2,1)} %get-tuple-element.43.w_ref, bf16[384,384]{1,0:T(8,128)(2,1)} %value_ref.3, f32[3,384]{1,0:T(4,128)} %taps_ref.4, f32[1,384]{1,0:T(1,128)} %reshape.44.bias_ref), custom_call_target="tpu_custom_call" | custom-call | flops 603979776 | bytes 3145728 | tf_op jit(solution)/shard_map/next_branch/pallas_call | solution.py:187
  144.0 0.0 collective-permute-done.4.refs_1_
  144.0 0.0 collective-permute-done.5.refs_2_
  144.0 0.0 copy-start.6
  144.0 0.0 collective-permute-done.6.refs_3_
  144.0 4.4 %collective-permute-start.10 = (bf16[48,2048]{1,0:T(8,128)(2,1)S(1)}, bf16[48,2048]{1,0:T(8,128)(2,1)S(1)}, u32[]{:S(2)}, u32[]{:S(2)}) collective-permute-start(bf16[48,2048]{1,0:T(8,128)(2,1)S(1)} %collective-permute-done.6.refs_3_), channel_id=1, source_target_pairs={{0,1},{1,0},{2,3},{3,2},{4,5},{5,4},{6,7},{7,6},{8,9},{9,8},{10,11... | collective-permute-start | bytes 589832 | tf_op jit(solution)/shard_map/ppermute | solution.py:25
  148.5 0.0 copy-done.4
  148.5 1.9 %collective-permute-start.7 = (bf16[48,2048]{1,0:T(8,128)(2,1)S(1)}, bf16[48,2048]{1,0:T(8,128)(2,1)S(1)}, u32[]{:S(2)}, u32[]{:S(2)}) collective-permute-start(bf16[48,2048]{1,0:T(8,128)(2,1)S(1)} %add_convert_fusion.1.refs_0_), channel_id=1, source_target_pairs={{0,1},{1,0},{2,3},{3,2},{4,5},{5,4},{6,7},{7,6},{8,9},{9,8},{10,11... | collective-permute-start | bytes 589832 | tf_op jit(solution)/shard_map/ppermute | solution.py:25
  150.4 2.4 %collective-permute-start.8 = (bf16[48,2048]{1,0:T(8,128)(2,1)S(1)}, bf16[48,2048]{1,0:T(8,128)(2,1)S(1)}, u32[]{:S(2)}, u32[]{:S(2)}) collective-permute-start(bf16[48,2048]{1,0:T(8,128)(2,1)S(1)} %collective-permute-done.4.refs_1_), channel_id=1, source_target_pairs={{0,1},{1,0},{2,3},{3,2},{4,5},{5,4},{6,7},{7,6},{8,9},{9,8},{10,11... | collective-permute-start | bytes 589832 | tf_op jit(solution)/shard_map/ppermute | solution.py:25
  152.8 1.9 %collective-permute-start.9 = (bf16[48,2048]{1,0:T(8,128)(2,1)S(1)}, bf16[48,2048]{1,0:T(8,128)(2,1)S(1)}, u32[]{:S(2)}, u32[]{:S(2)}) collective-permute-start(bf16[48,2048]{1,0:T(8,128)(2,1)S(1)} %collective-permute-done.5.refs_2_), channel_id=1, source_target_pairs={{0,1},{1,0},{2,3},{3,2},{4,5},{5,4},{6,7},{7,6},{8,9},{9,8},{10,11... | collective-permute-start | bytes 589832 | tf_op jit(solution)/shard_map/ppermute | solution.py:25
  154.7 0.0 copy-done.14
  154.7 0.6 reshape.48.bias_ref
  155.3 0.0 collective-permute-done.10.refs_7_
  155.3 0.0 collective-permute-done.7.refs_4_
  155.3 0.0 collective-permute-done.8.refs_5_
  155.4 0.8 collective-permute-done.9.refs_6_
  156.1 0.0 all-to-all-done.5.in_ref
  156.1 0.7 copy-done.3
  156.9 1.7 %last_sum.1 = (f32[64,384]{1,0:T(8,128)}, f32[3,384]{1,0:T(4,128)}, f32[1,384]{1,0:T(1,128)}) custom-call(bf16[4,80,384]{2,1,0:T(8,128)(2,1)} %copy-done.3, f32[64,384]{1,0:T(8,128)} %w_ref.1, f32[3,384]{1,0:T(4,128)} %taps_ref.5, f32[1,384]{1,0:T(1,128)} %reshape.48.bias_ref), custom_call_target="tpu_custom_call" | custom-call | flops 245760 | bytes 491520 | tf_op jit(solution)/shard_map/last_sum/pallas_call | solution.py:305
  158.6 1.2 reduce
  159.8 0.0 copy-done.5
  159.8 0.0 copy-done.9
  159.8 0.0 copy-done.10
  159.8 0.0 copy-done.11
  159.8 2.7 %put_in_order.1 = bf16[8,48,2048]{2,1,0:T(8,128)(2,1)} custom-call(bf16[48,2048]{1,0:T(8,128)(2,1)} %copy-done.4, bf16[48,2048]{1,0:T(8,128)(2,1)} %copy-done.5, bf16[48,2048]{1,0:T(8,128)(2,1)} %copy-done.6, bf16[48,2048]{1,0:T(8,128)(2,1)} %copy-done.7, bf16[48,2048]{1,0:T(8,128)(2,1)} %copy-done.9, bf16[48,2048]{1,0:T(8,128)(2,1)} %copy-done.10, ...), custom_call_target="tpu_custom_call" | custom-call | bytes 3145728 | tf_op jit(solution)/shard_map/put_in_order/pallas_call | solution.py:48
  (15 shorter events, 0.0 us)
Async XLA Ops:
  18.1 14.8 %all-to-all-start.1 = ((bf16[4,2,64,384]{3,2,1,0:T(8,128)(2,1)}), bf16[4,2,64,384]{3,2,1,0:T(8,128)(2,1)S(1)}, u32[]{:S(2)}, u32[]{:S(2)}) async-start(bf16[4,2,64,384]{3,2,1,0:T(8,128)(2,1)} %broadcast_in_dim.10), calls=%async_computation.1 | async-start | bytes 786432 | tf_op jit(solution)/shard_map/all_to_all | solution.py:16
  34.3 4.3 %copy-start.13 = (f32[384]{0:T(512)S(1)}, f32[384]{0:T(512)}, u32[]{:S(2)}) copy-start(f32[384]{0:T(512)} %param.18) | copy-start | bytes 4612
  34.3 21.1 %all-to-all-start.2 = ((bf16[4,4,2,64,384]{4,3,2,1,0:T(8,128)(2,1)}), bf16[4,4,2,64,384]{4,3,2,1,0:T(8,128)(2,1)S(1)}, u32[]{:S(2)}, u32[]{:S(2)}) async-start(bf16[4,4,2,64,384]{4,3,2,1,0:T(8,128)(2,1)} %broadcast_in_dim.11), calls=%async_computation.2 | async-start | bytes 3145728 | tf_op jit(solution)/shard_map/all_to_all | solution.py:16
  55.3 1.1 copy-start.2
  63.2 15.0 %collective-permute-start = (bf16[192,2048]{1,0:T(8,128)(2,1)}, bf16[192,2048]{1,0:T(8,128)(2,1)}, u32[]{:S(2)}, u32[]{:S(2)}) collective-permute-start(bf16[192,2048]{1,0:T(8,128)(2,1)} %get-tuple-element.44), channel_id=1, source_target_pairs={{0,1},{1,0},{2,3},{3,2},{4,5},{5,4},{6,7},{7,6},{8,9},{9,8},{10,11... | collective-permute-start | bytes 2359304 | tf_op jit(solution)/shard_map/ppermute | solution.py:25
  74.5 3.7 %copy-start.1 = (bf16[2048,384]{1,0:T(8,128)(2,1)S(1)}, bf16[2048,384]{1,0:T(8,128)(2,1)}, u32[]{:S(2)}) copy-start(bf16[2048,384]{1,0:T(8,128)(2,1)} %get-tuple-element.43.w_ref) | copy-start | bytes 4718596
  74.5 3.7 %copy-start.12 = (bf16[2,192,384]{2,1,0:T(8,128)(2,1)S(1)}, bf16[2,192,384]{2,1,0:T(8,128)(2,1)}, u32[]{:S(2)}) copy-start(bf16[2,192,384]{2,1,0:T(8,128)(2,1)} %get-tuple-element.42) | copy-start | bytes 884740
  74.5 25.0 %all-to-all-start.3 = ((bf16[4,528,384]{2,1,0:T(8,128)(2,1)}), bf16[4,528,384]{2,1,0:T(8,128)(2,1)S(1)}, u32[]{:S(2)}, u32[]{:S(2)}) async-start(bf16[4,528,384]{2,1,0:T(8,128)(2,1)} %weight_gradient.1), calls=%async_computation.3 | async-start | bytes 3244032 | tf_op jit(solution)/shard_map/all_to_all | solution.py:20
  80.1 10.6 %collective-permute-start.1 = (bf16[48,2048]{1,0:T(8,128)(2,1)S(1)}, bf16[48,2048]{1,0:T(8,128)(2,1)S(1)}, u32[]{:S(2)}, u32[]{:S(2)}) collective-permute-start(bf16[48,2048]{1,0:T(8,128)(2,1)S(1)} %get-tuple-element.68), channel_id=1, source_target_pairs={{0,2},{2,4},{4,6},{6,0},{1,3},{3,5},{5,7},{7,1},{8,10},{10,12},{12... | collective-permute-start | bytes 589832 | tf_op jit(solution)/shard_map/ppermute | solution.py:25
  83.3 11.6 %collective-permute-start.2 = (bf16[48,2048]{1,0:T(8,128)(2,1)S(1)}, bf16[48,2048]{1,0:T(8,128)(2,1)S(1)}, u32[]{:S(2)}, u32[]{:S(2)}) collective-permute-start(bf16[48,2048]{1,0:T(8,128)(2,1)S(1)} %get-tuple-element.67), channel_id=1, source_target_pairs={{0,4},{2,6},{4,0},{6,2},{1,5},{3,7},{5,1},{7,3},{8,12},{10,14},{12... | collective-permute-start | bytes 589832 | tf_op jit(solution)/shard_map/ppermute | solution.py:25
  87.6 8.7 %collective-permute-start.3 = (bf16[48,2048]{1,0:T(8,128)(2,1)S(1)}, bf16[48,2048]{1,0:T(8,128)(2,1)S(1)}, u32[]{:S(2)}, u32[]{:S(2)}) collective-permute-start(bf16[48,2048]{1,0:T(8,128)(2,1)S(1)} %get-tuple-element.66), channel_id=1, source_target_pairs={{0,6},{2,0},{4,2},{6,4},{1,7},{3,1},{5,3},{7,5},{8,14},{10,8},{12,... | collective-permute-start | bytes 589832 | tf_op jit(solution)/shard_map/ppermute | solution.py:25
  99.5 1.2 copy-start
  122.2 34.0 %all-to-all-start.5 = ((bf16[4,80,384]{2,1,0:T(8,128)(2,1)}), bf16[4,80,384]{2,1,0:T(8,128)(2,1)S(1)}, u32[]{:S(2)}, u32[]{:S(2)}) async-start(bf16[4,80,384]{2,1,0:T(8,128)(2,1)} %bitcast.13), calls=%async_computation.5 | async-start | bytes 491520 | tf_op jit(solution)/shard_map/all_to_all | solution.py:20
  128.8 19.6 %copy-start.4 = (bf16[48,2048]{1,0:T(8,128)(2,1)}, bf16[48,2048]{1,0:T(8,128)(2,1)S(1)}, u32[]{:S(2)}) copy-start(bf16[48,2048]{1,0:T(8,128)(2,1)S(1)} %add_convert_fusion.1.refs_0_) | copy-start | bytes 589828
  128.8 25.9 %copy-start.14 = (f32[384]{0:T(512)S(1)}, f32[384]{0:T(512)}, u32[]{:S(2)}) copy-start(f32[384]{0:T(512)} %param.21) | copy-start | bytes 4612
  128.8 15.1 %collective-permute-start.4 = (bf16[48,2048]{1,0:T(8,128)(2,1)S(1)}, bf16[48,2048]{1,0:T(8,128)(2,1)S(1)}, u32[]{:S(2)}, u32[]{:S(2)}) collective-permute-start(bf16[48,2048]{1,0:T(8,128)(2,1)S(1)} %add_convert_fusion.1.refs_0_), channel_id=1, source_target_pairs={{0,2},{2,4},{4,6},{6,0},{1,3},{3,5},{5,7},{7,1},{8,10},{10,12},{12... | collective-permute-start | bytes 589832 | tf_op jit(solution)/shard_map/ppermute | solution.py:25
  132.1 11.9 %collective-permute-start.5 = (bf16[48,2048]{1,0:T(8,128)(2,1)S(1)}, bf16[48,2048]{1,0:T(8,128)(2,1)S(1)}, u32[]{:S(2)}, u32[]{:S(2)}) collective-permute-start(bf16[48,2048]{1,0:T(8,128)(2,1)S(1)} %add_convert_fusion.1.refs_0_), channel_id=1, source_target_pairs={{0,4},{2,6},{4,0},{6,2},{1,5},{3,7},{5,1},{7,3},{8,12},{10,14},{12... | collective-permute-start | bytes 589832 | tf_op jit(solution)/shard_map/ppermute | solution.py:25
  136.5 7.6 %collective-permute-start.6 = (bf16[48,2048]{1,0:T(8,128)(2,1)S(1)}, bf16[48,2048]{1,0:T(8,128)(2,1)S(1)}, u32[]{:S(2)}, u32[]{:S(2)}) collective-permute-start(bf16[48,2048]{1,0:T(8,128)(2,1)S(1)} %add_convert_fusion.1.refs_0_), channel_id=1, source_target_pairs={{0,6},{2,0},{4,2},{6,4},{1,7},{3,1},{5,3},{7,5},{8,14},{10,8},{12,... | collective-permute-start | bytes 589832 | tf_op jit(solution)/shard_map/ppermute | solution.py:25
  144.0 15.8 %copy-start.5 = (bf16[48,2048]{1,0:T(8,128)(2,1)}, bf16[48,2048]{1,0:T(8,128)(2,1)S(1)}, u32[]{:S(2)}) copy-start(bf16[48,2048]{1,0:T(8,128)(2,1)S(1)} %collective-permute-done.4.refs_1_) | copy-start | bytes 589828
  144.0 15.8 %copy-start.6 = (bf16[48,2048]{1,0:T(8,128)(2,1)}, bf16[48,2048]{1,0:T(8,128)(2,1)S(1)}, u32[]{:S(2)}) copy-start(bf16[48,2048]{1,0:T(8,128)(2,1)S(1)} %collective-permute-done.5.refs_2_) | copy-start | bytes 589828
  144.0 15.7 %copy-start.7 = (bf16[48,2048]{1,0:T(8,128)(2,1)}, bf16[48,2048]{1,0:T(8,128)(2,1)S(1)}, u32[]{:S(2)}) copy-start(bf16[48,2048]{1,0:T(8,128)(2,1)S(1)} %collective-permute-done.6.refs_3_) | copy-start | bytes 589828
  144.0 11.3 %collective-permute-start.10 = (bf16[48,2048]{1,0:T(8,128)(2,1)S(1)}, bf16[48,2048]{1,0:T(8,128)(2,1)S(1)}, u32[]{:S(2)}, u32[]{:S(2)}) collective-permute-start(bf16[48,2048]{1,0:T(8,128)(2,1)S(1)} %collective-permute-done.6.refs_3_), channel_id=1, source_target_pairs={{0,1},{1,0},{2,3},{3,2},{4,5},{5,4},{6,7},{7,6},{8,9},{9,8},{10,11... | collective-permute-start | bytes 589832 | tf_op jit(solution)/shard_map/ppermute | solution.py:25
  148.5 6.9 %collective-permute-start.7 = (bf16[48,2048]{1,0:T(8,128)(2,1)S(1)}, bf16[48,2048]{1,0:T(8,128)(2,1)S(1)}, u32[]{:S(2)}, u32[]{:S(2)}) collective-permute-start(bf16[48,2048]{1,0:T(8,128)(2,1)S(1)} %add_convert_fusion.1.refs_0_), channel_id=1, source_target_pairs={{0,1},{1,0},{2,3},{3,2},{4,5},{5,4},{6,7},{7,6},{8,9},{9,8},{10,11... | collective-permute-start | bytes 589832 | tf_op jit(solution)/shard_map/ppermute | solution.py:25
  150.4 4.9 %collective-permute-start.8 = (bf16[48,2048]{1,0:T(8,128)(2,1)S(1)}, bf16[48,2048]{1,0:T(8,128)(2,1)S(1)}, u32[]{:S(2)}, u32[]{:S(2)}) collective-permute-start(bf16[48,2048]{1,0:T(8,128)(2,1)S(1)} %collective-permute-done.4.refs_1_), channel_id=1, source_target_pairs={{0,1},{1,0},{2,3},{3,2},{4,5},{5,4},{6,7},{7,6},{8,9},{9,8},{10,11... | collective-permute-start | bytes 589832 | tf_op jit(solution)/shard_map/ppermute | solution.py:25
  152.8 3.3 %collective-permute-start.9 = (bf16[48,2048]{1,0:T(8,128)(2,1)S(1)}, bf16[48,2048]{1,0:T(8,128)(2,1)S(1)}, u32[]{:S(2)}, u32[]{:S(2)}) collective-permute-start(bf16[48,2048]{1,0:T(8,128)(2,1)S(1)} %collective-permute-done.5.refs_2_), channel_id=1, source_target_pairs={{0,1},{1,0},{2,3},{3,2},{4,5},{5,4},{6,7},{7,6},{8,9},{9,8},{10,11... | collective-permute-start | bytes 589832 | tf_op jit(solution)/shard_map/ppermute | solution.py:25
  155.3 4.5 %copy-start.8 = (bf16[48,2048]{1,0:T(8,128)(2,1)}, bf16[48,2048]{1,0:T(8,128)(2,1)S(1)}, u32[]{:S(2)}) copy-start(bf16[48,2048]{1,0:T(8,128)(2,1)S(1)} %collective-permute-done.10.refs_7_) | copy-start | bytes 589828
  155.3 4.5 %copy-start.9 = (bf16[48,2048]{1,0:T(8,128)(2,1)}, bf16[48,2048]{1,0:T(8,128)(2,1)S(1)}, u32[]{:S(2)}) copy-start(bf16[48,2048]{1,0:T(8,128)(2,1)S(1)} %collective-permute-done.7.refs_4_) | copy-start | bytes 589828
  155.3 4.5 %copy-start.10 = (bf16[48,2048]{1,0:T(8,128)(2,1)}, bf16[48,2048]{1,0:T(8,128)(2,1)S(1)}, u32[]{:S(2)}) copy-start(bf16[48,2048]{1,0:T(8,128)(2,1)S(1)} %collective-permute-done.8.refs_5_) | copy-start | bytes 589828
  156.1 3.7 %copy-start.11 = (bf16[48,2048]{1,0:T(8,128)(2,1)}, bf16[48,2048]{1,0:T(8,128)(2,1)S(1)}, u32[]{:S(2)}) copy-start(bf16[48,2048]{1,0:T(8,128)(2,1)S(1)} %collective-permute-done.9.refs_6_) | copy-start | bytes 589828
  156.1 0.7 copy-start.3

commit v4 on v3

v4 whole, which is shorter than its diff:
```python
import jax
import jax.numpy as jnp
from jax import lax
from jax.experimental import pallas as pl
from jax.experimental.pallas import tpu as pltpu
from jax.sharding import Mesh
from jax.sharding import PartitionSpec as P


SEQ_LEN = 128
SMALL_ROWS = 8


def copies_to(block, axis, size):
    copies = jnp.broadcast_to(block, (size, *block.shape))
    return lax.all_to_all(copies, axis, 0, 0, tiled=True)


def exchange(blocks, axis):
    return lax.all_to_all(blocks, axis, 0, 0, tiled=True)


def send_on(block, axis, shift):
    size = lax.axis_size(axis)
    return lax.ppermute(block, axis, [(i, (i + shift) % size) for i in range(size)])


def near(array):
    return pltpu.with_memory_space_constraint(array, pltpu.VMEM)


VMEM = pl.BlockSpec(memory_space=pltpu.VMEM)
HBM = pl.BlockSpec(memory_space=pltpu.HBM)


def cost(flops, count, exps=0):
    return pl.CostEstimate(flops=flops, bytes_accessed=count, transcendentals=exps)


def put_in_order(own, other, n_c):
    n_x = len(own)
    rows, width = own[0].shape

    def body(*refs):
        out_ref = refs[-1]
        at_x, at_c = lax.axis_index("x"), lax.axis_index("c")
        for k in range(n_x):
            spot = (at_x + n_x - k) % n_x
            out_ref[at_c * n_x + spot] = refs[k][...]
            out_ref[(1 - at_c) * n_x + spot] = refs[n_x + k][...]

    return pl.pallas_call(
        body,
        in_specs=[VMEM] * (2 * n_x),
        out_shape=jax.ShapeDtypeStruct((n_c * n_x, rows, width), own[0].dtype),
        cost_estimate=cost(0, 32 * own[0].size),
        name="put_in_order",
        compiler_params=pltpu.CompilerParams(vmem_limit_bytes=24 * 2**20),
    )(*(near(block) for block in (*own, *other)))


def later(values, offset):
    if offset == 0:
        return values
    rows = lax.broadcasted_iota(jnp.int32, values.shape, 0) % SEQ_LEN
    return jnp.where(rows >= offset, pltpu.roll(values, offset, 0), 0.0)


def earlier(values, offset):
    if offset == 0:
        return values
    count = values.shape[0]
    rows = lax.broadcasted_iota(jnp.int32, values.shape, 0) % SEQ_LEN
    return jnp.where(rows < SEQ_LEN - offset, pltpu.roll(values, count - offset, 0), 0.0)


def gated(up, taps_ref, bias_ref):
    tap_count = taps_ref.shape[0]
    total = bias_ref[...][None, :]
    for j in range(tap_count):
        total = total + taps_ref[j : j + 1, :] * later(up, tap_count - 1 - j)
    return total


def high_and_low(rows):
    high = rows.astype(jnp.bfloat16).astype(jnp.float32)
    return jnp.concatenate([high, rows - high], axis=0).astype(jnp.bfloat16)


def previous_branch(x_prev, plane, cotangent, value_prev, conv_taps, conv_bias, grad_scale, n_c):
    row_count, width = x_prev.shape
    n_y, n_zq, n_zm, shard_rows, units = plane.shape
    tap_count = conv_taps.shape[0]
    n_x = lax.axis_size("x")
    half_rows = row_count // n_c
    block_rows = half_rows // n_x
    each = width // n_y

    def body(
        x_ref,
        w_ref,
        cot_ref,
        value_ref,
        taps_ref,
        bias_ref,
        gv_ref,
        natural_ref,
        keep_ref,
        send_ref,
        by_y_out,
        gu_ref,
        turned_ref,
        by_y_ref,
        sems,
    ):
        spots = [
            (y, q, m, ((m * n_zq + q) * n_y + y) * shard_rows)
            for y in range(n_y)
            for q in range(n_zq)
            for m in range(n_zm)
        ]
        own_half = lax.axis_index("zm")
        for y in range(n_y):
            for q in range(n_zq):
                for m in range(n_zm):
                    half_at = (own_half + m) % n_zm
                    at = ((half_at * n_zq + q) * n_y + y) * shard_rows
                    natural_ref[pl.ds(pl.multiple_of(at, shard_rows), shard_rows)] = w_ref[y, q, m]
        up = jnp.dot(x_ref[...], natural_ref[...], preferred_element_type=jnp.float32)
        up = up.astype(jnp.bfloat16).astype(jnp.float32)
        gate = gated(up, taps_ref, bias_ref)
        sig = jax.nn.sigmoid(gate)
        cot = cot_ref[...].astype(jnp.float32)
        gv_ref[...] = (cot * gate * sig).astype(jnp.bfloat16)
        grad_gate = cot * value_ref[...].astype(jnp.float32) * sig * (1.0 + gate * (1.0 - sig))
        grad_up = jnp.zeros_like(grad_gate)
        for j in range(tap_count):
            grad_up = grad_up + taps_ref[j : j + 1, :] * earlier(grad_gate, tap_count - 1 - j)
        gu_ref[...] = grad_up.astype(jnp.bfloat16)

        at_x, at_c = lax.axis_index("x"), lax.axis_index("c")
        for i, half_ref in ((1, turned_ref), (0, keep_ref)):
            core = (at_c + i) % n_c
            for k in range(n_x):
                row = core * half_rows + ((at_x + k) % n_x) * block_rows
                half_ref[k * block_rows : (k + 1) * block_rows] = gu_ref[
                    pl.ds(pl.multiple_of(row, block_rows), block_rows)
                ]
        send_ref[...] = lax.dot_general(
            turned_ref[...],
            natural_ref[...],
            (((1,), (1,)), ((), ())),
            preferred_element_type=jnp.float32,
        ).astype(jnp.bfloat16)

        grad_w = lax.dot_general(
            x_ref[...], gu_ref[...], (((0,), (0,)), ((), ())), preferred_element_type=jnp.float32
        )
        grad_w = (grad_w * grad_scale).astype(jnp.bfloat16)
        sums = [
            jnp.sum(grad_gate * later(up, tap_count - 1 - j), axis=0, keepdims=True)
            for j in range(tap_count)
        ] + [jnp.sum(grad_gate, axis=0, keepdims=True)]
        rest = jnp.zeros((SMALL_ROWS - len(sums), units), jnp.float32)
        small = high_and_low(jnp.concatenate([*sums, rest], axis=0) * grad_scale)
        moves = []
        for y in range(n_y):
            for at_y, q, m, at in spots:
                if at_y == y:
                    to = (q * n_zm + m) * shard_rows
                    by_y_ref[y, to : to + shard_rows] = grad_w[at : at + shard_rows]
            by_y_ref[y, each:] = small
            moves.append(pltpu.make_async_copy(by_y_ref.at[y], by_y_out.at[y], sems.at[y]))
            moves[-1].start()
        for move in moves:
            move.wait()

    half = jnp.bfloat16
    return pl.pallas_call(
        body,
        in_specs=[VMEM] * 6,
        out_specs=[pl.BlockSpec(), VMEM, VMEM, pl.BlockSpec(), HBM],
        out_shape=[
            jax.ShapeDtypeStruct((row_count, units), half),
            pltpu.VMEM((width, units), half),
            pltpu.VMEM((half_rows, units), half),
            jax.ShapeDtypeStruct((half_rows, width), half),
            pltpu.HBM((n_y, each + 2 * SMALL_ROWS, units), half),
        ],
        scratch_shapes=[
            pltpu.VMEM((row_count, units), half),
            pltpu.VMEM((half_rows, units), half),
            pltpu.VMEM((n_y, each + 2 * SMALL_ROWS, units), half),
            pltpu.SemaphoreType.DMA((n_y,)),
        ],
        cost_estimate=cost(5 * row_count * width * units, 8 * width * units, row_count * units),
        name="previous_branch",
        compiler_params=pltpu.CompilerParams(vmem_limit_bytes=24 * 2**20),
    )(
        near(x_prev),
        near(plane),
        near(cotangent),
        near(value_prev),
        near(conv_taps),
        near(conv_bias),
    )


def next_branch(x_next, weights, value_next, conv_taps, conv_bias):
    row_count, width = x_next.shape
    units = weights.shape[1]

    def body(x_ref, w_ref, value_ref, taps_ref, bias_ref, out_ref):
        up = jnp.dot(x_ref[...], w_ref[...], preferred_element_type=jnp.float32)
        gate = gated(up.astype(jnp.bfloat16).astype(jnp.float32), taps_ref, bias_ref)
        hidden = gate * jax.nn.sigmoid(gate) * value_ref[...].astype(jnp.float32)
        out_ref[...] = hidden.astype(jnp.bfloat16)

    return pl.pallas_call(
        body,
        in_specs=[VMEM] * 5,
        out_shape=jax.ShapeDtypeStruct((row_count, units), jnp.bfloat16),
        cost_estimate=cost(2 * row_count * width * units, 4 * width * units, row_count * units),
        name="next_branch",
        compiler_params=pltpu.CompilerParams(vmem_limit_bytes=24 * 2**20),
    )(near(x_next), near(weights), near(value_next), near(conv_taps), near(conv_bias))


def summed(block):
    return jnp.sum(block.astype(jnp.float32), axis=0)


def small_total(block):
    total = summed(block)
    return total[:SMALL_ROWS] + total[SMALL_ROWS:]


def sum_and_repack(arrived, parts, repeats):
    _, rows, units = arrived.shape
    extra = 2 * SMALL_ROWS
    each = (rows - extra) // parts

    def body(in_ref, out_ref, block_ref, sems):
        small = high_and_low(small_total(in_ref[:, rows - extra :]))
        moves = []
        for p in range(parts):
            main = summed(in_ref[:, p * each : (p + 1) * each]).astype(jnp.bfloat16)
            block_ref[p, :each] = main
            block_ref[p, each:] = small
            for r in range(repeats):
                to = r * parts + p
                move = pltpu.make_async_copy(block_ref.at[p], out_ref.at[to], sems.at[to])
                move.start()
                moves.append(move)
        for move in moves:
            move.wait()

    return pl.pallas_call(
        body,
        in_specs=[VMEM],
        out_specs=HBM,
        out_shape=pltpu.HBM((repeats * parts, each + extra, units), jnp.bfloat16),
        scratch_shapes=[
            pltpu.VMEM((parts, each + extra, units), jnp.bfloat16),
            pltpu.SemaphoreType.DMA((repeats * parts,)),
        ],
        cost_estimate=cost(2 * arrived.size, 4 * arrived.size),
        name="sum_and_repack",
        compiler_params=pltpu.CompilerParams(vmem_limit_bytes=24 * 2**20),
    )(near(arrived))


def last_sum(arrived, sum_w, sum_taps, sum_bias):
    rows, _ = sum_w.shape
    tap_count = sum_taps.shape[0]

    def body(in_ref, w_ref, taps_ref, bias_ref, new_w_ref, new_taps_ref, new_bias_ref):
        new_w_ref[...] = w_ref[...] + summed(in_ref[:, :rows])
        small = small_total(in_ref[:, rows:])
        new_taps_ref[...] = taps_ref[...] + small[:tap_count]
        new_bias_ref[...] = bias_ref[...] + small[tap_count]

    return pl.pallas_call(
        body,
        in_specs=[VMEM] * 4,
        out_shape=[
            jax.ShapeDtypeStruct(sum_w.shape, jnp.float32),
            jax.ShapeDtypeStruct(sum_taps.shape, jnp.float32),
            jax.ShapeDtypeStruct(sum_bias.shape, jnp.float32),
        ],
        cost_estimate=cost(2 * arrived.size, 4 * arrived.size),
        name="last_sum",
        compiler_params=pltpu.CompilerParams(vmem_limit_bytes=24 * 2**20),
    )(near(arrived), near(sum_w), near(sum_taps), near(sum_bias))


def per_device(
    x_next,
    value_next,
    x_prev,
    value_prev,
    cotangent,
    w_gate,
    conv_taps,
    conv_bias,
    sum_w,
    sum_taps,
    sum_bias,
):
    row_count, width = x_next.shape
    n_zh, n_zm, n_zq, n_y = (lax.axis_size(a) for a in ("zh", "zm", "zq", "y"))
    n_x, n_c = lax.axis_size("x"), lax.axis_size("c")

    pair = jnp.stack([w_gate, send_on(w_gate, "zm", 1)])
    quad = copies_to(pair, "zq", n_zq)
    plane = copies_to(quad, "y", n_y)
    grad_scale = float(row_count * n_zh * n_zm * n_zq * n_y) ** (-0.5)
    grad_value, gathered, keep, to_core, by_y = previous_branch(
        x_prev, plane, cotangent, value_prev, conv_taps, conv_bias, grad_scale, n_c
    )
    from_core = send_on(to_core, "c", 1)
    from_y = exchange(by_y, "y")

    block_rows = row_count // (n_x * n_c)
    kept = lax.dot_general(
        keep, gathered, (((1,), (1,)), ((), ())), preferred_element_type=jnp.float32
    )
    half = (kept + from_core.astype(jnp.float32)).astype(jnp.bfloat16)
    half = half.reshape(n_x, block_rows, width)
    arrived = [half[0]] + [send_on(half[k], "x", k) for k in range(1, n_x)]
    from_y, *arrived = lax.optimization_barrier((from_y, *arrived))
    eighth = sum(block.astype(jnp.float32) for block in arrived).astype(jnp.bfloat16)
    spread = [eighth]
    for k in range(1, n_x):
        spread.append(send_on(eighth, "x", k))

    from_q = exchange(sum_and_repack(from_y, n_zq, 1), "zq")
    by_half = sum_and_repack(from_q, n_zm, n_zh)
    by_half, x_next = lax.optimization_barrier((by_half, x_next))
    from_half = exchange(by_half, ("zh", "zm"))
    hidden_next = next_branch(x_next, gathered, value_next, conv_taps, conv_bias)
    hidden_next, *spread = lax.optimization_barrier((hidden_next, *spread))
    other = [send_on(block, "c", 1) for block in spread]
    grad_input = put_in_order(spread, other, n_c).reshape(row_count, width)
    from_half, grad_input = lax.optimization_barrier((from_half, grad_input))
    new_w, new_taps, new_bias = last_sum(from_half, sum_w, sum_taps, sum_bias)
    return hidden_next, grad_input, grad_value, new_w, new_taps, new_bias


def solution(mesh):
    n_fs, n_tp = mesh.shape["fs"], mesh.shape["tp"]
    n_y, n_zq, n_c = 4, 4, 2
    fine = Mesh(
        mesh.devices.reshape(
            mesh.shape["rep"], n_fs // (n_y * n_zq), n_zq, n_y, n_tp // n_c, n_c
        ),
        ("zh", "zm", "zq", "y", "x", "c"),
    )
    fs, tp = ("zm", "zq", "y"), ("x", "c")
    tokens = ("zh", *fs)
    in_specs = (
        P(tokens, None),
        P(tokens, tp),
        P(tokens, None),
        P(tokens, tp),
        P(tokens, tp),
        P(fs, tp),
        P(None, tp),
        P(tp),
        P(fs, tp),
        P(None, tp),
        P(tp),
    )
    out_specs = (
        P(tokens, tp),
        P(tokens, None),
        P(tokens, tp),
        P(fs, tp),
        P(None, tp),
        P(tp),
    )
    return jax.shard_map(
        per_device, mesh=fine, in_specs=in_specs, out_specs=out_specs, check_vma=False
    )
```

time: 164 us -> 146 us (0.89)
  blocking collectives: 32.2 us -> 56.5 us
  Pallas kernels: 30.9 us -> 11.2 us
  waiting for transfers between devices: 29.2 us -> 12.1 us
  local copies, waits for them, and re-layouts: 7.29 us -> 2.69 us
    all_to_all x1 -> x2, blocking collectives: 15.8 us -> 40.6 us  [copies_to(): return lax.all_to_all(copies, axis, 0, 0, tiled=True)]
    pallas_call x8 -> x6, Pallas kernels: 30.9 us -> 11.2 us  [the longest x1 5.68 us: previous_branch(): pl.pallas_call(body, in_specs=[VMEM] * 6, out_specs=[pl.BlockSpec(), VMEM...]
    all_to_all x2 -> x0, waiting for transfers between devices: 19.6 us -> none  [copies_to(): return lax.all_to_all(copies, axis, 0, 0, tiled=True)]
    all_to_all x2 -> x0, starting transfers between devices: 9.98 us -> none  [copies_to(): return lax.all_to_all(copies, axis, 0, 0, tiled=True)]
    ppermute x11 -> x12, starting transfers between devices: 38.7 us -> 46.3 us  [send_on(): lax.ppermute(block, axis, [(i, (i + shift) % size) for i in range(size)])]
    ppermute x11 -> x12, waiting for transfers between devices: 6.43 us -> 9.59 us  [send_on(): lax.ppermute(block, axis, [(i, (i + shift) % size) for i in range(size)])]
    broadcast_in_dim x3 -> x2, local copies, waits for them, and re-layouts: 2.98 us -> 0.28 us  [copies_to(): copies = jnp.broadcast_to(block, (size, *block.shape))]
  transfers between devices with their start and end apart: 15 -> 14, of which waited for: 6 -> 6; matrix products, arithmetic and copies ran while one was open for 2% -> 3% of each run, Pallas kernels for 9% -> 2%
where the time goes in v4:
time: 146 us; the launch traced here: 145 us
  starting transfers between devices  57.7 us (40%)
  blocking collectives  56.5 us (39%)
  waiting for transfers between devices  12.1 us (8%)
  Pallas kernels  11.2 us (8%)
  local copies, waits for them, and re-layouts  2.69 us (2%)
  other arithmetic  2.13 us (1%)
  matrix products  1.84 us (1%)
    ppermute x12, starting transfers between devices, send_on(): lax.ppermute(block, axis, [(i, (i + shift) % size) for i in range(size)])  46.3 us
    all_to_all x2, blocking collectives, copies_to(): return lax.all_to_all(copies, axis, 0, 0, tiled=True)  40.6 us
    all_to_all x1, blocking collectives, exchange(): return lax.all_to_all(blocks, axis, 0, 0, tiled=True)  15.9 us
    all_to_all x2, starting transfers between devices, exchange(): return lax.all_to_all(blocks, axis, 0, 0, tiled=True)  11.4 us
    ppermute x12, waiting for transfers between devices, send_on(): lax.ppermute(block, axis, [(i, (i + shift) % size) for i in range(size)])  9.59 us
    pallas_call x1, Pallas kernels, previous_branch(): pl.pallas_call(body, in_specs=[VMEM] * 6, out_specs=[pl.BlockSpec(), VMEM...  5.68 us
  transfers between devices with their start and end apart: 14, of which 6 were waited for; matrix products, arithmetic and copies ran while one was open for 3% of the time, Pallas kernels for 2%

profile of v4, /device:TPU:1, one launch (start us, length us, event | category | flops | bytes accessed | tf_op | source)
XLA Modules:
  0.0 145.1 jit_solution(5912685530007786250)
XLA Ops:
  0.6 9.6 %collective-permute-start = (bf16[64,384]{1,0:T(8,128)(2,1)}, bf16[64,384]{1,0:T(8,128)(2,1)S(1)}, u32[]{:S(2)}, u32[]{:S(2)}) collective-permute-start(bf16[64,384]{1,0:T(8,128)(2,1)} %param.16), channel_id=1, source_target_pairs={{0,128},{128,0},{1,129},{129,1},{2,130},{130,2},{3,131},{131,3},{4... | collective-permute-start | bytes 147464 | tf_op jit(solution)/shard_map/ppermute | solution.py:25
  10.3 1.7 %collective-permute-done = bf16[64,384]{1,0:T(8,128)(2,1)S(1)} collective-permute-done((bf16[64,384]{1,0:T(8,128)(2,1)}, bf16[64,384]{1,0:T(8,128)(2,1)S(1)}, u32[]{:S(2)}, u32[]{:S(2)}) %collective-permute-start) | collective-permute-done | bytes 49184 | tf_op jit(solution)/shard_map/ppermute | solution.py:25
  11.9 0.8 pad_maximum_fusion
  12.8 17.5 %all_to_all.25 = bf16[4,2,64,384]{3,2,1,0:T(8,128)(2,1)S(1)} all-to-all(bf16[4,2,64,384]{3,2,1,0:T(8,128)(2,1)S(1)} %broadcast_in_dim.6), channel_id=1, replica_groups=mesh['zh'=2,'zm'=2,'zq'=4,'y'=4,'x'=4,'c'=2] {'zq'}, dimensions={0} | all-to-all | bytes 786432 | tf_op jit(solution)/shard_map/all_to_all | solution.py:16
  30.3 0.2 broadcast_in_dim.7
  30.6 0.0 copy-start.3
  30.6 0.0 copy-start.5
  30.6 0.0 copy-start.7
  30.6 0.0 copy-start.8
  30.6 0.0 copy-start.9
  30.6 23.1 %all_to_all.26.w_ref = bf16[4,4,2,64,384]{4,3,2,1,0:T(8,128)(2,1)S(1)} all-to-all(bf16[4,4,2,64,384]{4,3,2,1,0:T(8,128)(2,1)S(1)} %broadcast_in_dim.7), channel_id=1, replica_groups=mesh['zh'=2,'zm'=2,'zq'=4,'y'=4,'x'=4,'c'=2] {'y'}, dimensions={0} | all-to-all | bytes 3145728 | tf_op jit(solution)/shard_map/all_to_all | solution.py:16
  53.8 0.0 copy-done.3
  53.8 0.0 copy-done.5
  53.8 0.0 copy-done.7
  53.8 0.0 copy-done.8
  53.8 0.0 copy-done.9
  53.8 5.7 %previous_branch.1 = (bf16[384,384]{1,0:T(8,128)(2,1)}, bf16[2048,384]{1,0:T(8,128)(2,1)S(1)}, bf16[192,384]{1,0:T(8,128)(2,1)S(1)}, bf16[192,2048]{1,0:T(8,128)(2,1)}, bf16[4,528,384]{2,1,0:T(8,128)(2,1)}) custom-call(bf16[384,2048]{1,0:T(8,128)(2,1)S(1)} %copy-done.7, bf16[4,4,2,64,384]{4,3,2,1,0:T(8,128)(2,1)S(1)} %all_to_all.26.w_ref, ...), custom_call_target="tpu_custom_call" | custom-call | flops 1509949440 | bytes 6291456 | tf_op jit(solution)/shard_map/previous_branch/pallas_call | solution.py:179
  59.5 5.1 %collective-permute-start.1 = (bf16[192,2048]{1,0:T(8,128)(2,1)}, bf16[192,2048]{1,0:T(8,128)(2,1)}, u32[]{:S(2)}, u32[]{:S(2)}) collective-permute-start(bf16[192,2048]{1,0:T(8,128)(2,1)} %get-tuple-element.31), channel_id=1, source_target_pairs={{0,1},{1,0},{2,3},{3,2},{4,5},{5,4},{6,7},{7,6},{8,9},{9,8},{10,11... | collective-permute-start | bytes 2359304 | tf_op jit(solution)/shard_map/ppermute | solution.py:25
  64.6 3.6 %all-to-all-start.2 = ((bf16[4,528,384]{2,1,0:T(8,128)(2,1)}), bf16[4,528,384]{2,1,0:T(8,128)(2,1)S(1)}, u32[]{:S(2)}, u32[]{:S(2)}) async-start(bf16[4,528,384]{2,1,0:T(8,128)(2,1)} %get-tuple-element.28), calls=%async_computation.2 | async-start | bytes 3244032 | tf_op jit(solution)/shard_map/all_to_all | solution.py:20
  68.2 0.0 collective-permute-done.1
  68.2 1.8 %add_convert_fusion = bf16[192,2048]{1,0:T(8,128)(2,1)S(1)} fusion(bf16[192,2048]{1,0:T(8,128)(2,1)} %collective-permute-done.1, bf16[192,384]{1,0:T(8,128)(2,1)S(1)} %get-tuple-element.29, bf16[2048,384]{1,0:T(8,128)(2,1)S(1)} %get-tuple-element.30.w_ref), kind=kOutput, calls=%fused_computation | convolution fusion | flops 303169536 | bytes 3293184 | tf_op jit(solution)/shard_map/dot_general | solution.py:325
  70.0 0.7 fusion
  70.8 3.1 %collective-permute-start.2 = (bf16[48,2048]{1,0:T(8,128)(2,1)S(1)}, bf16[48,2048]{1,0:T(8,128)(2,1)S(1)}, u32[]{:S(2)}, u32[]{:S(2)}) collective-permute-start(bf16[48,2048]{1,0:T(8,128)(2,1)S(1)} %get-tuple-element.52), channel_id=1, source_target_pairs={{0,2},{2,4},{4,6},{6,0},{1,3},{3,5},{5,7},{7,1},{8,10},{10,12},{12... | collective-permute-start | bytes 589832 | tf_op jit(solution)/shard_map/ppermute | solution.py:25
  73.9 4.4 %collective-permute-start.3 = (bf16[48,2048]{1,0:T(8,128)(2,1)S(1)}, bf16[48,2048]{1,0:T(8,128)(2,1)S(1)}, u32[]{:S(2)}, u32[]{:S(2)}) collective-permute-start(bf16[48,2048]{1,0:T(8,128)(2,1)S(1)} %get-tuple-element.51), channel_id=1, source_target_pairs={{0,4},{2,6},{4,0},{6,2},{1,5},{3,7},{5,1},{7,3},{8,12},{10,14},{12... | collective-permute-start | bytes 589832 | tf_op jit(solution)/shard_map/ppermute | solution.py:25
  78.2 3.1 %collective-permute-start.4 = (bf16[48,2048]{1,0:T(8,128)(2,1)S(1)}, bf16[48,2048]{1,0:T(8,128)(2,1)}, u32[]{:S(2)}, u32[]{:S(2)}) collective-permute-start(bf16[48,2048]{1,0:T(8,128)(2,1)S(1)} %get-tuple-element.50), channel_id=1, source_target_pairs={{0,6},{2,0},{4,2},{6,4},{1,7},{3,1},{5,3},{7,5},{8,14},{10,8},{12,... | collective-permute-start | bytes 589832 | tf_op jit(solution)/shard_map/ppermute | solution.py:25
  81.3 0.0 collective-permute-done.2
  81.3 0.0 copy-start.10
  81.3 4.2 %collective-permute-done.3 = bf16[48,2048]{1,0:T(8,128)(2,1)S(1)} collective-permute-done((bf16[48,2048]{1,0:T(8,128)(2,1)S(1)}, bf16[48,2048]{1,0:T(8,128)(2,1)S(1)}, u32[]{:S(2)}, u32[]{:S(2)}) %collective-permute-start.3) | collective-permute-done | bytes 196640 | tf_op jit(solution)/shard_map/ppermute | solution.py:25
  85.5 0.0 copy-done.10
  85.5 0.0 copy-start.11
  85.5 0.7 copy-done.11
  86.2 0.8 collective-permute-done.4
  87.0 2.5 %all-to-all-done.2.in_ref = bf16[4,528,384]{2,1,0:T(8,128)(2,1)S(1)} async-done(((bf16[4,528,384]{2,1,0:T(8,128)(2,1)}), bf16[4,528,384]{2,1,0:T(8,128)(2,1)S(1)}, u32[]{:S(2)}, u32[]{:S(2)}) %all-to-all-start.2) | async-done | bytes 1622048 | tf_op jit(solution)/shard_map/all_to_all | solution.py:20
  89.4 0.9 sum_and_repack.2
  90.3 0.0 copy-start
  90.4 15.9 %all_to_all.27.in_ref = bf16[4,144,384]{2,1,0:T(8,128)(2,1)S(1)} all-to-all(bf16[4,144,384]{2,1,0:T(8,128)(2,1)} %sum_and_repack.2), channel_id=1, replica_groups=mesh['zh'=2,'zm'=2,'zq'=4,'y'=4,'x'=4,'c'=2] {'zq'}, dimensions={0} | all-to-all | bytes 884736 | tf_op jit(solution)/shard_map/all_to_all | solution.py:20
  106.2 0.8 sum_and_repack.3
  107.0 7.8 %all-to-all-start.4 = ((bf16[4,80,384]{2,1,0:T(8,128)(2,1)}), bf16[4,80,384]{2,1,0:T(8,128)(2,1)S(1)}, u32[]{:S(2)}, u32[]{:S(2)}) async-start(bf16[4,80,384]{2,1,0:T(8,128)(2,1)} %sum_and_repack.3), calls=%async_computation.4 | async-start | bytes 491520 | tf_op jit(solution)/shard_map/all_to_all | solution.py:20
  114.8 1.3 add_convert_fusion.1.refs_0_
  116.1 3.1 %collective-permute-start.5 = (bf16[48,2048]{1,0:T(8,128)(2,1)S(1)}, bf16[48,2048]{1,0:T(8,128)(2,1)S(1)}, u32[]{:S(2)}, u32[]{:S(2)}) collective-permute-start(bf16[48,2048]{1,0:T(8,128)(2,1)S(1)} %add_convert_fusion.1.refs_0_), channel_id=1, source_target_pairs={{0,2},{2,4},{4,6},{6,0},{1,3},{3,5},{5,7},{7,1},{8,10},{10,12},{12... | collective-permute-start | bytes 589832 | tf_op jit(solution)/shard_map/ppermute | solution.py:25
  119.2 4.4 %collective-permute-start.6 = (bf16[48,2048]{1,0:T(8,128)(2,1)S(1)}, bf16[48,2048]{1,0:T(8,128)(2,1)S(1)}, u32[]{:S(2)}, u32[]{:S(2)}) collective-permute-start(bf16[48,2048]{1,0:T(8,128)(2,1)S(1)} %add_convert_fusion.1.refs_0_), channel_id=1, source_target_pairs={{0,4},{2,6},{4,0},{6,2},{1,5},{3,7},{5,1},{7,3},{8,12},{10,14},{12... | collective-permute-start | bytes 589832 | tf_op jit(solution)/shard_map/ppermute | solution.py:25
  123.6 3.0 %collective-permute-start.7 = (bf16[48,2048]{1,0:T(8,128)(2,1)S(1)}, bf16[48,2048]{1,0:T(8,128)(2,1)S(1)}, u32[]{:S(2)}, u32[]{:S(2)}) collective-permute-start(bf16[48,2048]{1,0:T(8,128)(2,1)S(1)} %add_convert_fusion.1.refs_0_), channel_id=1, source_target_pairs={{0,6},{2,0},{4,2},{6,4},{1,7},{3,1},{5,3},{7,5},{8,14},{10,8},{12,... | collective-permute-start | bytes 589832 | tf_op jit(solution)/shard_map/ppermute | solution.py:25
  126.7 0.0 copy-done
  126.7 0.0 copy-start.1
  126.7 1.0 copy-done.1
  127.6 1.9 %next_branch.1 = bf16[384,384]{1,0:T(8,128)(2,1)} custom-call(bf16[384,2048]{1,0:T(8,128)(2,1)S(1)} %copy-done, bf16[2048,384]{1,0:T(8,128)(2,1)S(1)} %get-tuple-element.30.w_ref, bf16[384,384]{1,0:T(8,128)(2,1)S(1)} %copy-done.1, f32[3,384]{1,0:T(4,128)S(1)} %copy-done.3, f32[384]{0:T(512)S(1)} %copy-done.5), custom_call_target="tpu_custom_call" | custom-call | flops 603979776 | bytes 3145728 | tf_op jit(solution)/shard_map/next_branch/pallas_call | solution.py:219
  129.6 0.0 copy-start.2
  129.6 0.0 collective-permute-done.5.refs_1_
  129.6 0.0 collective-permute-done.6.refs_2_
  129.6 1.6 %collective-permute-done.7.refs_3_ = bf16[48,2048]{1,0:T(8,128)(2,1)S(1)} collective-permute-done((bf16[48,2048]{1,0:T(8,128)(2,1)S(1)}, bf16[48,2048]{1,0:T(8,128)(2,1)S(1)}, u32[]{:S(2)}, u32[]{:S(2)}) %collective-permute-start.7) | collective-permute-done | bytes 196640 | tf_op jit(solution)/shard_map/ppermute | solution.py:25
  131.2 4.3 %collective-permute-start.10 = (bf16[48,2048]{1,0:T(8,128)(2,1)S(1)}, bf16[48,2048]{1,0:T(8,128)(2,1)S(1)}, u32[]{:S(2)}, u32[]{:S(2)}) collective-permute-start(bf16[48,2048]{1,0:T(8,128)(2,1)S(1)} %collective-permute-done.6.refs_2_), channel_id=1, source_target_pairs={{0,1},{1,0},{2,3},{3,2},{4,5},{5,4},{6,7},{7,6},{8,9},{9,8},{10,11... | collective-permute-start | bytes 589832 | tf_op jit(solution)/shard_map/ppermute | solution.py:25
  135.5 1.9 %collective-permute-start.11 = (bf16[48,2048]{1,0:T(8,128)(2,1)S(1)}, bf16[48,2048]{1,0:T(8,128)(2,1)S(1)}, u32[]{:S(2)}, u32[]{:S(2)}) collective-permute-start(bf16[48,2048]{1,0:T(8,128)(2,1)S(1)} %collective-permute-done.7.refs_3_), channel_id=1, source_target_pairs={{0,1},{1,0},{2,3},{3,2},{4,5},{5,4},{6,7},{7,6},{8,9},{9,8},{10,11... | collective-permute-start | bytes 589832 | tf_op jit(solution)/shard_map/ppermute | solution.py:25
  137.4 2.4 %collective-permute-start.8 = (bf16[48,2048]{1,0:T(8,128)(2,1)S(1)}, bf16[48,2048]{1,0:T(8,128)(2,1)S(1)}, u32[]{:S(2)}, u32[]{:S(2)}) collective-permute-start(bf16[48,2048]{1,0:T(8,128)(2,1)S(1)} %add_convert_fusion.1.refs_0_), channel_id=1, source_target_pairs={{0,1},{1,0},{2,3},{3,2},{4,5},{5,4},{6,7},{7,6},{8,9},{9,8},{10,11... | collective-permute-start | bytes 589832 | tf_op jit(solution)/shard_map/ppermute | solution.py:25
  139.8 1.9 %collective-permute-start.9 = (bf16[48,2048]{1,0:T(8,128)(2,1)S(1)}, bf16[48,2048]{1,0:T(8,128)(2,1)S(1)}, u32[]{:S(2)}, u32[]{:S(2)}) collective-permute-start(bf16[48,2048]{1,0:T(8,128)(2,1)S(1)} %collective-permute-done.5.refs_1_), channel_id=1, source_target_pairs={{0,1},{1,0},{2,3},{3,2},{4,5},{5,4},{6,7},{7,6},{8,9},{9,8},{10,11... | collective-permute-start | bytes 589832 | tf_op jit(solution)/shard_map/ppermute | solution.py:25
  141.7 0.0 collective-permute-done.10.refs_6_
  141.7 0.0 collective-permute-done.11.refs_7_
  141.7 0.0 collective-permute-done.8.refs_4_
  141.8 1.4 collective-permute-done.9.refs_5_
  143.1 1.3 put_in_order.1
  144.4 0.0 all-to-all-done.4.in_ref
  144.4 0.0 copy-done.2
  144.4 0.0 copy-done.4
  144.4 0.0 copy-done.6
  144.4 0.7 last_sum.1
  (3 shorter events, 0.0 us)
Async XLA Ops:
  0.6 11.3 %collective-permute-start = (bf16[64,384]{1,0:T(8,128)(2,1)}, bf16[64,384]{1,0:T(8,128)(2,1)S(1)}, u32[]{:S(2)}, u32[]{:S(2)}) collective-permute-start(bf16[64,384]{1,0:T(8,128)(2,1)} %param.16), channel_id=1, source_target_pairs={{0,128},{128,0},{1,129},{129,1},{2,130},{130,2},{3,131},{131,3},{4... | collective-permute-start | bytes 147464 | tf_op jit(solution)/shard_map/ppermute | solution.py:25
  30.6 23.2 %copy-start.3 = (f32[3,384]{1,0:T(4,128)S(1)}, f32[3,384]{1,0:T(4,128)}, u32[]{:S(2)}) copy-start(f32[3,384]{1,0:T(4,128)} %taps_ref.4) | copy-start | bytes 13828
  30.6 23.2 %copy-start.5 = (f32[384]{0:T(512)S(1)}, f32[384]{0:T(512)}, u32[]{:S(2)}) copy-start(f32[384]{0:T(512)} %bias_ref.4) | copy-start | bytes 4612
  30.6 23.2 %copy-start.7 = (bf16[384,2048]{1,0:T(8,128)(2,1)S(1)}, bf16[384,2048]{1,0:T(8,128)(2,1)}, u32[]{:S(2)}) copy-start(bf16[384,2048]{1,0:T(8,128)(2,1)} %x_ref.1) | copy-start | bytes 4718596
  30.6 23.2 %copy-start.8 = (bf16[384,384]{1,0:T(8,128)(2,1)S(1)}, bf16[384,384]{1,0:T(8,128)(2,1)}, u32[]{:S(2)}) copy-start(bf16[384,384]{1,0:T(8,128)(2,1)} %cot_ref.1) | copy-start | bytes 884740
  30.6 23.2 %copy-start.9 = (bf16[384,384]{1,0:T(8,128)(2,1)S(1)}, bf16[384,384]{1,0:T(8,128)(2,1)}, u32[]{:S(2)}) copy-start(bf16[384,384]{1,0:T(8,128)(2,1)} %value_ref.2) | copy-start | bytes 884740
  59.5 8.7 %collective-permute-start.1 = (bf16[192,2048]{1,0:T(8,128)(2,1)}, bf16[192,2048]{1,0:T(8,128)(2,1)}, u32[]{:S(2)}, u32[]{:S(2)}) collective-permute-start(bf16[192,2048]{1,0:T(8,128)(2,1)} %get-tuple-element.31), channel_id=1, source_target_pairs={{0,1},{1,0},{2,3},{3,2},{4,5},{5,4},{6,7},{7,6},{8,9},{9,8},{10,11... | collective-permute-start | bytes 2359304 | tf_op jit(solution)/shard_map/ppermute | solution.py:25
  64.6 24.9 %all-to-all-start.2 = ((bf16[4,528,384]{2,1,0:T(8,128)(2,1)}), bf16[4,528,384]{2,1,0:T(8,128)(2,1)S(1)}, u32[]{:S(2)}, u32[]{:S(2)}) async-start(bf16[4,528,384]{2,1,0:T(8,128)(2,1)} %get-tuple-element.28), calls=%async_computation.2 | async-start | bytes 3244032 | tf_op jit(solution)/shard_map/all_to_all | solution.py:20
  70.8 10.6 %collective-permute-start.2 = (bf16[48,2048]{1,0:T(8,128)(2,1)S(1)}, bf16[48,2048]{1,0:T(8,128)(2,1)S(1)}, u32[]{:S(2)}, u32[]{:S(2)}) collective-permute-start(bf16[48,2048]{1,0:T(8,128)(2,1)S(1)} %get-tuple-element.52), channel_id=1, source_target_pairs={{0,2},{2,4},{4,6},{6,0},{1,3},{3,5},{5,7},{7,1},{8,10},{10,12},{12... | collective-permute-start | bytes 589832 | tf_op jit(solution)/shard_map/ppermute | solution.py:25
  73.9 11.6 %collective-permute-start.3 = (bf16[48,2048]{1,0:T(8,128)(2,1)S(1)}, bf16[48,2048]{1,0:T(8,128)(2,1)S(1)}, u32[]{:S(2)}, u32[]{:S(2)}) collective-permute-start(bf16[48,2048]{1,0:T(8,128)(2,1)S(1)} %get-tuple-element.51), channel_id=1, source_target_pairs={{0,4},{2,6},{4,0},{6,2},{1,5},{3,7},{5,1},{7,3},{8,12},{10,14},{12... | collective-permute-start | bytes 589832 | tf_op jit(solution)/shard_map/ppermute | solution.py:25
  78.2 8.7 %collective-permute-start.4 = (bf16[48,2048]{1,0:T(8,128)(2,1)S(1)}, bf16[48,2048]{1,0:T(8,128)(2,1)}, u32[]{:S(2)}, u32[]{:S(2)}) collective-permute-start(bf16[48,2048]{1,0:T(8,128)(2,1)S(1)} %get-tuple-element.50), channel_id=1, source_target_pairs={{0,6},{2,0},{4,2},{6,4},{1,7},{3,1},{5,3},{7,5},{8,14},{10,8},{12,... | collective-permute-start | bytes 589832 | tf_op jit(solution)/shard_map/ppermute | solution.py:25
  81.3 4.2 %copy-start.10 = (bf16[48,2048]{1,0:T(8,128)(2,1)}, bf16[48,2048]{1,0:T(8,128)(2,1)S(1)}, u32[]{:S(2)}) copy-start(bf16[48,2048]{1,0:T(8,128)(2,1)S(1)} %collective-permute-done.2) | copy-start | bytes 589828
  85.5 0.7 copy-start.11
  90.3 36.3 %copy-start = (bf16[384,2048]{1,0:T(8,128)(2,1)S(1)}, bf16[384,2048]{1,0:T(8,128)(2,1)}, u32[]{:S(2)}) copy-start(bf16[384,2048]{1,0:T(8,128)(2,1)} %x_ref.2) | copy-start | bytes 4718596
  107.0 37.4 %all-to-all-start.4 = ((bf16[4,80,384]{2,1,0:T(8,128)(2,1)}), bf16[4,80,384]{2,1,0:T(8,128)(2,1)S(1)}, u32[]{:S(2)}, u32[]{:S(2)}) async-start(bf16[4,80,384]{2,1,0:T(8,128)(2,1)} %sum_and_repack.3), calls=%async_computation.4 | async-start | bytes 491520 | tf_op jit(solution)/shard_map/all_to_all | solution.py:20
  116.1 13.5 %collective-permute-start.5 = (bf16[48,2048]{1,0:T(8,128)(2,1)S(1)}, bf16[48,2048]{1,0:T(8,128)(2,1)S(1)}, u32[]{:S(2)}, u32[]{:S(2)}) collective-permute-start(bf16[48,2048]{1,0:T(8,128)(2,1)S(1)} %add_convert_fusion.1.refs_0_), channel_id=1, source_target_pairs={{0,2},{2,4},{4,6},{6,0},{1,3},{3,5},{5,7},{7,1},{8,10},{10,12},{12... | collective-permute-start | bytes 589832 | tf_op jit(solution)/shard_map/ppermute | solution.py:25
  119.2 10.4 %collective-permute-start.6 = (bf16[48,2048]{1,0:T(8,128)(2,1)S(1)}, bf16[48,2048]{1,0:T(8,128)(2,1)S(1)}, u32[]{:S(2)}, u32[]{:S(2)}) collective-permute-start(bf16[48,2048]{1,0:T(8,128)(2,1)S(1)} %add_convert_fusion.1.refs_0_), channel_id=1, source_target_pairs={{0,4},{2,6},{4,0},{6,2},{1,5},{3,7},{5,1},{7,3},{8,12},{10,14},{12... | collective-permute-start | bytes 589832 | tf_op jit(solution)/shard_map/ppermute | solution.py:25
  123.6 7.6 %collective-permute-start.7 = (bf16[48,2048]{1,0:T(8,128)(2,1)S(1)}, bf16[48,2048]{1,0:T(8,128)(2,1)S(1)}, u32[]{:S(2)}, u32[]{:S(2)}) collective-permute-start(bf16[48,2048]{1,0:T(8,128)(2,1)S(1)} %add_convert_fusion.1.refs_0_), channel_id=1, source_target_pairs={{0,6},{2,0},{4,2},{6,4},{1,7},{3,1},{5,3},{7,5},{8,14},{10,8},{12,... | collective-permute-start | bytes 589832 | tf_op jit(solution)/shard_map/ppermute | solution.py:25
  126.7 1.0 copy-start.1
  129.6 14.8 %copy-start.2 = (f32[64,384]{1,0:T(8,128)S(1)}, f32[64,384]{1,0:T(8,128)}, u32[]{:S(2)}) copy-start(f32[64,384]{1,0:T(8,128)} %w_ref.1) | copy-start | bytes 294916
  129.6 14.8 %copy-start.4 = (f32[3,384]{1,0:T(4,128)S(1)}, f32[3,384]{1,0:T(4,128)}, u32[]{:S(2)}) copy-start(f32[3,384]{1,0:T(4,128)} %taps_ref.5) | copy-start | bytes 13828
  129.6 14.8 %copy-start.6 = (f32[384]{0:T(512)S(1)}, f32[384]{0:T(512)}, u32[]{:S(2)}) copy-start(f32[384]{0:T(512)} %bias_ref.5) | copy-start | bytes 4612
  131.2 10.5 %collective-permute-start.10 = (bf16[48,2048]{1,0:T(8,128)(2,1)S(1)}, bf16[48,2048]{1,0:T(8,128)(2,1)S(1)}, u32[]{:S(2)}, u32[]{:S(2)}) collective-permute-start(bf16[48,2048]{1,0:T(8,128)(2,1)S(1)} %collective-permute-done.6.refs_2_), channel_id=1, source_target_pairs={{0,1},{1,0},{2,3},{3,2},{4,5},{5,4},{6,7},{7,6},{8,9},{9,8},{10,11... | collective-permute-start | bytes 589832 | tf_op jit(solution)/shard_map/ppermute | solution.py:25
  135.5 6.3 %collective-permute-start.11 = (bf16[48,2048]{1,0:T(8,128)(2,1)S(1)}, bf16[48,2048]{1,0:T(8,128)(2,1)S(1)}, u32[]{:S(2)}, u32[]{:S(2)}) collective-permute-start(bf16[48,2048]{1,0:T(8,128)(2,1)S(1)} %collective-permute-done.7.refs_3_), channel_id=1, source_target_pairs={{0,1},{1,0},{2,3},{3,2},{4,5},{5,4},{6,7},{7,6},{8,9},{9,8},{10,11... | collective-permute-start | bytes 589832 | tf_op jit(solution)/shard_map/ppermute | solution.py:25
  137.4 4.4 %collective-permute-start.8 = (bf16[48,2048]{1,0:T(8,128)(2,1)S(1)}, bf16[48,2048]{1,0:T(8,128)(2,1)S(1)}, u32[]{:S(2)}, u32[]{:S(2)}) collective-permute-start(bf16[48,2048]{1,0:T(8,128)(2,1)S(1)} %add_convert_fusion.1.refs_0_), channel_id=1, source_target_pairs={{0,1},{1,0},{2,3},{3,2},{4,5},{5,4},{6,7},{7,6},{8,9},{9,8},{10,11... | collective-permute-start | bytes 589832 | tf_op jit(solution)/shard_map/ppermute | solution.py:25
  139.8 3.3 %collective-permute-start.9 = (bf16[48,2048]{1,0:T(8,128)(2,1)S(1)}, bf16[48,2048]{1,0:T(8,128)(2,1)S(1)}, u32[]{:S(2)}, u32[]{:S(2)}) collective-permute-start(bf16[48,2048]{1,0:T(8,128)(2,1)S(1)} %collective-permute-done.5.refs_1_), channel_id=1, source_target_pairs={{0,1},{1,0},{2,3},{3,2},{4,5},{5,4},{6,7},{7,6},{8,9},{9,8},{10,11... | collective-permute-start | bytes 589832 | tf_op jit(solution)/shard_map/ppermute | solution.py:25

commit v5 on v4

--- a/solution.py
+++ b/solution.py
@@ -6,9 +6,9 @@
 from jax.sharding import Mesh
 from jax.sharding import PartitionSpec as P
 
-
 SEQ_LEN = 128
 SMALL_ROWS = 8
+FAR, NEAR = ("zm", "zp"), ("zl", "y")
 
 
 def copies_to(block, axis, size):
@@ -23,6 +23,10 @@
 def send_on(block, axis, shift):
     size = lax.axis_size(axis)
     return lax.ppermute(block, axis, [(i, (i + shift) % size) for i in range(size)])
+
+
+def whole(shape):
+    return pl.BlockSpec(shape, lambda *_: (0,) * len(shape))
 
 
 def near(array):
@@ -84,17 +88,18 @@
 
 def high_and_low(rows):
     high = rows.astype(jnp.bfloat16).astype(jnp.float32)
-    return jnp.concatenate([high, rows - high], axis=0).astype(jnp.bfloat16)
+    half = SMALL_ROWS // 2
+    return (high + pltpu.roll(rows - high, half, 0)).astype(jnp.bfloat16)
 
 
 def previous_branch(x_prev, plane, cotangent, value_prev, conv_taps, conv_bias, grad_scale, n_c):
     row_count, width = x_prev.shape
-    n_y, n_zq, n_zm, shard_rows, units = plane.shape
+    n_near, n_far, shard_rows, units = plane.shape
     tap_count = conv_taps.shape[0]
     n_x = lax.axis_size("x")
     half_rows = row_count // n_c
     block_rows = half_rows // n_x
-    each = width // n_y
+    each = n_far * shard_rows
 
     def body(
         x_ref,
@@ -107,25 +112,19 @@
         natural_ref,
         keep_ref,
         send_ref,
-        by_y_out,
+        sent_out,
         gu_ref,
         turned_ref,
-        by_y_ref,
+        sent_ref,
         sems,
     ):
         spots = [
-            (y, q, m, ((m * n_zq + q) * n_y + y) * shard_rows)
-            for y in range(n_y)
-            for q in range(n_zq)
-            for m in range(n_zm)
+            (near_at, far_at, (far_at * n_near + near_at) * shard_rows)
+            for near_at in range(n_near)
+            for far_at in range(n_far)
         ]
-        own_half = lax.axis_index("zm")
-        for y in range(n_y):
-            for q in range(n_zq):
-                for m in range(n_zm):
-                    half_at = (own_half + m) % n_zm
-                    at = ((half_at * n_zq + q) * n_y + y) * shard_rows
-                    natural_ref[pl.ds(pl.multiple_of(at, shard_rows), shard_rows)] = w_ref[y, q, m]
+        for near_at, far_at, at in spots:
+            natural_ref[at : at + shard_rows] = w_ref[near_at, far_at]
         up = jnp.dot(x_ref[...], natural_ref[...], preferred_element_type=jnp.float32)
         up = up.astype(jnp.bfloat16).astype(jnp.float32)
         gate = gated(up, taps_ref, bias_ref)
@@ -164,13 +163,15 @@
         rest = jnp.zeros((SMALL_ROWS - len(sums), units), jnp.float32)
         small = high_and_low(jnp.concatenate([*sums, rest], axis=0) * grad_scale)
         moves = []
-        for y in range(n_y):
-            for at_y, q, m, at in spots:
-                if at_y == y:
-                    to = (q * n_zm + m) * shard_rows
-                    by_y_ref[y, to : to + shard_rows] = grad_w[at : at + shard_rows]
-            by_y_ref[y, each:] = small
-            moves.append(pltpu.make_async_copy(by_y_ref.at[y], by_y_out.at[y], sems.at[y]))
+        for block in range(n_near):
+            for near_at, far_at, at in spots:
+                if near_at == block:
+                    to = far_at * shard_rows
+                    sent_ref[block, to : to + shard_rows] = grad_w[at : at + shard_rows]
+            sent_ref[block, each:] = small
+            moves.append(
+                pltpu.make_async_copy(sent_ref.at[block], sent_out.at[block], sems.at[block])
+            )
             moves[-1].start()
         for move in moves:
             move.wait()
@@ -185,13 +186,13 @@
             pltpu.VMEM((width, units), half),
             pltpu.VMEM((half_rows, units), half),
             jax.ShapeDtypeStruct((half_rows, width), half),
-            pltpu.HBM((n_y, each + 2 * SMALL_ROWS, units), half),
+            pltpu.HBM((n_near, each + SMALL_ROWS, units), half),
         ],
         scratch_shapes=[
             pltpu.VMEM((row_count, units), half),
             pltpu.VMEM((half_rows, units), half),
-            pltpu.VMEM((n_y, each + 2 * SMALL_ROWS, units), half),
-            pltpu.SemaphoreType.DMA((n_y,)),
+            pltpu.VMEM((n_near, each + SMALL_ROWS, units), half),
+            pltpu.SemaphoreType.DMA((n_near,)),
         ],
         cost_estimate=cost(5 * row_count * width * units, 8 * width * units, row_count * units),
         name="previous_branch",
@@ -232,12 +233,14 @@
 
 def small_total(block):
     total = summed(block)
-    return total[:SMALL_ROWS] + total[SMALL_ROWS:]
+    half = SMALL_ROWS // 2
+    rows = lax.broadcasted_iota(jnp.int32, total.shape, 0)
+    return jnp.where(rows < half, total + pltpu.roll(total, half, 0), 0.0)
 
 
 def sum_and_repack(arrived, parts, repeats):
-    _, rows, units = arrived.shape
-    extra = 2 * SMALL_ROWS
+    count, rows, units = arrived.shape
+    extra = SMALL_ROWS
     each = (rows - extra) // parts
 
     def body(in_ref, out_ref, block_ref, sems):
@@ -271,7 +274,7 @@
 
 
 def last_sum(arrived, sum_w, sum_taps, sum_bias):
-    rows, _ = sum_w.shape
+    rows, units = sum_w.shape
     tap_count = sum_taps.shape[0]
 
     def body(in_ref, w_ref, taps_ref, bias_ref, new_w_ref, new_taps_ref, new_bias_ref):
@@ -308,18 +311,17 @@
     sum_bias,
 ):
     row_count, width = x_next.shape
-    n_zh, n_zm, n_zq, n_y = (lax.axis_size(a) for a in ("zh", "zm", "zq", "y"))
-    n_x, n_c = lax.axis_size("x"), lax.axis_size("c")
-
-    pair = jnp.stack([w_gate, send_on(w_gate, "zm", 1)])
-    quad = copies_to(pair, "zq", n_zq)
-    plane = copies_to(quad, "y", n_y)
-    grad_scale = float(row_count * n_zh * n_zm * n_zq * n_y) ** (-0.5)
-    grad_value, gathered, keep, to_core, by_y = previous_branch(
+    shard_rows, units = w_gate.shape
+    n_zh, n_x, n_c = (lax.axis_size(a) for a in ("zh", "x", "c"))
+    n_far, n_near = lax.axis_size(FAR), lax.axis_size(NEAR)
+
+    plane = copies_to(copies_to(w_gate, FAR, n_far), NEAR, n_near)
+    grad_scale = float(row_count * n_zh * n_far * n_near) ** (-0.5)
+    grad_value, gathered, keep, to_core, sent = previous_branch(
         x_prev, plane, cotangent, value_prev, conv_taps, conv_bias, grad_scale, n_c
     )
     from_core = send_on(to_core, "c", 1)
-    from_y = exchange(by_y, "y")
+    from_near = exchange(sent, NEAR)
 
     block_rows = row_count // (n_x * n_c)
     kept = lax.dot_general(
@@ -328,35 +330,28 @@
     half = (kept + from_core.astype(jnp.float32)).astype(jnp.bfloat16)
     half = half.reshape(n_x, block_rows, width)
     arrived = [half[0]] + [send_on(half[k], "x", k) for k in range(1, n_x)]
-    from_y, *arrived = lax.optimization_barrier((from_y, *arrived))
+    hidden_next = next_branch(x_next, gathered, value_next, conv_taps, conv_bias)
+    from_near, hidden_next, *arrived = lax.optimization_barrier((from_near, hidden_next, *arrived))
     eighth = sum(block.astype(jnp.float32) for block in arrived).astype(jnp.bfloat16)
-    spread = [eighth]
-    for k in range(1, n_x):
-        spread.append(send_on(eighth, "x", k))
-
-    from_q = exchange(sum_and_repack(from_y, n_zq, 1), "zq")
-    by_half = sum_and_repack(from_q, n_zm, n_zh)
-    by_half, x_next = lax.optimization_barrier((by_half, x_next))
-    from_half = exchange(by_half, ("zh", "zm"))
-    hidden_next = next_branch(x_next, gathered, value_next, conv_taps, conv_bias)
-    hidden_next, *spread = lax.optimization_barrier((hidden_next, *spread))
+    spread = [eighth] + [send_on(eighth, "x", k) for k in range(1, n_x)]
     other = [send_on(block, "c", 1) for block in spread]
     grad_input = put_in_order(spread, other, n_c).reshape(row_count, width)
-    from_half, grad_input = lax.optimization_barrier((from_half, grad_input))
-    new_w, new_taps, new_bias = last_sum(from_half, sum_w, sum_taps, sum_bias)
+
+    from_far = exchange(sum_and_repack(from_near, n_far, n_zh), ("zh", *FAR))
+    from_far, grad_input = lax.optimization_barrier((from_far, grad_input))
+    new_w, new_taps, new_bias = last_sum(from_far, sum_w, sum_taps, sum_bias)
     return hidden_next, grad_input, grad_value, new_w, new_taps, new_bias
 
 
 def solution(mesh):
     n_fs, n_tp = mesh.shape["fs"], mesh.shape["tp"]
-    n_y, n_zq, n_c = 4, 4, 2
+    n_y, n_c = 4, 2
+    n_z = n_fs // n_y
     fine = Mesh(
-        mesh.devices.reshape(
-            mesh.shape["rep"], n_fs // (n_y * n_zq), n_zq, n_y, n_tp // n_c, n_c
-        ),
-        ("zh", "zm", "zq", "y", "x", "c"),
-    )
-    fs, tp = ("zm", "zq", "y"), ("x", "c")
+        mesh.devices.reshape(mesh.shape["rep"], n_z // 4, 2, 2, n_y, n_tp // n_c, n_c),
+        ("zh", *FAR, *NEAR, "x", "c"),
+    )
+    fs, tp = (*FAR, *NEAR), ("x", "c")
     tokens = ("zh", *fs)
     in_specs = (
         P(tokens, None),

time: 146 us -> 124 us (0.85)
  the two profiles are of different devices: /device:TPU:1 before, /device:TPU:34 now
where the time goes in v5:
time: 124 us; the launch traced here: 123 us
  blocking collectives  50.1 us (40%)
  starting transfers between devices  43.7 us (35%)
  waiting for transfers between devices  13.5 us (11%)
  Pallas kernels  10.2 us (8%)
  local copies, waits for them, and re-layouts  2.73 us (2%)
    all_to_all x2, blocking collectives, copies_to(): return lax.all_to_all(copies, axis, 0, 0, tiled=True)  50.1 us
    ppermute x11, starting transfers between devices, send_on(): lax.ppermute(block, axis, [(i, (i + shift) % size) for i in range(size)])  31.4 us
    all_to_all x2, starting transfers between devices, exchange(): return lax.all_to_all(blocks, axis, 0, 0, tiled=True)  12.3 us
    ppermute x11, waiting for transfers between devices, send_on(): lax.ppermute(block, axis, [(i, (i + shift) % size) for i in range(size)])  8.09 us
    all_to_all x2, waiting for transfers between devices, exchange(): return lax.all_to_all(blocks, axis, 0, 0, tiled=True)  5.36 us
    pallas_call x1, Pallas kernels, previous_branch(): pl.pallas_call(body, in_specs=[VMEM] * 6, out_specs=[pl.BlockSpec(), VMEM...  5.32 us
  transfers between devices with their start and end apart: 13, of which 5 were waited for; matrix products, arithmetic and copies ran while one was open for 1% of the time, Pallas kernels for 3%

profile of v5, /device:TPU:34, one launch (start us, length us, event | category | flops | bytes accessed | tf_op | source)
XLA Modules:
  0.0 122.8 jit_solution(13708763678988571777)
XLA Ops:
  0.6 0.8 broadcast_in_dim.6
  1.5 24.6 %all_to_all.20 = bf16[4,64,384]{2,1,0:T(8,128)(2,1)S(1)} all-to-all(bf16[4,64,384]{2,1,0:T(8,128)(2,1)S(1)} %broadcast_in_dim.6), channel_id=1, replica_groups=mesh['zh'=2,'zm'=2,'zp'=2,'zl'=2,'y'=4,'x'=4,'c'=2] {'zm','zp'}, dimensions={0} | all-to-all | bytes 393216 | tf_op jit(solution)/shard_map/all_to_all | solution.py:16
  26.1 0.2 broadcast_in_dim.7
  26.3 0.0 copy-start.3
  26.3 0.0 copy-start.5
  26.3 0.0 copy-start.7
  26.3 0.0 copy-start.9
  26.3 0.0 copy-start.10
  26.4 25.5 %all_to_all.21.w_ref = bf16[8,4,64,384]{3,2,1,0:T(8,128)(2,1)S(1)} all-to-all(bf16[8,4,64,384]{3,2,1,0:T(8,128)(2,1)S(1)} %broadcast_in_dim.7), channel_id=1, replica_groups=mesh['zh'=2,'zm'=2,'zp'=2,'zl'=2,'y'=4,'x'=4,'c'=2] {'zl','y'}, dimensions={0} | all-to-all | bytes 3145728 | tf_op jit(solution)/shard_map/all_to_all | solution.py:16
  51.8 0.0 copy-done.3
  51.8 0.0 copy-done.5
  51.8 0.0 copy-done.7
  51.8 0.0 copy-done.9
  51.9 0.0 copy-done.10
  51.9 5.3 %previous_branch.1 = (bf16[384,384]{1,0:T(8,128)(2,1)}, bf16[2048,384]{1,0:T(8,128)(2,1)S(1)}, bf16[192,384]{1,0:T(8,128)(2,1)S(1)}, bf16[192,2048]{1,0:T(8,128)(2,1)S(1)}, bf16[8,264,384]{2,1,0:T(8,128)(2,1)}) custom-call(bf16[384,2048]{1,0:T(8,128)(2,1)S(1)} %copy-done.7, bf16[8,4,64,384]{3,2,1,0:T(8,128)(2,1)S(1)} %all_to_all.21.w_ref, ...), custom_call_target="tpu_custom_call" | custom-call | flops 1509949440 | bytes 6291456 | tf_op jit(solution)/shard_map/previous_branch/pallas_call | solution.py:180
  57.2 0.0 copy-start.8
  57.2 0.9 copy-done.8
  58.1 4.9 %all-to-all-start.2 = ((bf16[8,264,384]{2,1,0:T(8,128)(2,1)}), bf16[8,264,384]{2,1,0:T(8,128)(2,1)S(1)}, u32[]{:S(2)}, u32[]{:S(2)}) async-start(bf16[8,264,384]{2,1,0:T(8,128)(2,1)} %get-tuple-element.22), calls=%async_computation.2 | async-start | bytes 3244032 | tf_op jit(solution)/shard_map/all_to_all | solution.py:20
  63.0 1.9 %collective-permute-start = (bf16[192,2048]{1,0:T(8,128)(2,1)}, bf16[192,2048]{1,0:T(8,128)(2,1)S(1)}, u32[]{:S(2)}, u32[]{:S(2)}) collective-permute-start(bf16[192,2048]{1,0:T(8,128)(2,1)} %copy-done.8), channel_id=1, source_target_pairs={{0,1},{1,0},{2,3},{3,2},{4,5},{5,4},{6,7},{7,6},{8,9},{9,8},{10,11... | collective-permute-start | bytes 2359304 | tf_op jit(solution)/shard_map/ppermute | solution.py:25
  64.9 2.5 %collective-permute-done = bf16[192,2048]{1,0:T(8,128)(2,1)S(1)} collective-permute-done((bf16[192,2048]{1,0:T(8,128)(2,1)}, bf16[192,2048]{1,0:T(8,128)(2,1)S(1)}, u32[]{:S(2)}, u32[]{:S(2)}) %collective-permute-start) | collective-permute-done | bytes 786464 | tf_op jit(solution)/shard_map/ppermute | solution.py:25
  67.3 0.0 copy-start.1
  67.3 0.7 add_convert_fusion
  68.0 0.0 copy-start
  68.1 0.1 fusion
  68.1 3.5 %collective-permute-start.1 = (bf16[48,2048]{1,0:T(8,128)(2,1)S(1)}, bf16[48,2048]{1,0:T(8,128)(2,1)S(1)}, u32[]{:S(2)}, u32[]{:S(2)}) collective-permute-start(bf16[48,2048]{1,0:T(8,128)(2,1)S(1)} %get-tuple-element.40), channel_id=1, source_target_pairs={{0,2},{2,4},{4,6},{6,0},{1,3},{3,5},{5,7},{7,1},{8,10},{10,12},{12... | collective-permute-start | bytes 589832 | tf_op jit(solution)/shard_map/ppermute | solution.py:25
  71.7 3.0 %collective-permute-start.2 = (bf16[48,2048]{1,0:T(8,128)(2,1)S(1)}, bf16[48,2048]{1,0:T(8,128)(2,1)S(1)}, u32[]{:S(2)}, u32[]{:S(2)}) collective-permute-start(bf16[48,2048]{1,0:T(8,128)(2,1)S(1)} %get-tuple-element.39), channel_id=1, source_target_pairs={{0,4},{2,6},{4,0},{6,2},{1,5},{3,7},{5,1},{7,3},{8,12},{10,14},{12... | collective-permute-start | bytes 589832 | tf_op jit(solution)/shard_map/ppermute | solution.py:25
  74.7 4.1 %collective-permute-start.3 = (bf16[48,2048]{1,0:T(8,128)(2,1)S(1)}, bf16[48,2048]{1,0:T(8,128)(2,1)}, u32[]{:S(2)}, u32[]{:S(2)}) collective-permute-start(bf16[48,2048]{1,0:T(8,128)(2,1)S(1)} %get-tuple-element.38), channel_id=1, source_target_pairs={{0,6},{2,0},{4,2},{6,4},{1,7},{3,1},{5,3},{7,5},{8,14},{10,8},{12,... | collective-permute-start | bytes 589832 | tf_op jit(solution)/shard_map/ppermute | solution.py:25
  78.8 0.0 copy-done.1
  78.8 0.0 copy-done
  78.8 2.0 %next_branch.1 = bf16[384,384]{1,0:T(8,128)(2,1)} custom-call(bf16[384,2048]{1,0:T(8,128)(2,1)S(1)} %copy-done, bf16[2048,384]{1,0:T(8,128)(2,1)S(1)} %get-tuple-element.23.w_ref, bf16[384,384]{1,0:T(8,128)(2,1)S(1)} %copy-done.1, f32[3,384]{1,0:T(4,128)S(1)} %copy-done.3, f32[384]{0:T(512)S(1)} %copy-done.5), custom_call_target="tpu_custom_call" | custom-call | flops 603979776 | bytes 3145728 | tf_op jit(solution)/shard_map/next_branch/pallas_call | solution.py:220
  80.8 0.0 collective-permute-done.1
  80.8 2.1 %collective-permute-done.2 = bf16[48,2048]{1,0:T(8,128)(2,1)S(1)} collective-permute-done((bf16[48,2048]{1,0:T(8,128)(2,1)S(1)}, bf16[48,2048]{1,0:T(8,128)(2,1)S(1)}, u32[]{:S(2)}, u32[]{:S(2)}) %collective-permute-start.2) | collective-permute-done | bytes 196640 | tf_op jit(solution)/shard_map/ppermute | solution.py:25
  82.9 0.0 copy-done.11
  82.9 0.7 copy-done.13
  83.6 2.5 %collective-permute-done.3 = bf16[48,2048]{1,0:T(8,128)(2,1)} collective-permute-done((bf16[48,2048]{1,0:T(8,128)(2,1)S(1)}, bf16[48,2048]{1,0:T(8,128)(2,1)}, u32[]{:S(2)}, u32[]{:S(2)}) %collective-permute-start.3) | collective-permute-done | bytes 196640 | tf_op jit(solution)/shard_map/ppermute | solution.py:25
  86.0 0.0 all-to-all-done.2.in_ref
  86.0 0.9 sum_and_repack.1
  87.0 7.4 %all-to-all-start.3 = ((bf16[8,72,384]{2,1,0:T(8,128)(2,1)}), bf16[8,72,384]{2,1,0:T(8,128)(2,1)S(1)}, u32[]{:S(2)}, u32[]{:S(2)}) async-start(bf16[8,72,384]{2,1,0:T(8,128)(2,1)} %sum_and_repack.1), calls=%async_computation.3 | async-start | bytes 884736 | tf_op jit(solution)/shard_map/all_to_all | solution.py:20
  94.4 0.0 copy-done.12
  94.4 0.0 copy-done.14
  94.4 1.0 add_convert_fusion.1.refs_0_
  95.4 0.0 copy-start.2
  95.5 0.0 copy-start.4
  95.5 0.0 copy-start.6
  95.5 2.1 %collective-permute-start.6 = (bf16[48,2048]{1,0:T(8,128)(2,1)S(1)}, bf16[48,2048]{1,0:T(8,128)(2,1)S(1)}, u32[]{:S(2)}, u32[]{:S(2)}) collective-permute-start(bf16[48,2048]{1,0:T(8,128)(2,1)S(1)} %add_convert_fusion.1.refs_0_), channel_id=1, source_target_pairs={{0,6},{2,0},{4,2},{6,4},{1,7},{3,1},{5,3},{7,5},{8,14},{10,8},{12,... | collective-permute-start | bytes 589832 | tf_op jit(solution)/shard_map/ppermute | solution.py:25
  97.5 3.9 %collective-permute-start.4 = (bf16[48,2048]{1,0:T(8,128)(2,1)S(1)}, bf16[48,2048]{1,0:T(8,128)(2,1)S(1)}, u32[]{:S(2)}, u32[]{:S(2)}) collective-permute-start(bf16[48,2048]{1,0:T(8,128)(2,1)S(1)} %add_convert_fusion.1.refs_0_), channel_id=1, source_target_pairs={{0,2},{2,4},{4,6},{6,0},{1,3},{3,5},{5,7},{7,1},{8,10},{10,12},{12... | collective-permute-start | bytes 589832 | tf_op jit(solution)/shard_map/ppermute | solution.py:25
  101.5 4.2 %collective-permute-start.5 = (bf16[48,2048]{1,0:T(8,128)(2,1)S(1)}, bf16[48,2048]{1,0:T(8,128)(2,1)S(1)}, u32[]{:S(2)}, u32[]{:S(2)}) collective-permute-start(bf16[48,2048]{1,0:T(8,128)(2,1)S(1)} %add_convert_fusion.1.refs_0_), channel_id=1, source_target_pairs={{0,4},{2,6},{4,0},{6,2},{1,5},{3,7},{5,1},{7,3},{8,12},{10,14},{12... | collective-permute-start | bytes 589832 | tf_op jit(solution)/shard_map/ppermute | solution.py:25
  105.7 1.9 %collective-permute-start.7 = (bf16[48,2048]{1,0:T(8,128)(2,1)S(1)}, bf16[48,2048]{1,0:T(8,128)(2,1)S(1)}, u32[]{:S(2)}, u32[]{:S(2)}) collective-permute-start(bf16[48,2048]{1,0:T(8,128)(2,1)S(1)} %add_convert_fusion.1.refs_0_), channel_id=1, source_target_pairs={{0,1},{1,0},{2,3},{3,2},{4,5},{5,4},{6,7},{7,6},{8,9},{9,8},{10,11... | collective-permute-start | bytes 589832 | tf_op jit(solution)/shard_map/ppermute | solution.py:25
  107.6 0.0 collective-permute-done.6.refs_3_
  107.7 2.4 %collective-permute-start.10 = (bf16[48,2048]{1,0:T(8,128)(2,1)S(1)}, bf16[48,2048]{1,0:T(8,128)(2,1)S(1)}, u32[]{:S(2)}, u32[]{:S(2)}) collective-permute-start(bf16[48,2048]{1,0:T(8,128)(2,1)S(1)} %collective-permute-done.6.refs_3_), channel_id=1, source_target_pairs={{0,1},{1,0},{2,3},{3,2},{4,5},{5,4},{6,7},{7,6},{8,9},{9,8},{10,11... | collective-permute-start | bytes 589832 | tf_op jit(solution)/shard_map/ppermute | solution.py:25
  110.1 0.0 collective-permute-done.4.refs_1_
  110.1 1.9 %collective-permute-start.8 = (bf16[48,2048]{1,0:T(8,128)(2,1)S(1)}, bf16[48,2048]{1,0:T(8,128)(2,1)S(1)}, u32[]{:S(2)}, u32[]{:S(2)}) collective-permute-start(bf16[48,2048]{1,0:T(8,128)(2,1)S(1)} %collective-permute-done.4.refs_1_), channel_id=1, source_target_pairs={{0,1},{1,0},{2,3},{3,2},{4,5},{5,4},{6,7},{7,6},{8,9},{9,8},{10,11... | collective-permute-start | bytes 589832 | tf_op jit(solution)/shard_map/ppermute | solution.py:25
  112.0 0.0 collective-permute-done.5.refs_2_
  112.0 2.4 %collective-permute-start.9 = (bf16[48,2048]{1,0:T(8,128)(2,1)S(1)}, bf16[48,2048]{1,0:T(8,128)(2,1)S(1)}, u32[]{:S(2)}, u32[]{:S(2)}) collective-permute-start(bf16[48,2048]{1,0:T(8,128)(2,1)S(1)} %collective-permute-done.5.refs_2_), channel_id=1, source_target_pairs={{0,1},{1,0},{2,3},{3,2},{4,5},{5,4},{6,7},{7,6},{8,9},{9,8},{10,11... | collective-permute-start | bytes 589832 | tf_op jit(solution)/shard_map/ppermute | solution.py:25
  114.4 0.0 collective-permute-done.7.refs_4_
  114.4 0.0 collective-permute-done.10.refs_7_
  114.5 0.0 collective-permute-done.8.refs_5_
  114.5 1.0 collective-permute-done.9.refs_6_
  115.5 1.3 %put_in_order.1 = bf16[8,48,2048]{2,1,0:T(8,128)(2,1)} custom-call(bf16[48,2048]{1,0:T(8,128)(2,1)S(1)} %add_convert_fusion.1.refs_0_, bf16[48,2048]{1,0:T(8,128)(2,1)S(1)} %collective-permute-done.4.refs_1_, bf16[48,2048]{1,0:T(8,128)(2,1)S(1)} %collective-permute-done.5.refs_2_, bf16[48,2048]{1,0:T(8,128)(2,1)S(1)} %collective-permute-done.6.refs_3_, ...), custom_call_target="tpu_custom_call" | custom-call | bytes 3145728 | tf_op jit(solution)/shard_map/put_in_order/pallas_call | solution.py:56
  116.8 5.4 %all-to-all-done.3.in_ref = bf16[8,72,384]{2,1,0:T(8,128)(2,1)S(1)} async-done(((bf16[8,72,384]{2,1,0:T(8,128)(2,1)}), bf16[8,72,384]{2,1,0:T(8,128)(2,1)S(1)}, u32[]{:S(2)}, u32[]{:S(2)}) %all-to-all-start.3) | async-done | bytes 442400 | tf_op jit(solution)/shard_map/all_to_all | solution.py:20
  122.1 0.0 copy-done.2
  122.1 0.0 copy-done.4
  122.1 0.0 copy-done.6
  122.1 0.7 last_sum.1
  (4 shorter events, 0.0 us)
Async XLA Ops:
  26.3 25.5 %copy-start.3 = (f32[3,384]{1,0:T(4,128)S(1)}, f32[3,384]{1,0:T(4,128)}, u32[]{:S(2)}) copy-start(f32[3,384]{1,0:T(4,128)} %taps_ref.4) | copy-start | bytes 13828
  26.3 25.5 %copy-start.5 = (f32[384]{0:T(512)S(1)}, f32[384]{0:T(512)}, u32[]{:S(2)}) copy-start(f32[384]{0:T(512)} %bias_ref.4) | copy-start | bytes 4612
  26.3 25.5 %copy-start.7 = (bf16[384,2048]{1,0:T(8,128)(2,1)S(1)}, bf16[384,2048]{1,0:T(8,128)(2,1)}, u32[]{:S(2)}) copy-start(bf16[384,2048]{1,0:T(8,128)(2,1)} %x_ref.2) | copy-start | bytes 4718596
  26.3 25.5 %copy-start.9 = (bf16[384,384]{1,0:T(8,128)(2,1)S(1)}, bf16[384,384]{1,0:T(8,128)(2,1)}, u32[]{:S(2)}) copy-start(bf16[384,384]{1,0:T(8,128)(2,1)} %cot_ref.1) | copy-start | bytes 884740
  26.3 25.5 %copy-start.10 = (bf16[384,384]{1,0:T(8,128)(2,1)S(1)}, bf16[384,384]{1,0:T(8,128)(2,1)}, u32[]{:S(2)}) copy-start(bf16[384,384]{1,0:T(8,128)(2,1)} %value_ref.2) | copy-start | bytes 884740
  57.2 0.9 copy-start.8
  58.1 28.0 %all-to-all-start.2 = ((bf16[8,264,384]{2,1,0:T(8,128)(2,1)}), bf16[8,264,384]{2,1,0:T(8,128)(2,1)S(1)}, u32[]{:S(2)}, u32[]{:S(2)}) async-start(bf16[8,264,384]{2,1,0:T(8,128)(2,1)} %get-tuple-element.22), calls=%async_computation.2 | async-start | bytes 3244032 | tf_op jit(solution)/shard_map/all_to_all | solution.py:20
  63.0 4.4 %collective-permute-start = (bf16[192,2048]{1,0:T(8,128)(2,1)}, bf16[192,2048]{1,0:T(8,128)(2,1)S(1)}, u32[]{:S(2)}, u32[]{:S(2)}) collective-permute-start(bf16[192,2048]{1,0:T(8,128)(2,1)} %copy-done.8), channel_id=1, source_target_pairs={{0,1},{1,0},{2,3},{3,2},{4,5},{5,4},{6,7},{7,6},{8,9},{9,8},{10,11... | collective-permute-start | bytes 2359304 | tf_op jit(solution)/shard_map/ppermute | solution.py:25
  67.3 11.4 %copy-start.1 = (bf16[384,384]{1,0:T(8,128)(2,1)S(1)}, bf16[384,384]{1,0:T(8,128)(2,1)}, u32[]{:S(2)}) copy-start(bf16[384,384]{1,0:T(8,128)(2,1)} %value_ref.3) | copy-start | bytes 884740
  68.0 10.7 %copy-start = (bf16[384,2048]{1,0:T(8,128)(2,1)S(1)}, bf16[384,2048]{1,0:T(8,128)(2,1)}, u32[]{:S(2)}) copy-start(bf16[384,2048]{1,0:T(8,128)(2,1)} %x_ref.3) | copy-start | bytes 4718596
  68.1 12.6 %collective-permute-start.1 = (bf16[48,2048]{1,0:T(8,128)(2,1)S(1)}, bf16[48,2048]{1,0:T(8,128)(2,1)S(1)}, u32[]{:S(2)}, u32[]{:S(2)}) collective-permute-start(bf16[48,2048]{1,0:T(8,128)(2,1)S(1)} %get-tuple-element.40), channel_id=1, source_target_pairs={{0,2},{2,4},{4,6},{6,0},{1,3},{3,5},{5,7},{7,1},{8,10},{10,12},{12... | collective-permute-start | bytes 589832 | tf_op jit(solution)/shard_map/ppermute | solution.py:25
  71.7 11.2 %collective-permute-start.2 = (bf16[48,2048]{1,0:T(8,128)(2,1)S(1)}, bf16[48,2048]{1,0:T(8,128)(2,1)S(1)}, u32[]{:S(2)}, u32[]{:S(2)}) collective-permute-start(bf16[48,2048]{1,0:T(8,128)(2,1)S(1)} %get-tuple-element.39), channel_id=1, source_target_pairs={{0,4},{2,6},{4,0},{6,2},{1,5},{3,7},{5,1},{7,3},{8,12},{10,14},{12... | collective-permute-start | bytes 589832 | tf_op jit(solution)/shard_map/ppermute | solution.py:25
  74.7 11.3 %collective-permute-start.3 = (bf16[48,2048]{1,0:T(8,128)(2,1)S(1)}, bf16[48,2048]{1,0:T(8,128)(2,1)}, u32[]{:S(2)}, u32[]{:S(2)}) collective-permute-start(bf16[48,2048]{1,0:T(8,128)(2,1)S(1)} %get-tuple-element.38), channel_id=1, source_target_pairs={{0,6},{2,0},{4,2},{6,4},{1,7},{3,1},{5,3},{7,5},{8,14},{10,8},{12,... | collective-permute-start | bytes 589832 | tf_op jit(solution)/shard_map/ppermute | solution.py:25
  80.8 2.1 %copy-start.11 = (bf16[48,2048]{1,0:T(8,128)(2,1)}, bf16[48,2048]{1,0:T(8,128)(2,1)S(1)}, u32[]{:S(2)}) copy-start(bf16[48,2048]{1,0:T(8,128)(2,1)S(1)} %collective-permute-done.1) | copy-start | bytes 589828
  82.9 0.7 copy-start.13
  86.0 8.4 %copy-start.12 = (bf16[48,2048]{1,0:T(8,128)(2,1)S(1)}, bf16[48,2048]{1,0:T(8,128)(2,1)}, u32[]{:S(2)}) copy-start(bf16[48,2048]{1,0:T(8,128)(2,1)} %copy-done.11) | copy-start | bytes 589828
  86.0 8.4 %copy-start.14 = (bf16[48,2048]{1,0:T(8,128)(2,1)S(1)}, bf16[48,2048]{1,0:T(8,128)(2,1)}, u32[]{:S(2)}) copy-start(bf16[48,2048]{1,0:T(8,128)(2,1)} %copy-done.13) | copy-start | bytes 589828
  87.0 35.1 %all-to-all-start.3 = ((bf16[8,72,384]{2,1,0:T(8,128)(2,1)}), bf16[8,72,384]{2,1,0:T(8,128)(2,1)S(1)}, u32[]{:S(2)}, u32[]{:S(2)}) async-start(bf16[8,72,384]{2,1,0:T(8,128)(2,1)} %sum_and_repack.1), calls=%async_computation.3 | async-start | bytes 884736 | tf_op jit(solution)/shard_map/all_to_all | solution.py:20
  95.4 26.7 %copy-start.2 = (f32[64,384]{1,0:T(8,128)S(1)}, f32[64,384]{1,0:T(8,128)}, u32[]{:S(2)}) copy-start(f32[64,384]{1,0:T(8,128)} %w_ref.1) | copy-start | bytes 294916
  95.5 26.7 %copy-start.4 = (f32[3,384]{1,0:T(4,128)S(1)}, f32[3,384]{1,0:T(4,128)}, u32[]{:S(2)}) copy-start(f32[3,384]{1,0:T(4,128)} %taps_ref.5) | copy-start | bytes 13828
  95.5 26.6 %copy-start.6 = (f32[384]{0:T(512)S(1)}, f32[384]{0:T(512)}, u32[]{:S(2)}) copy-start(f32[384]{0:T(512)} %bias_ref.5) | copy-start | bytes 4612
  95.5 12.2 %collective-permute-start.6 = (bf16[48,2048]{1,0:T(8,128)(2,1)S(1)}, bf16[48,2048]{1,0:T(8,128)(2,1)S(1)}, u32[]{:S(2)}, u32[]{:S(2)}) collective-permute-start(bf16[48,2048]{1,0:T(8,128)(2,1)S(1)} %add_convert_fusion.1.refs_0_), channel_id=1, source_target_pairs={{0,6},{2,0},{4,2},{6,4},{1,7},{3,1},{5,3},{7,5},{8,14},{10,8},{12,... | collective-permute-start | bytes 589832 | tf_op jit(solution)/shard_map/ppermute | solution.py:25
  97.5 12.5 %collective-permute-start.4 = (bf16[48,2048]{1,0:T(8,128)(2,1)S(1)}, bf16[48,2048]{1,0:T(8,128)(2,1)S(1)}, u32[]{:S(2)}, u32[]{:S(2)}) collective-permute-start(bf16[48,2048]{1,0:T(8,128)(2,1)S(1)} %add_convert_fusion.1.refs_0_), channel_id=1, source_target_pairs={{0,2},{2,4},{4,6},{6,0},{1,3},{3,5},{5,7},{7,1},{8,10},{10,12},{12... | collective-permute-start | bytes 589832 | tf_op jit(solution)/shard_map/ppermute | solution.py:25
  101.5 10.5 %collective-permute-start.5 = (bf16[48,2048]{1,0:T(8,128)(2,1)S(1)}, bf16[48,2048]{1,0:T(8,128)(2,1)S(1)}, u32[]{:S(2)}, u32[]{:S(2)}) collective-permute-start(bf16[48,2048]{1,0:T(8,128)(2,1)S(1)} %add_convert_fusion.1.refs_0_), channel_id=1, source_target_pairs={{0,4},{2,6},{4,0},{6,2},{1,5},{3,7},{5,1},{7,3},{8,12},{10,14},{12... | collective-permute-start | bytes 589832 | tf_op jit(solution)/shard_map/ppermute | solution.py:25
  105.7 8.7 %collective-permute-start.7 = (bf16[48,2048]{1,0:T(8,128)(2,1)S(1)}, bf16[48,2048]{1,0:T(8,128)(2,1)S(1)}, u32[]{:S(2)}, u32[]{:S(2)}) collective-permute-start(bf16[48,2048]{1,0:T(8,128)(2,1)S(1)} %add_convert_fusion.1.refs_0_), channel_id=1, source_target_pairs={{0,1},{1,0},{2,3},{3,2},{4,5},{5,4},{6,7},{7,6},{8,9},{9,8},{10,11... | collective-permute-start | bytes 589832 | tf_op jit(solution)/shard_map/ppermute | solution.py:25
  107.7 6.8 %collective-permute-start.10 = (bf16[48,2048]{1,0:T(8,128)(2,1)S(1)}, bf16[48,2048]{1,0:T(8,128)(2,1)S(1)}, u32[]{:S(2)}, u32[]{:S(2)}) collective-permute-start(bf16[48,2048]{1,0:T(8,128)(2,1)S(1)} %collective-permute-done.6.refs_3_), channel_id=1, source_target_pairs={{0,1},{1,0},{2,3},{3,2},{4,5},{5,4},{6,7},{7,6},{8,9},{9,8},{10,11... | collective-permute-start | bytes 589832 | tf_op jit(solution)/shard_map/ppermute | solution.py:25
  110.1 4.4 %collective-permute-start.8 = (bf16[48,2048]{1,0:T(8,128)(2,1)S(1)}, bf16[48,2048]{1,0:T(8,128)(2,1)S(1)}, u32[]{:S(2)}, u32[]{:S(2)}) collective-permute-start(bf16[48,2048]{1,0:T(8,128)(2,1)S(1)} %collective-permute-done.4.refs_1_), channel_id=1, source_target_pairs={{0,1},{1,0},{2,3},{3,2},{4,5},{5,4},{6,7},{7,6},{8,9},{9,8},{10,11... | collective-permute-start | bytes 589832 | tf_op jit(solution)/shard_map/ppermute | solution.py:25
  112.0 3.5 %collective-permute-start.9 = (bf16[48,2048]{1,0:T(8,128)(2,1)S(1)}, bf16[48,2048]{1,0:T(8,128)(2,1)S(1)}, u32[]{:S(2)}, u32[]{:S(2)}) collective-permute-start(bf16[48,2048]{1,0:T(8,128)(2,1)S(1)} %collective-permute-done.5.refs_2_), channel_id=1, source_target_pairs={{0,1},{1,0},{2,3},{3,2},{4,5},{5,4},{6,7},{7,6},{8,9},{9,8},{10,11... | collective-permute-start | bytes 589832 | tf_op jit(solution)/shard_map/ppermute | solution.py:25

commit v6 on v5

--- a/solution.py
+++ b/solution.py
@@ -6,6 +6,7 @@
 from jax.sharding import Mesh
 from jax.sharding import PartitionSpec as P
 
+
 SEQ_LEN = 128
 SMALL_ROWS = 8
 FAR, NEAR = ("zm", "zp"), ("zl", "y")
@@ -25,10 +26,6 @@
     return lax.ppermute(block, axis, [(i, (i + shift) % size) for i in range(size)])
 
 
-def whole(shape):
-    return pl.BlockSpec(shape, lambda *_: (0,) * len(shape))
-
-
 def near(array):
     return pltpu.with_memory_space_constraint(array, pltpu.VMEM)
 
@@ -42,25 +39,23 @@
 
 
 def put_in_order(own, other, n_c):
-    n_x = len(own)
-    rows, width = own[0].shape
-
-    def body(*refs):
-        out_ref = refs[-1]
+    n_x = own.shape[0]
+
+    def body(own_ref, other_ref, out_ref):
         at_x, at_c = lax.axis_index("x"), lax.axis_index("c")
         for k in range(n_x):
             spot = (at_x + n_x - k) % n_x
-            out_ref[at_c * n_x + spot] = refs[k][...]
-            out_ref[(1 - at_c) * n_x + spot] = refs[n_x + k][...]
-
-    return pl.pallas_call(
-        body,
-        in_specs=[VMEM] * (2 * n_x),
-        out_shape=jax.ShapeDtypeStruct((n_c * n_x, rows, width), own[0].dtype),
-        cost_estimate=cost(0, 32 * own[0].size),
+            out_ref[at_c * n_x + spot] = own_ref[k]
+            out_ref[(1 - at_c) * n_x + spot] = other_ref[k]
+
+    return pl.pallas_call(
+        body,
+        in_specs=[VMEM] * 2,
+        out_shape=jax.ShapeDtypeStruct((n_c * n_x, *own.shape[1:]), own.dtype),
+        cost_estimate=cost(0, 8 * own.size),
         name="put_in_order",
         compiler_params=pltpu.CompilerParams(vmem_limit_bytes=24 * 2**20),
-    )(*(near(block) for block in (*own, *other)))
+    )(near(own), near(other))
 
 
 def later(values, offset):
@@ -92,14 +87,13 @@
     return (high + pltpu.roll(rows - high, half, 0)).astype(jnp.bfloat16)
 
 
-def previous_branch(x_prev, plane, cotangent, value_prev, conv_taps, conv_bias, grad_scale, n_c):
+def previous_branch(x_prev, plane, cotangent, value_prev, conv_taps, conv_bias, n_c):
     row_count, width = x_prev.shape
     n_near, n_far, shard_rows, units = plane.shape
     tap_count = conv_taps.shape[0]
     n_x = lax.axis_size("x")
     half_rows = row_count // n_c
     block_rows = half_rows // n_x
-    each = n_far * shard_rows
 
     def body(
         x_ref,
@@ -111,12 +105,12 @@
         gv_ref,
         natural_ref,
         keep_ref,
+        send_out,
+        gu_ref,
+        small_ref,
+        turned_ref,
         send_ref,
-        sent_out,
-        gu_ref,
-        turned_ref,
-        sent_ref,
-        sems,
+        sem,
     ):
         spots = [
             (near_at, far_at, (far_at * n_near + near_at) * shard_rows)
@@ -151,50 +145,35 @@
             (((1,), (1,)), ((), ())),
             preferred_element_type=jnp.float32,
         ).astype(jnp.bfloat16)
-
-        grad_w = lax.dot_general(
-            x_ref[...], gu_ref[...], (((0,), (0,)), ((), ())), preferred_element_type=jnp.float32
-        )
-        grad_w = (grad_w * grad_scale).astype(jnp.bfloat16)
+        move = pltpu.make_async_copy(send_ref, send_out, sem)
+        move.start()
         sums = [
             jnp.sum(grad_gate * later(up, tap_count - 1 - j), axis=0, keepdims=True)
             for j in range(tap_count)
         ] + [jnp.sum(grad_gate, axis=0, keepdims=True)]
         rest = jnp.zeros((SMALL_ROWS - len(sums), units), jnp.float32)
-        small = high_and_low(jnp.concatenate([*sums, rest], axis=0) * grad_scale)
-        moves = []
-        for block in range(n_near):
-            for near_at, far_at, at in spots:
-                if near_at == block:
-                    to = far_at * shard_rows
-                    sent_ref[block, to : to + shard_rows] = grad_w[at : at + shard_rows]
-            sent_ref[block, each:] = small
-            moves.append(
-                pltpu.make_async_copy(sent_ref.at[block], sent_out.at[block], sems.at[block])
-            )
-            moves[-1].start()
-        for move in moves:
-            move.wait()
+        small_ref[...] = jnp.concatenate([*sums, rest], axis=0)
+        move.wait()
 
     half = jnp.bfloat16
     return pl.pallas_call(
         body,
         in_specs=[VMEM] * 6,
-        out_specs=[pl.BlockSpec(), VMEM, VMEM, pl.BlockSpec(), HBM],
+        out_specs=[pl.BlockSpec(), VMEM, VMEM, HBM, VMEM, VMEM],
         out_shape=[
             jax.ShapeDtypeStruct((row_count, units), half),
             pltpu.VMEM((width, units), half),
             pltpu.VMEM((half_rows, units), half),
-            jax.ShapeDtypeStruct((half_rows, width), half),
-            pltpu.HBM((n_near, each + SMALL_ROWS, units), half),
+            pltpu.HBM((half_rows, width), half),
+            pltpu.VMEM((row_count, units), half),
+            pltpu.VMEM((SMALL_ROWS, units), jnp.float32),
         ],
         scratch_shapes=[
-            pltpu.VMEM((row_count, units), half),
             pltpu.VMEM((half_rows, units), half),
-            pltpu.VMEM((n_near, each + SMALL_ROWS, units), half),
-            pltpu.SemaphoreType.DMA((n_near,)),
+            pltpu.VMEM((half_rows, width), half),
+            pltpu.SemaphoreType.DMA(()),
         ],
-        cost_estimate=cost(5 * row_count * width * units, 8 * width * units, row_count * units),
+        cost_estimate=cost(3 * row_count * width * units, 8 * width * units, row_count * units),
         name="previous_branch",
         compiler_params=pltpu.CompilerParams(vmem_limit_bytes=24 * 2**20),
     )(
@@ -207,6 +186,47 @@
     )
 
 
+def weight_gradient(x_prev, grad_up, small, grad_scale, n_near, n_far):
+    row_count, width = x_prev.shape
+    units = grad_up.shape[1]
+    each = width // n_near
+    shard_rows = each // n_far
+
+    def body(x_ref, g_ref, small_ref, sent_out, sent_ref, sems):
+        grad_w = lax.dot_general(
+            x_ref[...], g_ref[...], (((0,), (0,)), ((), ())), preferred_element_type=jnp.float32
+        )
+        grad_w = (grad_w * grad_scale).astype(jnp.bfloat16)
+        last = high_and_low(small_ref[...] * grad_scale)
+        moves = []
+        for block in range(n_near):
+            for far_at in range(n_far):
+                at, to = (far_at * n_near + block) * shard_rows, far_at * shard_rows
+                sent_ref[block, to : to + shard_rows] = grad_w[at : at + shard_rows]
+            sent_ref[block, each:] = last
+            moves.append(
+                pltpu.make_async_copy(sent_ref.at[block], sent_out.at[block], sems.at[block])
+            )
+            moves[-1].start()
+        for move in moves:
+            move.wait()
+
+    shape = (n_near, each + SMALL_ROWS, units)
+    return pl.pallas_call(
+        body,
+        in_specs=[VMEM] * 3,
+        out_specs=HBM,
+        out_shape=pltpu.HBM(shape, jnp.bfloat16),
+        scratch_shapes=[
+            pltpu.VMEM(shape, jnp.bfloat16),
+            pltpu.SemaphoreType.DMA((n_near,)),
+        ],
+        cost_estimate=cost(2 * row_count * width * units, 4 * width * units),
+        name="weight_gradient",
+        compiler_params=pltpu.CompilerParams(vmem_limit_bytes=24 * 2**20),
+    )(near(x_prev), near(grad_up), near(small))
+
+
 def next_branch(x_next, weights, value_next, conv_taps, conv_bias):
     row_count, width = x_next.shape
     units = weights.shape[1]
@@ -239,7 +259,7 @@
 
 
 def sum_and_repack(arrived, parts, repeats):
-    count, rows, units = arrived.shape
+    _, rows, units = arrived.shape
     extra = SMALL_ROWS
     each = (rows - extra) // parts
 
@@ -274,7 +294,7 @@
 
 
 def last_sum(arrived, sum_w, sum_taps, sum_bias):
-    rows, units = sum_w.shape
+    rows, _ = sum_w.shape
     tap_count = sum_taps.shape[0]
 
     def body(in_ref, w_ref, taps_ref, bias_ref, new_w_ref, new_taps_ref, new_bias_ref):
@@ -311,16 +331,17 @@
     sum_bias,
 ):
     row_count, width = x_next.shape
-    shard_rows, units = w_gate.shape
     n_zh, n_x, n_c = (lax.axis_size(a) for a in ("zh", "x", "c"))
     n_far, n_near = lax.axis_size(FAR), lax.axis_size(NEAR)
 
     plane = copies_to(copies_to(w_gate, FAR, n_far), NEAR, n_near)
     grad_scale = float(row_count * n_zh * n_far * n_near) ** (-0.5)
-    grad_value, gathered, keep, to_core, sent = previous_branch(
-        x_prev, plane, cotangent, value_prev, conv_taps, conv_bias, grad_scale, n_c
+    grad_value, gathered, keep, to_core, grad_up, small = previous_branch(
+        x_prev, plane, cotangent, value_prev, conv_taps, conv_bias, n_c
     )
     from_core = send_on(to_core, "c", 1)
+    sent = weight_gradient(x_prev, grad_up, small, grad_scale, n_near, n_far)
+    sent, keep, x_next = lax.optimization_barrier((sent, keep, x_next))
     from_near = exchange(sent, NEAR)
 
     block_rows = row_count // (n_x * n_c)
@@ -333,11 +354,14 @@
     hidden_next = next_branch(x_next, gathered, value_next, conv_taps, conv_bias)
     from_near, hidden_next, *arrived = lax.optimization_barrier((from_near, hidden_next, *arrived))
     eighth = sum(block.astype(jnp.float32) for block in arrived).astype(jnp.bfloat16)
-    spread = [eighth] + [send_on(eighth, "x", k) for k in range(1, n_x)]
-    other = [send_on(block, "c", 1) for block in spread]
-    grad_input = put_in_order(spread, other, n_c).reshape(row_count, width)
-
-    from_far = exchange(sum_and_repack(from_near, n_far, n_zh), ("zh", *FAR))
+    spread = [eighth]
+    for k in range(1, n_x):
+        spread.append(send_on(eighth, "x", k))
+    half = jnp.stack(spread)
+    grad_input = put_in_order(half, send_on(half, "c", 1), n_c).reshape(row_count, width)
+
+    by_far = sum_and_repack(from_near, n_far, n_zh)
+    from_far = exchange(by_far, ("zh", *FAR))
     from_far, grad_input = lax.optimization_barrier((from_far, grad_input))
     new_w, new_taps, new_bias = last_sum(from_far, sum_w, sum_taps, sum_bias)
     return hidden_next, grad_input, grad_value, new_w, new_taps, new_bias

time: 124 us -> 125 us (level)
  the two profiles are of different devices: /device:TPU:34 before, /device:TPU:32 now
where the time goes in v6:
time: 125 us; the launch traced here: 124 us
  blocking collectives  50.1 us (40%)
  starting transfers between devices  34.5 us (28%)
  waiting for transfers between devices  23.7 us (19%)
  Pallas kernels  11.3 us (9%)
  local copies, waits for them, and re-layouts  1.85 us (1%)
    all_to_all x2, blocking collectives, copies_to(): return lax.all_to_all(copies, axis, 0, 0, tiled=True)  50.1 us
    ppermute x8, starting transfers between devices, send_on(): lax.ppermute(block, axis, [(i, (i + shift) % size) for i in range(size)])  22.2 us
    ppermute x8, waiting for transfers between devices, send_on(): lax.ppermute(block, axis, [(i, (i + shift) % size) for i in range(size)])  18.9 us
    all_to_all x2, starting transfers between devices, exchange(): return lax.all_to_all(blocks, axis, 0, 0, tiled=True)  12.3 us
    all_to_all x2, waiting for transfers between devices, exchange(): return lax.all_to_all(blocks, axis, 0, 0, tiled=True)  4.78 us
    pallas_call x1, Pallas kernels, previous_branch(): pl.pallas_call(body, in_specs=[VMEM] * 6, out_specs=[pl.BlockSpec(), VMEM...  4.06 us
  transfers between devices with their start and end apart: 10, of which 9 were waited for; matrix products, arithmetic and copies ran while one was open for 2% of the time, Pallas kernels for 3%

profile of v6, /device:TPU:32, one launch (start us, length us, event | category | flops | bytes accessed | tf_op | source)
XLA Modules:
  0.0 124.1 jit_solution(11072774993102810541)
XLA Ops:
  0.6 0.8 broadcast_in_dim.6
  1.5 24.6 %all_to_all.20 = bf16[4,64,384]{2,1,0:T(8,128)(2,1)S(1)} all-to-all(bf16[4,64,384]{2,1,0:T(8,128)(2,1)S(1)} %broadcast_in_dim.6), channel_id=1, replica_groups=mesh['zh'=2,'zm'=2,'zp'=2,'zl'=2,'y'=4,'x'=4,'c'=2] {'zm','zp'}, dimensions={0} | all-to-all | bytes 393216 | tf_op jit(solution)/shard_map/all_to_all | solution.py:17
  26.1 0.2 broadcast_in_dim.7
  26.3 0.0 copy-start
  26.3 0.0 copy-start.2
  26.3 0.0 copy-start.3
  26.3 0.0 copy-start.6
  26.3 0.0 copy-start.7
  26.4 25.5 %all_to_all.21.w_ref = bf16[8,4,64,384]{3,2,1,0:T(8,128)(2,1)S(1)} all-to-all(bf16[8,4,64,384]{3,2,1,0:T(8,128)(2,1)S(1)} %broadcast_in_dim.7), channel_id=1, replica_groups=mesh['zh'=2,'zm'=2,'zp'=2,'zl'=2,'y'=4,'x'=4,'c'=2] {'zl','y'}, dimensions={0} | all-to-all | bytes 3145728 | tf_op jit(solution)/shard_map/all_to_all | solution.py:17
  51.8 0.0 copy-done
  51.8 0.0 copy-done.2
  51.8 0.0 copy-done.3
  51.8 0.0 copy-done.6
  51.9 0.0 copy-done.7
  51.9 4.1 %previous_branch.1 = (bf16[384,384]{1,0:T(8,128)(2,1)}, bf16[2048,384]{1,0:T(8,128)(2,1)S(1)}, bf16[192,384]{1,0:T(8,128)(2,1)S(1)}, bf16[192,2048]{1,0:T(8,128)...) custom-call(bf16[384,2048]{1,0:T(8,128)(2,1)S(1)} %copy-done, bf16[8,4,64,384]{3,2,1,0:T(8,128)(2,1)S(1)} %all_to_all.21.w_ref, ...), custom_call_target="tpu_custom_call" | custom-call | flops 905969664 | bytes 6291456 | tf_op jit(solution)/shard_map/previous_branch/pallas_call | solution.py:159
  55.9 2.4 %weight_gradient.1 = bf16[8,264,384]{2,1,0:T(8,128)(2,1)} custom-call(bf16[384,2048]{1,0:T(8,128)(2,1)S(1)} %copy-done, bf16[384,384]{1,0:T(8,128)(2,1)S(1)} %get-tuple-element.26.g_ref, f32[8,384]{1,0:T(8,128)S(1)} %get-tuple-element.27.small_ref), custom_call_target="tpu_custom_call" | custom-call | flops 603979776 | bytes 3145728 | tf_op jit(solution)/shard_map/weight_gradient/pallas_call | solution.py:215
  58.4 4.9 %all-to-all-start.2 = ((bf16[8,264,384]{2,1,0:T(8,128)(2,1)}), bf16[8,264,384]{2,1,0:T(8,128)(2,1)S(1)}, u32[]{:S(2)}, u32[]{:S(2)}) async-start(bf16[8,264,384]{2,1,0:T(8,128)(2,1)} %weight_gradient.1), calls=%async_computation.2 | async-start | bytes 3244032 | tf_op jit(solution)/shard_map/all_to_all | solution.py:21
  63.2 1.9 %collective-permute-start = (bf16[192,2048]{1,0:T(8,128)(2,1)}, bf16[192,2048]{1,0:T(8,128)(2,1)S(1)}, u32[]{:S(2)}, u32[]{:S(2)}) collective-permute-start(bf16[192,2048]{1,0:T(8,128)(2,1)} %get-tuple-element.33), channel_id=1, source_target_pairs={{0,1},{1,0},{2,3},{3,2},{4,5},{5,4},{6,7},{7,6},{8,9},{9,8},{10,11... | collective-permute-start | bytes 2359304 | tf_op jit(solution)/shard_map/ppermute | solution.py:26
  65.2 2.5 %collective-permute-done = bf16[192,2048]{1,0:T(8,128)(2,1)S(1)} collective-permute-done((bf16[192,2048]{1,0:T(8,128)(2,1)}, bf16[192,2048]{1,0:T(8,128)(2,1)S(1)}, u32[]{:S(2)}, u32[]{:S(2)}) %collective-permute-start) | collective-permute-done | bytes 786464 | tf_op jit(solution)/shard_map/ppermute | solution.py:26
  67.6 0.0 copy-start.4
  67.6 0.7 add_convert_fusion
  68.3 0.0 copy-start.1
  68.3 0.1 fusion
  68.4 4.8 %collective-permute-start.3 = (bf16[48,2048]{1,0:T(8,128)(2,1)S(1)}, bf16[48,2048]{1,0:T(8,128)(2,1)S(1)}, u32[]{:S(2)}, u32[]{:S(2)}) collective-permute-start(bf16[48,2048]{1,0:T(8,128)(2,1)S(1)} %get-tuple-element.46), channel_id=1, source_target_pairs={{0,6},{2,0},{4,2},{6,4},{1,7},{3,1},{5,3},{7,5},{8,14},{10,8},{12,... | collective-permute-start | bytes 589832 | tf_op jit(solution)/shard_map/ppermute | solution.py:26
  73.2 2.7 %collective-permute-start.2 = (bf16[48,2048]{1,0:T(8,128)(2,1)S(1)}, bf16[48,2048]{1,0:T(8,128)(2,1)S(1)}, u32[]{:S(2)}, u32[]{:S(2)}) collective-permute-start(bf16[48,2048]{1,0:T(8,128)(2,1)S(1)} %get-tuple-element.47), channel_id=1, source_target_pairs={{0,4},{2,6},{4,0},{6,2},{1,5},{3,7},{5,1},{7,3},{8,12},{10,14},{12... | collective-permute-start | bytes 589832 | tf_op jit(solution)/shard_map/ppermute | solution.py:26
  75.9 2.8 %collective-permute-start.1 = (bf16[48,2048]{1,0:T(8,128)(2,1)S(1)}, bf16[48,2048]{1,0:T(8,128)(2,1)}, u32[]{:S(2)}, u32[]{:S(2)}) collective-permute-start(bf16[48,2048]{1,0:T(8,128)(2,1)S(1)} %get-tuple-element.48), channel_id=1, source_target_pairs={{0,2},{2,4},{4,6},{6,0},{1,3},{3,5},{5,7},{7,1},{8,10},{10,12},{12... | collective-permute-start | bytes 589832 | tf_op jit(solution)/shard_map/ppermute | solution.py:26
  78.7 0.0 copy-done.4
  78.7 0.0 copy-done.1
  78.7 2.0 %next_branch.1 = bf16[384,384]{1,0:T(8,128)(2,1)} custom-call(bf16[384,2048]{1,0:T(8,128)(2,1)S(1)} %copy-done.1, bf16[2048,384]{1,0:T(8,128)(2,1)S(1)} %get-tuple-element.31.w_ref, bf16[384,384]{1,0:T(8,128)(2,1)S(1)} %copy-done.4, f32[3,384]{1,0:T(4,128)S(1)} %copy-done.6, f32[384]{0:T(512)S(1)} %copy-done.7), custom_call_target="tpu_custom_call" | custom-call | flops 603979776 | bytes 3145728 | tf_op jit(solution)/shard_map/next_branch/pallas_call | solution.py:240
  80.7 1.2 collective-permute-done.3
  81.9 0.0 copy-start.10
  81.9 2.5 %collective-permute-done.2 = bf16[48,2048]{1,0:T(8,128)(2,1)S(1)} collective-permute-done((bf16[48,2048]{1,0:T(8,128)(2,1)S(1)}, bf16[48,2048]{1,0:T(8,128)(2,1)S(1)}, u32[]{:S(2)}, u32[]{:S(2)}) %collective-permute-start.2) | collective-permute-done | bytes 196640 | tf_op jit(solution)/shard_map/ppermute | solution.py:26
  84.4 0.0 copy-done.10
  84.4 0.0 copy-start.12
  84.4 0.7 copy-done.12
  85.1 2.5 %collective-permute-done.1 = bf16[48,2048]{1,0:T(8,128)(2,1)} collective-permute-done((bf16[48,2048]{1,0:T(8,128)(2,1)S(1)}, bf16[48,2048]{1,0:T(8,128)(2,1)}, u32[]{:S(2)}, u32[]{:S(2)}) %collective-permute-start.1) | collective-permute-done | bytes 196640 | tf_op jit(solution)/shard_map/ppermute | solution.py:26
  87.6 0.0 copy-start.11
  87.6 0.0 copy-start.13
  87.6 0.0 all-to-all-done.2.in_ref
  87.6 0.9 sum_and_repack.1
  88.5 7.4 %all-to-all-start.3 = ((bf16[8,72,384]{2,1,0:T(8,128)(2,1)}), bf16[8,72,384]{2,1,0:T(8,128)(2,1)S(1)}, u32[]{:S(2)}, u32[]{:S(2)}) async-start(bf16[8,72,384]{2,1,0:T(8,128)(2,1)} %sum_and_repack.1), calls=%async_computation.3 | async-start | bytes 884736 | tf_op jit(solution)/shard_map/all_to_all | solution.py:21
  95.9 0.0 copy-done.11
  95.9 0.0 copy-done.13
  95.9 1.0 add_convert_fusion.1
  97.0 2.5 %collective-permute-start.6 = (bf16[48,2048]{1,0:T(8,128)(2,1)S(1)}, bf16[48,2048]{1,0:T(8,128)(2,1)S(1)}, u32[]{:S(2)}, u32[]{:S(2)}) collective-permute-start(bf16[48,2048]{1,0:T(8,128)(2,1)S(1)} %add_convert_fusion.1), channel_id=1, source_target_pairs={{0,6},{2,0},{4,2},{6,4},{1,7},{3,1},{5,3},{7,5},{8,14},{10,8},{12,... | collective-permute-start | bytes 589832 | tf_op jit(solution)/shard_map/ppermute | solution.py:26
  99.4 2.7 %collective-permute-start.5 = (bf16[48,2048]{1,0:T(8,128)(2,1)S(1)}, bf16[48,2048]{1,0:T(8,128)(2,1)S(1)}, u32[]{:S(2)}, u32[]{:S(2)}) collective-permute-start(bf16[48,2048]{1,0:T(8,128)(2,1)S(1)} %add_convert_fusion.1), channel_id=1, source_target_pairs={{0,4},{2,6},{4,0},{6,2},{1,5},{3,7},{5,1},{7,3},{8,12},{10,14},{12... | collective-permute-start | bytes 589832 | tf_op jit(solution)/shard_map/ppermute | solution.py:26
  102.2 2.8 %collective-permute-start.4 = (bf16[48,2048]{1,0:T(8,128)(2,1)S(1)}, bf16[48,2048]{1,0:T(8,128)(2,1)S(1)}, u32[]{:S(2)}, u32[]{:S(2)}) collective-permute-start(bf16[48,2048]{1,0:T(8,128)(2,1)S(1)} %add_convert_fusion.1), channel_id=1, source_target_pairs={{0,2},{2,4},{4,6},{6,0},{1,3},{3,5},{5,7},{7,1},{8,10},{10,12},{12... | collective-permute-start | bytes 589832 | tf_op jit(solution)/shard_map/ppermute | solution.py:26
  105.0 1.7 %collective-permute-done.6 = bf16[48,2048]{1,0:T(8,128)(2,1)S(1)} collective-permute-done((bf16[48,2048]{1,0:T(8,128)(2,1)S(1)}, bf16[48,2048]{1,0:T(8,128)(2,1)S(1)}, u32[]{:S(2)}, u32[]{:S(2)}) %collective-permute-start.6) | collective-permute-done | bytes 196640 | tf_op jit(solution)/shard_map/ppermute | solution.py:26
  106.6 2.3 %collective-permute-done.5 = bf16[48,2048]{1,0:T(8,128)(2,1)S(1)} collective-permute-done((bf16[48,2048]{1,0:T(8,128)(2,1)S(1)}, bf16[48,2048]{1,0:T(8,128)(2,1)S(1)}, u32[]{:S(2)}, u32[]{:S(2)}) %collective-permute-start.5) | collective-permute-done | bytes 196640 | tf_op jit(solution)/shard_map/ppermute | solution.py:26
  108.9 4.0 %collective-permute-done.4 = bf16[48,2048]{1,0:T(8,128)(2,1)S(1)} collective-permute-done((bf16[48,2048]{1,0:T(8,128)(2,1)S(1)}, bf16[48,2048]{1,0:T(8,128)(2,1)S(1)}, u32[]{:S(2)}, u32[]{:S(2)}) %collective-permute-start.4) | collective-permute-done | bytes 196640 | tf_op jit(solution)/shard_map/ppermute | solution.py:26
  112.9 0.1 pad_maximum_fusion.own_ref
  113.0 0.0 copy-start.5
  113.0 0.0 copy-start.8
  113.0 0.0 copy-start.9
  113.1 2.1 %collective-permute-start.7 = (bf16[4,48,2048]{2,1,0:T(8,128)(2,1)S(1)}, bf16[4,48,2048]{2,1,0:T(8,128)(2,1)S(1)}, u32[]{:S(2)}, u32[]{:S(2)}) collective-permute-start(bf16[4,48,2048]{2,1,0:T(8,128)(2,1)S(1)} %pad_maximum_fusion.own_ref), channel_id=1, source_target_pairs={{0,1},{1,0},{2,3},{3,2},{4,5},{5,4},{6,7},{7,6},{8,9},{9,8},{10,11... | collective-permute-start | bytes 2359304 | tf_op jit(solution)/shard_map/ppermute | solution.py:26
  115.1 2.3 %collective-permute-done.7.other_ref = bf16[4,48,2048]{2,1,0:T(8,128)(2,1)S(1)} collective-permute-done((bf16[4,48,2048]{2,1,0:T(8,128)(2,1)S(1)}, bf16[4,48,2048]{2,1,0:T(8,128)(2,1)S(1)}, u32[]{:S(2)}, u32[]{:S(2)}) %collective-permute-start.7) | collective-permute-done | bytes 786464 | tf_op jit(solution)/shard_map/ppermute | solution.py:26
  117.4 1.3 %put_in_order.1 = bf16[8,48,2048]{2,1,0:T(8,128)(2,1)} custom-call(bf16[4,48,2048]{2,1,0:T(8,128)(2,1)S(1)} %pad_maximum_fusion.own_ref, bf16[4,48,2048]{2,1,0:T(8,128)(2,1)S(1)} %collective-permute-done.7.other_ref), custom_call_target="tpu_custom_call" | custom-call | bytes 3145728 | tf_op jit(solution)/shard_map/put_in_order/pallas_call | solution.py:51
  118.6 4.8 %all-to-all-done.3.in_ref = bf16[8,72,384]{2,1,0:T(8,128)(2,1)S(1)} async-done(((bf16[8,72,384]{2,1,0:T(8,128)(2,1)}), bf16[8,72,384]{2,1,0:T(8,128)(2,1)S(1)}, u32[]{:S(2)}, u32[]{:S(2)}) %all-to-all-start.3) | async-done | bytes 442400 | tf_op jit(solution)/shard_map/all_to_all | solution.py:21
  123.4 0.0 copy-done.5
  123.4 0.0 copy-done.8
  123.4 0.0 copy-done.9
  123.4 0.7 last_sum.1
Async XLA Ops:
  26.3 25.5 %copy-start = (bf16[384,2048]{1,0:T(8,128)(2,1)S(1)}, bf16[384,2048]{1,0:T(8,128)(2,1)}, u32[]{:S(2)}) copy-start(bf16[384,2048]{1,0:T(8,128)(2,1)} %x_ref.3) | copy-start | bytes 4718596
  26.3 25.5 %copy-start.2 = (bf16[384,384]{1,0:T(8,128)(2,1)S(1)}, bf16[384,384]{1,0:T(8,128)(2,1)}, u32[]{:S(2)}) copy-start(bf16[384,384]{1,0:T(8,128)(2,1)} %cot_ref.1) | copy-start | bytes 884740
  26.3 25.5 %copy-start.3 = (bf16[384,384]{1,0:T(8,128)(2,1)S(1)}, bf16[384,384]{1,0:T(8,128)(2,1)}, u32[]{:S(2)}) copy-start(bf16[384,384]{1,0:T(8,128)(2,1)} %value_ref.2) | copy-start | bytes 884740
  26.3 25.5 %copy-start.6 = (f32[3,384]{1,0:T(4,128)S(1)}, f32[3,384]{1,0:T(4,128)}, u32[]{:S(2)}) copy-start(f32[3,384]{1,0:T(4,128)} %taps_ref.4) | copy-start | bytes 13828
  26.3 25.5 %copy-start.7 = (f32[384]{0:T(512)S(1)}, f32[384]{0:T(512)}, u32[]{:S(2)}) copy-start(f32[384]{0:T(512)} %bias_ref.4) | copy-start | bytes 4612
  58.4 29.3 %all-to-all-start.2 = ((bf16[8,264,384]{2,1,0:T(8,128)(2,1)}), bf16[8,264,384]{2,1,0:T(8,128)(2,1)S(1)}, u32[]{:S(2)}, u32[]{:S(2)}) async-start(bf16[8,264,384]{2,1,0:T(8,128)(2,1)} %weight_gradient.1), calls=%async_computation.2 | async-start | bytes 3244032 | tf_op jit(solution)/shard_map/all_to_all | solution.py:21
  63.2 4.4 %collective-permute-start = (bf16[192,2048]{1,0:T(8,128)(2,1)}, bf16[192,2048]{1,0:T(8,128)(2,1)S(1)}, u32[]{:S(2)}, u32[]{:S(2)}) collective-permute-start(bf16[192,2048]{1,0:T(8,128)(2,1)} %get-tuple-element.33), channel_id=1, source_target_pairs={{0,1},{1,0},{2,3},{3,2},{4,5},{5,4},{6,7},{7,6},{8,9},{9,8},{10,11... | collective-permute-start | bytes 2359304 | tf_op jit(solution)/shard_map/ppermute | solution.py:26
  67.6 11.1 %copy-start.4 = (bf16[384,384]{1,0:T(8,128)(2,1)S(1)}, bf16[384,384]{1,0:T(8,128)(2,1)}, u32[]{:S(2)}) copy-start(bf16[384,384]{1,0:T(8,128)(2,1)} %value_ref.3) | copy-start | bytes 884740
  68.3 10.4 %copy-start.1 = (bf16[384,2048]{1,0:T(8,128)(2,1)S(1)}, bf16[384,2048]{1,0:T(8,128)(2,1)}, u32[]{:S(2)}) copy-start(bf16[384,2048]{1,0:T(8,128)(2,1)} %x_ref.4) | copy-start | bytes 4718596
  68.4 13.5 %collective-permute-start.3 = (bf16[48,2048]{1,0:T(8,128)(2,1)S(1)}, bf16[48,2048]{1,0:T(8,128)(2,1)S(1)}, u32[]{:S(2)}, u32[]{:S(2)}) collective-permute-start(bf16[48,2048]{1,0:T(8,128)(2,1)S(1)} %get-tuple-element.46), channel_id=1, source_target_pairs={{0,6},{2,0},{4,2},{6,4},{1,7},{3,1},{5,3},{7,5},{8,14},{10,8},{12,... | collective-permute-start | bytes 589832 | tf_op jit(solution)/shard_map/ppermute | solution.py:26
  73.2 11.2 %collective-permute-start.2 = (bf16[48,2048]{1,0:T(8,128)(2,1)S(1)}, bf16[48,2048]{1,0:T(8,128)(2,1)S(1)}, u32[]{:S(2)}, u32[]{:S(2)}) collective-permute-start(bf16[48,2048]{1,0:T(8,128)(2,1)S(1)} %get-tuple-element.47), channel_id=1, source_target_pairs={{0,4},{2,6},{4,0},{6,2},{1,5},{3,7},{5,1},{7,3},{8,12},{10,14},{12... | collective-permute-start | bytes 589832 | tf_op jit(solution)/shard_map/ppermute | solution.py:26
  75.9 11.7 %collective-permute-start.1 = (bf16[48,2048]{1,0:T(8,128)(2,1)S(1)}, bf16[48,2048]{1,0:T(8,128)(2,1)}, u32[]{:S(2)}, u32[]{:S(2)}) collective-permute-start(bf16[48,2048]{1,0:T(8,128)(2,1)S(1)} %get-tuple-element.48), channel_id=1, source_target_pairs={{0,2},{2,4},{4,6},{6,0},{1,3},{3,5},{5,7},{7,1},{8,10},{10,12},{12... | collective-permute-start | bytes 589832 | tf_op jit(solution)/shard_map/ppermute | solution.py:26
  81.9 2.5 %copy-start.10 = (bf16[48,2048]{1,0:T(8,128)(2,1)}, bf16[48,2048]{1,0:T(8,128)(2,1)S(1)}, u32[]{:S(2)}) copy-start(bf16[48,2048]{1,0:T(8,128)(2,1)S(1)} %collective-permute-done.3) | copy-start | bytes 589828
  84.4 0.7 copy-start.12
  87.6 8.3 %copy-start.11 = (bf16[48,2048]{1,0:T(8,128)(2,1)S(1)}, bf16[48,2048]{1,0:T(8,128)(2,1)}, u32[]{:S(2)}) copy-start(bf16[48,2048]{1,0:T(8,128)(2,1)} %copy-done.10) | copy-start | bytes 589828
  87.6 8.3 %copy-start.13 = (bf16[48,2048]{1,0:T(8,128)(2,1)S(1)}, bf16[48,2048]{1,0:T(8,128)(2,1)}, u32[]{:S(2)}) copy-start(bf16[48,2048]{1,0:T(8,128)(2,1)} %copy-done.12) | copy-start | bytes 589828
  88.5 34.9 %all-to-all-start.3 = ((bf16[8,72,384]{2,1,0:T(8,128)(2,1)}), bf16[8,72,384]{2,1,0:T(8,128)(2,1)S(1)}, u32[]{:S(2)}, u32[]{:S(2)}) async-start(bf16[8,72,384]{2,1,0:T(8,128)(2,1)} %sum_and_repack.1), calls=%async_computation.3 | async-start | bytes 884736 | tf_op jit(solution)/shard_map/all_to_all | solution.py:21
  97.0 9.7 %collective-permute-start.6 = (bf16[48,2048]{1,0:T(8,128)(2,1)S(1)}, bf16[48,2048]{1,0:T(8,128)(2,1)S(1)}, u32[]{:S(2)}, u32[]{:S(2)}) collective-permute-start(bf16[48,2048]{1,0:T(8,128)(2,1)S(1)} %add_convert_fusion.1), channel_id=1, source_target_pairs={{0,6},{2,0},{4,2},{6,4},{1,7},{3,1},{5,3},{7,5},{8,14},{10,8},{12,... | collective-permute-start | bytes 589832 | tf_op jit(solution)/shard_map/ppermute | solution.py:26
  99.4 9.5 %collective-permute-start.5 = (bf16[48,2048]{1,0:T(8,128)(2,1)S(1)}, bf16[48,2048]{1,0:T(8,128)(2,1)S(1)}, u32[]{:S(2)}, u32[]{:S(2)}) collective-permute-start(bf16[48,2048]{1,0:T(8,128)(2,1)S(1)} %add_convert_fusion.1), channel_id=1, source_target_pairs={{0,4},{2,6},{4,0},{6,2},{1,5},{3,7},{5,1},{7,3},{8,12},{10,14},{12... | collective-permute-start | bytes 589832 | tf_op jit(solution)/shard_map/ppermute | solution.py:26
  102.2 10.7 %collective-permute-start.4 = (bf16[48,2048]{1,0:T(8,128)(2,1)S(1)}, bf16[48,2048]{1,0:T(8,128)(2,1)S(1)}, u32[]{:S(2)}, u32[]{:S(2)}) collective-permute-start(bf16[48,2048]{1,0:T(8,128)(2,1)S(1)} %add_convert_fusion.1), channel_id=1, source_target_pairs={{0,2},{2,4},{4,6},{6,0},{1,3},{3,5},{5,7},{7,1},{8,10},{10,12},{12... | collective-permute-start | bytes 589832 | tf_op jit(solution)/shard_map/ppermute | solution.py:26
  113.0 10.4 %copy-start.5 = (f32[64,384]{1,0:T(8,128)S(1)}, f32[64,384]{1,0:T(8,128)}, u32[]{:S(2)}) copy-start(f32[64,384]{1,0:T(8,128)} %w_ref.1) | copy-start | bytes 294916
  113.0 10.4 %copy-start.8 = (f32[3,384]{1,0:T(4,128)S(1)}, f32[3,384]{1,0:T(4,128)}, u32[]{:S(2)}) copy-start(f32[3,384]{1,0:T(4,128)} %taps_ref.5) | copy-start | bytes 13828
  113.0 10.4 %copy-start.9 = (f32[384]{0:T(512)S(1)}, f32[384]{0:T(512)}, u32[]{:S(2)}) copy-start(f32[384]{0:T(512)} %bias_ref.5) | copy-start | bytes 4612
  113.1 4.3 %collective-permute-start.7 = (bf16[4,48,2048]{2,1,0:T(8,128)(2,1)S(1)}, bf16[4,48,2048]{2,1,0:T(8,128)(2,1)S(1)}, u32[]{:S(2)}, u32[]{:S(2)}) collective-permute-start(bf16[4,48,2048]{2,1,0:T(8,128)(2,1)S(1)} %pad_maximum_fusion.own_ref), channel_id=1, source_target_pairs={{0,1},{1,0},{2,3},{3,2},{4,5},{5,4},{6,7},{7,6},{8,9},{9,8},{10,11... | collective-permute-start | bytes 2359304 | tf_op jit(solution)/shard_map/ppermute | solution.py:26

commit v7 on v5

--- a/solution.py
+++ b/solution.py
@@ -6,6 +6,7 @@
 from jax.sharding import Mesh
 from jax.sharding import PartitionSpec as P
 
+
 SEQ_LEN = 128
 SMALL_ROWS = 8
 FAR, NEAR = ("zm", "zp"), ("zl", "y")
@@ -25,10 +26,6 @@
     return lax.ppermute(block, axis, [(i, (i + shift) % size) for i in range(size)])
 
 
-def whole(shape):
-    return pl.BlockSpec(shape, lambda *_: (0,) * len(shape))
-
-
 def near(array):
     return pltpu.with_memory_space_constraint(array, pltpu.VMEM)
 
@@ -42,25 +39,23 @@
 
 
 def put_in_order(own, other, n_c):
-    n_x = len(own)
-    rows, width = own[0].shape
-
-    def body(*refs):
-        out_ref = refs[-1]
+    n_x = own.shape[0]
+
+    def body(own_ref, other_ref, out_ref):
         at_x, at_c = lax.axis_index("x"), lax.axis_index("c")
         for k in range(n_x):
             spot = (at_x + n_x - k) % n_x
-            out_ref[at_c * n_x + spot] = refs[k][...]
-            out_ref[(1 - at_c) * n_x + spot] = refs[n_x + k][...]
-
-    return pl.pallas_call(
-        body,
-        in_specs=[VMEM] * (2 * n_x),
-        out_shape=jax.ShapeDtypeStruct((n_c * n_x, rows, width), own[0].dtype),
-        cost_estimate=cost(0, 32 * own[0].size),
+            out_ref[at_c * n_x + spot] = own_ref[k]
+            out_ref[(1 - at_c) * n_x + spot] = other_ref[k]
+
+    return pl.pallas_call(
+        body,
+        in_specs=[VMEM] * 2,
+        out_shape=jax.ShapeDtypeStruct((n_c * n_x, *own.shape[1:]), own.dtype),
+        cost_estimate=cost(0, 8 * own.size),
         name="put_in_order",
         compiler_params=pltpu.CompilerParams(vmem_limit_bytes=24 * 2**20),
-    )(*(near(block) for block in (*own, *other)))
+    )(near(own), near(other))
 
 
 def later(values, offset):
@@ -111,10 +106,11 @@
         gv_ref,
         natural_ref,
         keep_ref,
-        send_ref,
+        send_out,
         sent_out,
         gu_ref,
         turned_ref,
+        send_ref,
         sent_ref,
         sems,
     ):
@@ -151,6 +147,8 @@
             (((1,), (1,)), ((), ())),
             preferred_element_type=jnp.float32,
         ).astype(jnp.bfloat16)
+        moves = [pltpu.make_async_copy(send_ref, send_out, sems.at[n_near])]
+        moves[0].start()
 
         grad_w = lax.dot_general(
             x_ref[...], gu_ref[...], (((0,), (0,)), ((), ())), preferred_element_type=jnp.float32
@@ -162,7 +160,6 @@
         ] + [jnp.sum(grad_gate, axis=0, keepdims=True)]
         rest = jnp.zeros((SMALL_ROWS - len(sums), units), jnp.float32)
         small = high_and_low(jnp.concatenate([*sums, rest], axis=0) * grad_scale)
-        moves = []
         for block in range(n_near):
             for near_at, far_at, at in spots:
                 if near_at == block:
@@ -180,19 +177,20 @@
     return pl.pallas_call(
         body,
         in_specs=[VMEM] * 6,
-        out_specs=[pl.BlockSpec(), VMEM, VMEM, pl.BlockSpec(), HBM],
+        out_specs=[pl.BlockSpec(), VMEM, VMEM, HBM, HBM],
         out_shape=[
             jax.ShapeDtypeStruct((row_count, units), half),
             pltpu.VMEM((width, units), half),
             pltpu.VMEM((half_rows, units), half),
-            jax.ShapeDtypeStruct((half_rows, width), half),
+            pltpu.HBM((half_rows, width), half),
             pltpu.HBM((n_near, each + SMALL_ROWS, units), half),
         ],
         scratch_shapes=[
             pltpu.VMEM((row_count, units), half),
             pltpu.VMEM((half_rows, units), half),
+            pltpu.VMEM((half_rows, width), half),
             pltpu.VMEM((n_near, each + SMALL_ROWS, units), half),
-            pltpu.SemaphoreType.DMA((n_near,)),
+            pltpu.SemaphoreType.DMA((n_near + 1,)),
         ],
         cost_estimate=cost(5 * row_count * width * units, 8 * width * units, row_count * units),
         name="previous_branch",
@@ -239,7 +237,7 @@
 
 
 def sum_and_repack(arrived, parts, repeats):
-    count, rows, units = arrived.shape
+    _, rows, units = arrived.shape
     extra = SMALL_ROWS
     each = (rows - extra) // parts
 
@@ -274,7 +272,7 @@
 
 
 def last_sum(arrived, sum_w, sum_taps, sum_bias):
-    rows, units = sum_w.shape
+    rows, _ = sum_w.shape
     tap_count = sum_taps.shape[0]
 
     def body(in_ref, w_ref, taps_ref, bias_ref, new_w_ref, new_taps_ref, new_bias_ref):
@@ -311,7 +309,6 @@
     sum_bias,
 ):
     row_count, width = x_next.shape
-    shard_rows, units = w_gate.shape
     n_zh, n_x, n_c = (lax.axis_size(a) for a in ("zh", "x", "c"))
     n_far, n_near = lax.axis_size(FAR), lax.axis_size(NEAR)
 
@@ -329,15 +326,17 @@
     )
     half = (kept + from_core.astype(jnp.float32)).astype(jnp.bfloat16)
     half = half.reshape(n_x, block_rows, width)
-    arrived = [half[0]] + [send_on(half[k], "x", k) for k in range(1, n_x)]
+    arrived = [half[0]]
+    for k in range(1, n_x):
+        arrived.append(send_on(half[k], "x", k))
     hidden_next = next_branch(x_next, gathered, value_next, conv_taps, conv_bias)
-    from_near, hidden_next, *arrived = lax.optimization_barrier((from_near, hidden_next, *arrived))
+    from_near, hidden_next = lax.optimization_barrier((from_near, hidden_next))
+    by_far = sum_and_repack(from_near, n_far, n_zh)
+    from_far = exchange(by_far, ("zh", *FAR))
+
     eighth = sum(block.astype(jnp.float32) for block in arrived).astype(jnp.bfloat16)
-    spread = [eighth] + [send_on(eighth, "x", k) for k in range(1, n_x)]
-    other = [send_on(block, "c", 1) for block in spread]
-    grad_input = put_in_order(spread, other, n_c).reshape(row_count, width)
-
-    from_far = exchange(sum_and_repack(from_near, n_far, n_zh), ("zh", *FAR))
+    half = jnp.stack([eighth] + [send_on(eighth, "x", k) for k in range(1, n_x)])
+    grad_input = put_in_order(half, send_on(half, "c", 1), n_c).reshape(row_count, width)
     from_far, grad_input = lax.optimization_barrier((from_far, grad_input))
     new_w, new_taps, new_bias = last_sum(from_far, sum_w, sum_taps, sum_bias)
     return hidden_next, grad_input, grad_value, new_w, new_taps, new_bias

time: 124 us -> 118 us (0.952)
  the two profiles are of different devices: /device:TPU:34 before, /device:TPU:32 now
where the time goes in v7:
time: 118 us
  blocking collectives  50.1 us (42%)
  starting transfers between devices  35.9 us (30%)
  waiting for transfers between devices  15.7 us (13%)
  Pallas kernels  10.2 us (9%)
  local copies, waits for them, and re-layouts  2.81 us (2%)
  other arithmetic  1.42 us (1%)
    all_to_all x2, blocking collectives, copies_to(): return lax.all_to_all(copies, axis, 0, 0, tiled=True)  50.1 us
    ppermute x8, starting transfers between devices, send_on(): lax.ppermute(block, axis, [(i, (i + shift) % size) for i in range(size)])  23.6 us
    ppermute x8, waiting for transfers between devices, send_on(): lax.ppermute(block, axis, [(i, (i + shift) % size) for i in range(size)])  12.5 us
    all_to_all x2, starting transfers between devices, exchange(): return lax.all_to_all(blocks, axis, 0, 0, tiled=True)  12.3 us
    pallas_call x1, Pallas kernels, previous_branch(): pl.pallas_call(body, in_specs=[VMEM] * 6, out_specs=[pl.BlockSpec(), VMEM...  5.32 us
    all_to_all x2, waiting for transfers between devices, exchange(): return lax.all_to_all(blocks, axis, 0, 0, tiled=True)  3.15 us
  transfers between devices with their start and end apart: 10, of which 6 were waited for; matrix products, arithmetic and copies ran while one was open for 3% of the time, Pallas kernels for 4%

profile of v7, /device:TPU:32, one launch (start us, length us, event | category | flops | bytes accessed | tf_op | source)
XLA Modules:
  0.0 117.6 jit_solution(17894608132642522827)
XLA Ops:
  0.6 0.8 broadcast_in_dim.6
  1.5 24.6 %all_to_all.20 = bf16[4,64,384]{2,1,0:T(8,128)(2,1)S(1)} all-to-all(bf16[4,64,384]{2,1,0:T(8,128)(2,1)S(1)} %broadcast_in_dim.6), channel_id=1, replica_groups=mesh['zh'=2,'zm'=2,'zp'=2,'zl'=2,'y'=4,'x'=4,'c'=2] {'zm','zp'}, dimensions={0} | all-to-all | bytes 393216 | tf_op jit(solution)/shard_map/all_to_all | solution.py:17
  26.1 0.2 broadcast_in_dim.7
  26.3 0.0 copy-start.3
  26.3 0.0 copy-start.5
  26.3 0.0 copy-start.7
  26.3 0.0 copy-start.8
  26.3 0.0 copy-start.9
  26.4 25.5 %all_to_all.21.w_ref = bf16[8,4,64,384]{3,2,1,0:T(8,128)(2,1)S(1)} all-to-all(bf16[8,4,64,384]{3,2,1,0:T(8,128)(2,1)S(1)} %broadcast_in_dim.7), channel_id=1, replica_groups=mesh['zh'=2,'zm'=2,'zp'=2,'zl'=2,'y'=4,'x'=4,'c'=2] {'zl','y'}, dimensions={0} | all-to-all | bytes 3145728 | tf_op jit(solution)/shard_map/all_to_all | solution.py:17
  51.8 0.0 copy-done.3
  51.8 0.0 copy-done.5
  51.8 0.0 copy-done.7
  51.8 0.0 copy-done.8
  51.9 0.0 copy-done.9
  51.9 5.3 %previous_branch.1 = (bf16[384,384]{1,0:T(8,128)(2,1)}, bf16[2048,384]{1,0:T(8,128)(2,1)S(1)}, bf16[192,384]{1,0:T(8,128)(2,1)S(1)}, bf16[192,2048]{1,0:T(8,128)(2,1)}, bf16[8,264,384]{2,1,0:T(8,128)(2,1)}) custom-call(bf16[384,2048]{1,0:T(8,128)(2,1)S(1)} %copy-done.7, bf16[8,4,64,384]{3,2,1,0:T(8,128)(2,1)S(1)} %all_to_all.21.w_ref, ...), custom_call_target="tpu_custom_call" | custom-call | flops 1509949440 | bytes 6291456 | tf_op jit(solution)/shard_map/previous_branch/pallas_call | solution.py:177
  57.2 4.9 %all-to-all-start.2 = ((bf16[8,264,384]{2,1,0:T(8,128)(2,1)}), bf16[8,264,384]{2,1,0:T(8,128)(2,1)S(1)}, u32[]{:S(2)}, u32[]{:S(2)}) async-start(bf16[8,264,384]{2,1,0:T(8,128)(2,1)} %get-tuple-element.18), calls=%async_computation.2 | async-start | bytes 3244032 | tf_op jit(solution)/shard_map/all_to_all | solution.py:21
  62.1 1.9 %collective-permute-start = (bf16[192,2048]{1,0:T(8,128)(2,1)}, bf16[192,2048]{1,0:T(8,128)(2,1)S(1)}, u32[]{:S(2)}, u32[]{:S(2)}) collective-permute-start(bf16[192,2048]{1,0:T(8,128)(2,1)} %get-tuple-element.23), channel_id=1, source_target_pairs={{0,1},{1,0},{2,3},{3,2},{4,5},{5,4},{6,7},{7,6},{8,9},{9,8},{10,11... | collective-permute-start | bytes 2359304 | tf_op jit(solution)/shard_map/ppermute | solution.py:26
  64.0 2.5 %collective-permute-done = bf16[192,2048]{1,0:T(8,128)(2,1)S(1)} collective-permute-done((bf16[192,2048]{1,0:T(8,128)(2,1)}, bf16[192,2048]{1,0:T(8,128)(2,1)S(1)}, u32[]{:S(2)}, u32[]{:S(2)}) %collective-permute-start) | collective-permute-done | bytes 786464 | tf_op jit(solution)/shard_map/ppermute | solution.py:26
  66.5 0.0 copy-start
  66.5 0.0 copy-start.1
  66.5 0.7 add_convert_fusion
  67.2 0.0 copy-start.10
  67.2 0.9 copy-done.10
  68.1 0.8 fusion
  68.9 3.4 %collective-permute-start.1 = (bf16[48,2048]{1,0:T(8,128)(2,1)}, bf16[48,2048]{1,0:T(8,128)(2,1)}, u32[]{:S(2)}, u32[]{:S(2)}) collective-permute-start(bf16[48,2048]{1,0:T(8,128)(2,1)} %get-tuple-element.30), channel_id=1, source_target_pairs={{0,2},{2,4},{4,6},{6,0},{1,3},{3,5},{5,7},{7,1},{8,10},{10,12},{12... | collective-permute-start | bytes 589832 | tf_op jit(solution)/shard_map/ppermute | solution.py:26
  72.3 3.7 %collective-permute-start.3 = (bf16[48,2048]{1,0:T(8,128)(2,1)}, bf16[48,2048]{1,0:T(8,128)(2,1)}, u32[]{:S(2)}, u32[]{:S(2)}) collective-permute-start(bf16[48,2048]{1,0:T(8,128)(2,1)} %get-tuple-element.31), channel_id=1, source_target_pairs={{0,6},{2,0},{4,2},{6,4},{1,7},{3,1},{5,3},{7,5},{8,14},{10,8},{12,... | collective-permute-start | bytes 589832 | tf_op jit(solution)/shard_map/ppermute | solution.py:26
  76.0 3.7 %collective-permute-start.2 = (bf16[48,2048]{1,0:T(8,128)(2,1)S(1)}, bf16[48,2048]{1,0:T(8,128)(2,1)}, u32[]{:S(2)}, u32[]{:S(2)}) collective-permute-start(bf16[48,2048]{1,0:T(8,128)(2,1)S(1)} %get-tuple-element.32), channel_id=1, source_target_pairs={{0,4},{2,6},{4,0},{6,2},{1,5},{3,7},{5,1},{7,3},{8,12},{10,14},{12... | collective-permute-start | bytes 589832 | tf_op jit(solution)/shard_map/ppermute | solution.py:26
  79.7 0.0 copy-done
  79.7 0.0 copy-done.1
  79.7 2.0 %next_branch.1 = bf16[384,384]{1,0:T(8,128)(2,1)} custom-call(bf16[384,2048]{1,0:T(8,128)(2,1)S(1)} %copy-done, bf16[2048,384]{1,0:T(8,128)(2,1)S(1)} %get-tuple-element.19.w_ref, bf16[384,384]{1,0:T(8,128)(2,1)S(1)} %copy-done.1, f32[3,384]{1,0:T(4,128)S(1)} %copy-done.3, f32[384]{0:T(512)S(1)} %copy-done.5), custom_call_target="tpu_custom_call" | custom-call | flops 603979776 | bytes 3145728 | tf_op jit(solution)/shard_map/next_branch/pallas_call | solution.py:218
  81.7 0.0 all-to-all-done.2.in_ref
  81.7 0.9 sum_and_repack.1
  82.6 7.4 %all-to-all-start.3 = ((bf16[8,72,384]{2,1,0:T(8,128)(2,1)}), bf16[8,72,384]{2,1,0:T(8,128)(2,1)S(1)}, u32[]{:S(2)}, u32[]{:S(2)}) async-start(bf16[8,72,384]{2,1,0:T(8,128)(2,1)} %sum_and_repack.1), calls=%async_computation.3 | async-start | bytes 884736 | tf_op jit(solution)/shard_map/all_to_all | solution.py:21
  90.0 0.0 collective-permute-done.1
  90.0 0.0 collective-permute-done.3
  90.0 0.0 collective-permute-done.2
  90.0 1.3 %add_convert_fusion.1 = bf16[48,2048]{1,0:T(8,128)(2,1)S(1)} fusion(bf16[48,2048]{1,0:T(8,128)(2,1)} %collective-permute-done.3, bf16[48,2048]{1,0:T(8,128)(2,1)} %collective-permute-done.2, bf16[48,2048]{1,0:T(8,128)(2,1)} %collective-permute-done.1, bf16[192,2048]{1,0:T(8,128)(2,1)} %copy-done.10), kind=kLoop, calls=%fused_computation.2 | loop fusion | flops 786432 | bytes 983040 | tf_op jit(solution)/shard_map/convert_element_type | solution.py:337
  91.3 3.0 %collective-permute-start.6 = (bf16[48,2048]{1,0:T(8,128)(2,1)S(1)}, bf16[48,2048]{1,0:T(8,128)(2,1)S(1)}, u32[]{:S(2)}, u32[]{:S(2)}) collective-permute-start(bf16[48,2048]{1,0:T(8,128)(2,1)S(1)} %add_convert_fusion.1), channel_id=1, source_target_pairs={{0,6},{2,0},{4,2},{6,4},{1,7},{3,1},{5,3},{7,5},{8,14},{10,8},{12,... | collective-permute-start | bytes 589832 | tf_op jit(solution)/shard_map/ppermute | solution.py:26
  94.4 3.4 %collective-permute-start.5 = (bf16[48,2048]{1,0:T(8,128)(2,1)S(1)}, bf16[48,2048]{1,0:T(8,128)(2,1)S(1)}, u32[]{:S(2)}, u32[]{:S(2)}) collective-permute-start(bf16[48,2048]{1,0:T(8,128)(2,1)S(1)} %add_convert_fusion.1), channel_id=1, source_target_pairs={{0,4},{2,6},{4,0},{6,2},{1,5},{3,7},{5,1},{7,3},{8,12},{10,14},{12... | collective-permute-start | bytes 589832 | tf_op jit(solution)/shard_map/ppermute | solution.py:26
  97.8 2.4 %collective-permute-start.4 = (bf16[48,2048]{1,0:T(8,128)(2,1)S(1)}, bf16[48,2048]{1,0:T(8,128)(2,1)S(1)}, u32[]{:S(2)}, u32[]{:S(2)}) collective-permute-start(bf16[48,2048]{1,0:T(8,128)(2,1)S(1)} %add_convert_fusion.1), channel_id=1, source_target_pairs={{0,2},{2,4},{4,6},{6,0},{1,3},{3,5},{5,7},{7,1},{8,10},{10,12},{12... | collective-permute-start | bytes 589832 | tf_op jit(solution)/shard_map/ppermute | solution.py:26
  100.2 0.2 collective-permute-done.6
  100.5 4.9 %collective-permute-done.5 = bf16[48,2048]{1,0:T(8,128)(2,1)S(1)} collective-permute-done((bf16[48,2048]{1,0:T(8,128)(2,1)S(1)}, bf16[48,2048]{1,0:T(8,128)(2,1)S(1)}, u32[]{:S(2)}, u32[]{:S(2)}) %collective-permute-start.5) | collective-permute-done | bytes 196640 | tf_op jit(solution)/shard_map/ppermute | solution.py:26
  105.4 2.6 %collective-permute-done.4 = bf16[48,2048]{1,0:T(8,128)(2,1)S(1)} collective-permute-done((bf16[48,2048]{1,0:T(8,128)(2,1)S(1)}, bf16[48,2048]{1,0:T(8,128)(2,1)S(1)}, u32[]{:S(2)}, u32[]{:S(2)}) %collective-permute-start.4) | collective-permute-done | bytes 196640 | tf_op jit(solution)/shard_map/ppermute | solution.py:26
  108.0 0.1 pad_maximum_fusion.own_ref
  108.2 0.0 copy-start.2
  108.2 0.0 copy-start.4
  108.2 0.0 copy-start.6
  108.2 2.1 %collective-permute-start.7 = (bf16[4,48,2048]{2,1,0:T(8,128)(2,1)S(1)}, bf16[4,48,2048]{2,1,0:T(8,128)(2,1)S(1)}, u32[]{:S(2)}, u32[]{:S(2)}) collective-permute-start(bf16[4,48,2048]{2,1,0:T(8,128)(2,1)S(1)} %pad_maximum_fusion.own_ref), channel_id=1, source_target_pairs={{0,1},{1,0},{2,3},{3,2},{4,5},{5,4},{6,7},{7,6},{8,9},{9,8},{10,11... | collective-permute-start | bytes 2359304 | tf_op jit(solution)/shard_map/ppermute | solution.py:26
  110.2 2.3 %collective-permute-done.7.other_ref = bf16[4,48,2048]{2,1,0:T(8,128)(2,1)S(1)} collective-permute-done((bf16[4,48,2048]{2,1,0:T(8,128)(2,1)S(1)}, bf16[4,48,2048]{2,1,0:T(8,128)(2,1)S(1)}, u32[]{:S(2)}, u32[]{:S(2)}) %collective-permute-start.7) | collective-permute-done | bytes 786464 | tf_op jit(solution)/shard_map/ppermute | solution.py:26
  112.5 1.3 %put_in_order.1 = bf16[8,48,2048]{2,1,0:T(8,128)(2,1)} custom-call(bf16[4,48,2048]{2,1,0:T(8,128)(2,1)S(1)} %pad_maximum_fusion.own_ref, bf16[4,48,2048]{2,1,0:T(8,128)(2,1)S(1)} %collective-permute-done.7.other_ref), custom_call_target="tpu_custom_call" | custom-call | bytes 3145728 | tf_op jit(solution)/shard_map/put_in_order/pallas_call | solution.py:51
  113.8 3.1 %all-to-all-done.3.in_ref = bf16[8,72,384]{2,1,0:T(8,128)(2,1)S(1)} async-done(((bf16[8,72,384]{2,1,0:T(8,128)(2,1)}), bf16[8,72,384]{2,1,0:T(8,128)(2,1)S(1)}, u32[]{:S(2)}, u32[]{:S(2)}) %all-to-all-start.3) | async-done | bytes 442400 | tf_op jit(solution)/shard_map/all_to_all | solution.py:21
  116.9 0.0 copy-done.2
  116.9 0.0 copy-done.4
  116.9 0.0 copy-done.6
  116.9 0.7 last_sum.1
Async XLA Ops:
  26.3 25.5 %copy-start.3 = (f32[3,384]{1,0:T(4,128)S(1)}, f32[3,384]{1,0:T(4,128)}, u32[]{:S(2)}) copy-start(f32[3,384]{1,0:T(4,128)} %taps_ref.4) | copy-start | bytes 13828
  26.3 25.5 %copy-start.5 = (f32[384]{0:T(512)S(1)}, f32[384]{0:T(512)}, u32[]{:S(2)}) copy-start(f32[384]{0:T(512)} %bias_ref.4) | copy-start | bytes 4612
  26.3 25.5 %copy-start.7 = (bf16[384,2048]{1,0:T(8,128)(2,1)S(1)}, bf16[384,2048]{1,0:T(8,128)(2,1)}, u32[]{:S(2)}) copy-start(bf16[384,2048]{1,0:T(8,128)(2,1)} %x_ref.2) | copy-start | bytes 4718596
  26.3 25.5 %copy-start.8 = (bf16[384,384]{1,0:T(8,128)(2,1)S(1)}, bf16[384,384]{1,0:T(8,128)(2,1)}, u32[]{:S(2)}) copy-start(bf16[384,384]{1,0:T(8,128)(2,1)} %cot_ref.1) | copy-start | bytes 884740
  26.3 25.5 %copy-start.9 = (bf16[384,384]{1,0:T(8,128)(2,1)S(1)}, bf16[384,384]{1,0:T(8,128)(2,1)}, u32[]{:S(2)}) copy-start(bf16[384,384]{1,0:T(8,128)(2,1)} %value_ref.2) | copy-start | bytes 884740
  57.2 24.5 %all-to-all-start.2 = ((bf16[8,264,384]{2,1,0:T(8,128)(2,1)}), bf16[8,264,384]{2,1,0:T(8,128)(2,1)S(1)}, u32[]{:S(2)}, u32[]{:S(2)}) async-start(bf16[8,264,384]{2,1,0:T(8,128)(2,1)} %get-tuple-element.18), calls=%async_computation.2 | async-start | bytes 3244032 | tf_op jit(solution)/shard_map/all_to_all | solution.py:21
  62.1 4.4 %collective-permute-start = (bf16[192,2048]{1,0:T(8,128)(2,1)}, bf16[192,2048]{1,0:T(8,128)(2,1)S(1)}, u32[]{:S(2)}, u32[]{:S(2)}) collective-permute-start(bf16[192,2048]{1,0:T(8,128)(2,1)} %get-tuple-element.23), channel_id=1, source_target_pairs={{0,1},{1,0},{2,3},{3,2},{4,5},{5,4},{6,7},{7,6},{8,9},{9,8},{10,11... | collective-permute-start | bytes 2359304 | tf_op jit(solution)/shard_map/ppermute | solution.py:26
  66.5 13.2 %copy-start = (bf16[384,2048]{1,0:T(8,128)(2,1)S(1)}, bf16[384,2048]{1,0:T(8,128)(2,1)}, u32[]{:S(2)}) copy-start(bf16[384,2048]{1,0:T(8,128)(2,1)} %x_ref.3) | copy-start | bytes 4718596
  66.5 13.2 %copy-start.1 = (bf16[384,384]{1,0:T(8,128)(2,1)S(1)}, bf16[384,384]{1,0:T(8,128)(2,1)}, u32[]{:S(2)}) copy-start(bf16[384,384]{1,0:T(8,128)(2,1)} %value_ref.3) | copy-start | bytes 884740
  67.2 0.9 copy-start.10
  68.9 21.1 %collective-permute-start.1 = (bf16[48,2048]{1,0:T(8,128)(2,1)}, bf16[48,2048]{1,0:T(8,128)(2,1)}, u32[]{:S(2)}, u32[]{:S(2)}) collective-permute-start(bf16[48,2048]{1,0:T(8,128)(2,1)} %get-tuple-element.30), channel_id=1, source_target_pairs={{0,2},{2,4},{4,6},{6,0},{1,3},{3,5},{5,7},{7,1},{8,10},{10,12},{12... | collective-permute-start | bytes 589832 | tf_op jit(solution)/shard_map/ppermute | solution.py:26
  72.3 17.7 %collective-permute-start.3 = (bf16[48,2048]{1,0:T(8,128)(2,1)}, bf16[48,2048]{1,0:T(8,128)(2,1)}, u32[]{:S(2)}, u32[]{:S(2)}) collective-permute-start(bf16[48,2048]{1,0:T(8,128)(2,1)} %get-tuple-element.31), channel_id=1, source_target_pairs={{0,6},{2,0},{4,2},{6,4},{1,7},{3,1},{5,3},{7,5},{8,14},{10,8},{12,... | collective-permute-start | bytes 589832 | tf_op jit(solution)/shard_map/ppermute | solution.py:26
  76.0 14.1 %collective-permute-start.2 = (bf16[48,2048]{1,0:T(8,128)(2,1)S(1)}, bf16[48,2048]{1,0:T(8,128)(2,1)}, u32[]{:S(2)}, u32[]{:S(2)}) collective-permute-start(bf16[48,2048]{1,0:T(8,128)(2,1)S(1)} %get-tuple-element.32), channel_id=1, source_target_pairs={{0,4},{2,6},{4,0},{6,2},{1,5},{3,7},{5,1},{7,3},{8,12},{10,14},{12... | collective-permute-start | bytes 589832 | tf_op jit(solution)/shard_map/ppermute | solution.py:26
  82.6 34.3 %all-to-all-start.3 = ((bf16[8,72,384]{2,1,0:T(8,128)(2,1)}), bf16[8,72,384]{2,1,0:T(8,128)(2,1)S(1)}, u32[]{:S(2)}, u32[]{:S(2)}) async-start(bf16[8,72,384]{2,1,0:T(8,128)(2,1)} %sum_and_repack.1), calls=%async_computation.3 | async-start | bytes 884736 | tf_op jit(solution)/shard_map/all_to_all | solution.py:21
  91.3 9.1 %collective-permute-start.6 = (bf16[48,2048]{1,0:T(8,128)(2,1)S(1)}, bf16[48,2048]{1,0:T(8,128)(2,1)S(1)}, u32[]{:S(2)}, u32[]{:S(2)}) collective-permute-start(bf16[48,2048]{1,0:T(8,128)(2,1)S(1)} %add_convert_fusion.1), channel_id=1, source_target_pairs={{0,6},{2,0},{4,2},{6,4},{1,7},{3,1},{5,3},{7,5},{8,14},{10,8},{12,... | collective-permute-start | bytes 589832 | tf_op jit(solution)/shard_map/ppermute | solution.py:26
  94.4 11.0 %collective-permute-start.5 = (bf16[48,2048]{1,0:T(8,128)(2,1)S(1)}, bf16[48,2048]{1,0:T(8,128)(2,1)S(1)}, u32[]{:S(2)}, u32[]{:S(2)}) collective-permute-start(bf16[48,2048]{1,0:T(8,128)(2,1)S(1)} %add_convert_fusion.1), channel_id=1, source_target_pairs={{0,4},{2,6},{4,0},{6,2},{1,5},{3,7},{5,1},{7,3},{8,12},{10,14},{12... | collective-permute-start | bytes 589832 | tf_op jit(solution)/shard_map/ppermute | solution.py:26
  97.8 10.2 %collective-permute-start.4 = (bf16[48,2048]{1,0:T(8,128)(2,1)S(1)}, bf16[48,2048]{1,0:T(8,128)(2,1)S(1)}, u32[]{:S(2)}, u32[]{:S(2)}) collective-permute-start(bf16[48,2048]{1,0:T(8,128)(2,1)S(1)} %add_convert_fusion.1), channel_id=1, source_target_pairs={{0,2},{2,4},{4,6},{6,0},{1,3},{3,5},{5,7},{7,1},{8,10},{10,12},{12... | collective-permute-start | bytes 589832 | tf_op jit(solution)/shard_map/ppermute | solution.py:26
  108.2 8.8 %copy-start.2 = (f32[64,384]{1,0:T(8,128)S(1)}, f32[64,384]{1,0:T(8,128)}, u32[]{:S(2)}) copy-start(f32[64,384]{1,0:T(8,128)} %w_ref.1) | copy-start | bytes 294916
  108.2 8.8 %copy-start.4 = (f32[3,384]{1,0:T(4,128)S(1)}, f32[3,384]{1,0:T(4,128)}, u32[]{:S(2)}) copy-start(f32[3,384]{1,0:T(4,128)} %taps_ref.5) | copy-start | bytes 13828
  108.2 8.7 %copy-start.6 = (f32[384]{0:T(512)S(1)}, f32[384]{0:T(512)}, u32[]{:S(2)}) copy-start(f32[384]{0:T(512)} %bias_ref.5) | copy-start | bytes 4612
  108.2 4.3 %collective-permute-start.7 = (bf16[4,48,2048]{2,1,0:T(8,128)(2,1)S(1)}, bf16[4,48,2048]{2,1,0:T(8,128)(2,1)S(1)}, u32[]{:S(2)}, u32[]{:S(2)}) collective-permute-start(bf16[4,48,2048]{2,1,0:T(8,128)(2,1)S(1)} %pad_maximum_fusion.own_ref), channel_id=1, source_target_pairs={{0,1},{1,0},{2,3},{3,2},{4,5},{5,4},{6,7},{7,6},{8,9},{9,8},{10,11... | collective-permute-start | bytes 2359304 | tf_op jit(solution)/shard_map/ppermute | solution.py:26

commit v8 on v7

--- a/solution.py
+++ b/solution.py
@@ -205,6 +205,42 @@
     )
 
 
+def add_halves(keep, weights, from_core, n_x):
+    rows, width = from_core.shape
+    each = rows // n_x
+
+    def body(keep_ref, w_ref, other_ref, *refs):
+        out_refs, blocks_ref, sems = refs[:n_x], refs[n_x], refs[n_x + 1]
+        total = lax.dot_general(
+            keep_ref[...],
+            w_ref[...],
+            (((1,), (1,)), ((), ())),
+            preferred_element_type=jnp.float32,
+        )
+        total = (total + other_ref[...].astype(jnp.float32)).astype(jnp.bfloat16)
+        moves = []
+        for k in range(n_x):
+            blocks_ref[k] = total[k * each : (k + 1) * each]
+            moves.append(pltpu.make_async_copy(blocks_ref.at[k], out_refs[k], sems.at[k]))
+            moves[-1].start()
+        for move in moves:
+            move.wait()
+
+    return pl.pallas_call(
+        body,
+        in_specs=[VMEM] * 3,
+        out_specs=[HBM] * n_x,
+        out_shape=[pltpu.HBM((each, width), jnp.bfloat16)] * n_x,
+        scratch_shapes=[
+            pltpu.VMEM((n_x, each, width), jnp.bfloat16),
+            pltpu.SemaphoreType.DMA((n_x,)),
+        ],
+        cost_estimate=cost(2 * keep.size * width, 8 * weights.size),
+        name="add_halves",
+        compiler_params=pltpu.CompilerParams(vmem_limit_bytes=16 * 2**20),
+    )(near(keep), near(weights), near(from_core))
+
+
 def next_branch(x_next, weights, value_next, conv_taps, conv_bias):
     row_count, width = x_next.shape
     units = weights.shape[1]
@@ -320,22 +356,21 @@
     from_core = send_on(to_core, "c", 1)
     from_near = exchange(sent, NEAR)
 
-    block_rows = row_count // (n_x * n_c)
-    kept = lax.dot_general(
-        keep, gathered, (((1,), (1,)), ((), ())), preferred_element_type=jnp.float32
-    )
-    half = (kept + from_core.astype(jnp.float32)).astype(jnp.bfloat16)
-    half = half.reshape(n_x, block_rows, width)
+    half = add_halves(keep, gathered, from_core, n_x)
     arrived = [half[0]]
     for k in range(1, n_x):
         arrived.append(send_on(half[k], "x", k))
-    hidden_next = next_branch(x_next, gathered, value_next, conv_taps, conv_bias)
-    from_near, hidden_next = lax.optimization_barrier((from_near, hidden_next))
     by_far = sum_and_repack(from_near, n_far, n_zh)
     from_far = exchange(by_far, ("zh", *FAR))
 
     eighth = sum(block.astype(jnp.float32) for block in arrived).astype(jnp.bfloat16)
-    half = jnp.stack([eighth] + [send_on(eighth, "x", k) for k in range(1, n_x)])
+    spread = [eighth]
+    for k in range(1, n_x):
+        spread.append(send_on(eighth, "x", k))
+    eighth, x_next = lax.optimization_barrier((eighth, x_next))
+    hidden_next = next_branch(x_next, gathered, value_next, conv_taps, conv_bias)
+    hidden_next, *spread = lax.optimization_barrier((hidden_next, *spread))
+    half = jnp.stack(spread)
     grad_input = put_in_order(half, send_on(half, "c", 1), n_c).reshape(row_count, width)
     from_far, grad_input = lax.optimization_barrier((from_far, grad_input))
     new_w, new_taps, new_bias = last_sum(from_far, sum_w, sum_taps, sum_bias)

time: 118 us -> 117 us (level)
  the two profiles are of different devices: /device:TPU:32 before, /device:TPU:44 now
where the time goes in v8:
time: 117 us; the launch traced here: 116 us
  blocking collectives  49.3 us (42%)
  starting transfers between devices  34.2 us (29%)
  waiting for transfers between devices  15.9 us (14%)
  Pallas kernels  11.8 us (10%)
  local copies, waits for them, and re-layouts  2.5 us (2%)
  other arithmetic  1.42 us (1%)
    all_to_all x2, blocking collectives, copies_to(): return lax.all_to_all(copies, axis, 0, 0, tiled=True)  49.3 us
    ppermute x8, starting transfers between devices, send_on(): lax.ppermute(block, axis, [(i, (i + shift) % size) for i in range(size)])  22 us
    all_to_all x2, starting transfers between devices, exchange(): return lax.all_to_all(blocks, axis, 0, 0, tiled=True)  12.2 us
    ppermute x8, waiting for transfers between devices, send_on(): lax.ppermute(block, axis, [(i, (i + shift) % size) for i in range(size)])  8.7 us
    all_to_all x2, waiting for transfers between devices, exchange(): return lax.all_to_all(blocks, axis, 0, 0, tiled=True)  7.2 us
    pallas_call x1, Pallas kernels, previous_branch(): pl.pallas_call(body, in_specs=[VMEM] * 6, out_specs=[pl.BlockSpec(), VMEM...  5.33 us
  transfers between devices with their start and end apart: 10, of which 6 were waited for; matrix products, arithmetic and copies ran while one was open for 1% of the time, Pallas kernels for 5%

profile of v8, /device:TPU:44, one launch (start us, length us, event | category | flops | bytes accessed | tf_op | source)
XLA Modules:
  0.0 116.0 jit_solution(3893693739055109977)
XLA Ops:
  0.6 0.8 broadcast_in_dim.6
  1.5 24.6 %all_to_all.20 = bf16[4,64,384]{2,1,0:T(8,128)(2,1)S(1)} all-to-all(bf16[4,64,384]{2,1,0:T(8,128)(2,1)S(1)} %broadcast_in_dim.6), channel_id=1, replica_groups=mesh['zh'=2,'zm'=2,'zp'=2,'zl'=2,'y'=4,'x'=4,'c'=2] {'zm','zp'}, dimensions={0} | all-to-all | bytes 393216 | tf_op jit(solution)/shard_map/all_to_all | solution.py:17
  26.1 0.2 broadcast_in_dim.7
  26.3 0.0 copy-start.3
  26.3 0.0 copy-start.5
  26.3 0.0 copy-start.7
  26.3 0.0 copy-start.8
  26.3 0.0 copy-start.9
  26.4 24.7 %all_to_all.21.w_ref = bf16[8,4,64,384]{3,2,1,0:T(8,128)(2,1)S(1)} all-to-all(bf16[8,4,64,384]{3,2,1,0:T(8,128)(2,1)S(1)} %broadcast_in_dim.7), channel_id=1, replica_groups=mesh['zh'=2,'zm'=2,'zp'=2,'zl'=2,'y'=4,'x'=4,'c'=2] {'zl','y'}, dimensions={0} | all-to-all | bytes 3145728 | tf_op jit(solution)/shard_map/all_to_all | solution.py:17
  51.1 0.0 copy-done.3
  51.1 0.0 copy-done.5
  51.1 0.0 copy-done.7
  51.1 0.0 copy-done.8
  51.1 0.0 copy-done.9
  51.1 5.3 %previous_branch.1 = (bf16[384,384]{1,0:T(8,128)(2,1)}, bf16[2048,384]{1,0:T(8,128)(2,1)S(1)}, bf16[192,384]{1,0:T(8,128)(2,1)S(1)}, bf16[192,2048]{1,0:T(8,128)(2,1)}, bf16[8,264,384]{2,1,0:T(8,128)(2,1)}) custom-call(bf16[384,2048]{1,0:T(8,128)(2,1)S(1)} %copy-done.7, bf16[8,4,64,384]{3,2,1,0:T(8,128)(2,1)S(1)} %all_to_all.21.w_ref, ...), custom_call_target="tpu_custom_call" | custom-call | flops 1509949440 | bytes 6291456 | tf_op jit(solution)/shard_map/previous_branch/pallas_call | solution.py:177
  56.4 5.5 %all-to-all-start.2 = ((bf16[8,264,384]{2,1,0:T(8,128)(2,1)}), bf16[8,264,384]{2,1,0:T(8,128)(2,1)S(1)}, u32[]{:S(2)}, u32[]{:S(2)}) async-start(bf16[8,264,384]{2,1,0:T(8,128)(2,1)} %get-tuple-element.35), calls=%async_computation.2 | async-start | bytes 3244032 | tf_op jit(solution)/shard_map/all_to_all | solution.py:21
  62.0 1.9 %collective-permute-start = (bf16[192,2048]{1,0:T(8,128)(2,1)}, bf16[192,2048]{1,0:T(8,128)(2,1)S(1)}, u32[]{:S(2)}, u32[]{:S(2)}) collective-permute-start(bf16[192,2048]{1,0:T(8,128)(2,1)} %get-tuple-element.28), channel_id=1, source_target_pairs={{0,1},{1,0},{2,3},{3,2},{4,5},{5,4},{6,7},{7,6},{8,9},{9,8},{10,11... | collective-permute-start | bytes 2359304 | tf_op jit(solution)/shard_map/ppermute | solution.py:26
  63.9 2.5 %collective-permute-done.other_ref = bf16[192,2048]{1,0:T(8,128)(2,1)S(1)} collective-permute-done((bf16[192,2048]{1,0:T(8,128)(2,1)}, bf16[192,2048]{1,0:T(8,128)(2,1)S(1)}, u32[]{:S(2)}, u32[]{:S(2)}) %collective-permute-start) | collective-permute-done | bytes 786464 | tf_op jit(solution)/shard_map/ppermute | solution.py:26
  66.4 1.6 %add_halves.1 = (bf16[48,2048]{1,0:T(8,128)(2,1)}, bf16[48,2048]{1,0:T(8,128)(2,1)}, bf16[48,2048]{1,0:T(8,128)(2,1)}, bf16[48,2048]{1,0:T(8,128)(2,1)}) custom-call(bf16[192,384]{1,0:T(8,128)(2,1)S(1)} %get-tuple-element.26.keep_ref, bf16[2048,384]{1,0:T(8,128)(2,1)S(1)} %get-tuple-element.27.w_ref, bf16[192,2048]{1,0:T(8,128)(2,1)S(1)} %collective-permute-done.other_ref), custom_call_target="tpu_custom_call" | custom-call | flops 301989888 | bytes 6291456 | tf_op jit(solution)/shard_map/add_halves/pallas_call | solution.py:229
  67.9 3.1 %collective-permute-start.1 = (bf16[48,2048]{1,0:T(8,128)(2,1)}, bf16[48,2048]{1,0:T(8,128)(2,1)}, u32[]{:S(2)}, u32[]{:S(2)}) collective-permute-start(bf16[48,2048]{1,0:T(8,128)(2,1)} %get-tuple-element.30), channel_id=1, source_target_pairs={{0,2},{2,4},{4,6},{6,0},{1,3},{3,5},{5,7},{7,1},{8,10},{10,12},{12... | collective-permute-start | bytes 589832 | tf_op jit(solution)/shard_map/ppermute | solution.py:26
  71.0 2.7 %collective-permute-start.2 = (bf16[48,2048]{1,0:T(8,128)(2,1)}, bf16[48,2048]{1,0:T(8,128)(2,1)}, u32[]{:S(2)}, u32[]{:S(2)}) collective-permute-start(bf16[48,2048]{1,0:T(8,128)(2,1)} %get-tuple-element.31), channel_id=1, source_target_pairs={{0,4},{2,6},{4,0},{6,2},{1,5},{3,7},{5,1},{7,3},{8,12},{10,14},{12... | collective-permute-start | bytes 589832 | tf_op jit(solution)/shard_map/ppermute | solution.py:26
  73.8 0.0 copy-start.1
  73.8 3.2 %collective-permute-start.3 = (bf16[48,2048]{1,0:T(8,128)(2,1)}, bf16[48,2048]{1,0:T(8,128)(2,1)}, u32[]{:S(2)}, u32[]{:S(2)}) collective-permute-start(bf16[48,2048]{1,0:T(8,128)(2,1)} %get-tuple-element.32), channel_id=1, source_target_pairs={{0,6},{2,0},{4,2},{6,4},{1,7},{3,1},{5,3},{7,5},{8,14},{10,8},{12,... | collective-permute-start | bytes 589832 | tf_op jit(solution)/shard_map/ppermute | solution.py:26
  77.0 3.1 %all-to-all-done.2.in_ref = bf16[8,264,384]{2,1,0:T(8,128)(2,1)S(1)} async-done(((bf16[8,264,384]{2,1,0:T(8,128)(2,1)}), bf16[8,264,384]{2,1,0:T(8,128)(2,1)S(1)}, u32[]{:S(2)}, u32[]{:S(2)}) %all-to-all-start.2) | async-done | bytes 1622048 | tf_op jit(solution)/shard_map/all_to_all | solution.py:21
  80.0 0.9 sum_and_repack.1
  81.0 6.7 %all-to-all-start.3 = ((bf16[8,72,384]{2,1,0:T(8,128)(2,1)}), bf16[8,72,384]{2,1,0:T(8,128)(2,1)S(1)}, u32[]{:S(2)}, u32[]{:S(2)}) async-start(bf16[8,72,384]{2,1,0:T(8,128)(2,1)} %sum_and_repack.1), calls=%async_computation.3 | async-start | bytes 884736 | tf_op jit(solution)/shard_map/all_to_all | solution.py:21
  87.7 0.0 collective-permute-done.1
  87.7 0.0 collective-permute-done.2
  87.7 0.0 collective-permute-done.3
  87.7 1.3 %add_convert_fusion = bf16[48,2048]{1,0:T(8,128)(2,1)S(1)} fusion(bf16[48,2048]{1,0:T(8,128)(2,1)} %collective-permute-done.3, bf16[48,2048]{1,0:T(8,128)(2,1)} %collective-permute-done.2, bf16[48,2048]{1,0:T(8,128)(2,1)} %collective-permute-done.1, bf16[48,2048]{1,0:T(8,128)(2,1)} %get-tuple-element.29), kind=kLoop, calls=%fused_computation.1 | loop fusion | flops 786432 | bytes 983040 | tf_op jit(solution)/shard_map/convert_element_type | solution.py:366
  89.0 3.1 %collective-permute-start.4 = (bf16[48,2048]{1,0:T(8,128)(2,1)S(1)}, bf16[48,2048]{1,0:T(8,128)(2,1)S(1)}, u32[]{:S(2)}, u32[]{:S(2)}) collective-permute-start(bf16[48,2048]{1,0:T(8,128)(2,1)S(1)} %add_convert_fusion), channel_id=1, source_target_pairs={{0,2},{2,4},{4,6},{6,0},{1,3},{3,5},{5,7},{7,1},{8,10},{10,12},{12... | collective-permute-start | bytes 589832 | tf_op jit(solution)/shard_map/ppermute | solution.py:26
  92.1 2.7 %collective-permute-start.5 = (bf16[48,2048]{1,0:T(8,128)(2,1)S(1)}, bf16[48,2048]{1,0:T(8,128)(2,1)S(1)}, u32[]{:S(2)}, u32[]{:S(2)}) collective-permute-start(bf16[48,2048]{1,0:T(8,128)(2,1)S(1)} %add_convert_fusion), channel_id=1, source_target_pairs={{0,4},{2,6},{4,0},{6,2},{1,5},{3,7},{5,1},{7,3},{8,12},{10,14},{12... | collective-permute-start | bytes 589832 | tf_op jit(solution)/shard_map/ppermute | solution.py:26
  94.8 3.2 %collective-permute-start.6 = (bf16[48,2048]{1,0:T(8,128)(2,1)S(1)}, bf16[48,2048]{1,0:T(8,128)(2,1)S(1)}, u32[]{:S(2)}, u32[]{:S(2)}) collective-permute-start(bf16[48,2048]{1,0:T(8,128)(2,1)S(1)} %add_convert_fusion), channel_id=1, source_target_pairs={{0,6},{2,0},{4,2},{6,4},{1,7},{3,1},{5,3},{7,5},{8,14},{10,8},{12,... | collective-permute-start | bytes 589832 | tf_op jit(solution)/shard_map/ppermute | solution.py:26
  98.1 0.0 copy-done.1
  98.1 0.0 copy-start
  98.1 1.4 %copy-done = bf16[384,2048]{1,0:T(8,128)(2,1)S(1)} copy-done((bf16[384,2048]{1,0:T(8,128)(2,1)S(1)}, bf16[384,2048]{1,0:T(8,128)(2,1)}, u32[]{:S(2)}) %copy-start) | copy-done | bytes 1572888
  99.5 1.9 %next_branch.1 = bf16[384,384]{1,0:T(8,128)(2,1)} custom-call(bf16[384,2048]{1,0:T(8,128)(2,1)S(1)} %copy-done, bf16[2048,384]{1,0:T(8,128)(2,1)S(1)} %get-tuple-element.27.w_ref, bf16[384,384]{1,0:T(8,128)(2,1)S(1)} %copy-done.1, f32[3,384]{1,0:T(4,128)S(1)} %copy-done.3, f32[384]{0:T(512)S(1)} %copy-done.5), custom_call_target="tpu_custom_call" | custom-call | flops 603979776 | bytes 3145728 | tf_op jit(solution)/shard_map/next_branch/pallas_call | solution.py:254
  101.5 0.0 collective-permute-done.4
  101.5 0.4 collective-permute-done.5
  101.8 3.6 %collective-permute-done.6 = bf16[48,2048]{1,0:T(8,128)(2,1)S(1)} collective-permute-done((bf16[48,2048]{1,0:T(8,128)(2,1)S(1)}, bf16[48,2048]{1,0:T(8,128)(2,1)S(1)}, u32[]{:S(2)}, u32[]{:S(2)}) %collective-permute-start.6) | collective-permute-done | bytes 196640 | tf_op jit(solution)/shard_map/ppermute | solution.py:26
  105.4 0.1 pad_maximum_fusion.own_ref
  105.5 0.0 copy-start.2
  105.5 0.0 copy-start.4
  105.6 0.0 copy-start.6
  105.6 2.1 %collective-permute-start.7 = (bf16[4,48,2048]{2,1,0:T(8,128)(2,1)S(1)}, bf16[4,48,2048]{2,1,0:T(8,128)(2,1)S(1)}, u32[]{:S(2)}, u32[]{:S(2)}) collective-permute-start(bf16[4,48,2048]{2,1,0:T(8,128)(2,1)S(1)} %pad_maximum_fusion.own_ref), channel_id=1, source_target_pairs={{0,1},{1,0},{2,3},{3,2},{4,5},{5,4},{6,7},{7,6},{8,9},{9,8},{10,11... | collective-permute-start | bytes 2359304 | tf_op jit(solution)/shard_map/ppermute | solution.py:26
  107.6 2.3 %collective-permute-done.7.other_ref = bf16[4,48,2048]{2,1,0:T(8,128)(2,1)S(1)} collective-permute-done((bf16[4,48,2048]{2,1,0:T(8,128)(2,1)S(1)}, bf16[4,48,2048]{2,1,0:T(8,128)(2,1)S(1)}, u32[]{:S(2)}, u32[]{:S(2)}) %collective-permute-start.7) | collective-permute-done | bytes 786464 | tf_op jit(solution)/shard_map/ppermute | solution.py:26
  109.9 1.3 %put_in_order.1 = bf16[8,48,2048]{2,1,0:T(8,128)(2,1)} custom-call(bf16[4,48,2048]{2,1,0:T(8,128)(2,1)S(1)} %pad_maximum_fusion.own_ref, bf16[4,48,2048]{2,1,0:T(8,128)(2,1)S(1)} %collective-permute-done.7.other_ref), custom_call_target="tpu_custom_call" | custom-call | bytes 3145728 | tf_op jit(solution)/shard_map/put_in_order/pallas_call | solution.py:51
  111.2 4.1 %all-to-all-done.3.in_ref = bf16[8,72,384]{2,1,0:T(8,128)(2,1)S(1)} async-done(((bf16[8,72,384]{2,1,0:T(8,128)(2,1)}), bf16[8,72,384]{2,1,0:T(8,128)(2,1)S(1)}, u32[]{:S(2)}, u32[]{:S(2)}) %all-to-all-start.3) | async-done | bytes 442400 | tf_op jit(solution)/shard_map/all_to_all | solution.py:21
  115.3 0.0 copy-done.2
  115.3 0.0 copy-done.4
  115.3 0.0 copy-done.6
  115.3 0.7 last_sum.1
Async XLA Ops:
  26.3 24.8 %copy-start.3 = (f32[3,384]{1,0:T(4,128)S(1)}, f32[3,384]{1,0:T(4,128)}, u32[]{:S(2)}) copy-start(f32[3,384]{1,0:T(4,128)} %taps_ref.4) | copy-start | bytes 13828
  26.3 24.8 %copy-start.5 = (f32[384]{0:T(512)S(1)}, f32[384]{0:T(512)}, u32[]{:S(2)}) copy-start(f32[384]{0:T(512)} %bias_ref.4) | copy-start | bytes 4612
  26.3 24.8 %copy-start.7 = (bf16[384,2048]{1,0:T(8,128)(2,1)S(1)}, bf16[384,2048]{1,0:T(8,128)(2,1)}, u32[]{:S(2)}) copy-start(bf16[384,2048]{1,0:T(8,128)(2,1)} %x_ref.1) | copy-start | bytes 4718596
  26.3 24.8 %copy-start.8 = (bf16[384,384]{1,0:T(8,128)(2,1)S(1)}, bf16[384,384]{1,0:T(8,128)(2,1)}, u32[]{:S(2)}) copy-start(bf16[384,384]{1,0:T(8,128)(2,1)} %cot_ref.1) | copy-start | bytes 884740
  26.3 24.8 %copy-start.9 = (bf16[384,384]{1,0:T(8,128)(2,1)S(1)}, bf16[384,384]{1,0:T(8,128)(2,1)}, u32[]{:S(2)}) copy-start(bf16[384,384]{1,0:T(8,128)(2,1)} %value_ref.2) | copy-start | bytes 884740
  56.4 23.6 %all-to-all-start.2 = ((bf16[8,264,384]{2,1,0:T(8,128)(2,1)}), bf16[8,264,384]{2,1,0:T(8,128)(2,1)S(1)}, u32[]{:S(2)}, u32[]{:S(2)}) async-start(bf16[8,264,384]{2,1,0:T(8,128)(2,1)} %get-tuple-element.35), calls=%async_computation.2 | async-start | bytes 3244032 | tf_op jit(solution)/shard_map/all_to_all | solution.py:21
  62.0 4.4 %collective-permute-start = (bf16[192,2048]{1,0:T(8,128)(2,1)}, bf16[192,2048]{1,0:T(8,128)(2,1)S(1)}, u32[]{:S(2)}, u32[]{:S(2)}) collective-permute-start(bf16[192,2048]{1,0:T(8,128)(2,1)} %get-tuple-element.28), channel_id=1, source_target_pairs={{0,1},{1,0},{2,3},{3,2},{4,5},{5,4},{6,7},{7,6},{8,9},{9,8},{10,11... | collective-permute-start | bytes 2359304 | tf_op jit(solution)/shard_map/ppermute | solution.py:26
  67.9 19.7 %collective-permute-start.1 = (bf16[48,2048]{1,0:T(8,128)(2,1)}, bf16[48,2048]{1,0:T(8,128)(2,1)}, u32[]{:S(2)}, u32[]{:S(2)}) collective-permute-start(bf16[48,2048]{1,0:T(8,128)(2,1)} %get-tuple-element.30), channel_id=1, source_target_pairs={{0,2},{2,4},{4,6},{6,0},{1,3},{3,5},{5,7},{7,1},{8,10},{10,12},{12... | collective-permute-start | bytes 589832 | tf_op jit(solution)/shard_map/ppermute | solution.py:26
  71.0 16.6 %collective-permute-start.2 = (bf16[48,2048]{1,0:T(8,128)(2,1)}, bf16[48,2048]{1,0:T(8,128)(2,1)}, u32[]{:S(2)}, u32[]{:S(2)}) collective-permute-start(bf16[48,2048]{1,0:T(8,128)(2,1)} %get-tuple-element.31), channel_id=1, source_target_pairs={{0,4},{2,6},{4,0},{6,2},{1,5},{3,7},{5,1},{7,3},{8,12},{10,14},{12... | collective-permute-start | bytes 589832 | tf_op jit(solution)/shard_map/ppermute | solution.py:26
  73.8 24.3 %copy-start.1 = (bf16[384,384]{1,0:T(8,128)(2,1)S(1)}, bf16[384,384]{1,0:T(8,128)(2,1)}, u32[]{:S(2)}) copy-start(bf16[384,384]{1,0:T(8,128)(2,1)} %value_ref.3) | copy-start | bytes 884740
  73.8 13.9 %collective-permute-start.3 = (bf16[48,2048]{1,0:T(8,128)(2,1)}, bf16[48,2048]{1,0:T(8,128)(2,1)}, u32[]{:S(2)}, u32[]{:S(2)}) collective-permute-start(bf16[48,2048]{1,0:T(8,128)(2,1)} %get-tuple-element.32), channel_id=1, source_target_pairs={{0,6},{2,0},{4,2},{6,4},{1,7},{3,1},{5,3},{7,5},{8,14},{10,8},{12,... | collective-permute-start | bytes 589832 | tf_op jit(solution)/shard_map/ppermute | solution.py:26
  81.0 34.3 %all-to-all-start.3 = ((bf16[8,72,384]{2,1,0:T(8,128)(2,1)}), bf16[8,72,384]{2,1,0:T(8,128)(2,1)S(1)}, u32[]{:S(2)}, u32[]{:S(2)}) async-start(bf16[8,72,384]{2,1,0:T(8,128)(2,1)} %sum_and_repack.1), calls=%async_computation.3 | async-start | bytes 884736 | tf_op jit(solution)/shard_map/all_to_all | solution.py:21
  89.0 12.4 %collective-permute-start.4 = (bf16[48,2048]{1,0:T(8,128)(2,1)S(1)}, bf16[48,2048]{1,0:T(8,128)(2,1)S(1)}, u32[]{:S(2)}, u32[]{:S(2)}) collective-permute-start(bf16[48,2048]{1,0:T(8,128)(2,1)S(1)} %add_convert_fusion), channel_id=1, source_target_pairs={{0,2},{2,4},{4,6},{6,0},{1,3},{3,5},{5,7},{7,1},{8,10},{10,12},{12... | collective-permute-start | bytes 589832 | tf_op jit(solution)/shard_map/ppermute | solution.py:26
  92.1 9.7 %collective-permute-start.5 = (bf16[48,2048]{1,0:T(8,128)(2,1)S(1)}, bf16[48,2048]{1,0:T(8,128)(2,1)S(1)}, u32[]{:S(2)}, u32[]{:S(2)}) collective-permute-start(bf16[48,2048]{1,0:T(8,128)(2,1)S(1)} %add_convert_fusion), channel_id=1, source_target_pairs={{0,4},{2,6},{4,0},{6,2},{1,5},{3,7},{5,1},{7,3},{8,12},{10,14},{12... | collective-permute-start | bytes 589832 | tf_op jit(solution)/shard_map/ppermute | solution.py:26
  94.8 10.6 %collective-permute-start.6 = (bf16[48,2048]{1,0:T(8,128)(2,1)S(1)}, bf16[48,2048]{1,0:T(8,128)(2,1)S(1)}, u32[]{:S(2)}, u32[]{:S(2)}) collective-permute-start(bf16[48,2048]{1,0:T(8,128)(2,1)S(1)} %add_convert_fusion), channel_id=1, source_target_pairs={{0,6},{2,0},{4,2},{6,4},{1,7},{3,1},{5,3},{7,5},{8,14},{10,8},{12,... | collective-permute-start | bytes 589832 | tf_op jit(solution)/shard_map/ppermute | solution.py:26
  98.1 1.4 %copy-start = (bf16[384,2048]{1,0:T(8,128)(2,1)S(1)}, bf16[384,2048]{1,0:T(8,128)(2,1)}, u32[]{:S(2)}) copy-start(bf16[384,2048]{1,0:T(8,128)(2,1)} %x_ref.2) | copy-start | bytes 4718596
  105.5 9.8 %copy-start.2 = (f32[64,384]{1,0:T(8,128)S(1)}, f32[64,384]{1,0:T(8,128)}, u32[]{:S(2)}) copy-start(f32[64,384]{1,0:T(8,128)} %w_ref.1) | copy-start | bytes 294916
  105.5 9.7 %copy-start.4 = (f32[3,384]{1,0:T(4,128)S(1)}, f32[3,384]{1,0:T(4,128)}, u32[]{:S(2)}) copy-start(f32[3,384]{1,0:T(4,128)} %taps_ref.5) | copy-start | bytes 13828
  105.6 9.7 %copy-start.6 = (f32[384]{0:T(512)S(1)}, f32[384]{0:T(512)}, u32[]{:S(2)}) copy-start(f32[384]{0:T(512)} %bias_ref.5) | copy-start | bytes 4612
  105.6 4.3 %collective-permute-start.7 = (bf16[4,48,2048]{2,1,0:T(8,128)(2,1)S(1)}, bf16[4,48,2048]{2,1,0:T(8,128)(2,1)S(1)}, u32[]{:S(2)}, u32[]{:S(2)}) collective-permute-start(bf16[4,48,2048]{2,1,0:T(8,128)(2,1)S(1)} %pad_maximum_fusion.own_ref), channel_id=1, source_target_pairs={{0,1},{1,0},{2,3},{3,2},{4,5},{5,4},{6,7},{7,6},{8,9},{9,8},{10,11... | collective-permute-start | bytes 2359304 | tf_op jit(solution)/shard_map/ppermute | solution.py:26

commit v9 on v8

--- a/solution.py
+++ b/solution.py
@@ -58,26 +58,43 @@
     )(near(own), near(other))
 
 
+EDGE = 8
+
+
 def later(values, offset):
     if offset == 0:
         return values
-    rows = lax.broadcasted_iota(jnp.int32, values.shape, 0) % SEQ_LEN
-    return jnp.where(rows >= offset, pltpu.roll(values, offset, 0), 0.0)
+    moved = pltpu.roll(values, offset, 0)
+    pieces = []
+    for start in range(0, values.shape[0], SEQ_LEN):
+        edge = moved[start : start + EDGE]
+        rows = lax.broadcasted_iota(jnp.int32, edge.shape, 0)
+        pieces.append(jnp.where(rows >= offset, edge, 0.0))
+        pieces.append(moved[start + EDGE : start + SEQ_LEN])
+    return jnp.concatenate(pieces, axis=0)
 
 
 def earlier(values, offset):
     if offset == 0:
         return values
-    count = values.shape[0]
-    rows = lax.broadcasted_iota(jnp.int32, values.shape, 0) % SEQ_LEN
-    return jnp.where(rows < SEQ_LEN - offset, pltpu.roll(values, count - offset, 0), 0.0)
-
-
-def gated(up, taps_ref, bias_ref):
-    tap_count = taps_ref.shape[0]
+    moved = pltpu.roll(values, values.shape[0] - offset, 0)
+    pieces = []
+    for end in range(SEQ_LEN, values.shape[0] + 1, SEQ_LEN):
+        pieces.append(moved[end - SEQ_LEN : end - EDGE])
+        edge = moved[end - EDGE : end]
+        rows = lax.broadcasted_iota(jnp.int32, edge.shape, 0)
+        pieces.append(jnp.where(rows < EDGE - offset, edge, 0.0))
+    return jnp.concatenate(pieces, axis=0)
+
+
+def lags_of(up, tap_count):
+    return [later(up, tap_count - 1 - j) for j in range(tap_count)]
+
+
+def gated(lags, taps_ref, bias_ref):
     total = bias_ref[...][None, :]
-    for j in range(tap_count):
-        total = total + taps_ref[j : j + 1, :] * later(up, tap_count - 1 - j)
+    for j, lag in enumerate(lags):
+        total = total + taps_ref[j : j + 1, :] * lag
     return total
 
 
@@ -87,13 +104,10 @@
     return (high + pltpu.roll(rows - high, half, 0)).astype(jnp.bfloat16)
 
 
-def previous_branch(x_prev, plane, cotangent, value_prev, conv_taps, conv_bias, grad_scale, n_c):
+def previous_branch(x_prev, plane, cotangent, value_prev, conv_taps, conv_bias, grad_scale):
     row_count, width = x_prev.shape
     n_near, n_far, shard_rows, units = plane.shape
     tap_count = conv_taps.shape[0]
-    n_x = lax.axis_size("x")
-    half_rows = row_count // n_c
-    block_rows = half_rows // n_x
     each = n_far * shard_rows
 
     def body(
@@ -105,12 +119,8 @@
         bias_ref,
         gv_ref,
         natural_ref,
-        keep_ref,
-        send_out,
+        gu_ref,
         sent_out,
-        gu_ref,
-        turned_ref,
-        send_ref,
         sent_ref,
         sems,
     ):
@@ -123,7 +133,8 @@
             natural_ref[at : at + shard_rows] = w_ref[near_at, far_at]
         up = jnp.dot(x_ref[...], natural_ref[...], preferred_element_type=jnp.float32)
         up = up.astype(jnp.bfloat16).astype(jnp.float32)
-        gate = gated(up, taps_ref, bias_ref)
+        lags = lags_of(up, tap_count)
+        gate = gated(lags, taps_ref, bias_ref)
         sig = jax.nn.sigmoid(gate)
         cot = cot_ref[...].astype(jnp.float32)
         gv_ref[...] = (cot * gate * sig).astype(jnp.bfloat16)
@@ -133,6 +144,64 @@
             grad_up = grad_up + taps_ref[j : j + 1, :] * earlier(grad_gate, tap_count - 1 - j)
         gu_ref[...] = grad_up.astype(jnp.bfloat16)
 
+        grad_w = lax.dot_general(
+            x_ref[...], gu_ref[...], (((0,), (0,)), ((), ())), preferred_element_type=jnp.float32
+        )
+        grad_w = (grad_w * grad_scale).astype(jnp.bfloat16)
+        sums = [
+            jnp.sum(grad_gate * lag, axis=0, keepdims=True) for lag in lags
+        ] + [jnp.sum(grad_gate, axis=0, keepdims=True)]
+        rest = jnp.zeros((SMALL_ROWS - len(sums), units), jnp.float32)
+        small = high_and_low(jnp.concatenate([*sums, rest], axis=0) * grad_scale)
+        moves = []
+        for block in range(n_near):
+            for near_at, far_at, at in spots:
+                if near_at == block:
+                    to = far_at * shard_rows
+                    sent_ref[block, to : to + shard_rows] = grad_w[at : at + shard_rows]
+            sent_ref[block, each:] = small
+            moves.append(
+                pltpu.make_async_copy(sent_ref.at[block], sent_out.at[block], sems.at[block])
+            )
+            moves[-1].start()
+        for move in moves:
+            move.wait()
+
+    half = jnp.bfloat16
+    return pl.pallas_call(
+        body,
+        in_specs=[VMEM] * 6,
+        out_specs=[pl.BlockSpec(), VMEM, VMEM, HBM],
+        out_shape=[
+            jax.ShapeDtypeStruct((row_count, units), half),
+            pltpu.VMEM((width, units), half),
+            pltpu.VMEM((row_count, units), half),
+            pltpu.HBM((n_near, each + SMALL_ROWS, units), half),
+        ],
+        scratch_shapes=[
+            pltpu.VMEM((n_near, each + SMALL_ROWS, units), half),
+            pltpu.SemaphoreType.DMA((n_near,)),
+        ],
+        cost_estimate=cost(4 * row_count * width * units, 8 * width * units, row_count * units),
+        name="previous_branch",
+        compiler_params=pltpu.CompilerParams(vmem_limit_bytes=24 * 2**20),
+    )(
+        near(x_prev),
+        near(plane),
+        near(cotangent),
+        near(value_prev),
+        near(conv_taps),
+        near(conv_bias),
+    )
+
+
+def core_halves(grad_up, weights, n_c, n_x):
+    row_count, units = grad_up.shape
+    width = weights.shape[0]
+    half_rows = row_count // n_c
+    block_rows = half_rows // n_x
+
+    def body(gu_ref, natural_ref, keep_ref, send_out, turned_ref, send_ref, sem):
         at_x, at_c = lax.axis_index("x"), lax.axis_index("c")
         for i, half_ref in ((1, turned_ref), (0, keep_ref)):
             core = (at_c + i) % n_c
@@ -147,62 +216,25 @@
             (((1,), (1,)), ((), ())),
             preferred_element_type=jnp.float32,
         ).astype(jnp.bfloat16)
-        moves = [pltpu.make_async_copy(send_ref, send_out, sems.at[n_near])]
-        moves[0].start()
-
-        grad_w = lax.dot_general(
-            x_ref[...], gu_ref[...], (((0,), (0,)), ((), ())), preferred_element_type=jnp.float32
-        )
-        grad_w = (grad_w * grad_scale).astype(jnp.bfloat16)
-        sums = [
-            jnp.sum(grad_gate * later(up, tap_count - 1 - j), axis=0, keepdims=True)
-            for j in range(tap_count)
-        ] + [jnp.sum(grad_gate, axis=0, keepdims=True)]
-        rest = jnp.zeros((SMALL_ROWS - len(sums), units), jnp.float32)
-        small = high_and_low(jnp.concatenate([*sums, rest], axis=0) * grad_scale)
-        for block in range(n_near):
-            for near_at, far_at, at in spots:
-                if near_at == block:
-                    to = far_at * shard_rows
-                    sent_ref[block, to : to + shard_rows] = grad_w[at : at + shard_rows]
-            sent_ref[block, each:] = small
-            moves.append(
-                pltpu.make_async_copy(sent_ref.at[block], sent_out.at[block], sems.at[block])
-            )
-            moves[-1].start()
-        for move in moves:
-            move.wait()
+        move = pltpu.make_async_copy(send_ref, send_out, sem)
+        move.start()
+        move.wait()
 
     half = jnp.bfloat16
     return pl.pallas_call(
         body,
-        in_specs=[VMEM] * 6,
-        out_specs=[pl.BlockSpec(), VMEM, VMEM, HBM, HBM],
-        out_shape=[
-            jax.ShapeDtypeStruct((row_count, units), half),
-            pltpu.VMEM((width, units), half),
-            pltpu.VMEM((half_rows, units), half),
-            pltpu.HBM((half_rows, width), half),
-            pltpu.HBM((n_near, each + SMALL_ROWS, units), half),
-        ],
+        in_specs=[VMEM] * 2,
+        out_specs=[VMEM, HBM],
+        out_shape=[pltpu.VMEM((half_rows, units), half), pltpu.HBM((half_rows, width), half)],
         scratch_shapes=[
-            pltpu.VMEM((row_count, units), half),
             pltpu.VMEM((half_rows, units), half),
             pltpu.VMEM((half_rows, width), half),
-            pltpu.VMEM((n_near, each + SMALL_ROWS, units), half),
-            pltpu.SemaphoreType.DMA((n_near + 1,)),
-        ],
-        cost_estimate=cost(5 * row_count * width * units, 8 * width * units, row_count * units),
-        name="previous_branch",
-        compiler_params=pltpu.CompilerParams(vmem_limit_bytes=24 * 2**20),
-    )(
-        near(x_prev),
-        near(plane),
-        near(cotangent),
-        near(value_prev),
-        near(conv_taps),
-        near(conv_bias),
-    )
+            pltpu.SemaphoreType.DMA(()),
+        ],
+        cost_estimate=cost(row_count * width * units, 4 * width * units),
+        name="core_halves",
+        compiler_params=pltpu.CompilerParams(vmem_limit_bytes=16 * 2**20),
+    )(near(grad_up), near(weights))
 
 
 def add_halves(keep, weights, from_core, n_x):
@@ -247,7 +279,8 @@
 
     def body(x_ref, w_ref, value_ref, taps_ref, bias_ref, out_ref):
         up = jnp.dot(x_ref[...], w_ref[...], preferred_element_type=jnp.float32)
-        gate = gated(up.astype(jnp.bfloat16).astype(jnp.float32), taps_ref, bias_ref)
+        up = up.astype(jnp.bfloat16).astype(jnp.float32)
+        gate = gated(lags_of(up, taps_ref.shape[0]), taps_ref, bias_ref)
         hidden = gate * jax.nn.sigmoid(gate) * value_ref[...].astype(jnp.float32)
         out_ref[...] = hidden.astype(jnp.bfloat16)
 
@@ -350,12 +383,14 @@
 
     plane = copies_to(copies_to(w_gate, FAR, n_far), NEAR, n_near)
     grad_scale = float(row_count * n_zh * n_far * n_near) ** (-0.5)
-    grad_value, gathered, keep, to_core, sent = previous_branch(
-        x_prev, plane, cotangent, value_prev, conv_taps, conv_bias, grad_scale, n_c
-    )
+    grad_value, gathered, grad_up, sent = previous_branch(
+        x_prev, plane, cotangent, value_prev, conv_taps, conv_bias, grad_scale
+    )
+    sent, grad_up = lax.optimization_barrier((sent, grad_up))
+    from_near = exchange(sent, NEAR)
+
+    keep, to_core = core_halves(grad_up, gathered, n_c, n_x)
     from_core = send_on(to_core, "c", 1)
-    from_near = exchange(sent, NEAR)
-
     half = add_halves(keep, gathered, from_core, n_x)
     arrived = [half[0]]
     for k in range(1, n_x):

time: 117 us -> 117 us (level)
  the two profiles are of different devices: /device:TPU:44 before, /device:TPU:34 now
where the time goes in v9:
time: 117 us; the launch traced here: 116 us
  blocking collectives  50.1 us (43%)
  starting transfers between devices  36.6 us (31%)
  Pallas kernels  12.9 us (11%)
  waiting for transfers between devices  11.7 us (10%)
  local copies, waits for them, and re-layouts  2.5 us (2%)
  other arithmetic  1.42 us (1%)
    all_to_all x2, blocking collectives, copies_to(): return lax.all_to_all(copies, axis, 0, 0, tiled=True)  50.1 us
    ppermute x8, starting transfers between devices, send_on(): lax.ppermute(block, axis, [(i, (i + shift) % size) for i in range(size)])  24.8 us
    all_to_all x2, starting transfers between devices, exchange(): return lax.all_to_all(blocks, axis, 0, 0, tiled=True)  11.8 us
    ppermute x8, waiting for transfers between devices, send_on(): lax.ppermute(block, axis, [(i, (i + shift) % size) for i in range(size)])  7.81 us
    pallas_call x1, Pallas kernels, previous_branch(): pl.pallas_call(body, in_specs=[VMEM] * 6, out_specs=[pl.BlockSpec(), VMEM...  4.91 us
    all_to_all x2, waiting for transfers between devices, exchange(): return lax.all_to_all(blocks, axis, 0, 0, tiled=True)  3.88 us
  transfers between devices with their start and end apart: 10, of which 6 were waited for; matrix products, arithmetic and copies ran while one was open for 1% of the time, Pallas kernels for 6%

profile of v9, /device:TPU:34, one launch (start us, length us, event | category | flops | bytes accessed | tf_op | source)
XLA Modules:
  0.0 116.1 jit_solution(16352836847099570000)
XLA Ops:
  0.6 0.8 broadcast_in_dim.6
  1.5 24.6 %all_to_all.20 = bf16[4,64,384]{2,1,0:T(8,128)(2,1)S(1)} all-to-all(bf16[4,64,384]{2,1,0:T(8,128)(2,1)S(1)} %broadcast_in_dim.6), channel_id=1, replica_groups=mesh['zh'=2,'zm'=2,'zp'=2,'zl'=2,'y'=4,'x'=4,'c'=2] {'zm','zp'}, dimensions={0} | all-to-all | bytes 393216 | tf_op jit(solution)/shard_map/all_to_all | solution.py:17
  26.1 0.2 broadcast_in_dim.7
  26.3 0.0 copy-start.3
  26.3 0.0 copy-start.5
  26.3 0.0 copy-start.7
  26.3 0.0 copy-start.8
  26.3 0.0 copy-start.9
  26.4 25.5 %all_to_all.21.w_ref = bf16[8,4,64,384]{3,2,1,0:T(8,128)(2,1)S(1)} all-to-all(bf16[8,4,64,384]{3,2,1,0:T(8,128)(2,1)S(1)} %broadcast_in_dim.7), channel_id=1, replica_groups=mesh['zh'=2,'zm'=2,'zp'=2,'zl'=2,'y'=4,'x'=4,'c'=2] {'zl','y'}, dimensions={0} | all-to-all | bytes 3145728 | tf_op jit(solution)/shard_map/all_to_all | solution.py:17
  51.8 0.0 copy-done.3
  51.8 0.0 copy-done.5
  51.8 0.0 copy-done.7
  51.8 0.0 copy-done.8
  51.9 0.0 copy-done.9
  51.9 4.9 %previous_branch.1 = (bf16[384,384]{1,0:T(8,128)(2,1)}, bf16[2048,384]{1,0:T(8,128)(2,1)S(1)}, bf16[384,384]{1,0:T(8,128)(2,1)S(1)}, bf16[8,264,384]{2,1,0:T(8,128)(2,1)}) custom-call(bf16[384,2048]{1,0:T(8,128)(2,1)S(1)} %copy-done.7, bf16[8,4,64,384]{3,2,1,0:T(8,128)(2,1)S(1)} %all_to_all.21.w_ref, bf16[384,384]{1,0:T(8,128)(2,1)S(1)} %copy-done.8, ...), custom_call_target="tpu_custom_call" | custom-call | flops 1207959552 | bytes 6291456 | tf_op jit(solution)/shard_map/previous_branch/pallas_call | solution.py:171
  56.8 4.9 %all-to-all-start.2 = ((bf16[8,264,384]{2,1,0:T(8,128)(2,1)}), bf16[8,264,384]{2,1,0:T(8,128)(2,1)S(1)}, u32[]{:S(2)}, u32[]{:S(2)}) async-start(bf16[8,264,384]{2,1,0:T(8,128)(2,1)} %get-tuple-element.41), calls=%async_computation.2 | async-start | bytes 3244032 | tf_op jit(solution)/shard_map/all_to_all | solution.py:21
  61.7 1.6 %core_halves.1 = (bf16[192,384]{1,0:T(8,128)(2,1)S(1)}, bf16[192,2048]{1,0:T(8,128)(2,1)}) custom-call(bf16[384,384]{1,0:T(8,128)(2,1)S(1)} %get-tuple-element.31.gu_ref, bf16[2048,384]{1,0:T(8,128)(2,1)S(1)} %get-tuple-element.32.natural_ref.w_ref), custom_call_target="tpu_custom_call" | custom-call | flops 301989888 | bytes 3145728 | tf_op jit(solution)/shard_map/core_halves/pallas_call | solution.py:224
  63.3 1.9 %collective-permute-start = (bf16[192,2048]{1,0:T(8,128)(2,1)}, bf16[192,2048]{1,0:T(8,128)(2,1)S(1)}, u32[]{:S(2)}, u32[]{:S(2)}) collective-permute-start(bf16[192,2048]{1,0:T(8,128)(2,1)} %get-tuple-element.34), channel_id=1, source_target_pairs={{0,1},{1,0},{2,3},{3,2},{4,5},{5,4},{6,7},{7,6},{8,9},{9,8},{10,11... | collective-permute-start | bytes 2359304 | tf_op jit(solution)/shard_map/ppermute | solution.py:26
  65.2 2.5 %collective-permute-done.other_ref = bf16[192,2048]{1,0:T(8,128)(2,1)S(1)} collective-permute-done((bf16[192,2048]{1,0:T(8,128)(2,1)}, bf16[192,2048]{1,0:T(8,128)(2,1)S(1)}, u32[]{:S(2)}, u32[]{:S(2)}) %collective-permute-start) | collective-permute-done | bytes 786464 | tf_op jit(solution)/shard_map/ppermute | solution.py:26
  67.7 1.6 %add_halves.1 = (bf16[48,2048]{1,0:T(8,128)(2,1)}, bf16[48,2048]{1,0:T(8,128)(2,1)}, bf16[48,2048]{1,0:T(8,128)(2,1)}, bf16[48,2048]{1,0:T(8,128)(2,1)}) custom-call(bf16[192,384]{1,0:T(8,128)(2,1)S(1)} %get-tuple-element.33.keep_ref, bf16[2048,384]{1,0:T(8,128)(2,1)S(1)} %get-tuple-element.32.natural_ref.w_ref, ...), custom_call_target="tpu_custom_call" | custom-call | flops 301989888 | bytes 6291456 | tf_op jit(solution)/shard_map/add_halves/pallas_call | solution.py:261
  69.2 2.4 %collective-permute-start.3 = (bf16[48,2048]{1,0:T(8,128)(2,1)}, bf16[48,2048]{1,0:T(8,128)(2,1)}, u32[]{:S(2)}, u32[]{:S(2)}) collective-permute-start(bf16[48,2048]{1,0:T(8,128)(2,1)} %get-tuple-element.38), channel_id=1, source_target_pairs={{0,6},{2,0},{4,2},{6,4},{1,7},{3,1},{5,3},{7,5},{8,14},{10,8},{12,... | collective-permute-start | bytes 589832 | tf_op jit(solution)/shard_map/ppermute | solution.py:26
  71.7 4.3 %collective-permute-start.2 = (bf16[48,2048]{1,0:T(8,128)(2,1)}, bf16[48,2048]{1,0:T(8,128)(2,1)}, u32[]{:S(2)}, u32[]{:S(2)}) collective-permute-start(bf16[48,2048]{1,0:T(8,128)(2,1)} %get-tuple-element.37), channel_id=1, source_target_pairs={{0,4},{2,6},{4,0},{6,2},{1,5},{3,7},{5,1},{7,3},{8,12},{10,14},{12... | collective-permute-start | bytes 589832 | tf_op jit(solution)/shard_map/ppermute | solution.py:26
  76.0 0.0 copy-start.1
  76.0 3.9 %collective-permute-start.1 = (bf16[48,2048]{1,0:T(8,128)(2,1)}, bf16[48,2048]{1,0:T(8,128)(2,1)}, u32[]{:S(2)}, u32[]{:S(2)}) collective-permute-start(bf16[48,2048]{1,0:T(8,128)(2,1)} %get-tuple-element.36), channel_id=1, source_target_pairs={{0,2},{2,4},{4,6},{6,0},{1,3},{3,5},{5,7},{7,1},{8,10},{10,12},{12... | collective-permute-start | bytes 589832 | tf_op jit(solution)/shard_map/ppermute | solution.py:26
  79.9 0.5 all-to-all-done.2.in_ref
  80.4 0.9 sum_and_repack.1
  81.3 6.9 %all-to-all-start.3 = ((bf16[8,72,384]{2,1,0:T(8,128)(2,1)}), bf16[8,72,384]{2,1,0:T(8,128)(2,1)S(1)}, u32[]{:S(2)}, u32[]{:S(2)}) async-start(bf16[8,72,384]{2,1,0:T(8,128)(2,1)} %sum_and_repack.1), calls=%async_computation.3 | async-start | bytes 884736 | tf_op jit(solution)/shard_map/all_to_all | solution.py:21
  88.2 0.0 collective-permute-done.3
  88.2 0.0 collective-permute-done.2
  88.2 0.0 collective-permute-done.1
  88.2 1.3 %add_convert_fusion = bf16[48,2048]{1,0:T(8,128)(2,1)S(1)} fusion(bf16[48,2048]{1,0:T(8,128)(2,1)} %collective-permute-done.3, bf16[48,2048]{1,0:T(8,128)(2,1)} %collective-permute-done.2, bf16[48,2048]{1,0:T(8,128)(2,1)} %collective-permute-done.1, bf16[48,2048]{1,0:T(8,128)(2,1)} %get-tuple-element.35), kind=kLoop, calls=%fused_computation.1 | loop fusion | flops 786432 | bytes 983040 | tf_op jit(solution)/shard_map/convert_element_type | solution.py:401
  89.6 3.1 %collective-permute-start.4 = (bf16[48,2048]{1,0:T(8,128)(2,1)S(1)}, bf16[48,2048]{1,0:T(8,128)(2,1)S(1)}, u32[]{:S(2)}, u32[]{:S(2)}) collective-permute-start(bf16[48,2048]{1,0:T(8,128)(2,1)S(1)} %add_convert_fusion), channel_id=1, source_target_pairs={{0,2},{2,4},{4,6},{6,0},{1,3},{3,5},{5,7},{7,1},{8,10},{10,12},{12... | collective-permute-start | bytes 589832 | tf_op jit(solution)/shard_map/ppermute | solution.py:26
  92.7 3.5 %collective-permute-start.5 = (bf16[48,2048]{1,0:T(8,128)(2,1)S(1)}, bf16[48,2048]{1,0:T(8,128)(2,1)S(1)}, u32[]{:S(2)}, u32[]{:S(2)}) collective-permute-start(bf16[48,2048]{1,0:T(8,128)(2,1)S(1)} %add_convert_fusion), channel_id=1, source_target_pairs={{0,4},{2,6},{4,0},{6,2},{1,5},{3,7},{5,1},{7,3},{8,12},{10,14},{12... | collective-permute-start | bytes 589832 | tf_op jit(solution)/shard_map/ppermute | solution.py:26
  96.3 3.5 %collective-permute-start.6 = (bf16[48,2048]{1,0:T(8,128)(2,1)S(1)}, bf16[48,2048]{1,0:T(8,128)(2,1)S(1)}, u32[]{:S(2)}, u32[]{:S(2)}) collective-permute-start(bf16[48,2048]{1,0:T(8,128)(2,1)S(1)} %add_convert_fusion), channel_id=1, source_target_pairs={{0,6},{2,0},{4,2},{6,4},{1,7},{3,1},{5,3},{7,5},{8,14},{10,8},{12,... | collective-permute-start | bytes 589832 | tf_op jit(solution)/shard_map/ppermute | solution.py:26
  99.8 0.0 copy-done.1
  99.8 0.0 copy-start
  99.8 1.4 %copy-done = bf16[384,2048]{1,0:T(8,128)(2,1)S(1)} copy-done((bf16[384,2048]{1,0:T(8,128)(2,1)S(1)}, bf16[384,2048]{1,0:T(8,128)(2,1)}, u32[]{:S(2)}) %copy-start) | copy-done | bytes 1572888
  101.2 2.0 %next_branch.1 = bf16[384,384]{1,0:T(8,128)(2,1)} custom-call(bf16[384,2048]{1,0:T(8,128)(2,1)S(1)} %copy-done, bf16[2048,384]{1,0:T(8,128)(2,1)S(1)} %get-tuple-element.32.natural_ref.w_ref, bf16[384,384]{1,0:T(8,128)(2,1)S(1)} %copy-done.1, f32[3,384]{1,0:T(4,128)S(1)} %copy-done.3, f32[384]{0:T(512)S(1)} %copy-done.5), custom_call_target="tpu_custom_call" | custom-call | flops 603979776 | bytes 3145728 | tf_op jit(solution)/shard_map/next_branch/pallas_call | solution.py:287
  103.2 0.0 collective-permute-done.4
  103.2 0.7 collective-permute-done.5
  103.9 2.4 %collective-permute-done.6 = bf16[48,2048]{1,0:T(8,128)(2,1)S(1)} collective-permute-done((bf16[48,2048]{1,0:T(8,128)(2,1)S(1)}, bf16[48,2048]{1,0:T(8,128)(2,1)S(1)}, u32[]{:S(2)}, u32[]{:S(2)}) %collective-permute-start.6) | collective-permute-done | bytes 196640 | tf_op jit(solution)/shard_map/ppermute | solution.py:26
  106.3 0.1 pad_maximum_fusion.own_ref
  106.4 0.0 copy-start.2
  106.4 0.0 copy-start.4
  106.4 0.0 copy-start.6
  106.4 2.1 %collective-permute-start.7 = (bf16[4,48,2048]{2,1,0:T(8,128)(2,1)S(1)}, bf16[4,48,2048]{2,1,0:T(8,128)(2,1)S(1)}, u32[]{:S(2)}, u32[]{:S(2)}) collective-permute-start(bf16[4,48,2048]{2,1,0:T(8,128)(2,1)S(1)} %pad_maximum_fusion.own_ref), channel_id=1, source_target_pairs={{0,1},{1,0},{2,3},{3,2},{4,5},{5,4},{6,7},{7,6},{8,9},{9,8},{10,11... | collective-permute-start | bytes 2359304 | tf_op jit(solution)/shard_map/ppermute | solution.py:26
  108.5 2.3 %collective-permute-done.7.other_ref = bf16[4,48,2048]{2,1,0:T(8,128)(2,1)S(1)} collective-permute-done((bf16[4,48,2048]{2,1,0:T(8,128)(2,1)S(1)}, bf16[4,48,2048]{2,1,0:T(8,128)(2,1)S(1)}, u32[]{:S(2)}, u32[]{:S(2)}) %collective-permute-start.7) | collective-permute-done | bytes 786464 | tf_op jit(solution)/shard_map/ppermute | solution.py:26
  110.7 1.3 %put_in_order.1 = bf16[8,48,2048]{2,1,0:T(8,128)(2,1)} custom-call(bf16[4,48,2048]{2,1,0:T(8,128)(2,1)S(1)} %pad_maximum_fusion.own_ref, bf16[4,48,2048]{2,1,0:T(8,128)(2,1)S(1)} %collective-permute-done.7.other_ref), custom_call_target="tpu_custom_call" | custom-call | bytes 3145728 | tf_op jit(solution)/shard_map/put_in_order/pallas_call | solution.py:51
  112.0 3.4 %all-to-all-done.3.in_ref = bf16[8,72,384]{2,1,0:T(8,128)(2,1)S(1)} async-done(((bf16[8,72,384]{2,1,0:T(8,128)(2,1)}), bf16[8,72,384]{2,1,0:T(8,128)(2,1)S(1)}, u32[]{:S(2)}, u32[]{:S(2)}) %all-to-all-start.3) | async-done | bytes 442400 | tf_op jit(solution)/shard_map/all_to_all | solution.py:21
  115.4 0.0 copy-done.2
  115.4 0.0 copy-done.4
  115.4 0.0 copy-done.6
  115.4 0.7 last_sum.1
Async XLA Ops:
  26.3 25.5 %copy-start.3 = (f32[3,384]{1,0:T(4,128)S(1)}, f32[3,384]{1,0:T(4,128)}, u32[]{:S(2)}) copy-start(f32[3,384]{1,0:T(4,128)} %taps_ref.4) | copy-start | bytes 13828
  26.3 25.5 %copy-start.5 = (f32[384]{0:T(512)S(1)}, f32[384]{0:T(512)}, u32[]{:S(2)}) copy-start(f32[384]{0:T(512)} %bias_ref.4) | copy-start | bytes 4612
  26.3 25.5 %copy-start.7 = (bf16[384,2048]{1,0:T(8,128)(2,1)S(1)}, bf16[384,2048]{1,0:T(8,128)(2,1)}, u32[]{:S(2)}) copy-start(bf16[384,2048]{1,0:T(8,128)(2,1)} %x_ref.1) | copy-start | bytes 4718596
  26.3 25.5 %copy-start.8 = (bf16[384,384]{1,0:T(8,128)(2,1)S(1)}, bf16[384,384]{1,0:T(8,128)(2,1)}, u32[]{:S(2)}) copy-start(bf16[384,384]{1,0:T(8,128)(2,1)} %cot_ref.1) | copy-start | bytes 884740
  26.3 25.5 %copy-start.9 = (bf16[384,384]{1,0:T(8,128)(2,1)S(1)}, bf16[384,384]{1,0:T(8,128)(2,1)}, u32[]{:S(2)}) copy-start(bf16[384,384]{1,0:T(8,128)(2,1)} %value_ref.2) | copy-start | bytes 884740
  56.8 23.6 %all-to-all-start.2 = ((bf16[8,264,384]{2,1,0:T(8,128)(2,1)}), bf16[8,264,384]{2,1,0:T(8,128)(2,1)S(1)}, u32[]{:S(2)}, u32[]{:S(2)}) async-start(bf16[8,264,384]{2,1,0:T(8,128)(2,1)} %get-tuple-element.41), calls=%async_computation.2 | async-start | bytes 3244032 | tf_op jit(solution)/shard_map/all_to_all | solution.py:21
  63.3 4.4 %collective-permute-start = (bf16[192,2048]{1,0:T(8,128)(2,1)}, bf16[192,2048]{1,0:T(8,128)(2,1)S(1)}, u32[]{:S(2)}, u32[]{:S(2)}) collective-permute-start(bf16[192,2048]{1,0:T(8,128)(2,1)} %get-tuple-element.34), channel_id=1, source_target_pairs={{0,1},{1,0},{2,3},{3,2},{4,5},{5,4},{6,7},{7,6},{8,9},{9,8},{10,11... | collective-permute-start | bytes 2359304 | tf_op jit(solution)/shard_map/ppermute | solution.py:26
  69.2 19.0 %collective-permute-start.3 = (bf16[48,2048]{1,0:T(8,128)(2,1)}, bf16[48,2048]{1,0:T(8,128)(2,1)}, u32[]{:S(2)}, u32[]{:S(2)}) collective-permute-start(bf16[48,2048]{1,0:T(8,128)(2,1)} %get-tuple-element.38), channel_id=1, source_target_pairs={{0,6},{2,0},{4,2},{6,4},{1,7},{3,1},{5,3},{7,5},{8,14},{10,8},{12,... | collective-permute-start | bytes 589832 | tf_op jit(solution)/shard_map/ppermute | solution.py:26
  71.7 16.5 %collective-permute-start.2 = (bf16[48,2048]{1,0:T(8,128)(2,1)}, bf16[48,2048]{1,0:T(8,128)(2,1)}, u32[]{:S(2)}, u32[]{:S(2)}) collective-permute-start(bf16[48,2048]{1,0:T(8,128)(2,1)} %get-tuple-element.37), channel_id=1, source_target_pairs={{0,4},{2,6},{4,0},{6,2},{1,5},{3,7},{5,1},{7,3},{8,12},{10,14},{12... | collective-permute-start | bytes 589832 | tf_op jit(solution)/shard_map/ppermute | solution.py:26
  76.0 23.8 %copy-start.1 = (bf16[384,384]{1,0:T(8,128)(2,1)S(1)}, bf16[384,384]{1,0:T(8,128)(2,1)}, u32[]{:S(2)}) copy-start(bf16[384,384]{1,0:T(8,128)(2,1)} %value_ref.3) | copy-start | bytes 884740
  76.0 12.2 %collective-permute-start.1 = (bf16[48,2048]{1,0:T(8,128)(2,1)}, bf16[48,2048]{1,0:T(8,128)(2,1)}, u32[]{:S(2)}, u32[]{:S(2)}) collective-permute-start(bf16[48,2048]{1,0:T(8,128)(2,1)} %get-tuple-element.36), channel_id=1, source_target_pairs={{0,2},{2,4},{4,6},{6,0},{1,3},{3,5},{5,7},{7,1},{8,10},{10,12},{12... | collective-permute-start | bytes 589832 | tf_op jit(solution)/shard_map/ppermute | solution.py:26
  81.3 34.1 %all-to-all-start.3 = ((bf16[8,72,384]{2,1,0:T(8,128)(2,1)}), bf16[8,72,384]{2,1,0:T(8,128)(2,1)S(1)}, u32[]{:S(2)}, u32[]{:S(2)}) async-start(bf16[8,72,384]{2,1,0:T(8,128)(2,1)} %sum_and_repack.1), calls=%async_computation.3 | async-start | bytes 884736 | tf_op jit(solution)/shard_map/all_to_all | solution.py:21
  89.6 13.6 %collective-permute-start.4 = (bf16[48,2048]{1,0:T(8,128)(2,1)S(1)}, bf16[48,2048]{1,0:T(8,128)(2,1)S(1)}, u32[]{:S(2)}, u32[]{:S(2)}) collective-permute-start(bf16[48,2048]{1,0:T(8,128)(2,1)S(1)} %add_convert_fusion), channel_id=1, source_target_pairs={{0,2},{2,4},{4,6},{6,0},{1,3},{3,5},{5,7},{7,1},{8,10},{10,12},{12... | collective-permute-start | bytes 589832 | tf_op jit(solution)/shard_map/ppermute | solution.py:26
  92.7 11.2 %collective-permute-start.5 = (bf16[48,2048]{1,0:T(8,128)(2,1)S(1)}, bf16[48,2048]{1,0:T(8,128)(2,1)S(1)}, u32[]{:S(2)}, u32[]{:S(2)}) collective-permute-start(bf16[48,2048]{1,0:T(8,128)(2,1)S(1)} %add_convert_fusion), channel_id=1, source_target_pairs={{0,4},{2,6},{4,0},{6,2},{1,5},{3,7},{5,1},{7,3},{8,12},{10,14},{12... | collective-permute-start | bytes 589832 | tf_op jit(solution)/shard_map/ppermute | solution.py:26
  96.3 10.0 %collective-permute-start.6 = (bf16[48,2048]{1,0:T(8,128)(2,1)S(1)}, bf16[48,2048]{1,0:T(8,128)(2,1)S(1)}, u32[]{:S(2)}, u32[]{:S(2)}) collective-permute-start(bf16[48,2048]{1,0:T(8,128)(2,1)S(1)} %add_convert_fusion), channel_id=1, source_target_pairs={{0,6},{2,0},{4,2},{6,4},{1,7},{3,1},{5,3},{7,5},{8,14},{10,8},{12,... | collective-permute-start | bytes 589832 | tf_op jit(solution)/shard_map/ppermute | solution.py:26
  99.8 1.4 %copy-start = (bf16[384,2048]{1,0:T(8,128)(2,1)S(1)}, bf16[384,2048]{1,0:T(8,128)(2,1)}, u32[]{:S(2)}) copy-start(bf16[384,2048]{1,0:T(8,128)(2,1)} %x_ref.2) | copy-start | bytes 4718596
  106.4 9.0 %copy-start.2 = (f32[64,384]{1,0:T(8,128)S(1)}, f32[64,384]{1,0:T(8,128)}, u32[]{:S(2)}) copy-start(f32[64,384]{1,0:T(8,128)} %w_ref.1) | copy-start | bytes 294916
  106.4 9.0 %copy-start.4 = (f32[3,384]{1,0:T(4,128)S(1)}, f32[3,384]{1,0:T(4,128)}, u32[]{:S(2)}) copy-start(f32[3,384]{1,0:T(4,128)} %taps_ref.5) | copy-start | bytes 13828
  106.4 9.0 %copy-start.6 = (f32[384]{0:T(512)S(1)}, f32[384]{0:T(512)}, u32[]{:S(2)}) copy-start(f32[384]{0:T(512)} %bias_ref.5) | copy-start | bytes 4612
  106.4 4.3 %collective-permute-start.7 = (bf16[4,48,2048]{2,1,0:T(8,128)(2,1)S(1)}, bf16[4,48,2048]{2,1,0:T(8,128)(2,1)S(1)}, u32[]{:S(2)}, u32[]{:S(2)}) collective-permute-start(bf16[4,48,2048]{2,1,0:T(8,128)(2,1)S(1)} %pad_maximum_fusion.own_ref), channel_id=1, source_target_pairs={{0,1},{1,0},{2,3},{3,2},{4,5},{5,4},{6,7},{7,6},{8,9},{9,8},{10,11... | collective-permute-start | bytes 2359304 | tf_op jit(solution)/shard_map/ppermute | solution.py:26

commit v10 on v9

--- a/solution.py
+++ b/solution.py
@@ -10,6 +10,7 @@
 SEQ_LEN = 128
 SMALL_ROWS = 8
 FAR, NEAR = ("zm", "zp"), ("zl", "y")
+FAR_SHIFTS = (0, 1, -1, 2)
 
 
 def copies_to(block, axis, size):
@@ -23,7 +24,7 @@
 
 def send_on(block, axis, shift):
     size = lax.axis_size(axis)
-    return lax.ppermute(block, axis, [(i, (i + shift) % size) for i in range(size)])
+    return lax.ppermute(block, axis, [(i, (i + shift + size) % size) for i in range(size)])
 
 
 def near(array):
@@ -104,15 +105,19 @@
     return (high + pltpu.roll(rows - high, half, 0)).astype(jnp.bfloat16)
 
 
-def previous_branch(x_prev, plane, cotangent, value_prev, conv_taps, conv_bias, grad_scale):
+def previous_branch(
+    x_prev, plane, rest, cotangent, value_prev, conv_taps, conv_bias, grad_scale
+):
     row_count, width = x_prev.shape
-    n_near, n_far, shard_rows, units = plane.shape
+    n_near, shard_rows, units = plane.shape
+    n_far = rest.shape[1] + 1
     tap_count = conv_taps.shape[0]
     each = n_far * shard_rows
 
     def body(
         x_ref,
         w_ref,
+        rest_ref,
         cot_ref,
         value_ref,
         taps_ref,
@@ -129,8 +134,13 @@
             for near_at in range(n_near)
             for far_at in range(n_far)
         ]
-        for near_at, far_at, at in spots:
-            natural_ref[at : at + shard_rows] = w_ref[near_at, far_at]
+        own_far = lax.axis_index("zm") * lax.axis_size("zp") + lax.axis_index("zp")
+        for near_at in range(n_near):
+            for k in range(n_far):
+                far_at = (own_far + n_far - FAR_SHIFTS[k]) % n_far
+                at = (far_at * n_near + near_at) * shard_rows
+                block = w_ref[near_at] if k == 0 else rest_ref[near_at, k - 1]
+                natural_ref[pl.ds(pl.multiple_of(at, shard_rows), shard_rows)] = block
         up = jnp.dot(x_ref[...], natural_ref[...], preferred_element_type=jnp.float32)
         up = up.astype(jnp.bfloat16).astype(jnp.float32)
         lags = lags_of(up, tap_count)
@@ -170,7 +180,7 @@
     half = jnp.bfloat16
     return pl.pallas_call(
         body,
-        in_specs=[VMEM] * 6,
+        in_specs=[VMEM] * 7,
         out_specs=[pl.BlockSpec(), VMEM, VMEM, HBM],
         out_shape=[
             jax.ShapeDtypeStruct((row_count, units), half),
@@ -188,6 +198,7 @@
     )(
         near(x_prev),
         near(plane),
+        near(rest),
         near(cotangent),
         near(value_prev),
         near(conv_taps),
@@ -381,10 +392,12 @@
     n_zh, n_x, n_c = (lax.axis_size(a) for a in ("zh", "x", "c"))
     n_far, n_near = lax.axis_size(FAR), lax.axis_size(NEAR)
 
-    plane = copies_to(copies_to(w_gate, FAR, n_far), NEAR, n_near)
+    plane = copies_to(w_gate, NEAR, n_near)
+    far_shards = [send_on(w_gate, ("zh", *FAR), shift) for shift in FAR_SHIFTS[1:]]
+    rest = copies_to(jnp.stack(far_shards), NEAR, n_near)
     grad_scale = float(row_count * n_zh * n_far * n_near) ** (-0.5)
     grad_value, gathered, grad_up, sent = previous_branch(
-        x_prev, plane, cotangent, value_prev, conv_taps, conv_bias, grad_scale
+        x_prev, plane, rest, cotangent, value_prev, conv_taps, conv_bias, grad_scale
     )
     sent, grad_up = lax.optimization_barrier((sent, grad_up))
     from_near = exchange(sent, NEAR)

time: 117 us -> 117 us (level)
  blocking collectives: 50.1 us -> 19.8 us
  starting transfers between devices: 36.6 us -> 61.2 us
  waiting for transfers between devices: 11.7 us -> 16.5 us
    all_to_all x2 -> x1, blocking collectives: 50.1 us -> 19.8 us  [copies_to(): return lax.all_to_all(copies, axis, 0, 0, tiled=True)]
    ppermute x8 -> x11, starting transfers between devices: 24.8 us -> 40.5 us  [send_on(): lax.ppermute(block, axis, [(i, (i + shift + size) % size) for i in range(...]
    all_to_all x0 -> x1, starting transfers between devices: none -> 5.93 us  [copies_to(): return lax.all_to_all(copies, axis, 0, 0, tiled=True)]
    ppermute x8 -> x11, waiting for transfers between devices: 7.81 us -> 12.5 us  [send_on(): lax.ppermute(block, axis, [(i, (i + shift + size) % size) for i in range(...]
    all_to_all x2, starting transfers between devices: 11.8 us -> 14.8 us  [exchange(): return lax.all_to_all(blocks, axis, 0, 0, tiled=True)]
  transfers between devices with their start and end apart: 10 -> 14, of which waited for: 6 -> 7; matrix products, arithmetic and copies ran while one was open for 1% -> 1% of each run, Pallas kernels for 6% -> 6%
where the time goes in v10:
time: 117 us; the launch traced here: 116 us
  starting transfers between devices  61.2 us (52%)
  blocking collectives  19.8 us (17%)
  waiting for transfers between devices  16.5 us (14%)
  Pallas kernels  13 us (11%)
  local copies, waits for them, and re-layouts  3.2 us (3%)
  other arithmetic  1.45 us (1%)
    ppermute x11, starting transfers between devices, send_on(): lax.ppermute(block, axis, [(i, (i + shift + size) % size) for i in range(...  40.5 us
    all_to_all x1, blocking collectives, copies_to(): return lax.all_to_all(copies, axis, 0, 0, tiled=True)  19.8 us
    all_to_all x2, starting transfers between devices, exchange(): return lax.all_to_all(blocks, axis, 0, 0, tiled=True)  14.8 us
    ppermute x11, waiting for transfers between devices, send_on(): lax.ppermute(block, axis, [(i, (i + shift + size) % size) for i in range(...  12.5 us
    all_to_all x1, starting transfers between devices, copies_to(): return lax.all_to_all(copies, axis, 0, 0, tiled=True)  5.93 us
    pallas_call x1, Pallas kernels, previous_branch(): pl.pallas_call(body, in_specs=[VMEM] * 7, out_specs=[pl.BlockSpec(), VMEM...  5.01 us
    all_to_all x2, waiting for transfers between devices, exchange(): return lax.all_to_all(blocks, axis, 0, 0, tiled=True)  4.03 us
  transfers between devices with their start and end apart: 14, of which 7 were waited for; matrix products, arithmetic and copies ran while one was open for 1% of the time, Pallas kernels for 6%

profile of v10, /device:TPU:34, one launch (start us, length us, event | category | flops | bytes accessed | tf_op | source)
XLA Modules:
  0.0 116.1 jit_solution(5502574900031139817)
XLA Ops:
  0.6 1.6 %broadcast_in_dim.6 = bf16[8,64,384]{2,1,0:T(8,128)(2,1)} broadcast(bf16[64,384]{1,0:T(8,128)(2,1)} %param.16), dimensions={1,2} | broadcast | bytes 442368 | tf_op jit(solution)/shard_map/broadcast_in_dim | solution.py:17
  2.2 5.9 %all-to-all-start = ((bf16[8,64,384]{2,1,0:T(8,128)(2,1)}), bf16[8,64,384]{2,1,0:T(8,128)(2,1)S(1)}, u32[]{:S(2)}, u32[]{:S(2)}) async-start(bf16[8,64,384]{2,1,0:T(8,128)(2,1)} %broadcast_in_dim.6), calls=%async_computation | async-start | bytes 786432 | tf_op jit(solution)/shard_map/all_to_all | solution.py:18
  8.1 9.1 %collective-permute-start.2 = (bf16[64,384]{1,0:T(8,128)(2,1)}, bf16[64,384]{1,0:T(8,128)(2,1)S(1)}, u32[]{:S(2)}, u32[]{:S(2)}) collective-permute-start(bf16[64,384]{1,0:T(8,128)(2,1)} %param.16), channel_id=1, source_target_pairs={{0,128},{64,192},{128,256},{192,320},{256,384},{320,448},{384,0},{... | collective-permute-start | bytes 147464 | tf_op jit(solution)/shard_map/ppermute | solution.py:27
  17.2 3.8 %collective-permute-start.1 = (bf16[64,384]{1,0:T(8,128)(2,1)}, bf16[64,384]{1,0:T(8,128)(2,1)S(1)}, u32[]{:S(2)}, u32[]{:S(2)}) collective-permute-start(bf16[64,384]{1,0:T(8,128)(2,1)} %param.16), channel_id=1, source_target_pairs={{0,448},{64,0},{128,64},{192,128},{256,192},{320,256},{384,320},{4... | collective-permute-start | bytes 147464 | tf_op jit(solution)/shard_map/ppermute | solution.py:27
  21.0 3.3 %collective-permute-start = (bf16[64,384]{1,0:T(8,128)(2,1)}, bf16[64,384]{1,0:T(8,128)(2,1)S(1)}, u32[]{:S(2)}, u32[]{:S(2)}) collective-permute-start(bf16[64,384]{1,0:T(8,128)(2,1)} %param.16), channel_id=1, source_target_pairs={{0,64},{64,128},{128,192},{192,256},{256,320},{320,384},{384,448},... | collective-permute-start | bytes 147464 | tf_op jit(solution)/shard_map/ppermute | solution.py:27
  24.4 0.0 collective-permute-done.2
  24.4 0.8 collective-permute-done.1
  25.2 4.3 %collective-permute-done = bf16[64,384]{1,0:T(8,128)(2,1)S(1)} collective-permute-done((bf16[64,384]{1,0:T(8,128)(2,1)}, bf16[64,384]{1,0:T(8,128)(2,1)S(1)}, u32[]{:S(2)}, u32[]{:S(2)}) %collective-permute-start) | collective-permute-done | bytes 49184 | tf_op jit(solution)/shard_map/ppermute | solution.py:27
  29.5 0.0 copy-start.3
  29.5 0.0 copy-start.5
  29.5 0.0 copy-start.8
  29.5 0.0 copy-start.9
  29.6 0.0 all-to-all-done.w_ref
  29.6 0.0 copy-start.7
  29.6 0.2 broadcast_in_dim.7
  29.7 19.8 %all_to_all.20.rest_ref = bf16[8,3,64,384]{3,2,1,0:T(8,128)(2,1)S(1)} all-to-all(bf16[8,3,64,384]{3,2,1,0:T(8,128)(2,1)S(1)} %broadcast_in_dim.7), channel_id=1, replica_groups=mesh['zh'=2,'zm'=2,'zp'=2,'zl'=2,'y'=4,'x'=4,'c'=2] {'zl','y'}, dimensions={0} | all-to-all | bytes 2359296 | tf_op jit(solution)/shard_map/all_to_all | solution.py:18
  49.5 0.0 copy-done.3
  49.5 0.0 copy-done.5
  49.5 0.0 copy-done.8
  49.5 0.0 copy-done.9
  49.5 0.0 copy-done.7
  49.6 5.0 %previous_branch.1 = (bf16[384,384]{1,0:T(8,128)(2,1)}, bf16[2048,384]{1,0:T(8,128)(2,1)S(1)}, bf16[384,384]{1,0:T(8,128)(2,1)S(1)}, bf16[8,264,384]{2,1,0:T(8,128)(2,1)}) custom-call(bf16[384,2048]{1,0:T(8,128)(2,1)S(1)} %copy-done.7, bf16[8,64,384]{2,1,0:T(8,128)(2,1)S(1)} %all-to-all-done.w_ref, bf16[8,3,64,384]{3,2,1,0:T(8,128)(2,1)S(1)} %all_to_all.20.rest_ref, ...), custom_call_target="tpu_custom_call" | custom-call | flops 1207959552 | bytes 6291456 | tf_op jit(solution)/shard_map/previous_branch/pallas_call | solution.py:181
  54.6 4.9 %all-to-all-start.2 = ((bf16[8,264,384]{2,1,0:T(8,128)(2,1)}), bf16[8,264,384]{2,1,0:T(8,128)(2,1)S(1)}, u32[]{:S(2)}, u32[]{:S(2)}) async-start(bf16[8,264,384]{2,1,0:T(8,128)(2,1)} %get-tuple-element.41), calls=%async_computation.2 | async-start | bytes 3244032 | tf_op jit(solution)/shard_map/all_to_all | solution.py:22
  59.4 1.6 %core_halves.1 = (bf16[192,384]{1,0:T(8,128)(2,1)S(1)}, bf16[192,2048]{1,0:T(8,128)(2,1)}) custom-call(bf16[384,384]{1,0:T(8,128)(2,1)S(1)} %get-tuple-element.31.gu_ref, bf16[2048,384]{1,0:T(8,128)(2,1)S(1)} %get-tuple-element.32.natural_ref.w_ref), custom_call_target="tpu_custom_call" | custom-call | flops 301989888 | bytes 3145728 | tf_op jit(solution)/shard_map/core_halves/pallas_call | solution.py:235
  61.0 1.9 %collective-permute-start.3 = (bf16[192,2048]{1,0:T(8,128)(2,1)}, bf16[192,2048]{1,0:T(8,128)(2,1)S(1)}, u32[]{:S(2)}, u32[]{:S(2)}) collective-permute-start(bf16[192,2048]{1,0:T(8,128)(2,1)} %get-tuple-element.34), channel_id=1, source_target_pairs={{0,1},{1,0},{2,3},{3,2},{4,5},{5,4},{6,7},{7,6},{8,9},{9,8},{10,11... | collective-permute-start | bytes 2359304 | tf_op jit(solution)/shard_map/ppermute | solution.py:27
  63.0 2.5 %collective-permute-done.3.other_ref = bf16[192,2048]{1,0:T(8,128)(2,1)S(1)} collective-permute-done((bf16[192,2048]{1,0:T(8,128)(2,1)}, bf16[192,2048]{1,0:T(8,128)(2,1)S(1)}, u32[]{:S(2)}, u32[]{:S(2)}) %collective-permute-start.3) | collective-permute-done | bytes 786464 | tf_op jit(solution)/shard_map/ppermute | solution.py:27
  65.4 1.6 %add_halves.1 = (bf16[48,2048]{1,0:T(8,128)(2,1)}, bf16[48,2048]{1,0:T(8,128)(2,1)}, bf16[48,2048]{1,0:T(8,128)(2,1)}, bf16[48,2048]{1,0:T(8,128)(2,1)}) custom-call(bf16[192,384]{1,0:T(8,128)(2,1)S(1)} %get-tuple-element.33.keep_ref, bf16[2048,384]{1,0:T(8,128)(2,1)S(1)} %get-tuple-element.32.natural_ref.w_ref, ...), custom_call_target="tpu_custom_call" | custom-call | flops 301989888 | bytes 6291456 | tf_op jit(solution)/shard_map/add_halves/pallas_call | solution.py:272
  67.0 2.4 %collective-permute-start.6 = (bf16[48,2048]{1,0:T(8,128)(2,1)}, bf16[48,2048]{1,0:T(8,128)(2,1)}, u32[]{:S(2)}, u32[]{:S(2)}) collective-permute-start(bf16[48,2048]{1,0:T(8,128)(2,1)} %get-tuple-element.38), channel_id=1, source_target_pairs={{0,6},{2,0},{4,2},{6,4},{1,7},{3,1},{5,3},{7,5},{8,14},{10,8},{12,... | collective-permute-start | bytes 589832 | tf_op jit(solution)/shard_map/ppermute | solution.py:27
  69.4 4.3 %collective-permute-start.5 = (bf16[48,2048]{1,0:T(8,128)(2,1)}, bf16[48,2048]{1,0:T(8,128)(2,1)}, u32[]{:S(2)}, u32[]{:S(2)}) collective-permute-start(bf16[48,2048]{1,0:T(8,128)(2,1)} %get-tuple-element.37), channel_id=1, source_target_pairs={{0,4},{2,6},{4,0},{6,2},{1,5},{3,7},{5,1},{7,3},{8,12},{10,14},{12... | collective-permute-start | bytes 589832 | tf_op jit(solution)/shard_map/ppermute | solution.py:27
  73.8 0.0 copy-start.1
  73.8 3.9 %collective-permute-start.4 = (bf16[48,2048]{1,0:T(8,128)(2,1)}, bf16[48,2048]{1,0:T(8,128)(2,1)}, u32[]{:S(2)}, u32[]{:S(2)}) collective-permute-start(bf16[48,2048]{1,0:T(8,128)(2,1)} %get-tuple-element.36), channel_id=1, source_target_pairs={{0,2},{2,4},{4,6},{6,0},{1,3},{3,5},{5,7},{7,1},{8,10},{10,12},{12... | collective-permute-start | bytes 589832 | tf_op jit(solution)/shard_map/ppermute | solution.py:27
  77.6 0.0 all-to-all-done.2.in_ref
  77.7 0.9 sum_and_repack.1
  78.6 9.9 %all-to-all-start.3 = ((bf16[8,72,384]{2,1,0:T(8,128)(2,1)}), bf16[8,72,384]{2,1,0:T(8,128)(2,1)S(1)}, u32[]{:S(2)}, u32[]{:S(2)}) async-start(bf16[8,72,384]{2,1,0:T(8,128)(2,1)} %sum_and_repack.1), calls=%async_computation.3 | async-start | bytes 884736 | tf_op jit(solution)/shard_map/all_to_all | solution.py:22
  88.5 0.0 collective-permute-done.6
  88.5 0.0 collective-permute-done.5
  88.5 0.0 collective-permute-done.4
  88.5 1.3 %add_convert_fusion = bf16[48,2048]{1,0:T(8,128)(2,1)S(1)} fusion(bf16[48,2048]{1,0:T(8,128)(2,1)} %collective-permute-done.6, bf16[48,2048]{1,0:T(8,128)(2,1)} %collective-permute-done.5, bf16[48,2048]{1,0:T(8,128)(2,1)} %collective-permute-done.4, bf16[48,2048]{1,0:T(8,128)(2,1)} %get-tuple-element.35), kind=kLoop, calls=%fused_computation.1 | loop fusion | flops 786432 | bytes 983040 | tf_op jit(solution)/shard_map/convert_element_type | solution.py:414
  89.9 2.3 %collective-permute-start.7 = (bf16[48,2048]{1,0:T(8,128)(2,1)S(1)}, bf16[48,2048]{1,0:T(8,128)(2,1)S(1)}, u32[]{:S(2)}, u32[]{:S(2)}) collective-permute-start(bf16[48,2048]{1,0:T(8,128)(2,1)S(1)} %add_convert_fusion), channel_id=1, source_target_pairs={{0,2},{2,4},{4,6},{6,0},{1,3},{3,5},{5,7},{7,1},{8,10},{10,12},{12... | collective-permute-start | bytes 589832 | tf_op jit(solution)/shard_map/ppermute | solution.py:27
  92.1 3.8 %collective-permute-start.8 = (bf16[48,2048]{1,0:T(8,128)(2,1)S(1)}, bf16[48,2048]{1,0:T(8,128)(2,1)S(1)}, u32[]{:S(2)}, u32[]{:S(2)}) collective-permute-start(bf16[48,2048]{1,0:T(8,128)(2,1)S(1)} %add_convert_fusion), channel_id=1, source_target_pairs={{0,4},{2,6},{4,0},{6,2},{1,5},{3,7},{5,1},{7,3},{8,12},{10,14},{12... | collective-permute-start | bytes 589832 | tf_op jit(solution)/shard_map/ppermute | solution.py:27
  96.0 3.7 %collective-permute-start.9 = (bf16[48,2048]{1,0:T(8,128)(2,1)S(1)}, bf16[48,2048]{1,0:T(8,128)(2,1)S(1)}, u32[]{:S(2)}, u32[]{:S(2)}) collective-permute-start(bf16[48,2048]{1,0:T(8,128)(2,1)S(1)} %add_convert_fusion), channel_id=1, source_target_pairs={{0,6},{2,0},{4,2},{6,4},{1,7},{3,1},{5,3},{7,5},{8,14},{10,8},{12,... | collective-permute-start | bytes 589832 | tf_op jit(solution)/shard_map/ppermute | solution.py:27
  99.6 0.0 copy-done.1
  99.7 0.0 copy-start
  99.7 1.4 %copy-done = bf16[384,2048]{1,0:T(8,128)(2,1)S(1)} copy-done((bf16[384,2048]{1,0:T(8,128)(2,1)S(1)}, bf16[384,2048]{1,0:T(8,128)(2,1)}, u32[]{:S(2)}) %copy-start) | copy-done | bytes 1572888
  101.1 2.0 %next_branch.1 = bf16[384,384]{1,0:T(8,128)(2,1)} custom-call(bf16[384,2048]{1,0:T(8,128)(2,1)S(1)} %copy-done, bf16[2048,384]{1,0:T(8,128)(2,1)S(1)} %get-tuple-element.32.natural_ref.w_ref, bf16[384,384]{1,0:T(8,128)(2,1)S(1)} %copy-done.1, f32[3,384]{1,0:T(4,128)S(1)} %copy-done.3, f32[384]{0:T(512)S(1)} %copy-done.5), custom_call_target="tpu_custom_call" | custom-call | flops 603979776 | bytes 3145728 | tf_op jit(solution)/shard_map/next_branch/pallas_call | solution.py:298
  103.0 0.0 collective-permute-done.7
  103.0 0.3 collective-permute-done.8
  103.3 2.4 %collective-permute-done.9 = bf16[48,2048]{1,0:T(8,128)(2,1)S(1)} collective-permute-done((bf16[48,2048]{1,0:T(8,128)(2,1)S(1)}, bf16[48,2048]{1,0:T(8,128)(2,1)S(1)}, u32[]{:S(2)}, u32[]{:S(2)}) %collective-permute-start.9) | collective-permute-done | bytes 196640 | tf_op jit(solution)/shard_map/ppermute | solution.py:27
  105.7 0.1 pad_maximum_fusion.own_ref
  105.8 0.0 copy-start.2
  105.8 0.0 copy-start.4
  105.8 0.0 copy-start.6
  105.8 2.1 %collective-permute-start.10 = (bf16[4,48,2048]{2,1,0:T(8,128)(2,1)S(1)}, bf16[4,48,2048]{2,1,0:T(8,128)(2,1)S(1)}, u32[]{:S(2)}, u32[]{:S(2)}) collective-permute-start(bf16[4,48,2048]{2,1,0:T(8,128)(2,1)S(1)} %pad_maximum_fusion.own_ref), channel_id=1, source_target_pairs={{0,1},{1,0},{2,3},{3,2},{4,5},{5,4},{6,7},{7,6},{8,9},{9,8},{10,11... | collective-permute-start | bytes 2359304 | tf_op jit(solution)/shard_map/ppermute | solution.py:27
  107.9 2.3 %collective-permute-done.10.other_ref = bf16[4,48,2048]{2,1,0:T(8,128)(2,1)S(1)} collective-permute-done((bf16[4,48,2048]{2,1,0:T(8,128)(2,1)S(1)}, bf16[4,48,2048]{2,1,0:T(8,128)(2,1)S(1)}, u32[]{:S(2)}, u32[]{:S(2)}) %collective-permute-start.10) | collective-permute-done | bytes 786464 | tf_op jit(solution)/shard_map/ppermute | solution.py:27
  110.1 1.3 %put_in_order.1 = bf16[8,48,2048]{2,1,0:T(8,128)(2,1)} custom-call(bf16[4,48,2048]{2,1,0:T(8,128)(2,1)S(1)} %pad_maximum_fusion.own_ref, bf16[4,48,2048]{2,1,0:T(8,128)(2,1)S(1)} %collective-permute-done.10.other_ref), custom_call_target="tpu_custom_call" | custom-call | bytes 3145728 | tf_op jit(solution)/shard_map/put_in_order/pallas_call | solution.py:52
  111.4 4.0 %all-to-all-done.3.in_ref = bf16[8,72,384]{2,1,0:T(8,128)(2,1)S(1)} async-done(((bf16[8,72,384]{2,1,0:T(8,128)(2,1)}), bf16[8,72,384]{2,1,0:T(8,128)(2,1)S(1)}, u32[]{:S(2)}, u32[]{:S(2)}) %all-to-all-start.3) | async-done | bytes 442400 | tf_op jit(solution)/shard_map/all_to_all | solution.py:22
  115.4 0.0 copy-done.2
  115.4 0.0 copy-done.4
  115.4 0.0 copy-done.6
  115.4 0.7 last_sum.1
  (1 shorter events, 0.0 us)
Async XLA Ops:
  2.2 27.3 %all-to-all-start = ((bf16[8,64,384]{2,1,0:T(8,128)(2,1)}), bf16[8,64,384]{2,1,0:T(8,128)(2,1)S(1)}, u32[]{:S(2)}, u32[]{:S(2)}) async-start(bf16[8,64,384]{2,1,0:T(8,128)(2,1)} %broadcast_in_dim.6), calls=%async_computation | async-start | bytes 786432 | tf_op jit(solution)/shard_map/all_to_all | solution.py:18
  8.1 16.2 %collective-permute-start.2 = (bf16[64,384]{1,0:T(8,128)(2,1)}, bf16[64,384]{1,0:T(8,128)(2,1)S(1)}, u32[]{:S(2)}, u32[]{:S(2)}) collective-permute-start(bf16[64,384]{1,0:T(8,128)(2,1)} %param.16), channel_id=1, source_target_pairs={{0,128},{64,192},{128,256},{192,320},{256,384},{320,448},{384,0},{... | collective-permute-start | bytes 147464 | tf_op jit(solution)/shard_map/ppermute | solution.py:27
  17.2 8.0 %collective-permute-start.1 = (bf16[64,384]{1,0:T(8,128)(2,1)}, bf16[64,384]{1,0:T(8,128)(2,1)S(1)}, u32[]{:S(2)}, u32[]{:S(2)}) collective-permute-start(bf16[64,384]{1,0:T(8,128)(2,1)} %param.16), channel_id=1, source_target_pairs={{0,448},{64,0},{128,64},{192,128},{256,192},{320,256},{384,320},{4... | collective-permute-start | bytes 147464 | tf_op jit(solution)/shard_map/ppermute | solution.py:27
  21.0 8.5 %collective-permute-start = (bf16[64,384]{1,0:T(8,128)(2,1)}, bf16[64,384]{1,0:T(8,128)(2,1)S(1)}, u32[]{:S(2)}, u32[]{:S(2)}) collective-permute-start(bf16[64,384]{1,0:T(8,128)(2,1)} %param.16), channel_id=1, source_target_pairs={{0,64},{64,128},{128,192},{192,256},{256,320},{320,384},{384,448},... | collective-permute-start | bytes 147464 | tf_op jit(solution)/shard_map/ppermute | solution.py:27
  29.5 20.0 %copy-start.3 = (f32[3,384]{1,0:T(4,128)S(1)}, f32[3,384]{1,0:T(4,128)}, u32[]{:S(2)}) copy-start(f32[3,384]{1,0:T(4,128)} %taps_ref.4) | copy-start | bytes 13828
  29.5 20.0 %copy-start.5 = (f32[384]{0:T(512)S(1)}, f32[384]{0:T(512)}, u32[]{:S(2)}) copy-start(f32[384]{0:T(512)} %bias_ref.4) | copy-start | bytes 4612
  29.5 20.0 %copy-start.8 = (bf16[384,384]{1,0:T(8,128)(2,1)S(1)}, bf16[384,384]{1,0:T(8,128)(2,1)}, u32[]{:S(2)}) copy-start(bf16[384,384]{1,0:T(8,128)(2,1)} %cot_ref.1) | copy-start | bytes 884740
  29.5 20.0 %copy-start.9 = (bf16[384,384]{1,0:T(8,128)(2,1)S(1)}, bf16[384,384]{1,0:T(8,128)(2,1)}, u32[]{:S(2)}) copy-start(bf16[384,384]{1,0:T(8,128)(2,1)} %value_ref.2) | copy-start | bytes 884740
  29.6 20.0 %copy-start.7 = (bf16[384,2048]{1,0:T(8,128)(2,1)S(1)}, bf16[384,2048]{1,0:T(8,128)(2,1)}, u32[]{:S(2)}) copy-start(bf16[384,2048]{1,0:T(8,128)(2,1)} %x_ref.1) | copy-start | bytes 4718596
  54.6 23.1 %all-to-all-start.2 = ((bf16[8,264,384]{2,1,0:T(8,128)(2,1)}), bf16[8,264,384]{2,1,0:T(8,128)(2,1)S(1)}, u32[]{:S(2)}, u32[]{:S(2)}) async-start(bf16[8,264,384]{2,1,0:T(8,128)(2,1)} %get-tuple-element.41), calls=%async_computation.2 | async-start | bytes 3244032 | tf_op jit(solution)/shard_map/all_to_all | solution.py:22
  61.0 4.4 %collective-permute-start.3 = (bf16[192,2048]{1,0:T(8,128)(2,1)}, bf16[192,2048]{1,0:T(8,128)(2,1)S(1)}, u32[]{:S(2)}, u32[]{:S(2)}) collective-permute-start(bf16[192,2048]{1,0:T(8,128)(2,1)} %get-tuple-element.34), channel_id=1, source_target_pairs={{0,1},{1,0},{2,3},{3,2},{4,5},{5,4},{6,7},{7,6},{8,9},{9,8},{10,11... | collective-permute-start | bytes 2359304 | tf_op jit(solution)/shard_map/ppermute | solution.py:27
  67.0 21.5 %collective-permute-start.6 = (bf16[48,2048]{1,0:T(8,128)(2,1)}, bf16[48,2048]{1,0:T(8,128)(2,1)}, u32[]{:S(2)}, u32[]{:S(2)}) collective-permute-start(bf16[48,2048]{1,0:T(8,128)(2,1)} %get-tuple-element.38), channel_id=1, source_target_pairs={{0,6},{2,0},{4,2},{6,4},{1,7},{3,1},{5,3},{7,5},{8,14},{10,8},{12,... | collective-permute-start | bytes 589832 | tf_op jit(solution)/shard_map/ppermute | solution.py:27
  69.4 19.1 %collective-permute-start.5 = (bf16[48,2048]{1,0:T(8,128)(2,1)}, bf16[48,2048]{1,0:T(8,128)(2,1)}, u32[]{:S(2)}, u32[]{:S(2)}) collective-permute-start(bf16[48,2048]{1,0:T(8,128)(2,1)} %get-tuple-element.37), channel_id=1, source_target_pairs={{0,4},{2,6},{4,0},{6,2},{1,5},{3,7},{5,1},{7,3},{8,12},{10,14},{12... | collective-permute-start | bytes 589832 | tf_op jit(solution)/shard_map/ppermute | solution.py:27
  73.8 25.9 %copy-start.1 = (bf16[384,384]{1,0:T(8,128)(2,1)S(1)}, bf16[384,384]{1,0:T(8,128)(2,1)}, u32[]{:S(2)}) copy-start(bf16[384,384]{1,0:T(8,128)(2,1)} %value_ref.3) | copy-start | bytes 884740
  73.8 14.7 %collective-permute-start.4 = (bf16[48,2048]{1,0:T(8,128)(2,1)}, bf16[48,2048]{1,0:T(8,128)(2,1)}, u32[]{:S(2)}, u32[]{:S(2)}) collective-permute-start(bf16[48,2048]{1,0:T(8,128)(2,1)} %get-tuple-element.36), channel_id=1, source_target_pairs={{0,2},{2,4},{4,6},{6,0},{1,3},{3,5},{5,7},{7,1},{8,10},{10,12},{12... | collective-permute-start | bytes 589832 | tf_op jit(solution)/shard_map/ppermute | solution.py:27
  78.6 36.8 %all-to-all-start.3 = ((bf16[8,72,384]{2,1,0:T(8,128)(2,1)}), bf16[8,72,384]{2,1,0:T(8,128)(2,1)S(1)}, u32[]{:S(2)}, u32[]{:S(2)}) async-start(bf16[8,72,384]{2,1,0:T(8,128)(2,1)} %sum_and_repack.1), calls=%async_computation.3 | async-start | bytes 884736 | tf_op jit(solution)/shard_map/all_to_all | solution.py:22
  89.9 13.2 %collective-permute-start.7 = (bf16[48,2048]{1,0:T(8,128)(2,1)S(1)}, bf16[48,2048]{1,0:T(8,128)(2,1)S(1)}, u32[]{:S(2)}, u32[]{:S(2)}) collective-permute-start(bf16[48,2048]{1,0:T(8,128)(2,1)S(1)} %add_convert_fusion), channel_id=1, source_target_pairs={{0,2},{2,4},{4,6},{6,0},{1,3},{3,5},{5,7},{7,1},{8,10},{10,12},{12... | collective-permute-start | bytes 589832 | tf_op jit(solution)/shard_map/ppermute | solution.py:27
  92.1 11.2 %collective-permute-start.8 = (bf16[48,2048]{1,0:T(8,128)(2,1)S(1)}, bf16[48,2048]{1,0:T(8,128)(2,1)S(1)}, u32[]{:S(2)}, u32[]{:S(2)}) collective-permute-start(bf16[48,2048]{1,0:T(8,128)(2,1)S(1)} %add_convert_fusion), channel_id=1, source_target_pairs={{0,4},{2,6},{4,0},{6,2},{1,5},{3,7},{5,1},{7,3},{8,12},{10,14},{12... | collective-permute-start | bytes 589832 | tf_op jit(solution)/shard_map/ppermute | solution.py:27
  96.0 9.7 %collective-permute-start.9 = (bf16[48,2048]{1,0:T(8,128)(2,1)S(1)}, bf16[48,2048]{1,0:T(8,128)(2,1)S(1)}, u32[]{:S(2)}, u32[]{:S(2)}) collective-permute-start(bf16[48,2048]{1,0:T(8,128)(2,1)S(1)} %add_convert_fusion), channel_id=1, source_target_pairs={{0,6},{2,0},{4,2},{6,4},{1,7},{3,1},{5,3},{7,5},{8,14},{10,8},{12,... | collective-permute-start | bytes 589832 | tf_op jit(solution)/shard_map/ppermute | solution.py:27
  99.7 1.4 %copy-start = (bf16[384,2048]{1,0:T(8,128)(2,1)S(1)}, bf16[384,2048]{1,0:T(8,128)(2,1)}, u32[]{:S(2)}) copy-start(bf16[384,2048]{1,0:T(8,128)(2,1)} %x_ref.2) | copy-start | bytes 4718596
  105.8 9.6 %copy-start.2 = (f32[64,384]{1,0:T(8,128)S(1)}, f32[64,384]{1,0:T(8,128)}, u32[]{:S(2)}) copy-start(f32[64,384]{1,0:T(8,128)} %w_ref.1) | copy-start | bytes 294916
  105.8 9.6 %copy-start.4 = (f32[3,384]{1,0:T(4,128)S(1)}, f32[3,384]{1,0:T(4,128)}, u32[]{:S(2)}) copy-start(f32[3,384]{1,0:T(4,128)} %taps_ref.5) | copy-start | bytes 13828
  105.8 9.6 %copy-start.6 = (f32[384]{0:T(512)S(1)}, f32[384]{0:T(512)}, u32[]{:S(2)}) copy-start(f32[384]{0:T(512)} %bias_ref.5) | copy-start | bytes 4612
  105.8 4.3 %collective-permute-start.10 = (bf16[4,48,2048]{2,1,0:T(8,128)(2,1)S(1)}, bf16[4,48,2048]{2,1,0:T(8,128)(2,1)S(1)}, u32[]{:S(2)}, u32[]{:S(2)}) collective-permute-start(bf16[4,48,2048]{2,1,0:T(8,128)(2,1)S(1)} %pad_maximum_fusion.own_ref), channel_id=1, source_target_pairs={{0,1},{1,0},{2,3},{3,2},{4,5},{5,4},{6,7},{7,6},{8,9},{9,8},{10,11... | collective-permute-start | bytes 2359304 | tf_op jit(solution)/shard_map/ppermute | solution.py:27

commit v11 on v8

--- a/solution.py
+++ b/solution.py
@@ -10,6 +10,7 @@
 SEQ_LEN = 128
 SMALL_ROWS = 8
 FAR, NEAR = ("zm", "zp"), ("zl", "y")
+FAR_SHIFTS = (0, 1, -1, 2)
 
 
 def copies_to(block, axis, size):
@@ -23,7 +24,7 @@
 
 def send_on(block, axis, shift):
     size = lax.axis_size(axis)
-    return lax.ppermute(block, axis, [(i, (i + shift) % size) for i in range(size)])
+    return lax.ppermute(block, axis, [(i, (i + shift + size) % size) for i in range(size)])
 
 
 def near(array):
@@ -58,26 +59,43 @@
     )(near(own), near(other))
 
 
+EDGE = 8
+
+
 def later(values, offset):
     if offset == 0:
         return values
-    rows = lax.broadcasted_iota(jnp.int32, values.shape, 0) % SEQ_LEN
-    return jnp.where(rows >= offset, pltpu.roll(values, offset, 0), 0.0)
+    moved = pltpu.roll(values, offset, 0)
+    pieces = []
+    for start in range(0, values.shape[0], SEQ_LEN):
+        edge = moved[start : start + EDGE]
+        rows = lax.broadcasted_iota(jnp.int32, edge.shape, 0)
+        pieces.append(jnp.where(rows >= offset, edge, 0.0))
+        pieces.append(moved[start + EDGE : start + SEQ_LEN])
+    return jnp.concatenate(pieces, axis=0)
 
 
 def earlier(values, offset):
     if offset == 0:
         return values
-    count = values.shape[0]
-    rows = lax.broadcasted_iota(jnp.int32, values.shape, 0) % SEQ_LEN
-    return jnp.where(rows < SEQ_LEN - offset, pltpu.roll(values, count - offset, 0), 0.0)
-
-
-def gated(up, taps_ref, bias_ref):
-    tap_count = taps_ref.shape[0]
+    moved = pltpu.roll(values, values.shape[0] - offset, 0)
+    pieces = []
+    for end in range(SEQ_LEN, values.shape[0] + 1, SEQ_LEN):
+        pieces.append(moved[end - SEQ_LEN : end - EDGE])
+        edge = moved[end - EDGE : end]
+        rows = lax.broadcasted_iota(jnp.int32, edge.shape, 0)
+        pieces.append(jnp.where(rows < EDGE - offset, edge, 0.0))
+    return jnp.concatenate(pieces, axis=0)
+
+
+def lags_of(up, tap_count):
+    return [later(up, tap_count - 1 - j) for j in range(tap_count)]
+
+
+def gated(lags, taps_ref, bias_ref):
     total = bias_ref[...][None, :]
-    for j in range(tap_count):
-        total = total + taps_ref[j : j + 1, :] * later(up, tap_count - 1 - j)
+    for j, lag in enumerate(lags):
+        total = total + taps_ref[j : j + 1, :] * lag
     return total
 
 
@@ -87,9 +105,12 @@
     return (high + pltpu.roll(rows - high, half, 0)).astype(jnp.bfloat16)
 
 
-def previous_branch(x_prev, plane, cotangent, value_prev, conv_taps, conv_bias, grad_scale, n_c):
+def previous_branch(
+    x_prev, plane, rest, cotangent, value_prev, conv_taps, conv_bias, grad_scale, n_c
+):
     row_count, width = x_prev.shape
-    n_near, n_far, shard_rows, units = plane.shape
+    n_near, shard_rows, units = plane.shape
+    n_far = rest.shape[1] + 1
     tap_count = conv_taps.shape[0]
     n_x = lax.axis_size("x")
     half_rows = row_count // n_c
@@ -99,6 +120,7 @@
     def body(
         x_ref,
         w_ref,
+        rest_ref,
         cot_ref,
         value_ref,
         taps_ref,
@@ -119,11 +141,17 @@
             for near_at in range(n_near)
             for far_at in range(n_far)
         ]
-        for near_at, far_at, at in spots:
-            natural_ref[at : at + shard_rows] = w_ref[near_at, far_at]
+        own_far = lax.axis_index("zm") * lax.axis_size("zp") + lax.axis_index("zp")
+        for near_at in range(n_near):
+            for k in range(n_far):
+                far_at = (own_far + n_far - FAR_SHIFTS[k]) % n_far
+                at = (far_at * n_near + near_at) * shard_rows
+                block = w_ref[near_at] if k == 0 else rest_ref[near_at, k - 1]
+                natural_ref[pl.ds(pl.multiple_of(at, shard_rows), shard_rows)] = block
         up = jnp.dot(x_ref[...], natural_ref[...], preferred_element_type=jnp.float32)
         up = up.astype(jnp.bfloat16).astype(jnp.float32)
-        gate = gated(up, taps_ref, bias_ref)
+        lags = lags_of(up, tap_count)
+        gate = gated(lags, taps_ref, bias_ref)
         sig = jax.nn.sigmoid(gate)
         cot = cot_ref[...].astype(jnp.float32)
         gv_ref[...] = (cot * gate * sig).astype(jnp.bfloat16)
@@ -155,8 +183,7 @@
         )
         grad_w = (grad_w * grad_scale).astype(jnp.bfloat16)
         sums = [
-            jnp.sum(grad_gate * later(up, tap_count - 1 - j), axis=0, keepdims=True)
-            for j in range(tap_count)
+            jnp.sum(grad_gate * lag, axis=0, keepdims=True) for lag in lags
         ] + [jnp.sum(grad_gate, axis=0, keepdims=True)]
         rest = jnp.zeros((SMALL_ROWS - len(sums), units), jnp.float32)
         small = high_and_low(jnp.concatenate([*sums, rest], axis=0) * grad_scale)
@@ -176,7 +203,7 @@
     half = jnp.bfloat16
     return pl.pallas_call(
         body,
-        in_specs=[VMEM] * 6,
+        in_specs=[VMEM] * 7,
         out_specs=[pl.BlockSpec(), VMEM, VMEM, HBM, HBM],
         out_shape=[
             jax.ShapeDtypeStruct((row_count, units), half),
@@ -198,6 +225,7 @@
     )(
         near(x_prev),
         near(plane),
+        near(rest),
         near(cotangent),
         near(value_prev),
         near(conv_taps),
@@ -247,7 +275,8 @@
 
     def body(x_ref, w_ref, value_ref, taps_ref, bias_ref, out_ref):
         up = jnp.dot(x_ref[...], w_ref[...], preferred_element_type=jnp.float32)
-        gate = gated(up.astype(jnp.bfloat16).astype(jnp.float32), taps_ref, bias_ref)
+        up = up.astype(jnp.bfloat16).astype(jnp.float32)
+        gate = gated(lags_of(up, taps_ref.shape[0]), taps_ref, bias_ref)
         hidden = gate * jax.nn.sigmoid(gate) * value_ref[...].astype(jnp.float32)
         out_ref[...] = hidden.astype(jnp.bfloat16)
 
@@ -348,10 +377,12 @@
     n_zh, n_x, n_c = (lax.axis_size(a) for a in ("zh", "x", "c"))
     n_far, n_near = lax.axis_size(FAR), lax.axis_size(NEAR)
 
-    plane = copies_to(copies_to(w_gate, FAR, n_far), NEAR, n_near)
+    plane = copies_to(w_gate, NEAR, n_near)
+    far_shards = [send_on(w_gate, ("zh", *FAR), shift) for shift in FAR_SHIFTS[1:]]
+    rest = copies_to(jnp.stack(far_shards), NEAR, n_near)
     grad_scale = float(row_count * n_zh * n_far * n_near) ** (-0.5)
     grad_value, gathered, keep, to_core, sent = previous_branch(
-        x_prev, plane, cotangent, value_prev, conv_taps, conv_bias, grad_scale, n_c
+        x_prev, plane, rest, cotangent, value_prev, conv_taps, conv_bias, grad_scale, n_c
     )
     from_core = send_on(to_core, "c", 1)
     from_near = exchange(sent, NEAR)

time: 117 us -> 119 us (1.017)
  the two profiles are of different devices: /device:TPU:44 before, /device:TPU:32 now
where the time goes in v11:
time: 119 us; the launch traced here: 118 us
  starting transfers between devices  64.9 us (55%)
  blocking collectives  18.9 us (16%)
  waiting for transfers between devices  17 us (14%)
  Pallas kernels  11.9 us (10%)
  local copies, waits for them, and re-layouts  3.2 us (3%)
  other arithmetic  1.45 us (1%)
    ppermute x11, starting transfers between devices, send_on(): lax.ppermute(block, axis, [(i, (i + shift + size) % size) for i in range(...  41 us
    all_to_all x1, blocking collectives, copies_to(): return lax.all_to_all(copies, axis, 0, 0, tiled=True)  18.9 us
    all_to_all x2, starting transfers between devices, exchange(): return lax.all_to_all(blocks, axis, 0, 0, tiled=True)  15.1 us
    ppermute x11, waiting for transfers between devices, send_on(): lax.ppermute(block, axis, [(i, (i + shift + size) % size) for i in range(...  12.9 us
    all_to_all x1, starting transfers between devices, copies_to(): return lax.all_to_all(copies, axis, 0, 0, tiled=True)  8.83 us
    pallas_call x1, Pallas kernels, previous_branch(): pl.pallas_call(body, in_specs=[VMEM] * 7, out_specs=[pl.BlockSpec(), VMEM...  5.46 us
    all_to_all x2, waiting for transfers between devices, exchange(): return lax.all_to_all(blocks, axis, 0, 0, tiled=True)  4.16 us
  transfers between devices with their start and end apart: 14, of which 5 were waited for; matrix products, arithmetic and copies ran while one was open for 1% of the time, Pallas kernels for 5%

profile of v11, /device:TPU:32, one launch (start us, length us, event | category | flops | bytes accessed | tf_op | source)
XLA Modules:
  0.0 118.4 jit_solution(3286808175284361579)
XLA Ops:
  0.6 1.6 %broadcast_in_dim.6 = bf16[8,64,384]{2,1,0:T(8,128)(2,1)} broadcast(bf16[64,384]{1,0:T(8,128)(2,1)} %param.16), dimensions={1,2} | broadcast | bytes 442368 | tf_op jit(solution)/shard_map/broadcast_in_dim | solution.py:17
  2.2 8.8 %all-to-all-start = ((bf16[8,64,384]{2,1,0:T(8,128)(2,1)}), bf16[8,64,384]{2,1,0:T(8,128)(2,1)S(1)}, u32[]{:S(2)}, u32[]{:S(2)}) async-start(bf16[8,64,384]{2,1,0:T(8,128)(2,1)} %broadcast_in_dim.6), calls=%async_computation | async-start | bytes 786432 | tf_op jit(solution)/shard_map/all_to_all | solution.py:18
  11.0 2.3 %collective-permute-start = (bf16[64,384]{1,0:T(8,128)(2,1)}, bf16[64,384]{1,0:T(8,128)(2,1)S(1)}, u32[]{:S(2)}, u32[]{:S(2)}) collective-permute-start(bf16[64,384]{1,0:T(8,128)(2,1)} %param.16), channel_id=1, source_target_pairs={{0,64},{64,128},{128,192},{192,256},{256,320},{320,384},{384,448},... | collective-permute-start | bytes 147464 | tf_op jit(solution)/shard_map/ppermute | solution.py:27
  13.3 7.7 %collective-permute-start.1 = (bf16[64,384]{1,0:T(8,128)(2,1)}, bf16[64,384]{1,0:T(8,128)(2,1)S(1)}, u32[]{:S(2)}, u32[]{:S(2)}) collective-permute-start(bf16[64,384]{1,0:T(8,128)(2,1)} %param.16), channel_id=1, source_target_pairs={{0,448},{64,0},{128,64},{192,128},{256,192},{320,256},{384,320},{4... | collective-permute-start | bytes 147464 | tf_op jit(solution)/shard_map/ppermute | solution.py:27
  21.0 4.2 %collective-permute-start.2 = (bf16[64,384]{1,0:T(8,128)(2,1)}, bf16[64,384]{1,0:T(8,128)(2,1)S(1)}, u32[]{:S(2)}, u32[]{:S(2)}) collective-permute-start(bf16[64,384]{1,0:T(8,128)(2,1)} %param.16), channel_id=1, source_target_pairs={{0,128},{64,192},{128,256},{192,320},{256,384},{320,448},{384,0},{... | collective-permute-start | bytes 147464 | tf_op jit(solution)/shard_map/ppermute | solution.py:27
  25.2 0.0 collective-permute-done
  25.2 0.0 collective-permute-done.1
  25.2 6.9 %collective-permute-done.2 = bf16[64,384]{1,0:T(8,128)(2,1)S(1)} collective-permute-done((bf16[64,384]{1,0:T(8,128)(2,1)}, bf16[64,384]{1,0:T(8,128)(2,1)S(1)}, u32[]{:S(2)}, u32[]{:S(2)}) %collective-permute-start.2) | collective-permute-done | bytes 49184 | tf_op jit(solution)/shard_map/ppermute | solution.py:27
  32.2 0.0 copy-start.3
  32.2 0.0 copy-start.5
  32.2 0.0 copy-start.8
  32.2 0.0 copy-start.9
  32.2 0.0 all-to-all-done.w_ref
  32.2 0.0 copy-start.7
  32.2 0.2 broadcast_in_dim.7
  32.4 18.9 %all_to_all.20.rest_ref = bf16[8,3,64,384]{3,2,1,0:T(8,128)(2,1)S(1)} all-to-all(bf16[8,3,64,384]{3,2,1,0:T(8,128)(2,1)S(1)} %broadcast_in_dim.7), channel_id=1, replica_groups=mesh['zh'=2,'zm'=2,'zp'=2,'zl'=2,'y'=4,'x'=4,'c'=2] {'zl','y'}, dimensions={0} | all-to-all | bytes 2359296 | tf_op jit(solution)/shard_map/all_to_all | solution.py:18
  51.3 0.0 copy-done.3
  51.3 0.0 copy-done.5
  51.3 0.0 copy-done.8
  51.3 0.0 copy-done.9
  51.3 0.0 copy-done.7
  51.4 5.5 %previous_branch.1 = (bf16[384,384]{1,0:T(8,128)(2,1)}, bf16[2048,384]{1,0:T(8,128)(2,1)S(1)}, bf16[192,384]{1,0:T(8,128)(2,1)S(1)}, bf16[192,2048]{1,0:T(8,128)(2,1)}, bf16[8,264,384]{2,1,0:T(8,128)(2,1)}) custom-call(bf16[384,2048]{1,0:T(8,128)(2,1)S(1)} %copy-done.7, bf16[8,64,384]{2,1,0:T(8,128)(2,1)S(1)} %all-to-all-done.w_ref, ...), custom_call_target="tpu_custom_call" | custom-call | flops 1509949440 | bytes 6291456 | tf_op jit(solution)/shard_map/previous_branch/pallas_call | solution.py:204
  56.8 4.9 %all-to-all-start.2 = ((bf16[8,264,384]{2,1,0:T(8,128)(2,1)}), bf16[8,264,384]{2,1,0:T(8,128)(2,1)S(1)}, u32[]{:S(2)}, u32[]{:S(2)}) async-start(bf16[8,264,384]{2,1,0:T(8,128)(2,1)} %get-tuple-element.35), calls=%async_computation.2 | async-start | bytes 3244032 | tf_op jit(solution)/shard_map/all_to_all | solution.py:22
  61.7 1.9 %collective-permute-start.3 = (bf16[192,2048]{1,0:T(8,128)(2,1)}, bf16[192,2048]{1,0:T(8,128)(2,1)S(1)}, u32[]{:S(2)}, u32[]{:S(2)}) collective-permute-start(bf16[192,2048]{1,0:T(8,128)(2,1)} %get-tuple-element.28), channel_id=1, source_target_pairs={{0,1},{1,0},{2,3},{3,2},{4,5},{5,4},{6,7},{7,6},{8,9},{9,8},{10,11... | collective-permute-start | bytes 2359304 | tf_op jit(solution)/shard_map/ppermute | solution.py:27
  63.6 2.5 %collective-permute-done.3.other_ref = bf16[192,2048]{1,0:T(8,128)(2,1)S(1)} collective-permute-done((bf16[192,2048]{1,0:T(8,128)(2,1)}, bf16[192,2048]{1,0:T(8,128)(2,1)S(1)}, u32[]{:S(2)}, u32[]{:S(2)}) %collective-permute-start.3) | collective-permute-done | bytes 786464 | tf_op jit(solution)/shard_map/ppermute | solution.py:27
  66.1 1.6 %add_halves.1 = (bf16[48,2048]{1,0:T(8,128)(2,1)}, bf16[48,2048]{1,0:T(8,128)(2,1)}, bf16[48,2048]{1,0:T(8,128)(2,1)}, bf16[48,2048]{1,0:T(8,128)(2,1)}) custom-call(bf16[192,384]{1,0:T(8,128)(2,1)S(1)} %get-tuple-element.26.keep_ref, bf16[2048,384]{1,0:T(8,128)(2,1)S(1)} %get-tuple-element.27.w_ref, bf16[192,2048]{1,0:T(8,128)(2,1)S(1)} %collective-permute-done.3.other_ref), custom_call_target="tpu_custom_call" | custom-call | flops 301989888 | bytes 6291456 | tf_op jit(solution)/shard_map/add_halves/pallas_call | solution.py:257
  67.7 3.4 %collective-permute-start.4 = (bf16[48,2048]{1,0:T(8,128)(2,1)}, bf16[48,2048]{1,0:T(8,128)(2,1)}, u32[]{:S(2)}, u32[]{:S(2)}) collective-permute-start(bf16[48,2048]{1,0:T(8,128)(2,1)} %get-tuple-element.30), channel_id=1, source_target_pairs={{0,2},{2,4},{4,6},{6,0},{1,3},{3,5},{5,7},{7,1},{8,10},{10,12},{12... | collective-permute-start | bytes 589832 | tf_op jit(solution)/shard_map/ppermute | solution.py:27
  71.1 4.6 %collective-permute-start.5 = (bf16[48,2048]{1,0:T(8,128)(2,1)}, bf16[48,2048]{1,0:T(8,128)(2,1)}, u32[]{:S(2)}, u32[]{:S(2)}) collective-permute-start(bf16[48,2048]{1,0:T(8,128)(2,1)} %get-tuple-element.31), channel_id=1, source_target_pairs={{0,4},{2,6},{4,0},{6,2},{1,5},{3,7},{5,1},{7,3},{8,12},{10,14},{12... | collective-permute-start | bytes 589832 | tf_op jit(solution)/shard_map/ppermute | solution.py:27
  75.7 0.0 copy-start.1
  75.8 3.5 %collective-permute-start.6 = (bf16[48,2048]{1,0:T(8,128)(2,1)}, bf16[48,2048]{1,0:T(8,128)(2,1)}, u32[]{:S(2)}, u32[]{:S(2)}) collective-permute-start(bf16[48,2048]{1,0:T(8,128)(2,1)} %get-tuple-element.32), channel_id=1, source_target_pairs={{0,6},{2,0},{4,2},{6,4},{1,7},{3,1},{5,3},{7,5},{8,14},{10,8},{12,... | collective-permute-start | bytes 589832 | tf_op jit(solution)/shard_map/ppermute | solution.py:27
  79.2 0.0 all-to-all-done.2.in_ref
  79.2 0.9 sum_and_repack.1
  80.2 10.2 %all-to-all-start.3 = ((bf16[8,72,384]{2,1,0:T(8,128)(2,1)}), bf16[8,72,384]{2,1,0:T(8,128)(2,1)S(1)}, u32[]{:S(2)}, u32[]{:S(2)}) async-start(bf16[8,72,384]{2,1,0:T(8,128)(2,1)} %sum_and_repack.1), calls=%async_computation.3 | async-start | bytes 884736 | tf_op jit(solution)/shard_map/all_to_all | solution.py:22
  90.4 0.0 collective-permute-done.4
  90.4 0.0 collective-permute-done.5
  90.4 0.0 collective-permute-done.6
  90.4 1.3 %add_convert_fusion = bf16[48,2048]{1,0:T(8,128)(2,1)S(1)} fusion(bf16[48,2048]{1,0:T(8,128)(2,1)} %collective-permute-done.6, bf16[48,2048]{1,0:T(8,128)(2,1)} %collective-permute-done.5, bf16[48,2048]{1,0:T(8,128)(2,1)} %collective-permute-done.4, bf16[48,2048]{1,0:T(8,128)(2,1)} %get-tuple-element.29), kind=kLoop, calls=%fused_computation.1 | loop fusion | flops 786432 | bytes 983040 | tf_op jit(solution)/shard_map/convert_element_type | solution.py:397
  91.8 3.4 %collective-permute-start.7 = (bf16[48,2048]{1,0:T(8,128)(2,1)S(1)}, bf16[48,2048]{1,0:T(8,128)(2,1)S(1)}, u32[]{:S(2)}, u32[]{:S(2)}) collective-permute-start(bf16[48,2048]{1,0:T(8,128)(2,1)S(1)} %add_convert_fusion), channel_id=1, source_target_pairs={{0,2},{2,4},{4,6},{6,0},{1,3},{3,5},{5,7},{7,1},{8,10},{10,12},{12... | collective-permute-start | bytes 589832 | tf_op jit(solution)/shard_map/ppermute | solution.py:27
  95.1 4.6 %collective-permute-start.8 = (bf16[48,2048]{1,0:T(8,128)(2,1)S(1)}, bf16[48,2048]{1,0:T(8,128)(2,1)S(1)}, u32[]{:S(2)}, u32[]{:S(2)}) collective-permute-start(bf16[48,2048]{1,0:T(8,128)(2,1)S(1)} %add_convert_fusion), channel_id=1, source_target_pairs={{0,4},{2,6},{4,0},{6,2},{1,5},{3,7},{5,1},{7,3},{8,12},{10,14},{12... | collective-permute-start | bytes 589832 | tf_op jit(solution)/shard_map/ppermute | solution.py:27
  99.8 3.3 %collective-permute-start.9 = (bf16[48,2048]{1,0:T(8,128)(2,1)S(1)}, bf16[48,2048]{1,0:T(8,128)(2,1)S(1)}, u32[]{:S(2)}, u32[]{:S(2)}) collective-permute-start(bf16[48,2048]{1,0:T(8,128)(2,1)S(1)} %add_convert_fusion), channel_id=1, source_target_pairs={{0,6},{2,0},{4,2},{6,4},{1,7},{3,1},{5,3},{7,5},{8,14},{10,8},{12,... | collective-permute-start | bytes 589832 | tf_op jit(solution)/shard_map/ppermute | solution.py:27
  103.1 0.0 copy-done.1
  103.1 0.0 copy-start
  103.2 1.4 %copy-done = bf16[384,2048]{1,0:T(8,128)(2,1)S(1)} copy-done((bf16[384,2048]{1,0:T(8,128)(2,1)S(1)}, bf16[384,2048]{1,0:T(8,128)(2,1)}, u32[]{:S(2)}) %copy-start) | copy-done | bytes 1572888
  104.6 2.0 %next_branch.1 = bf16[384,384]{1,0:T(8,128)(2,1)} custom-call(bf16[384,2048]{1,0:T(8,128)(2,1)S(1)} %copy-done, bf16[2048,384]{1,0:T(8,128)(2,1)S(1)} %get-tuple-element.27.w_ref, bf16[384,384]{1,0:T(8,128)(2,1)S(1)} %copy-done.1, f32[3,384]{1,0:T(4,128)S(1)} %copy-done.3, f32[384]{0:T(512)S(1)} %copy-done.5), custom_call_target="tpu_custom_call" | custom-call | flops 603979776 | bytes 3145728 | tf_op jit(solution)/shard_map/next_branch/pallas_call | solution.py:283
  106.5 0.0 collective-permute-done.7
  106.5 0.0 collective-permute-done.8
  106.5 1.2 %collective-permute-done.9 = bf16[48,2048]{1,0:T(8,128)(2,1)S(1)} collective-permute-done((bf16[48,2048]{1,0:T(8,128)(2,1)S(1)}, bf16[48,2048]{1,0:T(8,128)(2,1)S(1)}, u32[]{:S(2)}, u32[]{:S(2)}) %collective-permute-start.9) | collective-permute-done | bytes 196640 | tf_op jit(solution)/shard_map/ppermute | solution.py:27
  107.8 0.1 pad_maximum_fusion.own_ref
  107.9 0.0 copy-start.2
  107.9 0.0 copy-start.4
  107.9 0.0 copy-start.6
  107.9 2.1 %collective-permute-start.10 = (bf16[4,48,2048]{2,1,0:T(8,128)(2,1)S(1)}, bf16[4,48,2048]{2,1,0:T(8,128)(2,1)S(1)}, u32[]{:S(2)}, u32[]{:S(2)}) collective-permute-start(bf16[4,48,2048]{2,1,0:T(8,128)(2,1)S(1)} %pad_maximum_fusion.own_ref), channel_id=1, source_target_pairs={{0,1},{1,0},{2,3},{3,2},{4,5},{5,4},{6,7},{7,6},{8,9},{9,8},{10,11... | collective-permute-start | bytes 2359304 | tf_op jit(solution)/shard_map/ppermute | solution.py:27
  110.0 2.3 %collective-permute-done.10.other_ref = bf16[4,48,2048]{2,1,0:T(8,128)(2,1)S(1)} collective-permute-done((bf16[4,48,2048]{2,1,0:T(8,128)(2,1)S(1)}, bf16[4,48,2048]{2,1,0:T(8,128)(2,1)S(1)}, u32[]{:S(2)}, u32[]{:S(2)}) %collective-permute-start.10) | collective-permute-done | bytes 786464 | tf_op jit(solution)/shard_map/ppermute | solution.py:27
  112.2 1.3 %put_in_order.1 = bf16[8,48,2048]{2,1,0:T(8,128)(2,1)} custom-call(bf16[4,48,2048]{2,1,0:T(8,128)(2,1)S(1)} %pad_maximum_fusion.own_ref, bf16[4,48,2048]{2,1,0:T(8,128)(2,1)S(1)} %collective-permute-done.10.other_ref), custom_call_target="tpu_custom_call" | custom-call | bytes 3145728 | tf_op jit(solution)/shard_map/put_in_order/pallas_call | solution.py:52
  113.5 4.2 %all-to-all-done.3.in_ref = bf16[8,72,384]{2,1,0:T(8,128)(2,1)S(1)} async-done(((bf16[8,72,384]{2,1,0:T(8,128)(2,1)}), bf16[8,72,384]{2,1,0:T(8,128)(2,1)S(1)}, u32[]{:S(2)}, u32[]{:S(2)}) %all-to-all-start.3) | async-done | bytes 442400 | tf_op jit(solution)/shard_map/all_to_all | solution.py:22
  117.7 0.0 copy-done.2
  117.7 0.0 copy-done.4
  117.7 0.0 copy-done.6
  117.7 0.7 last_sum.1
  (1 shorter events, 0.0 us)
Async XLA Ops:
  2.2 30.0 %all-to-all-start = ((bf16[8,64,384]{2,1,0:T(8,128)(2,1)}), bf16[8,64,384]{2,1,0:T(8,128)(2,1)S(1)}, u32[]{:S(2)}, u32[]{:S(2)}) async-start(bf16[8,64,384]{2,1,0:T(8,128)(2,1)} %broadcast_in_dim.6), calls=%async_computation | async-start | bytes 786432 | tf_op jit(solution)/shard_map/all_to_all | solution.py:18
  11.0 14.2 %collective-permute-start = (bf16[64,384]{1,0:T(8,128)(2,1)}, bf16[64,384]{1,0:T(8,128)(2,1)S(1)}, u32[]{:S(2)}, u32[]{:S(2)}) collective-permute-start(bf16[64,384]{1,0:T(8,128)(2,1)} %param.16), channel_id=1, source_target_pairs={{0,64},{64,128},{128,192},{192,256},{256,320},{320,384},{384,448},... | collective-permute-start | bytes 147464 | tf_op jit(solution)/shard_map/ppermute | solution.py:27
  13.3 11.9 %collective-permute-start.1 = (bf16[64,384]{1,0:T(8,128)(2,1)}, bf16[64,384]{1,0:T(8,128)(2,1)S(1)}, u32[]{:S(2)}, u32[]{:S(2)}) collective-permute-start(bf16[64,384]{1,0:T(8,128)(2,1)} %param.16), channel_id=1, source_target_pairs={{0,448},{64,0},{128,64},{192,128},{256,192},{320,256},{384,320},{4... | collective-permute-start | bytes 147464 | tf_op jit(solution)/shard_map/ppermute | solution.py:27
  21.0 11.1 %collective-permute-start.2 = (bf16[64,384]{1,0:T(8,128)(2,1)}, bf16[64,384]{1,0:T(8,128)(2,1)S(1)}, u32[]{:S(2)}, u32[]{:S(2)}) collective-permute-start(bf16[64,384]{1,0:T(8,128)(2,1)} %param.16), channel_id=1, source_target_pairs={{0,128},{64,192},{128,256},{192,320},{256,384},{320,448},{384,0},{... | collective-permute-start | bytes 147464 | tf_op jit(solution)/shard_map/ppermute | solution.py:27
  32.2 19.2 %copy-start.3 = (f32[3,384]{1,0:T(4,128)S(1)}, f32[3,384]{1,0:T(4,128)}, u32[]{:S(2)}) copy-start(f32[3,384]{1,0:T(4,128)} %taps_ref.4) | copy-start | bytes 13828
  32.2 19.1 %copy-start.5 = (f32[384]{0:T(512)S(1)}, f32[384]{0:T(512)}, u32[]{:S(2)}) copy-start(f32[384]{0:T(512)} %bias_ref.4) | copy-start | bytes 4612
  32.2 19.1 %copy-start.8 = (bf16[384,384]{1,0:T(8,128)(2,1)S(1)}, bf16[384,384]{1,0:T(8,128)(2,1)}, u32[]{:S(2)}) copy-start(bf16[384,384]{1,0:T(8,128)(2,1)} %cot_ref.1) | copy-start | bytes 884740
  32.2 19.1 %copy-start.9 = (bf16[384,384]{1,0:T(8,128)(2,1)S(1)}, bf16[384,384]{1,0:T(8,128)(2,1)}, u32[]{:S(2)}) copy-start(bf16[384,384]{1,0:T(8,128)(2,1)} %value_ref.2) | copy-start | bytes 884740
  32.2 19.1 %copy-start.7 = (bf16[384,2048]{1,0:T(8,128)(2,1)S(1)}, bf16[384,2048]{1,0:T(8,128)(2,1)}, u32[]{:S(2)}) copy-start(bf16[384,2048]{1,0:T(8,128)(2,1)} %x_ref.1) | copy-start | bytes 4718596
  56.8 22.4 %all-to-all-start.2 = ((bf16[8,264,384]{2,1,0:T(8,128)(2,1)}), bf16[8,264,384]{2,1,0:T(8,128)(2,1)S(1)}, u32[]{:S(2)}, u32[]{:S(2)}) async-start(bf16[8,264,384]{2,1,0:T(8,128)(2,1)} %get-tuple-element.35), calls=%async_computation.2 | async-start | bytes 3244032 | tf_op jit(solution)/shard_map/all_to_all | solution.py:22
  61.7 4.4 %collective-permute-start.3 = (bf16[192,2048]{1,0:T(8,128)(2,1)}, bf16[192,2048]{1,0:T(8,128)(2,1)S(1)}, u32[]{:S(2)}, u32[]{:S(2)}) collective-permute-start(bf16[192,2048]{1,0:T(8,128)(2,1)} %get-tuple-element.28), channel_id=1, source_target_pairs={{0,1},{1,0},{2,3},{3,2},{4,5},{5,4},{6,7},{7,6},{8,9},{9,8},{10,11... | collective-permute-start | bytes 2359304 | tf_op jit(solution)/shard_map/ppermute | solution.py:27
  67.7 22.7 %collective-permute-start.4 = (bf16[48,2048]{1,0:T(8,128)(2,1)}, bf16[48,2048]{1,0:T(8,128)(2,1)}, u32[]{:S(2)}, u32[]{:S(2)}) collective-permute-start(bf16[48,2048]{1,0:T(8,128)(2,1)} %get-tuple-element.30), channel_id=1, source_target_pairs={{0,2},{2,4},{4,6},{6,0},{1,3},{3,5},{5,7},{7,1},{8,10},{10,12},{12... | collective-permute-start | bytes 589832 | tf_op jit(solution)/shard_map/ppermute | solution.py:27
  71.1 19.3 %collective-permute-start.5 = (bf16[48,2048]{1,0:T(8,128)(2,1)}, bf16[48,2048]{1,0:T(8,128)(2,1)}, u32[]{:S(2)}, u32[]{:S(2)}) collective-permute-start(bf16[48,2048]{1,0:T(8,128)(2,1)} %get-tuple-element.31), channel_id=1, source_target_pairs={{0,4},{2,6},{4,0},{6,2},{1,5},{3,7},{5,1},{7,3},{8,12},{10,14},{12... | collective-permute-start | bytes 589832 | tf_op jit(solution)/shard_map/ppermute | solution.py:27
  75.7 27.4 %copy-start.1 = (bf16[384,384]{1,0:T(8,128)(2,1)S(1)}, bf16[384,384]{1,0:T(8,128)(2,1)}, u32[]{:S(2)}) copy-start(bf16[384,384]{1,0:T(8,128)(2,1)} %value_ref.3) | copy-start | bytes 884740
  75.8 14.7 %collective-permute-start.6 = (bf16[48,2048]{1,0:T(8,128)(2,1)}, bf16[48,2048]{1,0:T(8,128)(2,1)}, u32[]{:S(2)}, u32[]{:S(2)}) collective-permute-start(bf16[48,2048]{1,0:T(8,128)(2,1)} %get-tuple-element.32), channel_id=1, source_target_pairs={{0,6},{2,0},{4,2},{6,4},{1,7},{3,1},{5,3},{7,5},{8,14},{10,8},{12,... | collective-permute-start | bytes 589832 | tf_op jit(solution)/shard_map/ppermute | solution.py:27
  80.2 37.5 %all-to-all-start.3 = ((bf16[8,72,384]{2,1,0:T(8,128)(2,1)}), bf16[8,72,384]{2,1,0:T(8,128)(2,1)S(1)}, u32[]{:S(2)}, u32[]{:S(2)}) async-start(bf16[8,72,384]{2,1,0:T(8,128)(2,1)} %sum_and_repack.1), calls=%async_computation.3 | async-start | bytes 884736 | tf_op jit(solution)/shard_map/all_to_all | solution.py:22
  91.8 14.8 %collective-permute-start.7 = (bf16[48,2048]{1,0:T(8,128)(2,1)S(1)}, bf16[48,2048]{1,0:T(8,128)(2,1)S(1)}, u32[]{:S(2)}, u32[]{:S(2)}) collective-permute-start(bf16[48,2048]{1,0:T(8,128)(2,1)S(1)} %add_convert_fusion), channel_id=1, source_target_pairs={{0,2},{2,4},{4,6},{6,0},{1,3},{3,5},{5,7},{7,1},{8,10},{10,12},{12... | collective-permute-start | bytes 589832 | tf_op jit(solution)/shard_map/ppermute | solution.py:27
  95.1 11.4 %collective-permute-start.8 = (bf16[48,2048]{1,0:T(8,128)(2,1)S(1)}, bf16[48,2048]{1,0:T(8,128)(2,1)S(1)}, u32[]{:S(2)}, u32[]{:S(2)}) collective-permute-start(bf16[48,2048]{1,0:T(8,128)(2,1)S(1)} %add_convert_fusion), channel_id=1, source_target_pairs={{0,4},{2,6},{4,0},{6,2},{1,5},{3,7},{5,1},{7,3},{8,12},{10,14},{12... | collective-permute-start | bytes 589832 | tf_op jit(solution)/shard_map/ppermute | solution.py:27
  99.8 8.0 %collective-permute-start.9 = (bf16[48,2048]{1,0:T(8,128)(2,1)S(1)}, bf16[48,2048]{1,0:T(8,128)(2,1)S(1)}, u32[]{:S(2)}, u32[]{:S(2)}) collective-permute-start(bf16[48,2048]{1,0:T(8,128)(2,1)S(1)} %add_convert_fusion), channel_id=1, source_target_pairs={{0,6},{2,0},{4,2},{6,4},{1,7},{3,1},{5,3},{7,5},{8,14},{10,8},{12,... | collective-permute-start | bytes 589832 | tf_op jit(solution)/shard_map/ppermute | solution.py:27
  103.1 1.4 %copy-start = (bf16[384,2048]{1,0:T(8,128)(2,1)S(1)}, bf16[384,2048]{1,0:T(8,128)(2,1)}, u32[]{:S(2)}) copy-start(bf16[384,2048]{1,0:T(8,128)(2,1)} %x_ref.2) | copy-start | bytes 4718596
  107.9 9.8 %copy-start.2 = (f32[64,384]{1,0:T(8,128)S(1)}, f32[64,384]{1,0:T(8,128)}, u32[]{:S(2)}) copy-start(f32[64,384]{1,0:T(8,128)} %w_ref.1) | copy-start | bytes 294916
  107.9 9.8 %copy-start.4 = (f32[3,384]{1,0:T(4,128)S(1)}, f32[3,384]{1,0:T(4,128)}, u32[]{:S(2)}) copy-start(f32[3,384]{1,0:T(4,128)} %taps_ref.5) | copy-start | bytes 13828
  107.9 9.8 %copy-start.6 = (f32[384]{0:T(512)S(1)}, f32[384]{0:T(512)}, u32[]{:S(2)}) copy-start(f32[384]{0:T(512)} %bias_ref.5) | copy-start | bytes 4612
  107.9 4.3 %collective-permute-start.10 = (bf16[4,48,2048]{2,1,0:T(8,128)(2,1)S(1)}, bf16[4,48,2048]{2,1,0:T(8,128)(2,1)S(1)}, u32[]{:S(2)}, u32[]{:S(2)}) collective-permute-start(bf16[4,48,2048]{2,1,0:T(8,128)(2,1)S(1)} %pad_maximum_fusion.own_ref), channel_id=1, source_target_pairs={{0,1},{1,0},{2,3},{3,2},{4,5},{5,4},{6,7},{7,6},{8,9},{9,8},{10,11... | collective-permute-start | bytes 2359304 | tf_op jit(solution)/shard_map/ppermute | solution.py:27

commit v12 on v11

--- a/solution.py
+++ b/solution.py
@@ -10,7 +10,6 @@
 SEQ_LEN = 128
 SMALL_ROWS = 8
 FAR, NEAR = ("zm", "zp"), ("zl", "y")
-FAR_SHIFTS = (0, 1, -1, 2)
 
 
 def copies_to(block, axis, size):
@@ -24,7 +23,7 @@
 
 def send_on(block, axis, shift):
     size = lax.axis_size(axis)
-    return lax.ppermute(block, axis, [(i, (i + shift + size) % size) for i in range(size)])
+    return lax.ppermute(block, axis, [(i, (i + shift) % size) for i in range(size)])
 
 
 def near(array):
@@ -105,12 +104,9 @@
     return (high + pltpu.roll(rows - high, half, 0)).astype(jnp.bfloat16)
 
 
-def previous_branch(
-    x_prev, plane, rest, cotangent, value_prev, conv_taps, conv_bias, grad_scale, n_c
-):
+def previous_branch(x_prev, plane, cotangent, value_prev, conv_taps, conv_bias, grad_scale, n_c):
     row_count, width = x_prev.shape
-    n_near, shard_rows, units = plane.shape
-    n_far = rest.shape[1] + 1
+    n_near, n_far, shard_rows, units = plane.shape
     tap_count = conv_taps.shape[0]
     n_x = lax.axis_size("x")
     half_rows = row_count // n_c
@@ -120,7 +116,6 @@
     def body(
         x_ref,
         w_ref,
-        rest_ref,
         cot_ref,
         value_ref,
         taps_ref,
@@ -141,13 +136,8 @@
             for near_at in range(n_near)
             for far_at in range(n_far)
         ]
-        own_far = lax.axis_index("zm") * lax.axis_size("zp") + lax.axis_index("zp")
-        for near_at in range(n_near):
-            for k in range(n_far):
-                far_at = (own_far + n_far - FAR_SHIFTS[k]) % n_far
-                at = (far_at * n_near + near_at) * shard_rows
-                block = w_ref[near_at] if k == 0 else rest_ref[near_at, k - 1]
-                natural_ref[pl.ds(pl.multiple_of(at, shard_rows), shard_rows)] = block
+        for near_at, far_at, at in spots:
+            natural_ref[at : at + shard_rows] = w_ref[near_at, far_at]
         up = jnp.dot(x_ref[...], natural_ref[...], preferred_element_type=jnp.float32)
         up = up.astype(jnp.bfloat16).astype(jnp.float32)
         lags = lags_of(up, tap_count)
@@ -203,7 +193,7 @@
     half = jnp.bfloat16
     return pl.pallas_call(
         body,
-        in_specs=[VMEM] * 7,
+        in_specs=[VMEM] * 6,
         out_specs=[pl.BlockSpec(), VMEM, VMEM, HBM, HBM],
         out_shape=[
             jax.ShapeDtypeStruct((row_count, units), half),
@@ -225,7 +215,6 @@
     )(
         near(x_prev),
         near(plane),
-        near(rest),
         near(cotangent),
         near(value_prev),
         near(conv_taps),
@@ -377,12 +366,10 @@
     n_zh, n_x, n_c = (lax.axis_size(a) for a in ("zh", "x", "c"))
     n_far, n_near = lax.axis_size(FAR), lax.axis_size(NEAR)
 
-    plane = copies_to(w_gate, NEAR, n_near)
-    far_shards = [send_on(w_gate, ("zh", *FAR), shift) for shift in FAR_SHIFTS[1:]]
-    rest = copies_to(jnp.stack(far_shards), NEAR, n_near)
+    plane = copies_to(copies_to(w_gate, FAR, n_far), NEAR, n_near)
     grad_scale = float(row_count * n_zh * n_far * n_near) ** (-0.5)
     grad_value, gathered, keep, to_core, sent = previous_branch(
-        x_prev, plane, rest, cotangent, value_prev, conv_taps, conv_bias, grad_scale, n_c
+        x_prev, plane, cotangent, value_prev, conv_taps, conv_bias, grad_scale, n_c
     )
     from_core = send_on(to_core, "c", 1)
     from_near = exchange(sent, NEAR)

time: 119 us -> 117 us (0.983)
  the two profiles are of different devices: /device:TPU:32 before, /device:TPU:46 now
where the time goes in v12:
time: 117 us; the launch traced here: 116 us
  blocking collectives  49.3 us (42%)
  starting transfers between devices  33.6 us (29%)
  waiting for transfers between devices  16.5 us (14%)
  Pallas kernels  11.8 us (10%)
  local copies, waits for them, and re-layouts  2.5 us (2%)
  other arithmetic  1.42 us (1%)
    all_to_all x2, blocking collectives, copies_to(): return lax.all_to_all(copies, axis, 0, 0, tiled=True)  49.3 us
    ppermute x8, starting transfers between devices, send_on(): lax.ppermute(block, axis, [(i, (i + shift) % size) for i in range(size)])  21.4 us
    all_to_all x2, starting transfers between devices, exchange(): return lax.all_to_all(blocks, axis, 0, 0, tiled=True)  12.2 us
    ppermute x8, waiting for transfers between devices, send_on(): lax.ppermute(block, axis, [(i, (i + shift) % size) for i in range(size)])  8.9 us
    all_to_all x2, waiting for transfers between devices, exchange(): return lax.all_to_all(blocks, axis, 0, 0, tiled=True)  7.65 us
    pallas_call x1, Pallas kernels, previous_branch(): pl.pallas_call(body, in_specs=[VMEM] * 6, out_specs=[pl.BlockSpec(), VMEM...  5.33 us
  transfers between devices with their start and end apart: 10, of which 6 were waited for; matrix products, arithmetic and copies ran while one was open for 1% of the time, Pallas kernels for 5%

profile of v12, /device:TPU:46, one launch (start us, length us, event | category | flops | bytes accessed | tf_op | source)
XLA Modules:
  0.0 116.0 jit_solution(11311864193284393742)
XLA Ops:
  0.6 0.8 broadcast_in_dim.6
  1.5 24.6 %all_to_all.20 = bf16[4,64,384]{2,1,0:T(8,128)(2,1)S(1)} all-to-all(bf16[4,64,384]{2,1,0:T(8,128)(2,1)S(1)} %broadcast_in_dim.6), channel_id=1, replica_groups=mesh['zh'=2,'zm'=2,'zp'=2,'zl'=2,'y'=4,'x'=4,'c'=2] {'zm','zp'}, dimensions={0} | all-to-all | bytes 393216 | tf_op jit(solution)/shard_map/all_to_all | solution.py:17
  26.1 0.2 broadcast_in_dim.7
  26.3 0.0 copy-start.3
  26.3 0.0 copy-start.5
  26.3 0.0 copy-start.7
  26.3 0.0 copy-start.8
  26.3 0.0 copy-start.9
  26.4 24.7 %all_to_all.21.w_ref = bf16[8,4,64,384]{3,2,1,0:T(8,128)(2,1)S(1)} all-to-all(bf16[8,4,64,384]{3,2,1,0:T(8,128)(2,1)S(1)} %broadcast_in_dim.7), channel_id=1, replica_groups=mesh['zh'=2,'zm'=2,'zp'=2,'zl'=2,'y'=4,'x'=4,'c'=2] {'zl','y'}, dimensions={0} | all-to-all | bytes 3145728 | tf_op jit(solution)/shard_map/all_to_all | solution.py:17
  51.1 0.0 copy-done.3
  51.1 0.0 copy-done.5
  51.1 0.0 copy-done.7
  51.1 0.0 copy-done.8
  51.1 0.0 copy-done.9
  51.1 5.3 %previous_branch.1 = (bf16[384,384]{1,0:T(8,128)(2,1)}, bf16[2048,384]{1,0:T(8,128)(2,1)S(1)}, bf16[192,384]{1,0:T(8,128)(2,1)S(1)}, bf16[192,2048]{1,0:T(8,128)(2,1)}, bf16[8,264,384]{2,1,0:T(8,128)(2,1)}) custom-call(bf16[384,2048]{1,0:T(8,128)(2,1)S(1)} %copy-done.7, bf16[8,4,64,384]{3,2,1,0:T(8,128)(2,1)S(1)} %all_to_all.21.w_ref, ...), custom_call_target="tpu_custom_call" | custom-call | flops 1509949440 | bytes 6291456 | tf_op jit(solution)/shard_map/previous_branch/pallas_call | solution.py:194
  56.4 5.5 %all-to-all-start.2 = ((bf16[8,264,384]{2,1,0:T(8,128)(2,1)}), bf16[8,264,384]{2,1,0:T(8,128)(2,1)S(1)}, u32[]{:S(2)}, u32[]{:S(2)}) async-start(bf16[8,264,384]{2,1,0:T(8,128)(2,1)} %get-tuple-element.35), calls=%async_computation.2 | async-start | bytes 3244032 | tf_op jit(solution)/shard_map/all_to_all | solution.py:21
  62.0 1.9 %collective-permute-start = (bf16[192,2048]{1,0:T(8,128)(2,1)}, bf16[192,2048]{1,0:T(8,128)(2,1)S(1)}, u32[]{:S(2)}, u32[]{:S(2)}) collective-permute-start(bf16[192,2048]{1,0:T(8,128)(2,1)} %get-tuple-element.28), channel_id=1, source_target_pairs={{0,1},{1,0},{2,3},{3,2},{4,5},{5,4},{6,7},{7,6},{8,9},{9,8},{10,11... | collective-permute-start | bytes 2359304 | tf_op jit(solution)/shard_map/ppermute | solution.py:26
  63.9 2.5 %collective-permute-done.other_ref = bf16[192,2048]{1,0:T(8,128)(2,1)S(1)} collective-permute-done((bf16[192,2048]{1,0:T(8,128)(2,1)}, bf16[192,2048]{1,0:T(8,128)(2,1)S(1)}, u32[]{:S(2)}, u32[]{:S(2)}) %collective-permute-start) | collective-permute-done | bytes 786464 | tf_op jit(solution)/shard_map/ppermute | solution.py:26
  66.4 1.6 %add_halves.1 = (bf16[48,2048]{1,0:T(8,128)(2,1)}, bf16[48,2048]{1,0:T(8,128)(2,1)}, bf16[48,2048]{1,0:T(8,128)(2,1)}, bf16[48,2048]{1,0:T(8,128)(2,1)}) custom-call(bf16[192,384]{1,0:T(8,128)(2,1)S(1)} %get-tuple-element.26.keep_ref, bf16[2048,384]{1,0:T(8,128)(2,1)S(1)} %get-tuple-element.27.w_ref, bf16[192,2048]{1,0:T(8,128)(2,1)S(1)} %collective-permute-done.other_ref), custom_call_target="tpu_custom_call" | custom-call | flops 301989888 | bytes 6291456 | tf_op jit(solution)/shard_map/add_halves/pallas_call | solution.py:246
  67.9 2.4 %collective-permute-start.1 = (bf16[48,2048]{1,0:T(8,128)(2,1)}, bf16[48,2048]{1,0:T(8,128)(2,1)}, u32[]{:S(2)}, u32[]{:S(2)}) collective-permute-start(bf16[48,2048]{1,0:T(8,128)(2,1)} %get-tuple-element.30), channel_id=1, source_target_pairs={{0,2},{2,4},{4,6},{6,0},{1,3},{3,5},{5,7},{7,1},{8,10},{10,12},{12... | collective-permute-start | bytes 589832 | tf_op jit(solution)/shard_map/ppermute | solution.py:26
  70.3 4.3 %collective-permute-start.2 = (bf16[48,2048]{1,0:T(8,128)(2,1)}, bf16[48,2048]{1,0:T(8,128)(2,1)}, u32[]{:S(2)}, u32[]{:S(2)}) collective-permute-start(bf16[48,2048]{1,0:T(8,128)(2,1)} %get-tuple-element.31), channel_id=1, source_target_pairs={{0,4},{2,6},{4,0},{6,2},{1,5},{3,7},{5,1},{7,3},{8,12},{10,14},{12... | collective-permute-start | bytes 589832 | tf_op jit(solution)/shard_map/ppermute | solution.py:26
  74.7 0.0 copy-start.1
  74.7 2.1 %collective-permute-start.3 = (bf16[48,2048]{1,0:T(8,128)(2,1)}, bf16[48,2048]{1,0:T(8,128)(2,1)}, u32[]{:S(2)}, u32[]{:S(2)}) collective-permute-start(bf16[48,2048]{1,0:T(8,128)(2,1)} %get-tuple-element.32), channel_id=1, source_target_pairs={{0,6},{2,0},{4,2},{6,4},{1,7},{3,1},{5,3},{7,5},{8,14},{10,8},{12,... | collective-permute-start | bytes 589832 | tf_op jit(solution)/shard_map/ppermute | solution.py:26
  76.8 3.3 %all-to-all-done.2.in_ref = bf16[8,264,384]{2,1,0:T(8,128)(2,1)S(1)} async-done(((bf16[8,264,384]{2,1,0:T(8,128)(2,1)}), bf16[8,264,384]{2,1,0:T(8,128)(2,1)S(1)}, u32[]{:S(2)}, u32[]{:S(2)}) %all-to-all-start.2) | async-done | bytes 1622048 | tf_op jit(solution)/shard_map/all_to_all | solution.py:21
  80.0 0.9 sum_and_repack.1
  81.0 6.7 %all-to-all-start.3 = ((bf16[8,72,384]{2,1,0:T(8,128)(2,1)}), bf16[8,72,384]{2,1,0:T(8,128)(2,1)S(1)}, u32[]{:S(2)}, u32[]{:S(2)}) async-start(bf16[8,72,384]{2,1,0:T(8,128)(2,1)} %sum_and_repack.1), calls=%async_computation.3 | async-start | bytes 884736 | tf_op jit(solution)/shard_map/all_to_all | solution.py:21
  87.7 0.0 collective-permute-done.1
  87.7 0.0 collective-permute-done.2
  87.7 0.0 collective-permute-done.3
  87.7 1.3 %add_convert_fusion = bf16[48,2048]{1,0:T(8,128)(2,1)S(1)} fusion(bf16[48,2048]{1,0:T(8,128)(2,1)} %collective-permute-done.3, bf16[48,2048]{1,0:T(8,128)(2,1)} %collective-permute-done.2, bf16[48,2048]{1,0:T(8,128)(2,1)} %collective-permute-done.1, bf16[48,2048]{1,0:T(8,128)(2,1)} %get-tuple-element.29), kind=kLoop, calls=%fused_computation.1 | loop fusion | flops 786432 | bytes 983040 | tf_op jit(solution)/shard_map/convert_element_type | solution.py:384
  89.0 2.6 %collective-permute-start.4 = (bf16[48,2048]{1,0:T(8,128)(2,1)S(1)}, bf16[48,2048]{1,0:T(8,128)(2,1)S(1)}, u32[]{:S(2)}, u32[]{:S(2)}) collective-permute-start(bf16[48,2048]{1,0:T(8,128)(2,1)S(1)} %add_convert_fusion), channel_id=1, source_target_pairs={{0,2},{2,4},{4,6},{6,0},{1,3},{3,5},{5,7},{7,1},{8,10},{10,12},{12... | collective-permute-start | bytes 589832 | tf_op jit(solution)/shard_map/ppermute | solution.py:26
  91.6 4.2 %collective-permute-start.5 = (bf16[48,2048]{1,0:T(8,128)(2,1)S(1)}, bf16[48,2048]{1,0:T(8,128)(2,1)S(1)}, u32[]{:S(2)}, u32[]{:S(2)}) collective-permute-start(bf16[48,2048]{1,0:T(8,128)(2,1)S(1)} %add_convert_fusion), channel_id=1, source_target_pairs={{0,4},{2,6},{4,0},{6,2},{1,5},{3,7},{5,1},{7,3},{8,12},{10,14},{12... | collective-permute-start | bytes 589832 | tf_op jit(solution)/shard_map/ppermute | solution.py:26
  95.7 1.9 %collective-permute-start.6 = (bf16[48,2048]{1,0:T(8,128)(2,1)S(1)}, bf16[48,2048]{1,0:T(8,128)(2,1)S(1)}, u32[]{:S(2)}, u32[]{:S(2)}) collective-permute-start(bf16[48,2048]{1,0:T(8,128)(2,1)S(1)} %add_convert_fusion), channel_id=1, source_target_pairs={{0,6},{2,0},{4,2},{6,4},{1,7},{3,1},{5,3},{7,5},{8,14},{10,8},{12,... | collective-permute-start | bytes 589832 | tf_op jit(solution)/shard_map/ppermute | solution.py:26
  97.7 0.0 copy-done.1
  97.7 0.0 copy-start
  97.7 1.4 %copy-done = bf16[384,2048]{1,0:T(8,128)(2,1)S(1)} copy-done((bf16[384,2048]{1,0:T(8,128)(2,1)S(1)}, bf16[384,2048]{1,0:T(8,128)(2,1)}, u32[]{:S(2)}) %copy-start) | copy-done | bytes 1572888
  99.1 2.0 %next_branch.1 = bf16[384,384]{1,0:T(8,128)(2,1)} custom-call(bf16[384,2048]{1,0:T(8,128)(2,1)S(1)} %copy-done, bf16[2048,384]{1,0:T(8,128)(2,1)S(1)} %get-tuple-element.27.w_ref, bf16[384,384]{1,0:T(8,128)(2,1)S(1)} %copy-done.1, f32[3,384]{1,0:T(4,128)S(1)} %copy-done.3, f32[384]{0:T(512)S(1)} %copy-done.5), custom_call_target="tpu_custom_call" | custom-call | flops 603979776 | bytes 3145728 | tf_op jit(solution)/shard_map/next_branch/pallas_call | solution.py:272
  101.0 0.0 collective-permute-done.4
  101.0 0.3 collective-permute-done.5
  101.3 3.9 %collective-permute-done.6 = bf16[48,2048]{1,0:T(8,128)(2,1)S(1)} collective-permute-done((bf16[48,2048]{1,0:T(8,128)(2,1)S(1)}, bf16[48,2048]{1,0:T(8,128)(2,1)S(1)}, u32[]{:S(2)}, u32[]{:S(2)}) %collective-permute-start.6) | collective-permute-done | bytes 196640 | tf_op jit(solution)/shard_map/ppermute | solution.py:26
  105.2 0.1 pad_maximum_fusion.own_ref
  105.3 0.0 copy-start.2
  105.3 0.0 copy-start.4
  105.3 0.0 copy-start.6
  105.4 2.1 %collective-permute-start.7 = (bf16[4,48,2048]{2,1,0:T(8,128)(2,1)S(1)}, bf16[4,48,2048]{2,1,0:T(8,128)(2,1)S(1)}, u32[]{:S(2)}, u32[]{:S(2)}) collective-permute-start(bf16[4,48,2048]{2,1,0:T(8,128)(2,1)S(1)} %pad_maximum_fusion.own_ref), channel_id=1, source_target_pairs={{0,1},{1,0},{2,3},{3,2},{4,5},{5,4},{6,7},{7,6},{8,9},{9,8},{10,11... | collective-permute-start | bytes 2359304 | tf_op jit(solution)/shard_map/ppermute | solution.py:26
  107.4 2.3 %collective-permute-done.7.other_ref = bf16[4,48,2048]{2,1,0:T(8,128)(2,1)S(1)} collective-permute-done((bf16[4,48,2048]{2,1,0:T(8,128)(2,1)S(1)}, bf16[4,48,2048]{2,1,0:T(8,128)(2,1)S(1)}, u32[]{:S(2)}, u32[]{:S(2)}) %collective-permute-start.7) | collective-permute-done | bytes 786464 | tf_op jit(solution)/shard_map/ppermute | solution.py:26
  109.7 1.3 %put_in_order.1 = bf16[8,48,2048]{2,1,0:T(8,128)(2,1)} custom-call(bf16[4,48,2048]{2,1,0:T(8,128)(2,1)S(1)} %pad_maximum_fusion.own_ref, bf16[4,48,2048]{2,1,0:T(8,128)(2,1)S(1)} %collective-permute-done.7.other_ref), custom_call_target="tpu_custom_call" | custom-call | bytes 3145728 | tf_op jit(solution)/shard_map/put_in_order/pallas_call | solution.py:51
  110.9 4.4 %all-to-all-done.3.in_ref = bf16[8,72,384]{2,1,0:T(8,128)(2,1)S(1)} async-done(((bf16[8,72,384]{2,1,0:T(8,128)(2,1)}), bf16[8,72,384]{2,1,0:T(8,128)(2,1)S(1)}, u32[]{:S(2)}, u32[]{:S(2)}) %all-to-all-start.3) | async-done | bytes 442400 | tf_op jit(solution)/shard_map/all_to_all | solution.py:21
  115.3 0.0 copy-done.2
  115.3 0.0 copy-done.4
  115.3 0.0 copy-done.6
  115.3 0.7 last_sum.1
Async XLA Ops:
  26.3 24.8 %copy-start.3 = (f32[3,384]{1,0:T(4,128)S(1)}, f32[3,384]{1,0:T(4,128)}, u32[]{:S(2)}) copy-start(f32[3,384]{1,0:T(4,128)} %taps_ref.4) | copy-start | bytes 13828
  26.3 24.8 %copy-start.5 = (f32[384]{0:T(512)S(1)}, f32[384]{0:T(512)}, u32[]{:S(2)}) copy-start(f32[384]{0:T(512)} %bias_ref.4) | copy-start | bytes 4612
  26.3 24.8 %copy-start.7 = (bf16[384,2048]{1,0:T(8,128)(2,1)S(1)}, bf16[384,2048]{1,0:T(8,128)(2,1)}, u32[]{:S(2)}) copy-start(bf16[384,2048]{1,0:T(8,128)(2,1)} %x_ref.1) | copy-start | bytes 4718596
  26.3 24.8 %copy-start.8 = (bf16[384,384]{1,0:T(8,128)(2,1)S(1)}, bf16[384,384]{1,0:T(8,128)(2,1)}, u32[]{:S(2)}) copy-start(bf16[384,384]{1,0:T(8,128)(2,1)} %cot_ref.1) | copy-start | bytes 884740
  26.3 24.8 %copy-start.9 = (bf16[384,384]{1,0:T(8,128)(2,1)S(1)}, bf16[384,384]{1,0:T(8,128)(2,1)}, u32[]{:S(2)}) copy-start(bf16[384,384]{1,0:T(8,128)(2,1)} %value_ref.2) | copy-start | bytes 884740
  56.4 23.6 %all-to-all-start.2 = ((bf16[8,264,384]{2,1,0:T(8,128)(2,1)}), bf16[8,264,384]{2,1,0:T(8,128)(2,1)S(1)}, u32[]{:S(2)}, u32[]{:S(2)}) async-start(bf16[8,264,384]{2,1,0:T(8,128)(2,1)} %get-tuple-element.35), calls=%async_computation.2 | async-start | bytes 3244032 | tf_op jit(solution)/shard_map/all_to_all | solution.py:21
  62.0 4.4 %collective-permute-start = (bf16[192,2048]{1,0:T(8,128)(2,1)}, bf16[192,2048]{1,0:T(8,128)(2,1)S(1)}, u32[]{:S(2)}, u32[]{:S(2)}) collective-permute-start(bf16[192,2048]{1,0:T(8,128)(2,1)} %get-tuple-element.28), channel_id=1, source_target_pairs={{0,1},{1,0},{2,3},{3,2},{4,5},{5,4},{6,7},{7,6},{8,9},{9,8},{10,11... | collective-permute-start | bytes 2359304 | tf_op jit(solution)/shard_map/ppermute | solution.py:26
  67.9 19.7 %collective-permute-start.1 = (bf16[48,2048]{1,0:T(8,128)(2,1)}, bf16[48,2048]{1,0:T(8,128)(2,1)}, u32[]{:S(2)}, u32[]{:S(2)}) collective-permute-start(bf16[48,2048]{1,0:T(8,128)(2,1)} %get-tuple-element.30), channel_id=1, source_target_pairs={{0,2},{2,4},{4,6},{6,0},{1,3},{3,5},{5,7},{7,1},{8,10},{10,12},{12... | collective-permute-start | bytes 589832 | tf_op jit(solution)/shard_map/ppermute | solution.py:26
  70.3 17.3 %collective-permute-start.2 = (bf16[48,2048]{1,0:T(8,128)(2,1)}, bf16[48,2048]{1,0:T(8,128)(2,1)}, u32[]{:S(2)}, u32[]{:S(2)}) collective-permute-start(bf16[48,2048]{1,0:T(8,128)(2,1)} %get-tuple-element.31), channel_id=1, source_target_pairs={{0,4},{2,6},{4,0},{6,2},{1,5},{3,7},{5,1},{7,3},{8,12},{10,14},{12... | collective-permute-start | bytes 589832 | tf_op jit(solution)/shard_map/ppermute | solution.py:26
  74.7 23.0 %copy-start.1 = (bf16[384,384]{1,0:T(8,128)(2,1)S(1)}, bf16[384,384]{1,0:T(8,128)(2,1)}, u32[]{:S(2)}) copy-start(bf16[384,384]{1,0:T(8,128)(2,1)} %value_ref.3) | copy-start | bytes 884740
  74.7 13.0 %collective-permute-start.3 = (bf16[48,2048]{1,0:T(8,128)(2,1)}, bf16[48,2048]{1,0:T(8,128)(2,1)}, u32[]{:S(2)}, u32[]{:S(2)}) collective-permute-start(bf16[48,2048]{1,0:T(8,128)(2,1)} %get-tuple-element.32), channel_id=1, source_target_pairs={{0,6},{2,0},{4,2},{6,4},{1,7},{3,1},{5,3},{7,5},{8,14},{10,8},{12,... | collective-permute-start | bytes 589832 | tf_op jit(solution)/shard_map/ppermute | solution.py:26
  81.0 34.3 %all-to-all-start.3 = ((bf16[8,72,384]{2,1,0:T(8,128)(2,1)}), bf16[8,72,384]{2,1,0:T(8,128)(2,1)S(1)}, u32[]{:S(2)}, u32[]{:S(2)}) async-start(bf16[8,72,384]{2,1,0:T(8,128)(2,1)} %sum_and_repack.1), calls=%async_computation.3 | async-start | bytes 884736 | tf_op jit(solution)/shard_map/all_to_all | solution.py:21
  89.0 12.0 %collective-permute-start.4 = (bf16[48,2048]{1,0:T(8,128)(2,1)S(1)}, bf16[48,2048]{1,0:T(8,128)(2,1)S(1)}, u32[]{:S(2)}, u32[]{:S(2)}) collective-permute-start(bf16[48,2048]{1,0:T(8,128)(2,1)S(1)} %add_convert_fusion), channel_id=1, source_target_pairs={{0,2},{2,4},{4,6},{6,0},{1,3},{3,5},{5,7},{7,1},{8,10},{10,12},{12... | collective-permute-start | bytes 589832 | tf_op jit(solution)/shard_map/ppermute | solution.py:26
  91.6 9.7 %collective-permute-start.5 = (bf16[48,2048]{1,0:T(8,128)(2,1)S(1)}, bf16[48,2048]{1,0:T(8,128)(2,1)S(1)}, u32[]{:S(2)}, u32[]{:S(2)}) collective-permute-start(bf16[48,2048]{1,0:T(8,128)(2,1)S(1)} %add_convert_fusion), channel_id=1, source_target_pairs={{0,4},{2,6},{4,0},{6,2},{1,5},{3,7},{5,1},{7,3},{8,12},{10,14},{12... | collective-permute-start | bytes 589832 | tf_op jit(solution)/shard_map/ppermute | solution.py:26
  95.7 9.5 %collective-permute-start.6 = (bf16[48,2048]{1,0:T(8,128)(2,1)S(1)}, bf16[48,2048]{1,0:T(8,128)(2,1)S(1)}, u32[]{:S(2)}, u32[]{:S(2)}) collective-permute-start(bf16[48,2048]{1,0:T(8,128)(2,1)S(1)} %add_convert_fusion), channel_id=1, source_target_pairs={{0,6},{2,0},{4,2},{6,4},{1,7},{3,1},{5,3},{7,5},{8,14},{10,8},{12,... | collective-permute-start | bytes 589832 | tf_op jit(solution)/shard_map/ppermute | solution.py:26
  97.7 1.4 %copy-start = (bf16[384,2048]{1,0:T(8,128)(2,1)S(1)}, bf16[384,2048]{1,0:T(8,128)(2,1)}, u32[]{:S(2)}) copy-start(bf16[384,2048]{1,0:T(8,128)(2,1)} %x_ref.2) | copy-start | bytes 4718596
  105.3 10.0 %copy-start.2 = (f32[64,384]{1,0:T(8,128)S(1)}, f32[64,384]{1,0:T(8,128)}, u32[]{:S(2)}) copy-start(f32[64,384]{1,0:T(8,128)} %w_ref.1) | copy-start | bytes 294916
  105.3 10.0 %copy-start.4 = (f32[3,384]{1,0:T(4,128)S(1)}, f32[3,384]{1,0:T(4,128)}, u32[]{:S(2)}) copy-start(f32[3,384]{1,0:T(4,128)} %taps_ref.5) | copy-start | bytes 13828
  105.3 10.0 %copy-start.6 = (f32[384]{0:T(512)S(1)}, f32[384]{0:T(512)}, u32[]{:S(2)}) copy-start(f32[384]{0:T(512)} %bias_ref.5) | copy-start | bytes 4612
  105.4 4.3 %collective-permute-start.7 = (bf16[4,48,2048]{2,1,0:T(8,128)(2,1)S(1)}, bf16[4,48,2048]{2,1,0:T(8,128)(2,1)S(1)}, u32[]{:S(2)}, u32[]{:S(2)}) collective-permute-start(bf16[4,48,2048]{2,1,0:T(8,128)(2,1)S(1)} %pad_maximum_fusion.own_ref), channel_id=1, source_target_pairs={{0,1},{1,0},{2,3},{3,2},{4,5},{5,4},{6,7},{7,6},{8,9},{9,8},{10,11... | collective-permute-start | bytes 2359304 | tf_op jit(solution)/shard_map/ppermute | solution.py:26
